TPU v7x, 512 devices: a whole 4x4x16 slice. The times are simulated.
512 devices in a mesh: rep: 2 (over z_hi), fs: 32 (over z_lo, y), tp: 8 (over x, core).
Axes of the slice: x: 4, y: 4, z: 16 (z_hi: 2, z_lo: 8; z = z_hi * 8 + z_lo), core: 2. Of those that a mesh axis runs over, the one named last changes fastest.
Arguments:
- tokens: bfloat16 [64, 1024, 1024], P(('rep', 'fs'), 'tp'), may hold values from -6 to 6
- mixer_in_gain: float32 [1024], replicated, may hold values from 0.5 to 1.5
- query_weight: bfloat16 [1024, 1024], P('fs', 'tp'), may hold values from -0.1875 to 0.1875
- key_weight: bfloat16 [1024, 1024], P('fs', 'tp'), may hold values from -0.1875 to 0.1875
- value_weight: bfloat16 [1024, 2048], P('fs', 'tp'), may hold values from -0.1875 to 0.1875
- gate_weight: bfloat16 [1024, 2048], P('fs', 'tp'), may hold values from -0.1875 to 0.1875
- decay_logits: float32 [2, 8], P(None, 'tp'), may hold values from 3.4 to 6.2
- mixer_output: bfloat16 [2048, 1024], P('tp', 'fs'), may hold values from -0.125 to 0.125
- mixer_out_gain: float32 [1024], replicated, may hold values from 0.5 to 1.5
- channel_in_gain: float32 [1024], replicated, may hold values from 0.5 to 1.5
- gelu_weight: bfloat16 [1024, 2816], P('fs', 'tp'), may hold values from -0.1875 to 0.1875
- linear_weight: bfloat16 [1024, 2816], P('fs', 'tp'), may hold values from -0.1875 to 0.1875
- gelu_kernel: float32 [3, 2816], P(None, 'tp'), may hold values from -3.5 to 3.5
- linear_kernel: float32 [3, 2816], P(None, 'tp'), may hold values from -3.5 to 3.5
- gelu_bias: float32 [2816], P('tp'), may hold values from -1.2 to 1.2
- linear_bias: float32 [2816], P('tp'), may hold values from -1.2 to 1.2
- down_weight: bfloat16 [2816, 1024], P('tp', 'fs'), may hold values from -0.109375 to 0.109375
- channel_out_gain: float32 [1024], replicated, may hold values from 0.5 to 1.5
Outputs:
- layer_output: bfloat16 [64, 1024, 1024], P(('rep', 'fs'), 'tp')
All inputs are finite; a program needn't handle non-finite values.
Results may differ from a plain program's by a relative error of at most 0.02.
Values may be sent and summed in bfloat16 or wider, within the bound.
No kernel may reach another device: no remote copies, remote signals or barrier semaphores. Data moves between devices by JAX's collectives and lax.ppermute only.
A program may use at most 64 MiB of HBM per device.

v0:
```python
import functools

import jax
import jax.numpy as jnp
from jax import lax
from jax.experimental import pallas as pl
from jax.experimental.pallas import tpu as pltpu
from jax.sharding import Mesh
from jax.sharding import PartitionSpec as P


DK = 128
DV = 256
TP = ("x", "c")
FS = ("z", "y")
RING = ("rep", "z")
SWAP = ((0, 1), (1, 0))
PAD = 384
FIRST, SECOND, THIRD = 2 * DK + 2 * DV, DV, 3 * PAD
Z_SHIFTS = (4, 3, 2, 1, 0, -1, -2, -3)
Z_ISSUE = (4, -3, 3, -2, 2, -1, 1)
Y_SHIFTS = (0, 1, 2, -1)
Y_ISSUE = (2, 1, -1)
epsilon = 1e-06
rope_base = 10000.0
bf16 = jnp.bfloat16
f32 = jnp.float32

VMEM = pl.BlockSpec(memory_space=pltpu.VMEM)
SMEM = pl.BlockSpec(memory_space=pltpu.SMEM)


def call(body, out_shapes, *args, flops=0, moved=0, smem=0, **options):
    specs = [SMEM] * smem + [VMEM] * (len(args) - smem)
    single = not isinstance(out_shapes, (list, tuple))
    return pl.pallas_call(
        body,
        out_shape=out_shapes,
        in_specs=specs,
        out_specs=VMEM if single else [VMEM] * len(out_shapes),
        cost_estimate=pl.CostEstimate(
            flops=max(flops, 1 << 20), bytes_accessed=max(moved, 1 << 20), transcendentals=0
        ),
        **options,
    )(*args)


def shape(dims, kind=bf16):
    return jax.ShapeDtypeStruct(dims, kind)


def permuted(value, axes, shift, size):
    return lax.ppermute(value, axes, [(i, (i + shift) % size) for i in range(size)])


def swap(value):
    return lax.ppermute(value, "c", SWAP)


def exchanged(value):
    return lax.all_to_all(value, "x", 0, 0, tiled=True)


def rms_rows(values, gain):
    return values * lax.rsqrt(jnp.mean(values * values, axis=-1, keepdims=True) + epsilon) * gain


def pack_body(width, q, k, v, g, mo, ge, li, dn, out):
    out[:, :DK] = q[...]
    out[:, DK : 2 * DK] = k[...]
    out[:, 2 * DK : 2 * DK + DV] = v[...]
    out[:, 2 * DK + DV : FIRST] = g[...]
    out[:, FIRST : FIRST + SECOND] = mo[...]
    gap = jnp.zeros((out.shape[0], PAD - width), bf16)
    for place, piece in enumerate((ge, li, dn)):
        at = FIRST + SECOND + place * PAD
        out[:, at : at + PAD] = jnp.concatenate([piece[...], gap], axis=1)


def first_norm_body(tokens, gain, out):
    rows = rms_rows(tokens[...].astype(f32), gain[...]).astype(bf16)
    for k in range(out.shape[0]):
        out[k] = rows


def ring_order_body(index, *refs):
    pieces, (one, two, three) = refs[:8], refs[8:]
    for shift, piece in zip(Z_SHIFTS, pieces):
        at = lax.rem(index[0] - shift + 8, 8)
        one[at] = piece[:, :FIRST]
        two[at] = piece[:, FIRST : FIRST + SECOND]
        three[at] = piece[:, FIRST + SECOND :]


def line_order_body(index, *refs):
    pieces, out = refs[:4], refs[4]
    for shift, piece in zip(Y_SHIFTS, pieces):
        at = lax.rem(index[0] - shift + 4, 4)
        for z in range(8):
            out[z, at] = piece[z]


def middle_body(pieces, tokens, out_gain, in_gain, after_mix, channel_in):
    mixed = pieces[0].astype(f32)
    for k in range(1, pieces.shape[0]):
        mixed = mixed + pieces[k].astype(f32)
    mix = (tokens[...].astype(f32) + rms_rows(mixed, out_gain[...])).astype(bf16)
    after_mix[...] = mix
    rows = rms_rows(mix.astype(f32), in_gain[...]).astype(bf16)
    for k in range(channel_in.shape[0]):
        channel_in[k] = rows


def final_body(pieces, after_mix, gain, out):
    total = pieces[0].astype(f32)
    for k in range(1, pieces.shape[0]):
        total = total + pieces[k].astype(f32)
    out[...] = (after_mix[...].astype(f32) + rms_rows(total, gain[...])).astype(bf16)


def rotate(values, positions):
    half_width = values.shape[-1] // 2
    frequency = 1.0 / rope_base ** (jnp.arange(half_width, dtype=f32) / half_width)
    angles = positions.astype(f32)[:, None] * frequency[None, :]
    cosine = jnp.cos(angles)
    sine_part = jnp.sin(angles)
    first_half = values[..., :half_width]
    second = values[..., half_width:]
    return jnp.concatenate(
        [first_half * cosine - second * sine_part, first_half * sine_part + second * cosine],
        axis=-1,
    )


def head_norm(values):
    centred = values - jnp.mean(values, axis=-1, keepdims=True)
    return centred * lax.rsqrt(jnp.mean(centred * centred, axis=-1, keepdims=True) + epsilon)


def dot(a, b):
    return jnp.dot(a, b, preferred_element_type=f32)


def dot_nt(a, b):
    return lax.dot_general(a, b, (((1,), (1,)), ((), ())), preferred_element_type=f32)


def line_gather(piece):
    got = {0: piece}
    for shift in Y_ISSUE:
        got[shift] = permuted(piece, "y", shift, 4)
    return [got[s] for s in Y_SHIFTS]


def in_line_order(pieces, y_index):
    columns = pieces[0].shape[-1]
    ordered = call(
        line_order_body, shape((8, 4, 32, columns)), y_index, *pieces, smem=1
    )
    return ordered.reshape(1024, columns)


def layer(
    tokens,
    mixer_in_gain,
    query_weight,
    key_weight,
    value_weight,
    gate_weight,
    decay_logits,
    mixer_output,
    mixer_out_gain,
    channel_in_gain,
    gelu_weight,
    linear_weight,
    gelu_kernel,
    linear_kernel,
    gelu_bias,
    linear_bias,
    down_weight,
    channel_out_gain,
):
    core = lax.axis_index("c")
    y_index = lax.axis_index("y").astype(jnp.int32)[None]
    z_index = lax.axis_index("z").astype(jnp.int32)[None]
    token_rows = tokens[0]
    own, model = token_rows.shape
    chips = lax.axis_size("x")
    width = gelu_weight.shape[1]

    def gain_row(gain):
        return gain.reshape(1, -1)

    packed = call(
        functools.partial(pack_body, width),
        shape((32, FIRST + SECOND + THIRD)),
        query_weight,
        key_weight,
        value_weight,
        gate_weight,
        mixer_output.T,
        gelu_weight,
        linear_weight,
        down_weight.T,
    )
    got = {0: packed}
    for shift in Z_ISSUE:
        got[shift] = permuted(packed, RING, shift, 16)
    spread = call(
        first_norm_body, shape((chips, own, model)), token_rows, gain_row(mixer_in_gain)
    )
    normed_own = exchanged(spread).reshape(chips * own, model)
    normed_other = swap(normed_own)

    def padded(value):
        return jnp.pad(value, ((0, 0), (0, PAD - width)))

    taps = padded(
        jnp.concatenate([gelu_kernel, linear_kernel, gelu_bias[None], linear_bias[None]], axis=0)
    )
    taps_other = swap(taps)

    first_z, second_z, third_z = call(
        ring_order_body,
        [shape((8, 32, FIRST)), shape((8, 32, SECOND)), shape((8, 32, THIRD))],
        z_index,
        *[got[s] for s in Z_SHIFTS],
        smem=1,
    )
    first_pieces = line_gather(first_z)
    second_pieces = line_gather(second_z)
    third_pieces = line_gather(third_z)
    qkvg = in_line_order(first_pieces, y_index)

    block = jnp.arange(chips, dtype=jnp.int32)[:, None] * (2 * own)
    inside = jnp.arange(own, dtype=jnp.int32)[None, :]
    own_positions = (block + inside + core * own).reshape(-1)
    other_positions = (block + inside + (1 - core) * own).reshape(-1)
    positions = jnp.concatenate([own_positions, other_positions])
    rows = jnp.concatenate([normed_own, normed_other], axis=0)
    projected = dot(rows, qkvg)
    queries = rotate(projected[:, :DK], positions).astype(bf16)
    keys = (rotate(projected[:, DK : 2 * DK], positions) * DK ** (-0.5)).astype(bf16)
    values = projected[:, 2 * DK : 2 * DK + DV].astype(bf16)
    gates = projected[:, 2 * DK + DV :]
    log_forward = jax.nn.log_sigmoid(decay_logits[0, 0])
    log_backward = jax.nn.log_sigmoid(decay_logits[1, 0])
    offset = (positions[:, None] - positions[None, :]).astype(f32)
    decay = jnp.exp(jnp.where(offset >= 0, offset * log_forward, -offset * log_backward))
    scores = (dot_nt(queries, keys) * decay).astype(bf16)
    retained = dot(scores, values)
    gated = (head_norm(retained) * jax.nn.silu(gates)).astype(bf16)
    half = chips * own
    gated_partner = swap(gated[half:])
    out_own = in_line_order(second_pieces, y_index)
    out_other = swap(out_own)
    mixed = dot_nt(gated[:half], out_own) + dot_nt(gated_partner, out_other)
    mix_pieces = exchanged(mixed.astype(bf16).reshape(chips, own, model))
    after_mix, channel_spread = call(
        middle_body,
        [shape((own, model)), shape((chips, own, model))],
        mix_pieces,
        token_rows,
        gain_row(mixer_out_gain),
        gain_row(channel_in_gain),
    )
    channel_rows = exchanged(channel_spread)
    third_own = in_line_order(third_pieces, y_index)
    third_other = swap(third_own)

    edges = jnp.stack([channel_rows[:, 0], channel_rows[:, own - 1]], axis=0)
    edges_other = swap(edges)
    zero = jnp.zeros((1, model), bf16)
    firsts, lasts = edges_other[0], edges_other[1]
    before = jnp.where(core == 0, jnp.concatenate([zero, lasts[:-1]], 0), lasts)
    behind = jnp.where(core == 0, firsts, jnp.concatenate([firsts[1:], zero], 0))
    edge_rows = jnp.concatenate([before, behind], axis=0)
    hidden_parts = []
    flat_rows = channel_rows.reshape(half, model)
    for weights, tap in ((third_own, taps), (third_other, taps_other)):
        up = weights[:, : 2 * PAD]
        main = dot(flat_rows, up).reshape(chips, own, 2 * PAD)
        edge = dot(edge_rows, up).reshape(2, chips, 1, 2 * PAD)
        prev = jnp.concatenate([edge[0], main[:, :-1]], axis=1)
        nxt = jnp.concatenate([main[:, 1:], edge[1]], axis=1)
        kernel = jnp.concatenate([tap[0:3], tap[3:6]], axis=1)
        bias = jnp.concatenate([tap[6], tap[7]], axis=0)
        conv = kernel[0] * prev + kernel[1] * main + kernel[2] * nxt + bias
        hidden = (jax.nn.gelu(conv[..., :PAD]) * conv[..., PAD:]).astype(bf16)
        hidden_parts.append(hidden.reshape(half, PAD))
    channel = sum(
        dot_nt(hidden, weights[:, 2 * PAD :])
        for hidden, weights in zip(hidden_parts, (third_own, third_other))
    )
    channel_pieces = exchanged(channel.astype(bf16).reshape(chips, own, model))
    result = call(
        final_body, shape((own, model)), channel_pieces, after_mix, gain_row(channel_out_gain)
    )
    return result[None]


def solution(mesh):
    fs = mesh.shape["fs"]
    tp = mesh.shape["tp"]
    split = Mesh(
        mesh.devices.reshape(mesh.shape["rep"], fs // 4, 4, tp // 2, 2),
        ("rep", "z", "y", "x", "c"),
    )
    in_specs = (
        P(("rep", "z", "y"), TP, None),
        P(),
        P(FS, TP),
        P(FS, TP),
        P(FS, TP),
        P(FS, TP),
        P(None, TP),
        P(TP, FS),
        P(),
        P(),
        P(FS, TP),
        P(FS, TP),
        P(None, TP),
        P(None, TP),
        P(TP),
        P(TP),
        P(TP, FS),
        P(),
    )
    out_specs = P(("rep", "z", "y"), TP, None)
    return jax.shard_map(layer, mesh=split, in_specs=in_specs, out_specs=out_specs, check_vma=False)
```

profile of v0, /device:TPU:96, one launch (start us, length us, event | category | flops | bytes accessed | tf_op | source)
XLA Modules:
  0.0 243.4 jit_solution(13798900653284451704)
XLA Ops:
  0.0 2.1 shard_map.172
  2.1 19.5 %all_to_all.20 = bf16[4,128,1024]{2,1,0:T(8,128)(2,1)S(1)} all-to-all(bf16[4,128,1024]{2,1,0:T(8,128)(2,1)} %shard_map.172), channel_id=1, replica_groups=mesh['rep'=2,'z'=8,'y'=4,'x'=4,'c'=2] {'x'}, dimensions={0} | all-to-all | bytes 2097152 | tf_op jit(solution)/shard_map/all_to_all | solution.py:61
  21.6 1.9 collective-permute-start
  23.5 1.5 shard_map.173.refs_4_
  25.1 9.1 %collective-permute-start.1 = (bf16[32,2176]{1,0:T(8,128)(2,1)}, bf16[32,2176]{1,0:T(8,128)(2,1)S(1)}, u32[]{:S(2)}, u32[]{:S(2)}) collective-permute-start(bf16[32,2176]{1,0:T(8,128)(2,1)} %shard_map.173.refs_4_), channel_id=1, source_target_pairs={{0,128},{32,160},{64,192},{96,224},{128,256},{160,288},{192,320},{... | collective-permute-start | bytes 417800 | tf_op jit(solution)/shard_map/ppermute | solution.py:53
  34.2 5.9 %collective-permute-start.2 = (bf16[32,2176]{1,0:T(8,128)(2,1)}, bf16[32,2176]{1,0:T(8,128)(2,1)S(1)}, u32[]{:S(2)}, u32[]{:S(2)}) collective-permute-start(bf16[32,2176]{1,0:T(8,128)(2,1)} %shard_map.173.refs_4_), channel_id=1, source_target_pairs={{0,96},{32,128},{64,160},{96,192},{128,224},{160,256},{192,288},{2... | collective-permute-start | bytes 417800 | tf_op jit(solution)/shard_map/ppermute | solution.py:53
  40.1 3.4 %collective-permute-start.3 = (bf16[32,2176]{1,0:T(8,128)(2,1)}, bf16[32,2176]{1,0:T(8,128)(2,1)S(1)}, u32[]{:S(2)}, u32[]{:S(2)}) collective-permute-start(bf16[32,2176]{1,0:T(8,128)(2,1)} %shard_map.173.refs_4_), channel_id=1, source_target_pairs={{0,64},{32,96},{64,128},{96,160},{128,192},{160,224},{192,256},{22... | collective-permute-start | bytes 417800 | tf_op jit(solution)/shard_map/ppermute | solution.py:53
  43.5 2.9 %collective-permute-start.4 = (bf16[32,2176]{1,0:T(8,128)(2,1)}, bf16[32,2176]{1,0:T(8,128)(2,1)S(1)}, u32[]{:S(2)}, u32[]{:S(2)}) collective-permute-start(bf16[32,2176]{1,0:T(8,128)(2,1)} %shard_map.173.refs_4_), channel_id=1, source_target_pairs={{0,32},{32,64},{64,96},{96,128},{128,160},{160,192},{192,224},{224... | collective-permute-start | bytes 417800 | tf_op jit(solution)/shard_map/ppermute | solution.py:53
  46.5 8.9 %collective-permute-start.5 = (bf16[32,2176]{1,0:T(8,128)(2,1)}, bf16[32,2176]{1,0:T(8,128)(2,1)S(1)}, u32[]{:S(2)}, u32[]{:S(2)}) collective-permute-start(bf16[32,2176]{1,0:T(8,128)(2,1)} %shard_map.173.refs_4_), channel_id=1, source_target_pairs={{0,480},{32,0},{64,32},{96,64},{128,96},{160,128},{192,160},{224,1... | collective-permute-start | bytes 417800 | tf_op jit(solution)/shard_map/ppermute | solution.py:53
  55.4 2.7 %collective-permute-done.2.refs_1_ = bf16[32,2176]{1,0:T(8,128)(2,1)S(1)} collective-permute-done((bf16[32,2176]{1,0:T(8,128)(2,1)}, bf16[32,2176]{1,0:T(8,128)(2,1)S(1)}, u32[]{:S(2)}, u32[]{:S(2)}) %collective-permute-start.2) | collective-permute-done | bytes 139296 | tf_op jit(solution)/shard_map/ppermute | solution.py:53
  58.1 1.9 collective-permute-start.6
  61.5 4.3 %collective-permute-start.7 = (bf16[32,2176]{1,0:T(8,128)(2,1)}, bf16[32,2176]{1,0:T(8,128)(2,1)S(1)}, u32[]{:S(2)}, u32[]{:S(2)}) collective-permute-start(bf16[32,2176]{1,0:T(8,128)(2,1)} %shard_map.173.refs_4_), channel_id=1, source_target_pairs={{0,416},{32,448},{64,480},{96,0},{128,32},{160,64},{192,96},{224,1... | collective-permute-start | bytes 417800 | tf_op jit(solution)/shard_map/ppermute | solution.py:53
  65.9 5.3 %collective-permute-done.6.refs_6_ = bf16[32,2176]{1,0:T(8,128)(2,1)S(1)} collective-permute-done((bf16[32,2176]{1,0:T(8,128)(2,1)}, bf16[32,2176]{1,0:T(8,128)(2,1)S(1)}, u32[]{:S(2)}, u32[]{:S(2)}) %collective-permute-start.6) | collective-permute-done | bytes 139296 | tf_op jit(solution)/shard_map/ppermute | solution.py:53
  71.1 10.1 %collective-permute-done.7.refs_7_ = bf16[32,2176]{1,0:T(8,128)(2,1)S(1)} collective-permute-done((bf16[32,2176]{1,0:T(8,128)(2,1)}, bf16[32,2176]{1,0:T(8,128)(2,1)S(1)}, u32[]{:S(2)}, u32[]{:S(2)}) %collective-permute-start.7) | collective-permute-done | bytes 139296 | tf_op jit(solution)/shard_map/ppermute | solution.py:53
  81.9 2.4 shard_map.174
  84.3 3.5 %collective-permute-start.11 = (bf16[8,32,256]{2,1,0:T(8,128)(2,1)}, bf16[8,32,256]{2,1,0:T(8,128)(2,1)S(1)}, u32[]{:S(2)}, u32[]{:S(2)}) collective-permute-start(bf16[8,32,256]{2,1,0:T(8,128)(2,1)} %get-tuple-element.11.refs_0_), channel_id=1, source_target_pairs={{0,8},{8,16},{16,24},{24,0},{1,9},{9,17},{17,25},{25,1},{2,10},{10... | collective-permute-start | bytes 393224 | tf_op jit(solution)/shard_map/ppermute | solution.py:53
  87.8 3.6 %collective-permute-start.10 = (bf16[8,32,768]{2,1,0:T(8,128)(2,1)}, bf16[8,32,768]{2,1,0:T(8,128)(2,1)S(1)}, u32[]{:S(2)}, u32[]{:S(2)}) collective-permute-start(bf16[8,32,768]{2,1,0:T(8,128)(2,1)} %get-tuple-element.10.refs_0_), channel_id=1, source_target_pairs={{0,24},{8,0},{16,8},{24,16},{1,25},{9,1},{17,9},{25,17},{2,26},{10... | collective-permute-start | bytes 1179656 | tf_op jit(solution)/shard_map/ppermute | solution.py:53
  91.4 2.3 collective-permute-start.8
  93.6 4.8 %collective-permute-start.9 = (bf16[8,32,768]{2,1,0:T(8,128)(2,1)}, bf16[8,32,768]{2,1,0:T(8,128)(2,1)S(1)}, u32[]{:S(2)}, u32[]{:S(2)}) collective-permute-start(bf16[8,32,768]{2,1,0:T(8,128)(2,1)} %get-tuple-element.10.refs_0_), channel_id=1, source_target_pairs={{0,16},{8,24},{16,0},{24,8},{1,17},{9,25},{17,1},{25,9},{2,18},{10... | collective-permute-start | bytes 1179656 | tf_op jit(solution)/shard_map/ppermute | solution.py:53
  98.5 2.5 %collective-permute-start.12 = (bf16[8,32,256]{2,1,0:T(8,128)(2,1)}, bf16[8,32,256]{2,1,0:T(8,128)(2,1)S(1)}, u32[]{:S(2)}, u32[]{:S(2)}) collective-permute-start(bf16[8,32,256]{2,1,0:T(8,128)(2,1)} %get-tuple-element.11.refs_0_), channel_id=1, source_target_pairs={{0,16},{8,24},{16,0},{24,8},{1,17},{9,25},{17,1},{25,9},{2,18},{10... | collective-permute-start | bytes 393224 | tf_op jit(solution)/shard_map/ppermute | solution.py:53
  101.7 14.8 %collective-permute-done.12.refs_2_ = bf16[8,32,256]{2,1,0:T(8,128)(2,1)S(1)} collective-permute-done((bf16[8,32,256]{2,1,0:T(8,128)(2,1)}, bf16[8,32,256]{2,1,0:T(8,128)(2,1)S(1)}, u32[]{:S(2)}, u32[]{:S(2)}) %collective-permute-start.12) | collective-permute-done | bytes 131104 | tf_op jit(solution)/shard_map/ppermute | solution.py:53
  116.5 1.9 collective-permute-start.13
  119.8 3.8 %collective-permute-done.13.refs_3_ = bf16[8,32,256]{2,1,0:T(8,128)(2,1)S(1)} collective-permute-done((bf16[8,32,256]{2,1,0:T(8,128)(2,1)}, bf16[8,32,256]{2,1,0:T(8,128)(2,1)S(1)}, u32[]{:S(2)}, u32[]{:S(2)}) %collective-permute-start.13) | collective-permute-done | bytes 131104 | tf_op jit(solution)/shard_map/ppermute | solution.py:53
  124.2 1.9 shard_map.176
  126.1 1.9 collective-permute-start.15
  129.7 2.6 %shard_map.175 = bf16[8,4,32,768]{3,2,1,0:T(8,128)(2,1)} custom-call(s32[1]{0:T(128)} %bitcast.3.index, bf16[8,32,768]{2,1,0:T(8,128)(2,1)} %get-tuple-element.10.refs_0_, bf16[8,32,768]{2,1,0:T(8,128)(2,1)} %copy-done.8, bf16[8,32,768]{2,1,0:T(8,128)(2,1)} %copy-done.9, bf16[8,32,768]{2,1,0:T(8,128)(2,1)} %copy-done.7), custom_call_target="tpu_custom_call" | custom-call | flops 1048576 | bytes 1048576 | tf_op jit(solution)/shard_map/pallas_call | solution.py:36
  132.4 3.6 %fusion = f32[1024,768]{0,1:T(8,128)S(1)} fusion(bf16[1024,768]{1,0:T(8,128)(2,1)} %bitcast.65, bf16[512,1024]{1,0:T(8,128)(2,1)} %collective-permute-done, bf16[512,1024]{1,0:T(8,128)(2,1)S(1)} %bitcast.71), kind=kOutput, calls=%fused_computation.2 | convolution fusion | flops 1614807040 | bytes 6815744 | tf_op jit(solution)/shard_map/dot_general | solution.py:141
  137.6 3.3 %fusion.90 = (f32[1024]{0:T(1024)S(1)}, f32[1024,256]{0,1:T(8,128)S(1)}) fusion(f32[1024,768]{0,1:T(8,128)} %copy-done.3, f32[]{:T(128)S(6)} %neg.43, f32[]{:T(128)S(6)} %neg.38, s32[1024]{0:T(1024)S(1)} %get-tuple-element.48, f32[1024,64]{0,1:T(8,128)S(1)} %get-tuple-element.27, f32[1024,64]{0,1:T(8,128)S(1)} %get-tuple-element.26, ...), kind=kOutput, calls=%fused_computation.131 | convolution fusion | flops 815922176 | bytes 2371592 | tf_op jit(solution)/shard_map/dot_general | solution.py:141
  141.1 1.6 multiply_convert_fusion.1
  142.8 2.5 %collective-permute-start.14 = (bf16[512,256]{0,1:T(8,128)(2,1)S(1)}, bf16[512,256]{0,1:T(8,128)(2,1)S(1)}, u32[]{:S(2)}, u32[]{:S(2)}) collective-permute-start(bf16[512,256]{0,1:T(8,128)(2,1)S(1)} %slice.214), channel_id=1, source_target_pairs={{0,1},{1,0},{2,3},{3,2},{4,5},{5,4},{6,7},{7,6},{8,9},{9,8},{10,11... | collective-permute-start | bytes 786440 | tf_op jit(solution)/shard_map/ppermute | solution.py:57
  145.3 1.9 collective-permute-start.17
  147.3 4.6 %collective-permute-start.18 = (bf16[8,32,1152]{2,1,0:T(8,128)(2,1)S(1)}, bf16[8,32,1152]{2,1,0:T(8,128)(2,1)S(1)}, u32[]{:S(2)}, u32[]{:S(2)}) collective-permute-start(bf16[8,32,1152]{2,1,0:T(8,128)(2,1)S(1)} %copy-done.4), channel_id=1, source_target_pairs={{0,16},{8,24},{16,0},{24,8},{1,17},{9,25},{17,1},{25,9},{2,18},{10... | collective-permute-start | bytes 1769480 | tf_op jit(solution)/shard_map/ppermute | solution.py:53
  151.9 2.5 %collective-permute-start.19 = (bf16[8,32,1152]{2,1,0:T(8,128)(2,1)S(1)}, bf16[8,32,1152]{2,1,0:T(8,128)(2,1)}, u32[]{:S(2)}, u32[]{:S(2)}) collective-permute-start(bf16[8,32,1152]{2,1,0:T(8,128)(2,1)S(1)} %copy-done.4), channel_id=1, source_target_pairs={{0,24},{8,0},{16,8},{24,16},{1,25},{9,1},{17,9},{25,17},{2,26},{10... | collective-permute-start | bytes 1769480 | tf_op jit(solution)/shard_map/ppermute | solution.py:53
  156.4 3.5 %all-to-all-start.1 = ((bf16[4,128,1024]{2,1,0:T(8,128)(2,1)}), bf16[4,128,1024]{2,1,0:T(8,128)(2,1)S(1)}, u32[]{:S(2)}, u32[]{:S(2)}) async-start(bf16[4,128,1024]{2,1,0:T(8,128)(2,1)} %bitcast.13), calls=%async_computation.1 | async-start | bytes 2097152 | tf_op jit(solution)/shard_map/all_to_all | solution.py:61
  160.0 16.3 %collective-permute-done.17.refs_1_ = bf16[8,32,1152]{2,1,0:T(8,128)(2,1)S(1)} collective-permute-done((bf16[8,32,1152]{2,1,0:T(8,128)(2,1)S(1)}, bf16[8,32,1152]{2,1,0:T(8,128)(2,1)S(1)}, u32[]{:S(2)}, u32[]{:S(2)}) %collective-permute-start.17) | collective-permute-done | bytes 589856 | tf_op jit(solution)/shard_map/ppermute | solution.py:53
  176.3 2.6 %collective-permute-done.19.refs_3_ = bf16[8,32,1152]{2,1,0:T(8,128)(2,1)} collective-permute-done((bf16[8,32,1152]{2,1,0:T(8,128)(2,1)S(1)}, bf16[8,32,1152]{2,1,0:T(8,128)(2,1)}, u32[]{:S(2)}, u32[]{:S(2)}) %collective-permute-start.19) | collective-permute-done | bytes 589856 | tf_op jit(solution)/shard_map/ppermute | solution.py:53
  179.0 3.2 %shard_map.178 = bf16[8,4,32,1152]{3,2,1,0:T(8,128)(2,1)} custom-call(s32[1]{0:T(128)} %bitcast.3.index, bf16[8,32,1152]{2,1,0:T(8,128)(2,1)} %get-tuple-element.13.refs_0_, bf16[8,32,1152]{2,1,0:T(8,128)(2,1)} %copy-done.5, bf16[8,32,1152]{2,1,0:T(8,128)(2,1)} %copy-done.6, bf16[8,32,1152]{2,1,0:T(8,128)(2,1)} %collective-permute-done.19.refs_3_), custom_call_target="tpu_custom_call" | custom-call | flops 1048576 | bytes 1048576 | tf_op jit(solution)/shard_map/pallas_call | solution.py:36
  182.2 1.9 collective-permute-start.21
  184.2 2.4 collective-permute-start.20
  187.6 2.8 %shard_map.177 = (bf16[128,1024]{1,0:T(8,128)(2,1)}, bf16[4,128,1024]{2,1,0:T(8,128)(2,1)}) custom-call(bf16[4,128,1024]{2,1,0:T(8,128)(2,1)} %copy-done.1, bf16[128,1024]{1,0:T(8,128)(2,1)} %bitcast.69, f32[1,1024]{1,0:T(1,128)} %bitcast.75, f32[1,1024]{1,0:T(1,128)} %bitcast.76), custom_call_target="tpu_custom_call" | custom-call | flops 1048576 | bytes 1048576 | tf_op jit(solution)/shard_map/pallas_call | solution.py:36
  190.5 3.5 %all-to-all-start.2 = ((bf16[4,128,1024]{2,1,0:T(8,128)(2,1)}), bf16[4,128,1024]{2,1,0:T(8,128)(2,1)S(1)}, u32[]{:S(2)}, u32[]{:S(2)}) async-start(bf16[4,128,1024]{2,1,0:T(8,128)(2,1)} %get-tuple-element.12), calls=%async_computation.2 | async-start | bytes 2097152 | tf_op jit(solution)/shard_map/all_to_all | solution.py:61
  194.2 15.3 %all-to-all-done.2 = bf16[4,128,1024]{2,1,0:T(8,128)(2,1)S(1)} async-done(((bf16[4,128,1024]{2,1,0:T(8,128)(2,1)}), bf16[4,128,1024]{2,1,0:T(8,128)(2,1)S(1)}, u32[]{:S(2)}, u32[]{:S(2)}) %all-to-all-start.2) | async-done | bytes 1048608 | tf_op jit(solution)/shard_map/all_to_all | solution.py:61
  209.6 2.1 collective-permute-start.16
  213.0 2.4 fusion.10
  216.8 1.7 fusion.15
  219.3 1.9 fusion.39
  221.9 19.2 %all_to_all.21.pieces = bf16[4,128,1024]{2,1,0:T(8,128)(2,1)} all-to-all(bf16[4,128,1024]{2,1,0:T(8,128)(2,1)S(1)} %bitcast.62), channel_id=1, replica_groups=mesh['rep'=2,'z'=8,'y'=4,'x'=4,'c'=2] {'x'}, dimensions={0} | all-to-all | bytes 2097152 | tf_op jit(solution)/shard_map/all_to_all | solution.py:61
  241.1 2.3 shard_map.179
  (109 shorter events, 14.4 us)
Async XLA Ops:
  2.1 99.0 %copy-start.24 = (f32[2,1]{0,1:T(1,128)S(1)}, f32[2,1]{0,1:T(1,128)}, u32[]{:S(2)}) copy-start(f32[2,1]{0,1:T(1,128)} %param.24) | copy-start | bytes 28
  21.6 110.8 %collective-permute-start = (bf16[512,1024]{1,0:T(8,128)(2,1)S(1)}, bf16[512,1024]{1,0:T(8,128)(2,1)}, u32[]{:S(2)}, u32[]{:S(2)}) collective-permute-start(bf16[512,1024]{1,0:T(8,128)(2,1)S(1)} %bitcast.70), channel_id=1, source_target_pairs={{0,1},{1,0},{2,3},{3,2},{4,5},{5,4},{6,7},{7,6},{8,9},{9,8},{10,11... | collective-permute-start | bytes 3145736 | tf_op jit(solution)/shard_map/ppermute | solution.py:57
  25.1 21.4 %collective-permute-start.1 = (bf16[32,2176]{1,0:T(8,128)(2,1)}, bf16[32,2176]{1,0:T(8,128)(2,1)S(1)}, u32[]{:S(2)}, u32[]{:S(2)}) collective-permute-start(bf16[32,2176]{1,0:T(8,128)(2,1)} %shard_map.173.refs_4_), channel_id=1, source_target_pairs={{0,128},{32,160},{64,192},{96,224},{128,256},{160,288},{192,320},{... | collective-permute-start | bytes 417800 | tf_op jit(solution)/shard_map/ppermute | solution.py:53
  34.2 23.9 %collective-permute-start.2 = (bf16[32,2176]{1,0:T(8,128)(2,1)}, bf16[32,2176]{1,0:T(8,128)(2,1)S(1)}, u32[]{:S(2)}, u32[]{:S(2)}) collective-permute-start(bf16[32,2176]{1,0:T(8,128)(2,1)} %shard_map.173.refs_4_), channel_id=1, source_target_pairs={{0,96},{32,128},{64,160},{96,192},{128,224},{160,256},{192,288},{2... | collective-permute-start | bytes 417800 | tf_op jit(solution)/shard_map/ppermute | solution.py:53
  40.1 21.4 %collective-permute-start.3 = (bf16[32,2176]{1,0:T(8,128)(2,1)}, bf16[32,2176]{1,0:T(8,128)(2,1)S(1)}, u32[]{:S(2)}, u32[]{:S(2)}) collective-permute-start(bf16[32,2176]{1,0:T(8,128)(2,1)} %shard_map.173.refs_4_), channel_id=1, source_target_pairs={{0,64},{32,96},{64,128},{96,160},{128,192},{160,224},{192,256},{22... | collective-permute-start | bytes 417800 | tf_op jit(solution)/shard_map/ppermute | solution.py:53
  43.5 22.3 %collective-permute-start.4 = (bf16[32,2176]{1,0:T(8,128)(2,1)}, bf16[32,2176]{1,0:T(8,128)(2,1)S(1)}, u32[]{:S(2)}, u32[]{:S(2)}) collective-permute-start(bf16[32,2176]{1,0:T(8,128)(2,1)} %shard_map.173.refs_4_), channel_id=1, source_target_pairs={{0,32},{32,64},{64,96},{96,128},{128,160},{160,192},{192,224},{224... | collective-permute-start | bytes 417800 | tf_op jit(solution)/shard_map/ppermute | solution.py:53
  46.4 34.8 %copy-start.10 = (bf16[32,2176]{1,0:T(8,128)(2,1)}, bf16[32,2176]{1,0:T(8,128)(2,1)S(1)}, u32[]{:S(2)}) copy-start(bf16[32,2176]{1,0:T(8,128)(2,1)S(1)} %collective-permute-done.1.refs_0_) | copy-start | bytes 417796
  46.5 19.4 %collective-permute-start.5 = (bf16[32,2176]{1,0:T(8,128)(2,1)}, bf16[32,2176]{1,0:T(8,128)(2,1)S(1)}, u32[]{:S(2)}, u32[]{:S(2)}) collective-permute-start(bf16[32,2176]{1,0:T(8,128)(2,1)} %shard_map.173.refs_4_), channel_id=1, source_target_pairs={{0,480},{32,0},{64,32},{96,64},{128,96},{160,128},{192,160},{224,1... | collective-permute-start | bytes 417800 | tf_op jit(solution)/shard_map/ppermute | solution.py:53
  58.1 23.2 %copy-start.11 = (bf16[32,2176]{1,0:T(8,128)(2,1)}, bf16[32,2176]{1,0:T(8,128)(2,1)S(1)}, u32[]{:S(2)}) copy-start(bf16[32,2176]{1,0:T(8,128)(2,1)S(1)} %collective-permute-done.2.refs_1_) | copy-start | bytes 417796
  58.1 13.1 %collective-permute-start.6 = (bf16[32,2176]{1,0:T(8,128)(2,1)}, bf16[32,2176]{1,0:T(8,128)(2,1)S(1)}, u32[]{:S(2)}, u32[]{:S(2)}) collective-permute-start(bf16[32,2176]{1,0:T(8,128)(2,1)} %shard_map.173.refs_4_), channel_id=1, source_target_pairs={{0,448},{32,480},{64,0},{96,32},{128,64},{160,96},{192,128},{224,1... | collective-permute-start | bytes 417800 | tf_op jit(solution)/shard_map/ppermute | solution.py:53
  61.5 19.8 %copy-start.12 = (bf16[32,2176]{1,0:T(8,128)(2,1)}, bf16[32,2176]{1,0:T(8,128)(2,1)S(1)}, u32[]{:S(2)}) copy-start(bf16[32,2176]{1,0:T(8,128)(2,1)S(1)} %collective-permute-done.3.refs_2_) | copy-start | bytes 417796
  61.5 19.8 %collective-permute-start.7 = (bf16[32,2176]{1,0:T(8,128)(2,1)}, bf16[32,2176]{1,0:T(8,128)(2,1)S(1)}, u32[]{:S(2)}, u32[]{:S(2)}) collective-permute-start(bf16[32,2176]{1,0:T(8,128)(2,1)} %shard_map.173.refs_4_), channel_id=1, source_target_pairs={{0,416},{32,448},{64,480},{96,0},{128,32},{160,64},{192,96},{224,1... | collective-permute-start | bytes 417800 | tf_op jit(solution)/shard_map/ppermute | solution.py:53
  65.8 15.4 %copy-start.13 = (bf16[32,2176]{1,0:T(8,128)(2,1)}, bf16[32,2176]{1,0:T(8,128)(2,1)S(1)}, u32[]{:S(2)}) copy-start(bf16[32,2176]{1,0:T(8,128)(2,1)S(1)} %collective-permute-done.4.refs_3_) | copy-start | bytes 417796
  65.9 15.4 %copy-start.14 = (bf16[32,2176]{1,0:T(8,128)(2,1)}, bf16[32,2176]{1,0:T(8,128)(2,1)S(1)}, u32[]{:S(2)}) copy-start(bf16[32,2176]{1,0:T(8,128)(2,1)S(1)} %collective-permute-done.5.refs_5_) | copy-start | bytes 417796
  71.1 10.2 %copy-start.15 = (bf16[32,2176]{1,0:T(8,128)(2,1)}, bf16[32,2176]{1,0:T(8,128)(2,1)S(1)}, u32[]{:S(2)}) copy-start(bf16[32,2176]{1,0:T(8,128)(2,1)S(1)} %collective-permute-done.6.refs_6_) | copy-start | bytes 417796
  84.3 14.2 %collective-permute-start.11 = (bf16[8,32,256]{2,1,0:T(8,128)(2,1)}, bf16[8,32,256]{2,1,0:T(8,128)(2,1)S(1)}, u32[]{:S(2)}, u32[]{:S(2)}) collective-permute-start(bf16[8,32,256]{2,1,0:T(8,128)(2,1)} %get-tuple-element.11.refs_0_), channel_id=1, source_target_pairs={{0,8},{8,16},{16,24},{24,0},{1,9},{9,17},{17,25},{25,1},{2,10},{10... | collective-permute-start | bytes 393224 | tf_op jit(solution)/shard_map/ppermute | solution.py:53
  87.8 40.3 %collective-permute-start.10 = (bf16[8,32,768]{2,1,0:T(8,128)(2,1)}, bf16[8,32,768]{2,1,0:T(8,128)(2,1)S(1)}, u32[]{:S(2)}, u32[]{:S(2)}) collective-permute-start(bf16[8,32,768]{2,1,0:T(8,128)(2,1)} %get-tuple-element.10.refs_0_), channel_id=1, source_target_pairs={{0,24},{8,0},{16,8},{24,16},{1,25},{9,1},{17,9},{25,17},{2,26},{10... | collective-permute-start | bytes 1179656 | tf_op jit(solution)/shard_map/ppermute | solution.py:53
  91.4 36.7 %collective-permute-start.8 = (bf16[8,32,768]{2,1,0:T(8,128)(2,1)}, bf16[8,32,768]{2,1,0:T(8,128)(2,1)S(1)}, u32[]{:S(2)}, u32[]{:S(2)}) collective-permute-start(bf16[8,32,768]{2,1,0:T(8,128)(2,1)} %get-tuple-element.10.refs_0_), channel_id=1, source_target_pairs={{0,8},{8,16},{16,24},{24,0},{1,9},{9,17},{17,25},{25,1},{2,10},{10... | collective-permute-start | bytes 1179656 | tf_op jit(solution)/shard_map/ppermute | solution.py:53
  93.6 34.4 %collective-permute-start.9 = (bf16[8,32,768]{2,1,0:T(8,128)(2,1)}, bf16[8,32,768]{2,1,0:T(8,128)(2,1)S(1)}, u32[]{:S(2)}, u32[]{:S(2)}) collective-permute-start(bf16[8,32,768]{2,1,0:T(8,128)(2,1)} %get-tuple-element.10.refs_0_), channel_id=1, source_target_pairs={{0,16},{8,24},{16,0},{24,8},{1,17},{9,25},{17,1},{25,9},{2,18},{10... | collective-permute-start | bytes 1179656 | tf_op jit(solution)/shard_map/ppermute | solution.py:53
  98.5 25.1 %copy-start.17 = (bf16[8,32,256]{2,1,0:T(8,128)(2,1)}, bf16[8,32,256]{2,1,0:T(8,128)(2,1)S(1)}, u32[]{:S(2)}) copy-start(bf16[8,32,256]{2,1,0:T(8,128)(2,1)S(1)} %collective-permute-done.11.refs_1_) | copy-start | bytes 393220
  98.5 18.0 %collective-permute-start.12 = (bf16[8,32,256]{2,1,0:T(8,128)(2,1)}, bf16[8,32,256]{2,1,0:T(8,128)(2,1)S(1)}, u32[]{:S(2)}, u32[]{:S(2)}) collective-permute-start(bf16[8,32,256]{2,1,0:T(8,128)(2,1)} %get-tuple-element.11.refs_0_), channel_id=1, source_target_pairs={{0,16},{8,24},{16,0},{24,8},{1,17},{9,25},{17,1},{25,9},{2,18},{10... | collective-permute-start | bytes 393224 | tf_op jit(solution)/shard_map/ppermute | solution.py:53
  116.5 7.1 %copy-start.18 = (bf16[8,32,256]{2,1,0:T(8,128)(2,1)}, bf16[8,32,256]{2,1,0:T(8,128)(2,1)S(1)}, u32[]{:S(2)}) copy-start(bf16[8,32,256]{2,1,0:T(8,128)(2,1)S(1)} %collective-permute-done.12.refs_2_) | copy-start | bytes 393220
  116.5 7.1 %collective-permute-start.13 = (bf16[8,32,256]{2,1,0:T(8,128)(2,1)}, bf16[8,32,256]{2,1,0:T(8,128)(2,1)S(1)}, u32[]{:S(2)}, u32[]{:S(2)}) collective-permute-start(bf16[8,32,256]{2,1,0:T(8,128)(2,1)} %get-tuple-element.11.refs_0_), channel_id=1, source_target_pairs={{0,24},{8,0},{16,8},{24,16},{1,25},{9,1},{17,9},{25,17},{2,26},{10... | collective-permute-start | bytes 393224 | tf_op jit(solution)/shard_map/ppermute | solution.py:53
  123.5 0.7 copy-start.19
  126.1 28.3 %collective-permute-start.15 = (bf16[1024,256]{1,0:T(8,128)(2,1)}, bf16[1024,256]{1,0:T(8,128)(2,1)S(1)}, u32[]{:S(2)}, u32[]{:S(2)}) collective-permute-start(bf16[1024,256]{1,0:T(8,128)(2,1)} %bitcast.63), channel_id=1, source_target_pairs={{0,1},{1,0},{2,3},{3,2},{4,5},{5,4},{6,7},{7,6},{8,9},{9,8},{10,11... | collective-permute-start | bytes 1572872 | tf_op jit(solution)/shard_map/ppermute | solution.py:57
  128.0 0.8 copy-start.7
  128.1 0.9 copy-start.8
  129.0 0.8 copy-start.9
  136.0 1.6 copy-start.3
  141.1 4.2 %copy-start.4 = (bf16[8,32,1152]{2,1,0:T(8,128)(2,1)S(1)}, bf16[8,32,1152]{2,1,0:T(8,128)(2,1)}, u32[]{:S(2)}) copy-start(bf16[8,32,1152]{2,1,0:T(8,128)(2,1)} %get-tuple-element.13.refs_0_) | copy-start | bytes 1769476
  142.8 12.2 %copy-start.2 = (bf16[8,4,32,256]{3,2,1,0:T(8,128)(2,1)S(1)}, bf16[8,4,32,256]{3,2,1,0:T(8,128)(2,1)}, u32[]{:S(2)}) copy-start(bf16[8,4,32,256]{3,2,1,0:T(8,128)(2,1)} %shard_map.176) | copy-start | bytes 1572868
  142.8 11.6 %collective-permute-start.14 = (bf16[512,256]{0,1:T(8,128)(2,1)S(1)}, bf16[512,256]{0,1:T(8,128)(2,1)S(1)}, u32[]{:S(2)}, u32[]{:S(2)}) collective-permute-start(bf16[512,256]{0,1:T(8,128)(2,1)S(1)} %slice.214), channel_id=1, source_target_pairs={{0,1},{1,0},{2,3},{3,2},{4,5},{5,4},{6,7},{7,6},{8,9},{9,8},{10,11... | collective-permute-start | bytes 786440 | tf_op jit(solution)/shard_map/ppermute | solution.py:57
  145.3 31.0 %collective-permute-start.17 = (bf16[8,32,1152]{2,1,0:T(8,128)(2,1)S(1)}, bf16[8,32,1152]{2,1,0:T(8,128)(2,1)S(1)}, u32[]{:S(2)}, u32[]{:S(2)}) collective-permute-start(bf16[8,32,1152]{2,1,0:T(8,128)(2,1)S(1)} %copy-done.4), channel_id=1, source_target_pairs={{0,8},{8,16},{16,24},{24,0},{1,9},{9,17},{17,25},{25,1},{2,10},{10... | collective-permute-start | bytes 1769480 | tf_op jit(solution)/shard_map/ppermute | solution.py:53
  147.3 29.1 %collective-permute-start.18 = (bf16[8,32,1152]{2,1,0:T(8,128)(2,1)S(1)}, bf16[8,32,1152]{2,1,0:T(8,128)(2,1)S(1)}, u32[]{:S(2)}, u32[]{:S(2)}) collective-permute-start(bf16[8,32,1152]{2,1,0:T(8,128)(2,1)S(1)} %copy-done.4), channel_id=1, source_target_pairs={{0,16},{8,24},{16,0},{24,8},{1,17},{9,25},{17,1},{25,9},{2,18},{10... | collective-permute-start | bytes 1769480 | tf_op jit(solution)/shard_map/ppermute | solution.py:53
  151.9 27.1 %collective-permute-start.19 = (bf16[8,32,1152]{2,1,0:T(8,128)(2,1)S(1)}, bf16[8,32,1152]{2,1,0:T(8,128)(2,1)}, u32[]{:S(2)}, u32[]{:S(2)}) collective-permute-start(bf16[8,32,1152]{2,1,0:T(8,128)(2,1)S(1)} %copy-done.4), channel_id=1, source_target_pairs={{0,24},{8,0},{16,8},{24,16},{1,25},{9,1},{17,9},{25,17},{2,26},{10... | collective-permute-start | bytes 1769480 | tf_op jit(solution)/shard_map/ppermute | solution.py:53
  156.4 30.2 %all-to-all-start.1 = ((bf16[4,128,1024]{2,1,0:T(8,128)(2,1)}), bf16[4,128,1024]{2,1,0:T(8,128)(2,1)S(1)}, u32[]{:S(2)}, u32[]{:S(2)}) async-start(bf16[4,128,1024]{2,1,0:T(8,128)(2,1)} %bitcast.13), calls=%async_computation.1 | async-start | bytes 2097152 | tf_op jit(solution)/shard_map/all_to_all | solution.py:61
  160.0 24.1 %copy-start.22 = (f32[352]{0:T(512)S(1)}, f32[352]{0:T(512)}, u32[]{:S(2)}) copy-start(f32[352]{0:T(512)} %param.32) | copy-start | bytes 4228
  160.0 24.1 %copy-start.23 = (f32[352]{0:T(512)S(1)}, f32[352]{0:T(512)}, u32[]{:S(2)}) copy-start(f32[352]{0:T(512)} %param.33) | copy-start | bytes 4228
  160.0 24.1 %copy-start.20 = (f32[3,352]{1,0:T(4,128)S(1)}, f32[3,352]{1,0:T(4,128)}, u32[]{:S(2)}) copy-start(f32[3,352]{1,0:T(4,128)} %param.31) | copy-start | bytes 12676
  160.0 24.1 %copy-start.21 = (f32[3,352]{1,0:T(4,128)S(1)}, f32[3,352]{1,0:T(4,128)}, u32[]{:S(2)}) copy-start(f32[3,352]{1,0:T(4,128)} %param.30) | copy-start | bytes 12676
  176.3 2.6 %copy-start.5 = (bf16[8,32,1152]{2,1,0:T(8,128)(2,1)}, bf16[8,32,1152]{2,1,0:T(8,128)(2,1)S(1)}, u32[]{:S(2)}) copy-start(bf16[8,32,1152]{2,1,0:T(8,128)(2,1)S(1)} %collective-permute-done.17.refs_1_) | copy-start | bytes 1769476
  176.3 2.6 %copy-start.6 = (bf16[8,32,1152]{2,1,0:T(8,128)(2,1)}, bf16[8,32,1152]{2,1,0:T(8,128)(2,1)S(1)}, u32[]{:S(2)}) copy-start(bf16[8,32,1152]{2,1,0:T(8,128)(2,1)S(1)} %collective-permute-done.18.refs_2_) | copy-start | bytes 1769476
  182.2 30.8 %collective-permute-start.21 = (bf16[1024,1152]{1,0:T(8,128)(2,1)}, bf16[1024,1152]{1,0:T(8,128)(2,1)}, u32[]{:S(2)}, u32[]{:S(2)}) collective-permute-start(bf16[1024,1152]{1,0:T(8,128)(2,1)} %bitcast.58), channel_id=1, source_target_pairs={{0,1},{1,0},{2,3},{3,2},{4,5},{5,4},{6,7},{7,6},{8,9},{9,8},{10,11... | collective-permute-start | bytes 7077896 | tf_op jit(solution)/shard_map/ppermute | solution.py:57
  184.2 9.9 %collective-permute-start.20 = (f32[8,384]{1,0:T(8,128)S(1)}, f32[8,384]{1,0:T(8,128)S(1)}, u32[]{:S(2)}, u32[]{:S(2)}) collective-permute-start(f32[8,384]{1,0:T(8,128)S(1)} %select_maximum_fusion), channel_id=1, source_target_pairs={{0,1},{1,0},{2,3},{3,2},{4,5},{5,4},{6,7},{7,6},{8,9},{9,8},{10,11... | collective-permute-start | bytes 36872 | tf_op jit(solution)/shard_map/ppermute | solution.py:57
  186.6 1.0 copy-start.1
  187.6 24.1 %copy-start = (bf16[8,4,32,1152]{3,2,1,0:T(8,128)(2,1)S(1)}, bf16[8,4,32,1152]{3,2,1,0:T(8,128)(2,1)}, u32[]{:S(2)}) copy-start(bf16[8,4,32,1152]{3,2,1,0:T(8,128)(2,1)} %shard_map.178) | copy-start | bytes 7077892
  190.5 19.0 %all-to-all-start.2 = ((bf16[4,128,1024]{2,1,0:T(8,128)(2,1)}), bf16[4,128,1024]{2,1,0:T(8,128)(2,1)S(1)}, u32[]{:S(2)}, u32[]{:S(2)}) async-start(bf16[4,128,1024]{2,1,0:T(8,128)(2,1)} %get-tuple-element.12), calls=%async_computation.2 | async-start | bytes 2097152 | tf_op jit(solution)/shard_map/all_to_all | solution.py:61
  209.6 6.1 %collective-permute-start.16 = (bf16[2,4,1024]{2,1,0:T(4,128)(2,1)S(1)}, bf16[2,4,1024]{2,1,0:T(4,128)(2,1)S(1)}, u32[]{:S(2)}, u32[]{:S(2)}) collective-permute-start(bf16[2,4,1024]{2,1,0:T(4,128)(2,1)S(1)} %pad_maximum_fusion), channel_id=1, source_target_pairs={{0,1},{1,0},{2,3},{3,2},{4,5},{5,4},{6,7},{7,6},{8,9},{9,8},{10,11... | collective-permute-start | bytes 49160 | tf_op jit(solution)/shard_map/ppermute | solution.py:57
  (1 other events, 0.6 us)
where the time goes:
time: 245 us; the launch traced here: 243 us
  starting transfers between devices  83.9 us (34%)
  waiting for transfers between devices  72.5 us (30%)
  blocking collectives  38.7 us (16%)
  Pallas kernels  18.9 us (8%)
  matrix products  17 us (7%)
  local copies, waits for them, and re-layouts  5.7 us (2%)
  other arithmetic  4.68 us (2%)
    ppermute x16, starting transfers between devices, permuted(): lax.ppermute(value, axes, [(i, (i + shift) % size) for i in range(size)])  64.1 us
    ppermute x16, waiting for transfers between devices, permuted(): lax.ppermute(value, axes, [(i, (i + shift) % size) for i in range(size)])  57.1 us
    all_to_all x2, blocking collectives, exchanged(): return lax.all_to_all(value, 'x', 0, 0, tiled=True)  38.7 us
    pallas_call x8, Pallas kernels, call(): pl.pallas_call(body, out_shape=out_shapes, in_specs=specs, out_specs=VMEM...  18.9 us
    all_to_all x2, waiting for transfers between devices, exchanged(): return lax.all_to_all(value, 'x', 0, 0, tiled=True)  15.3 us
    ppermute x6, starting transfers between devices, swap(): return lax.ppermute(value, 'c', SWAP)  12.8 us
    dot_general x6, matrix products, dot(): return jnp.dot(a, b, preferred_element_type=f32)  12.4 us
    all_to_all x2, starting transfers between devices, exchanged(): return lax.all_to_all(value, 'x', 0, 0, tiled=True)  7.03 us
  transfers between devices with their start and end apart: 24, of which 9 were waited for; matrix products, arithmetic and copies ran while one was open for 7% of the time, Pallas kernels for 6%

commit v1 on v0

v1 whole, which is shorter than its diff:
```python
import functools

import jax
import jax.numpy as jnp
from jax import lax
from jax.experimental import pallas as pl
from jax.experimental.pallas import tpu as pltpu
from jax.sharding import Mesh
from jax.sharding import PartitionSpec as P


DK = 128
DV = 256
TP = ("x", "c")
FS = ("z", "y")
RING = ("rep", "z")
SWAP = ((0, 1), (1, 0))
PAD = 384
FIRST, SECOND, THIRD = 2 * DK + 2 * DV, DV, 3 * PAD
Z_SHIFTS = (4, 3, 2, 1, 0, -1, -2, -3)
Z_ISSUE = (4, -3, 3, -2, 2, -1, 1)
Y_SHIFTS = (0, 1, 2, -1)
Y_ISSUE = (2, 1, -1)
epsilon = 1e-06
rope_base = 10000.0
bf16 = jnp.bfloat16
f32 = jnp.float32

VMEM = pl.BlockSpec(memory_space=pltpu.VMEM)
SMEM = pl.BlockSpec(memory_space=pltpu.SMEM)


def call(body, out_shapes, *args, flops=0, smem=0, scratch=()):
    specs = [SMEM] * smem + [VMEM] * (len(args) - smem)
    single = not isinstance(out_shapes, (list, tuple))
    return pl.pallas_call(
        body,
        out_shape=out_shapes,
        in_specs=specs,
        out_specs=VMEM if single else [VMEM] * len(out_shapes),
        scratch_shapes=list(scratch),
        cost_estimate=pl.CostEstimate(
            flops=max(flops, 1 << 24), bytes_accessed=1 << 21, transcendentals=0
        ),
    )(*args)


def shape(dims, kind=bf16):
    return jax.ShapeDtypeStruct(dims, kind)


def permuted(value, axes, shift, size):
    return lax.ppermute(value, axes, [(i, (i + shift) % size) for i in range(size)])


def swap(value):
    return lax.ppermute(value, "c", SWAP)


def exchanged(value):
    return lax.all_to_all(value, "x", 0, 0, tiled=True)


def rms_rows(values, gain):
    return values * lax.rsqrt(jnp.mean(values * values, axis=-1, keepdims=True) + epsilon) * gain


def to_pieces(values):
    return jnp.concatenate(
        [values[:, z * 128 + y * 32 : z * 128 + y * 32 + 32] for y in range(4) for z in range(8)],
        axis=1,
    )


def from_pieces(values):
    return jnp.concatenate(
        [values[:, y * 256 + z * 32 : y * 256 + z * 32 + 32] for z in range(8) for y in range(4)],
        axis=1,
    )


def pack_body(width, q, k, v, g, mo, ge, li, dn, out):
    out[:, :DK] = q[...]
    out[:, DK : 2 * DK] = k[...]
    out[:, 2 * DK : 2 * DK + DV] = v[...]
    out[:, 2 * DK + DV : FIRST] = g[...]
    out[:, FIRST : FIRST + SECOND] = mo[...]
    gap = jnp.zeros((out.shape[0], PAD - width), bf16)
    for place, piece in enumerate((ge, li, dn)):
        at = FIRST + SECOND + place * PAD
        out[:, at : at + PAD] = jnp.concatenate([piece[...], gap], axis=1)


def taps_body(width, ge_kernel, li_kernel, ge_bias, li_bias, out):
    out[...] = jnp.zeros(out.shape, f32)
    out[0:3, :width] = ge_kernel[...]
    out[3:6, :width] = li_kernel[...]
    out[6:7, :width] = ge_bias[...]
    out[7:8, :width] = li_bias[...]


def first_norm_body(tokens, gain, out):
    rows = to_pieces(rms_rows(tokens[...].astype(f32), gain[...])).astype(bf16)
    for k in range(out.shape[0]):
        out[k] = rows


def ring_order_body(index, *refs):
    pieces, (one, two, three) = refs[:8], refs[8:]
    for shift, piece in zip(Z_SHIFTS, pieces):
        at = lax.rem(index[0] - shift + 8, 8)
        one[at] = piece[:, :FIRST]
        two[at] = piece[:, FIRST : FIRST + SECOND]
        three[at] = piece[:, FIRST + SECOND :]


def line_order_body(index, *refs):
    pieces, out = refs[:4], refs[4]
    for shift, piece in zip(Y_SHIFTS, pieces):
        out[lax.rem(index[0] - shift + 4, 4)] = piece[...]


def summed(pieces):
    total = pieces[0].astype(f32)
    for k in range(1, pieces.shape[0]):
        total = total + pieces[k].astype(f32)
    inverse = lax.rsqrt(jnp.mean(total * total, axis=-1, keepdims=True) + epsilon)
    return from_pieces(total * inverse)


def middle_body(pieces, tokens, out_gain, in_gain, after_mix, channel_in):
    mix = (tokens[...].astype(f32) + summed(pieces) * out_gain[...]).astype(bf16)
    after_mix[...] = mix
    rows = to_pieces(rms_rows(mix.astype(f32), in_gain[...])).astype(bf16)
    for k in range(channel_in.shape[0]):
        channel_in[k] = rows


def final_body(pieces, after_mix, gain, out):
    out[...] = (after_mix[...].astype(f32) + summed(pieces) * gain[...]).astype(bf16)


def log_sigmoid_tile(logit):
    value = jnp.full((8, 128), logit, f32)
    tile = jnp.minimum(value, 0.0) - jnp.log1p(jnp.exp(-jnp.abs(value)))
    return tile[0:1, 0:1]


def attend_body(
    index, logits, own, other, p0, p1, p2, p3, cosine, sine, out_own, out_other, w, qs, ks, vs, gs
):
    y, core = index[0], index[1]
    for shift, piece in zip(Y_SHIFTS, (p0, p1, p2, p3)):
        at = lax.rem(y - shift + 4, 4) * 256
        w[pl.ds(pl.multiple_of(at, 256), 256), :] = piece[...]
    step = 256
    for r in range(0, 1024, step):
        rows = own[r : r + step, :] if r < 512 else other[r - 512 : r - 512 + step, :]
        projected = dot(rows, w[...])
        cos, sin = cosine[r : r + step, :], sine[r : r + step, :]
        q = projected[:, :DK]
        k = projected[:, DK : 2 * DK]
        qs[r : r + step, :] = (q * cos + pltpu.roll(q, DK // 2, 1) * sin).astype(bf16)
        ks[r : r + step, :] = (
            (k * cos + pltpu.roll(k, DK // 2, 1) * sin) * DK ** (-0.5)
        ).astype(bf16)
        vs[r : r + step, :] = projected[:, 2 * DK : 2 * DK + DV].astype(bf16)
        gs[r : r + step, :] = projected[:, 2 * DK + DV :]
    forward = log_sigmoid_tile(logits[0])
    backward = log_sigmoid_tile(logits[1])
    lag = (
        lax.broadcasted_iota(jnp.int32, (128, 128), 0)
        - lax.broadcasted_iota(jnp.int32, (128, 128), 1)
    ).astype(f32)
    ahead, behind = lag * forward, lag * -backward
    side = ((2 * core - 1) * 128).astype(f32)
    for r in range(8):
        decays = []
        for c in range(8):
            gap = float((r % 4 - c % 4) * 256)
            if r < 4 <= c:
                gap = gap + side
            if c < 4 <= r:
                gap = gap - side
            decays.append(jnp.exp(jnp.minimum(ahead + gap * forward, behind - gap * backward)))
        rows = slice(r * 128, r * 128 + 128)
        scores = dot_nt(qs[rows, :], ks[...])
        weighted = (scores * jnp.concatenate(decays, axis=1)).astype(bf16)
        kept = head_norm(dot(weighted, vs[...]))
        gate = gs[rows, :]
        gated = (kept * (gate / (1.0 + jnp.exp(-gate)))).astype(bf16)
        if r < 4:
            out_own[rows, :] = gated
        else:
            out_other[r * 128 - 512 : r * 128 - 384, :] = gated


def output_body(index, mine, theirs, p0, p1, p2, p3, out):
    for shift, piece in zip(Y_SHIFTS, (p0, p1, p2, p3)):
        at = lax.rem(index[0] - shift + 4, 4) * 256
        part = dot_nt(mine[...], piece[:, :DV]) + dot_nt(theirs[...], piece[:, DV:])
        out[:, pl.ds(pl.multiple_of(at, 256), 256)] = part.astype(bf16)


def feed_body(index, rows, edges, mine, theirs, my_taps, their_taps, out, hidden):
    core = index[0]
    line = lax.broadcasted_iota(jnp.int32, (128, 1), 0)
    for part, (weights, taps) in enumerate(((mine, my_taps), (theirs, their_taps))):
        kernel = [
            jnp.concatenate([taps[t : t + 1, :], taps[t + 3 : t + 4, :]], axis=1) for t in range(3)
        ]
        bias = jnp.concatenate([taps[6:7, :], taps[7:8, :]], axis=1)
        edge = dot(edges[...], weights[:, : 2 * PAD])
        none = jnp.zeros((1, 2 * PAD), f32)
        for x in range(4):
            main = dot(rows[x * 128 : x * 128 + 128, :], weights[:, : 2 * PAD])
            last = edge[4 + x : 5 + x, :]
            sooner = edge[3 + x : 4 + x, :] if x else none
            first = edge[x : x + 1, :]
            later = edge[x + 1 : x + 2, :] if x < 3 else none
            before = jnp.where(core == 0, sooner, last)
            after = jnp.where(core == 0, first, later)
            prev = jnp.where(line == 0, before, pltpu.roll(main, 1, 0))
            nxt = jnp.where(line == 127, after, pltpu.roll(main, 127, 0))
            conv = kernel[0] * prev + kernel[1] * main + kernel[2] * nxt + bias
            value = conv[:, :PAD]
            bent = value * (
                0.5 + 0.5 * jnp.tanh(0.7978845608028654 * (value + 0.044715 * value**3))
            )
            hidden[x * 128 : x * 128 + 128, part * PAD : part * PAD + PAD] = (
                bent * conv[:, PAD:]
            ).astype(bf16)
    for d in range(0, 1024, 256):
        total = dot_nt(hidden[:, :PAD], mine[d : d + 256, 2 * PAD :]) + dot_nt(
            hidden[:, PAD:], theirs[d : d + 256, 2 * PAD :]
        )
        out[:, d : d + 256] = total.astype(bf16)


def head_norm(values):
    centred = values - jnp.mean(values, axis=-1, keepdims=True)
    return centred * lax.rsqrt(jnp.mean(centred * centred, axis=-1, keepdims=True) + epsilon)


def dot(a, b):
    return jnp.dot(a, b, preferred_element_type=f32)


def dot_nt(a, b):
    return lax.dot_general(a, b, (((1,), (1,)), ((), ())), preferred_element_type=f32)


def line_gather(piece):
    got = {0: piece}
    for shift in Y_ISSUE:
        got[shift] = permuted(piece, "y", shift, 4)
    return [got[s].reshape(256, piece.shape[-1]) for s in Y_SHIFTS]


def rope_tables(core, chips, own):
    block = jnp.arange(chips, dtype=jnp.int32)[:, None] * (2 * own)
    inside = jnp.arange(own, dtype=jnp.int32)[None, :]
    positions = jnp.concatenate(
        [(block + inside + side * own).reshape(-1) for side in (core, 1 - core)]
    )
    half = DK // 2
    frequency = 1.0 / rope_base ** (jnp.arange(half, dtype=f32) / half)
    angles = positions.astype(f32)[:, None] * frequency[None, :]
    cosine, sine = jnp.cos(angles), jnp.sin(angles)
    return jnp.concatenate([cosine, cosine], axis=1), jnp.concatenate([-sine, sine], axis=1)


def layer(
    tokens,
    mixer_in_gain,
    query_weight,
    key_weight,
    value_weight,
    gate_weight,
    decay_logits,
    mixer_output,
    mixer_out_gain,
    channel_in_gain,
    gelu_weight,
    linear_weight,
    gelu_kernel,
    linear_kernel,
    gelu_bias,
    linear_bias,
    down_weight,
    channel_out_gain,
):
    core = lax.axis_index("c").astype(jnp.int32)
    y_index = lax.axis_index("y").astype(jnp.int32)
    z_index = lax.axis_index("z").astype(jnp.int32)
    token_rows = tokens[0]
    own, model = token_rows.shape
    chips = lax.axis_size("x")
    half = chips * own
    width = gelu_weight.shape[1]

    def row(vector):
        return vector.reshape(1, -1)

    packed = call(
        functools.partial(pack_body, width),
        shape((32, FIRST + SECOND + THIRD)),
        query_weight,
        key_weight,
        value_weight,
        gate_weight,
        mixer_output.T,
        gelu_weight,
        linear_weight,
        down_weight.T,
    )
    got = {0: packed}
    for shift in Z_ISSUE:
        got[shift] = permuted(packed, RING, shift, 16)
    spread = call(first_norm_body, shape((chips, own, model)), token_rows, row(mixer_in_gain))
    normed_own = exchanged(spread).reshape(half, model)
    normed_other = swap(normed_own)
    first_z, second_z, third_z = call(
        ring_order_body,
        [shape((8, 32, FIRST)), shape((8, 32, SECOND)), shape((8, 32, THIRD))],
        z_index[None],
        *[got[s] for s in Z_SHIFTS],
        smem=1,
    )
    first_pieces = line_gather(first_z)
    second_both = jnp.concatenate([second_z, swap(second_z)], axis=2)
    second_pieces = line_gather(second_both)
    third_pieces = line_gather(third_z)
    cosine, sine = rope_tables(core, chips, own)
    gated_own, gated_other = call(
        attend_body,
        [shape((half, DV)), shape((half, DV))],
        jnp.stack([y_index, core]),
        decay_logits[:, 0],
        normed_own,
        normed_other,
        *first_pieces,
        cosine,
        sine,
        flops=1 << 32,
        smem=2,
        scratch=[
            pltpu.VMEM((model, FIRST), bf16),
            pltpu.VMEM((2 * half, DK), bf16),
            pltpu.VMEM((2 * half, DK), bf16),
            pltpu.VMEM((2 * half, DV), bf16),
            pltpu.VMEM((2 * half, DV), f32),
        ],
    )
    gated_partner = swap(gated_other)
    mixed = call(
        output_body,
        shape((half, model)),
        y_index[None],
        gated_own,
        gated_partner,
        *second_pieces,
        flops=1 << 30,
        smem=1,
    )
    mix_pieces = exchanged(mixed.reshape(chips, own, model))
    taps = call(
        functools.partial(taps_body, width),
        shape((8, PAD), f32),
        gelu_kernel,
        linear_kernel,
        row(gelu_bias),
        row(linear_bias),
    )
    taps_other = swap(taps)
    after_mix, channel_spread = call(
        middle_body,
        [shape((own, model)), shape((chips, own, model))],
        mix_pieces,
        token_rows,
        row(mixer_out_gain),
        row(channel_in_gain),
    )
    channel_rows = exchanged(channel_spread)
    third_own = call(
        line_order_body, shape((4, 256, THIRD)), y_index[None], *third_pieces, smem=1
    ).reshape(model, THIRD)
    third_other = swap(third_own)
    edges = jnp.concatenate([channel_rows[:, 0], channel_rows[:, own - 1]], axis=0)
    edges_other = swap(edges)
    channel = call(
        feed_body,
        shape((half, model)),
        core[None],
        channel_rows.reshape(half, model),
        edges_other,
        third_own,
        third_other,
        taps,
        taps_other,
        flops=1 << 32,
        smem=1,
        scratch=[pltpu.VMEM((half, 2 * PAD), bf16)],
    )
    channel_pieces = exchanged(channel.reshape(chips, own, model))
    result = call(final_body, shape((own, model)), channel_pieces, after_mix, row(channel_out_gain))
    return result[None]


def solution(mesh):
    fs = mesh.shape["fs"]
    tp = mesh.shape["tp"]
    split = Mesh(
        mesh.devices.reshape(mesh.shape["rep"], fs // 4, 4, tp // 2, 2),
        ("rep", "z", "y", "x", "c"),
    )
    in_specs = (
        P(("rep", "z", "y"), TP, None),
        P(),
        P(FS, TP),
        P(FS, TP),
        P(FS, TP),
        P(FS, TP),
        P(None, TP),
        P(TP, FS),
        P(),
        P(),
        P(FS, TP),
        P(FS, TP),
        P(None, TP),
        P(None, TP),
        P(TP),
        P(TP),
        P(TP, FS),
        P(),
    )
    out_specs = P(("rep", "z", "y"), TP, None)
    return jax.shard_map(layer, mesh=split, in_specs=in_specs, out_specs=out_specs, check_vma=False)
```

time: 245 us -> 213 us (0.87)
  the two profiles are of different devices: /device:TPU:96 before, /device:TPU:8 now
where the time goes in v1:
time: 213 us; the launch traced here: 211 us
  starting transfers between devices  96.2 us (45%)
  blocking collectives  59.3 us (28%)
  Pallas kernels  34.3 us (16%)
  waiting for transfers between devices  13.8 us (6%)
  other arithmetic  4 us (2%)
  local copies, waits for them, and re-layouts  3.12 us (1%)
    ppermute x16, starting transfers between devices, permuted(): lax.ppermute(value, axes, [(i, (i + shift) % size) for i in range(size)])  79.1 us
    all_to_all x3, blocking collectives, exchanged(): return lax.all_to_all(value, 'x', 0, 0, tiled=True)  59.3 us
    pallas_call x10, Pallas kernels, call(): pl.pallas_call(body, out_shape=out_shapes, in_specs=specs, out_specs=VMEM...  34.3 us
    ppermute x6, starting transfers between devices, swap(): return lax.ppermute(value, 'c', SWAP)  12.8 us
    ppermute x16, waiting for transfers between devices, permuted(): lax.ppermute(value, axes, [(i, (i + shift) % size) for i in range(size)])  11.7 us
    all_to_all x1, starting transfers between devices, exchanged(): return lax.all_to_all(value, 'x', 0, 0, tiled=True)  4.29 us
  transfers between devices with their start and end apart: 23, of which 6 were waited for; matrix products, arithmetic and copies ran while one was open for 2% of the time, Pallas kernels for 10%

profile of v1, /device:TPU:8, one launch (start us, length us, event | category | flops | bytes accessed | tf_op | source)
XLA Modules:
  0.0 211.3 jit_solution(371240939996580711)
XLA Ops:
  0.0 2.4 %shard_map.172 = bf16[4,128,1024]{2,1,0:T(8,128)(2,1)} custom-call(bf16[128,1024]{1,0:T(8,128)(2,1)} %bitcast.42, f32[1,1024]{1,0:T(1,128)} %bitcast.55), custom_call_target="tpu_custom_call" | custom-call | flops 16777216 | bytes 2097152 | tf_op jit(solution)/shard_map/pallas_call | solution.py:36
  2.4 4.3 %all-to-all-start = ((bf16[4,128,1024]{2,1,0:T(8,128)(2,1)}), bf16[4,128,1024]{2,1,0:T(8,128)(2,1)S(1)}, u32[]{:S(2)}, u32[]{:S(2)}) async-start(bf16[4,128,1024]{2,1,0:T(8,128)(2,1)} %shard_map.172), calls=%async_computation | async-start | bytes 2097152 | tf_op jit(solution)/shard_map/all_to_all | solution.py:61
  6.7 1.5 shard_map.173.refs_4_
  8.2 9.1 %collective-permute-start.1 = (bf16[32,2176]{1,0:T(8,128)(2,1)}, bf16[32,2176]{1,0:T(8,128)(2,1)S(1)}, u32[]{:S(2)}, u32[]{:S(2)}) collective-permute-start(bf16[32,2176]{1,0:T(8,128)(2,1)} %shard_map.173.refs_4_), channel_id=1, source_target_pairs={{0,128},{32,160},{64,192},{96,224},{128,256},{160,288},{192,320},{... | collective-permute-start | bytes 417800 | tf_op jit(solution)/shard_map/ppermute | solution.py:53
  17.3 6.5 %collective-permute-start.2 = (bf16[32,2176]{1,0:T(8,128)(2,1)}, bf16[32,2176]{1,0:T(8,128)(2,1)S(1)}, u32[]{:S(2)}, u32[]{:S(2)}) collective-permute-start(bf16[32,2176]{1,0:T(8,128)(2,1)} %shard_map.173.refs_4_), channel_id=1, source_target_pairs={{0,96},{32,128},{64,160},{96,192},{128,224},{160,256},{192,288},{2... | collective-permute-start | bytes 417800 | tf_op jit(solution)/shard_map/ppermute | solution.py:53
  23.9 5.5 %collective-permute-start.3 = (bf16[32,2176]{1,0:T(8,128)(2,1)}, bf16[32,2176]{1,0:T(8,128)(2,1)S(1)}, u32[]{:S(2)}, u32[]{:S(2)}) collective-permute-start(bf16[32,2176]{1,0:T(8,128)(2,1)} %shard_map.173.refs_4_), channel_id=1, source_target_pairs={{0,64},{32,96},{64,128},{96,160},{128,192},{160,224},{192,256},{22... | collective-permute-start | bytes 417800 | tf_op jit(solution)/shard_map/ppermute | solution.py:53
  29.4 2.9 %collective-permute-start.4 = (bf16[32,2176]{1,0:T(8,128)(2,1)}, bf16[32,2176]{1,0:T(8,128)(2,1)S(1)}, u32[]{:S(2)}, u32[]{:S(2)}) collective-permute-start(bf16[32,2176]{1,0:T(8,128)(2,1)} %shard_map.173.refs_4_), channel_id=1, source_target_pairs={{0,32},{32,64},{64,96},{96,128},{128,160},{160,192},{192,224},{224... | collective-permute-start | bytes 417800 | tf_op jit(solution)/shard_map/ppermute | solution.py:53
  32.3 4.1 %collective-permute-start.5 = (bf16[32,2176]{1,0:T(8,128)(2,1)}, bf16[32,2176]{1,0:T(8,128)(2,1)S(1)}, u32[]{:S(2)}, u32[]{:S(2)}) collective-permute-start(bf16[32,2176]{1,0:T(8,128)(2,1)} %shard_map.173.refs_4_), channel_id=1, source_target_pairs={{0,480},{32,0},{64,32},{96,64},{128,96},{160,128},{192,160},{224,1... | collective-permute-start | bytes 417800 | tf_op jit(solution)/shard_map/ppermute | solution.py:53
  36.5 5.3 %collective-permute-start.6 = (bf16[32,2176]{1,0:T(8,128)(2,1)}, bf16[32,2176]{1,0:T(8,128)(2,1)S(1)}, u32[]{:S(2)}, u32[]{:S(2)}) collective-permute-start(bf16[32,2176]{1,0:T(8,128)(2,1)} %shard_map.173.refs_4_), channel_id=1, source_target_pairs={{0,448},{32,480},{64,0},{96,32},{128,64},{160,96},{192,128},{224,1... | collective-permute-start | bytes 417800 | tf_op jit(solution)/shard_map/ppermute | solution.py:53
  41.8 2.9 %collective-permute-done.2.refs_1_ = bf16[32,2176]{1,0:T(8,128)(2,1)S(1)} collective-permute-done((bf16[32,2176]{1,0:T(8,128)(2,1)}, bf16[32,2176]{1,0:T(8,128)(2,1)S(1)}, u32[]{:S(2)}, u32[]{:S(2)}) %collective-permute-start.2) | collective-permute-done | bytes 139296 | tf_op jit(solution)/shard_map/ppermute | solution.py:53
  44.7 4.2 %collective-permute-start.7 = (bf16[32,2176]{1,0:T(8,128)(2,1)}, bf16[32,2176]{1,0:T(8,128)(2,1)S(1)}, u32[]{:S(2)}, u32[]{:S(2)}) collective-permute-start(bf16[32,2176]{1,0:T(8,128)(2,1)} %shard_map.173.refs_4_), channel_id=1, source_target_pairs={{0,416},{32,448},{64,480},{96,0},{128,32},{160,64},{192,96},{224,1... | collective-permute-start | bytes 417800 | tf_op jit(solution)/shard_map/ppermute | solution.py:53
  48.9 1.3 collective-permute-done.4.refs_3_
  50.2 7.2 %collective-permute-done.7.refs_7_ = bf16[32,2176]{1,0:T(8,128)(2,1)S(1)} collective-permute-done((bf16[32,2176]{1,0:T(8,128)(2,1)}, bf16[32,2176]{1,0:T(8,128)(2,1)S(1)}, u32[]{:S(2)}, u32[]{:S(2)}) %collective-permute-start.7) | collective-permute-done | bytes 139296 | tf_op jit(solution)/shard_map/ppermute | solution.py:53
  57.5 0.6 copy-done.9
  58.1 2.4 %shard_map.174 = (bf16[8,32,768]{2,1,0:T(8,128)(2,1)}, bf16[8,32,256]{2,1,0:T(8,128)(2,1)}, bf16[8,32,1152]{2,1,0:T(8,128)(2,1)}) custom-call(s32[1]{0:T(128)} %bitcast.6.index, bf16[32,2176]{1,0:T(8,128)(2,1)} %copy-done.3, bf16[32,2176]{1,0:T(8,128)(2,1)} %copy-done.4, bf16[32,2176]{1,0:T(8,128)(2,1)} %copy-done.5, bf16[32,2176]{1,0:T(8,128)(2,1)} %copy-done.6, ...), custom_call_target="tpu_custom_call" | custom-call | flops 16777216 | bytes 2097152 | tf_op jit(solution)/shard_map/pallas_call | solution.py:36
  60.5 3.6 %collective-permute-start.17 = (bf16[8,32,1152]{2,1,0:T(8,128)(2,1)}, bf16[8,32,1152]{2,1,0:T(8,128)(2,1)S(1)}, u32[]{:S(2)}, u32[]{:S(2)}) collective-permute-start(bf16[8,32,1152]{2,1,0:T(8,128)(2,1)} %get-tuple-element.17), channel_id=1, source_target_pairs={{0,8},{8,16},{16,24},{24,0},{1,9},{9,17},{17,25},{25,1},{2,10},{10... | collective-permute-start | bytes 1769480 | tf_op jit(solution)/shard_map/ppermute | solution.py:53
  64.1 2.9 %collective-permute-start.18 = (bf16[8,32,1152]{2,1,0:T(8,128)(2,1)}, bf16[8,32,1152]{2,1,0:T(8,128)(2,1)}, u32[]{:S(2)}, u32[]{:S(2)}) collective-permute-start(bf16[8,32,1152]{2,1,0:T(8,128)(2,1)} %get-tuple-element.17), channel_id=1, source_target_pairs={{0,16},{8,24},{16,0},{24,8},{1,17},{9,25},{17,1},{25,9},{2,18},{10... | collective-permute-start | bytes 1769480 | tf_op jit(solution)/shard_map/ppermute | solution.py:53
  67.0 1.9 collective-permute-start
  69.0 4.3 %collective-permute-start.19 = (bf16[8,32,1152]{2,1,0:T(8,128)(2,1)}, bf16[8,32,1152]{2,1,0:T(8,128)(2,1)}, u32[]{:S(2)}, u32[]{:S(2)}) collective-permute-start(bf16[8,32,1152]{2,1,0:T(8,128)(2,1)} %get-tuple-element.17), channel_id=1, source_target_pairs={{0,24},{8,0},{16,8},{24,16},{1,25},{9,1},{17,9},{25,17},{2,26},{10... | collective-permute-start | bytes 1769480 | tf_op jit(solution)/shard_map/ppermute | solution.py:53
  73.3 2.1 %collective-permute-start.12 = (bf16[8,32,256]{2,1,0:T(8,128)(2,1)}, bf16[8,32,256]{2,1,0:T(8,128)(2,1)S(1)}, u32[]{:S(2)}, u32[]{:S(2)}) collective-permute-start(bf16[8,32,256]{2,1,0:T(8,128)(2,1)} %get-tuple-element.15), channel_id=1, source_target_pairs={{0,1},{1,0},{2,3},{3,2},{4,5},{5,4},{6,7},{7,6},{8,9},{9,8},{10,11... | collective-permute-start | bytes 393224 | tf_op jit(solution)/shard_map/ppermute | solution.py:57
  75.5 1.9 fusion
  77.4 1.9 collective-permute-start.8
  79.3 5.3 %collective-permute-start.9 = (bf16[8,32,768]{2,1,0:T(8,128)(2,1)}, bf16[8,32,768]{2,1,0:T(8,128)(2,1)}, u32[]{:S(2)}, u32[]{:S(2)}) collective-permute-start(bf16[8,32,768]{2,1,0:T(8,128)(2,1)} %get-tuple-element.12), channel_id=1, source_target_pairs={{0,16},{8,24},{16,0},{24,8},{1,17},{9,25},{17,1},{25,9},{2,18},{10... | collective-permute-start | bytes 1179656 | tf_op jit(solution)/shard_map/ppermute | solution.py:53
  84.7 11.8 %collective-permute-start.10 = (bf16[8,32,768]{2,1,0:T(8,128)(2,1)}, bf16[8,32,768]{2,1,0:T(8,128)(2,1)}, u32[]{:S(2)}, u32[]{:S(2)}) collective-permute-start(bf16[8,32,768]{2,1,0:T(8,128)(2,1)} %get-tuple-element.12), channel_id=1, source_target_pairs={{0,24},{8,0},{16,8},{24,16},{1,25},{9,1},{17,9},{25,17},{2,26},{10... | collective-permute-start | bytes 1179656 | tf_op jit(solution)/shard_map/ppermute | solution.py:53
  96.5 0.6 pad_add_fusion.index
  97.1 1.4 pad_maximum_fusion
  98.6 1.9 collective-permute-start.13
  100.5 3.2 %shard_map.178 = bf16[4,256,1152]{2,1,0:T(8,128)(2,1)} custom-call(s32[1]{0:T(128)} %bitcast.1.index, bf16[256,1152]{1,0:T(8,128)(2,1)} %bitcast.48, bf16[256,1152]{1,0:T(8,128)(2,1)} %bitcast.49, bf16[256,1152]{1,0:T(8,128)(2,1)} %bitcast.27.refs_2_, bf16[256,1152]{1,0:T(8,128)(2,1)} %bitcast.28.refs_3_), custom_call_target="tpu_custom_call" | custom-call | flops 16777216 | bytes 2097152 | tf_op jit(solution)/shard_map/pallas_call | solution.py:36
  103.7 4.0 %collective-permute-start.14 = (bf16[8,32,512]{2,1,0:T(8,128)(2,1)S(1)}, bf16[8,32,512]{2,1,0:T(8,128)(2,1)S(1)}, u32[]{:S(2)}, u32[]{:S(2)}) collective-permute-start(bf16[8,32,512]{2,1,0:T(8,128)(2,1)S(1)} %constant_dynamic-update-slice_fusion), channel_id=1, source_target_pairs={{0,16},{8,24},{16,0},{24,8},{1,17},{9,25},{17,1},{25,9},{2,18},{10... | collective-permute-start | bytes 786440 | tf_op jit(solution)/shard_map/ppermute | solution.py:53
  107.7 5.7 %collective-permute-start.15 = (bf16[8,32,512]{2,1,0:T(8,128)(2,1)S(1)}, bf16[8,32,512]{2,1,0:T(8,128)(2,1)S(1)}, u32[]{:S(2)}, u32[]{:S(2)}) collective-permute-start(bf16[8,32,512]{2,1,0:T(8,128)(2,1)S(1)} %constant_dynamic-update-slice_fusion), channel_id=1, source_target_pairs={{0,24},{8,0},{16,8},{24,16},{1,25},{9,1},{17,9},{25,17},{2,26},{10... | collective-permute-start | bytes 786440 | tf_op jit(solution)/shard_map/ppermute | solution.py:53
  113.7 1.9 collective-permute-start.20
  115.6 6.4 %shard_map.175 = (bf16[512,256]{1,0:T(8,128)(2,1)}, bf16[512,256]{1,0:T(8,128)(2,1)}) custom-call(s32[2]{0:T(128)} %pad_add_fusion.index, f32[2]{0:T(128)} %bitcast.63, bf16[512,1024]{1,0:T(8,128)(2,1)} %bitcast.45, bf16[512,1024]{1,0:T(8,128)(2,1)} %collective-permute-done.other, bf16[256,768]{1,0:T(8,128)(2,1)} %bitcast.59, bf16[256,768]{1,0:T(8,128)(2,1)} %bitcast.10.p1, ...), custom_call_target="tpu_custom_call" | custom-call | flops 4294967296 | bytes 2097152 | tf_op jit(solution)/shard_map/pallas_call | solution.py:36
  122.0 2.4 %collective-permute-start.11 = (bf16[512,256]{1,0:T(8,128)(2,1)}, bf16[512,256]{1,0:T(8,128)(2,1)S(1)}, u32[]{:S(2)}, u32[]{:S(2)}) collective-permute-start(bf16[512,256]{1,0:T(8,128)(2,1)} %get-tuple-element.14), channel_id=1, source_target_pairs={{0,1},{1,0},{2,3},{3,2},{4,5},{5,4},{6,7},{7,6},{8,9},{9,8},{10,11... | collective-permute-start | bytes 786440 | tf_op jit(solution)/shard_map/ppermute | solution.py:57
  124.5 1.3 collective-permute-done.11.theirs
  125.8 0.7 copy-done.17
  126.5 3.1 %shard_map.176 = bf16[512,1024]{1,0:T(8,128)(2,1)} custom-call(s32[1]{0:T(128)} %bitcast.1.index, bf16[512,256]{1,0:T(8,128)(2,1)} %get-tuple-element.13.mine, bf16[512,256]{1,0:T(8,128)(2,1)} %copy-done.17, bf16[256,512]{1,0:T(8,128)(2,1)} %bitcast.50, bf16[256,512]{1,0:T(8,128)(2,1)} %bitcast.60, bf16[256,512]{1,0:T(8,128)(2,1)} %bitcast.61, ...), custom_call_target="tpu_custom_call" | custom-call | flops 1073741824 | bytes 2097152 | tf_op jit(solution)/shard_map/pallas_call | solution.py:36
  129.6 20.8 %all_to_all.20.pieces = bf16[4,128,1024]{2,1,0:T(8,128)(2,1)} all-to-all(bf16[4,128,1024]{2,1,0:T(8,128)(2,1)} %bitcast.46), channel_id=1, replica_groups=mesh['rep'=2,'z'=8,'y'=4,'x'=4,'c'=2] {'x'}, dimensions={0} | all-to-all | bytes 2097152 | tf_op jit(solution)/shard_map/all_to_all | solution.py:61
  150.4 3.5 %shard_map.177 = (bf16[128,1024]{1,0:T(8,128)(2,1)}, bf16[4,128,1024]{2,1,0:T(8,128)(2,1)}) custom-call(bf16[4,128,1024]{2,1,0:T(8,128)(2,1)} %all_to_all.20.pieces, bf16[128,1024]{1,0:T(8,128)(2,1)} %bitcast.43, f32[1,1024]{1,0:T(1,128)} %bitcast.56, f32[1,1024]{1,0:T(1,128)} %bitcast.57), custom_call_target="tpu_custom_call" | custom-call | flops 16777216 | bytes 2097152 | tf_op jit(solution)/shard_map/pallas_call | solution.py:36
  153.9 18.3 %all_to_all.21 = bf16[4,128,1024]{2,1,0:T(8,128)(2,1)S(1)} all-to-all(bf16[4,128,1024]{2,1,0:T(8,128)(2,1)} %get-tuple-element.16), channel_id=1, replica_groups=mesh['rep'=2,'z'=8,'y'=4,'x'=4,'c'=2] {'x'}, dimensions={0} | all-to-all | bytes 2097152 | tf_op jit(solution)/shard_map/all_to_all | solution.py:61
  172.3 1.9 collective-permute-start.16
  174.2 0.6 reshape.129.ge_bias
  175.3 1.3 shard_map.179.my_taps
  176.6 2.6 %collective-permute-start.21 = (f32[8,384]{1,0:T(8,128)}, f32[8,384]{1,0:T(8,128)S(1)}, u32[]{:S(2)}, u32[]{:S(2)}) collective-permute-start(f32[8,384]{1,0:T(8,128)} %shard_map.179.my_taps), channel_id=1, source_target_pairs={{0,1},{1,0},{2,3},{3,2},{4,5},{5,4},{6,7},{7,6},{8,9},{9,8},{10,11... | collective-permute-start | bytes 36872 | tf_op jit(solution)/shard_map/ppermute | solution.py:57
  179.2 0.8 collective-permute-done.21.their_taps
  180.1 0.6 copy-done.19
  180.7 7.7 %shard_map.180 = bf16[512,1024]{1,0:T(8,128)(2,1)} custom-call(s32[1]{0:T(128)} %bitcast.index, bf16[512,1024]{1,0:T(8,128)(2,1)} %bitcast.41, bf16[8,1024]{1,0:T(8,128)(2,1)} %copy-done.18, bf16[1024,1152]{1,0:T(8,128)(2,1)} %bitcast.40, bf16[1024,1152]{1,0:T(8,128)(2,1)} %collective-permute-done.20.theirs, f32[8,384]{1,0:T(8,128)} %shard_map.179.my_taps, ...), custom_call_target="tpu_custom_call" | custom-call | flops 4294967296 | bytes 2097152 | tf_op jit(solution)/shard_map/pallas_call | solution.py:36
  188.4 20.2 %all_to_all.22.pieces = bf16[4,128,1024]{2,1,0:T(8,128)(2,1)} all-to-all(bf16[4,128,1024]{2,1,0:T(8,128)(2,1)} %bitcast.47), channel_id=1, replica_groups=mesh['rep'=2,'z'=8,'y'=4,'x'=4,'c'=2] {'x'}, dimensions={0} | all-to-all | bytes 2097152 | tf_op jit(solution)/shard_map/all_to_all | solution.py:61
  208.6 2.7 %shard_map.181 = bf16[128,1024]{1,0:T(8,128)(2,1)} custom-call(bf16[4,128,1024]{2,1,0:T(8,128)(2,1)} %all_to_all.22.pieces, bf16[128,1024]{1,0:T(8,128)(2,1)} %get-tuple-element.18.after_mix, f32[1,1024]{1,0:T(1,128)} %bitcast.58), custom_call_target="tpu_custom_call" | custom-call | flops 16777216 | bytes 2097152 | tf_op jit(solution)/shard_map/pallas_call | solution.py:36
  (66 shorter events, 1.1 us)
Async XLA Ops:
  2.4 64.6 %all-to-all-start = ((bf16[4,128,1024]{2,1,0:T(8,128)(2,1)}), bf16[4,128,1024]{2,1,0:T(8,128)(2,1)S(1)}, u32[]{:S(2)}, u32[]{:S(2)}) async-start(bf16[4,128,1024]{2,1,0:T(8,128)(2,1)} %shard_map.172), calls=%async_computation | async-start | bytes 2097152 | tf_op jit(solution)/shard_map/all_to_all | solution.py:61
  8.2 28.2 %collective-permute-start.1 = (bf16[32,2176]{1,0:T(8,128)(2,1)}, bf16[32,2176]{1,0:T(8,128)(2,1)S(1)}, u32[]{:S(2)}, u32[]{:S(2)}) collective-permute-start(bf16[32,2176]{1,0:T(8,128)(2,1)} %shard_map.173.refs_4_), channel_id=1, source_target_pairs={{0,128},{32,160},{64,192},{96,224},{128,256},{160,288},{192,320},{... | collective-permute-start | bytes 417800 | tf_op jit(solution)/shard_map/ppermute | solution.py:53
  17.3 27.4 %collective-permute-start.2 = (bf16[32,2176]{1,0:T(8,128)(2,1)}, bf16[32,2176]{1,0:T(8,128)(2,1)S(1)}, u32[]{:S(2)}, u32[]{:S(2)}) collective-permute-start(bf16[32,2176]{1,0:T(8,128)(2,1)} %shard_map.173.refs_4_), channel_id=1, source_target_pairs={{0,96},{32,128},{64,160},{96,192},{128,224},{160,256},{192,288},{2... | collective-permute-start | bytes 417800 | tf_op jit(solution)/shard_map/ppermute | solution.py:53
  23.9 25.0 %collective-permute-start.3 = (bf16[32,2176]{1,0:T(8,128)(2,1)}, bf16[32,2176]{1,0:T(8,128)(2,1)S(1)}, u32[]{:S(2)}, u32[]{:S(2)}) collective-permute-start(bf16[32,2176]{1,0:T(8,128)(2,1)} %shard_map.173.refs_4_), channel_id=1, source_target_pairs={{0,64},{32,96},{64,128},{96,160},{128,192},{160,224},{192,256},{22... | collective-permute-start | bytes 417800 | tf_op jit(solution)/shard_map/ppermute | solution.py:53
  29.4 20.8 %collective-permute-start.4 = (bf16[32,2176]{1,0:T(8,128)(2,1)}, bf16[32,2176]{1,0:T(8,128)(2,1)S(1)}, u32[]{:S(2)}, u32[]{:S(2)}) collective-permute-start(bf16[32,2176]{1,0:T(8,128)(2,1)} %shard_map.173.refs_4_), channel_id=1, source_target_pairs={{0,32},{32,64},{64,96},{96,128},{128,160},{160,192},{192,224},{224... | collective-permute-start | bytes 417800 | tf_op jit(solution)/shard_map/ppermute | solution.py:53
  32.3 17.9 %collective-permute-start.5 = (bf16[32,2176]{1,0:T(8,128)(2,1)}, bf16[32,2176]{1,0:T(8,128)(2,1)S(1)}, u32[]{:S(2)}, u32[]{:S(2)}) collective-permute-start(bf16[32,2176]{1,0:T(8,128)(2,1)} %shard_map.173.refs_4_), channel_id=1, source_target_pairs={{0,480},{32,0},{64,32},{96,64},{128,96},{160,128},{192,160},{224,1... | collective-permute-start | bytes 417800 | tf_op jit(solution)/shard_map/ppermute | solution.py:53
  36.5 21.0 %copy-start.3 = (bf16[32,2176]{1,0:T(8,128)(2,1)}, bf16[32,2176]{1,0:T(8,128)(2,1)S(1)}, u32[]{:S(2)}) copy-start(bf16[32,2176]{1,0:T(8,128)(2,1)S(1)} %collective-permute-done.1.refs_0_) | copy-start | bytes 417796
  36.5 13.7 %collective-permute-start.6 = (bf16[32,2176]{1,0:T(8,128)(2,1)}, bf16[32,2176]{1,0:T(8,128)(2,1)S(1)}, u32[]{:S(2)}, u32[]{:S(2)}) collective-permute-start(bf16[32,2176]{1,0:T(8,128)(2,1)} %shard_map.173.refs_4_), channel_id=1, source_target_pairs={{0,448},{32,480},{64,0},{96,32},{128,64},{160,96},{192,128},{224,1... | collective-permute-start | bytes 417800 | tf_op jit(solution)/shard_map/ppermute | solution.py:53
  44.7 12.8 %copy-start.4 = (bf16[32,2176]{1,0:T(8,128)(2,1)}, bf16[32,2176]{1,0:T(8,128)(2,1)S(1)}, u32[]{:S(2)}) copy-start(bf16[32,2176]{1,0:T(8,128)(2,1)S(1)} %collective-permute-done.2.refs_1_) | copy-start | bytes 417796
  44.7 12.7 %collective-permute-start.7 = (bf16[32,2176]{1,0:T(8,128)(2,1)}, bf16[32,2176]{1,0:T(8,128)(2,1)S(1)}, u32[]{:S(2)}, u32[]{:S(2)}) collective-permute-start(bf16[32,2176]{1,0:T(8,128)(2,1)} %shard_map.173.refs_4_), channel_id=1, source_target_pairs={{0,416},{32,448},{64,480},{96,0},{128,32},{160,64},{192,96},{224,1... | collective-permute-start | bytes 417800 | tf_op jit(solution)/shard_map/ppermute | solution.py:53
  48.9 8.5 %copy-start.5 = (bf16[32,2176]{1,0:T(8,128)(2,1)}, bf16[32,2176]{1,0:T(8,128)(2,1)S(1)}, u32[]{:S(2)}) copy-start(bf16[32,2176]{1,0:T(8,128)(2,1)S(1)} %collective-permute-done.3.refs_2_) | copy-start | bytes 417796
  50.2 7.3 %copy-start.6 = (bf16[32,2176]{1,0:T(8,128)(2,1)}, bf16[32,2176]{1,0:T(8,128)(2,1)S(1)}, u32[]{:S(2)}) copy-start(bf16[32,2176]{1,0:T(8,128)(2,1)S(1)} %collective-permute-done.4.refs_3_) | copy-start | bytes 417796
  50.2 7.3 %copy-start.7 = (bf16[32,2176]{1,0:T(8,128)(2,1)}, bf16[32,2176]{1,0:T(8,128)(2,1)S(1)}, u32[]{:S(2)}) copy-start(bf16[32,2176]{1,0:T(8,128)(2,1)S(1)} %collective-permute-done.5.refs_5_) | copy-start | bytes 417796
  50.2 7.3 %copy-start.8 = (bf16[32,2176]{1,0:T(8,128)(2,1)}, bf16[32,2176]{1,0:T(8,128)(2,1)S(1)}, u32[]{:S(2)}) copy-start(bf16[32,2176]{1,0:T(8,128)(2,1)S(1)} %collective-permute-done.6.refs_6_) | copy-start | bytes 417796
  57.4 0.6 copy-start.9
  60.5 38.0 %copy-start.10 = (bf16[8,32,256]{2,1,0:T(8,128)(2,1)S(1)}, bf16[8,32,256]{2,1,0:T(8,128)(2,1)}, u32[]{:S(2)}) copy-start(bf16[8,32,256]{2,1,0:T(8,128)(2,1)} %get-tuple-element.15) | copy-start | bytes 393220
  60.5 18.8 %collective-permute-start.17 = (bf16[8,32,1152]{2,1,0:T(8,128)(2,1)}, bf16[8,32,1152]{2,1,0:T(8,128)(2,1)S(1)}, u32[]{:S(2)}, u32[]{:S(2)}) collective-permute-start(bf16[8,32,1152]{2,1,0:T(8,128)(2,1)} %get-tuple-element.17), channel_id=1, source_target_pairs={{0,8},{8,16},{16,24},{24,0},{1,9},{9,17},{17,25},{25,1},{2,10},{10... | collective-permute-start | bytes 1769480 | tf_op jit(solution)/shard_map/ppermute | solution.py:53
  64.1 20.5 %collective-permute-start.18 = (bf16[8,32,1152]{2,1,0:T(8,128)(2,1)}, bf16[8,32,1152]{2,1,0:T(8,128)(2,1)}, u32[]{:S(2)}, u32[]{:S(2)}) collective-permute-start(bf16[8,32,1152]{2,1,0:T(8,128)(2,1)} %get-tuple-element.17), channel_id=1, source_target_pairs={{0,16},{8,24},{16,0},{24,8},{1,17},{9,25},{17,1},{25,9},{2,18},{10... | collective-permute-start | bytes 1769480 | tf_op jit(solution)/shard_map/ppermute | solution.py:53
  67.0 31.6 %copy-start.1 = (bf16[4,128,1024]{2,1,0:T(8,128)(2,1)}, bf16[4,128,1024]{2,1,0:T(8,128)(2,1)S(1)}, u32[]{:S(2)}) copy-start(bf16[4,128,1024]{2,1,0:T(8,128)(2,1)S(1)} %all-to-all-done) | copy-start | bytes 3145732
  67.0 48.6 %collective-permute-start = (bf16[512,1024]{1,0:T(8,128)(2,1)S(1)}, bf16[512,1024]{1,0:T(8,128)(2,1)}, u32[]{:S(2)}, u32[]{:S(2)}) collective-permute-start(bf16[512,1024]{1,0:T(8,128)(2,1)S(1)} %bitcast.44), channel_id=1, source_target_pairs={{0,1},{1,0},{2,3},{3,2},{4,5},{5,4},{6,7},{7,6},{8,9},{9,8},{10,11... | collective-permute-start | bytes 3145736 | tf_op jit(solution)/shard_map/ppermute | solution.py:57
  69.0 29.5 %collective-permute-start.19 = (bf16[8,32,1152]{2,1,0:T(8,128)(2,1)}, bf16[8,32,1152]{2,1,0:T(8,128)(2,1)}, u32[]{:S(2)}, u32[]{:S(2)}) collective-permute-start(bf16[8,32,1152]{2,1,0:T(8,128)(2,1)} %get-tuple-element.17), channel_id=1, source_target_pairs={{0,24},{8,0},{16,8},{24,16},{1,25},{9,1},{17,9},{25,17},{2,26},{10... | collective-permute-start | bytes 1769480 | tf_op jit(solution)/shard_map/ppermute | solution.py:53
  73.3 4.0 %collective-permute-start.12 = (bf16[8,32,256]{2,1,0:T(8,128)(2,1)}, bf16[8,32,256]{2,1,0:T(8,128)(2,1)S(1)}, u32[]{:S(2)}, u32[]{:S(2)}) collective-permute-start(bf16[8,32,256]{2,1,0:T(8,128)(2,1)} %get-tuple-element.15), channel_id=1, source_target_pairs={{0,1},{1,0},{2,3},{3,2},{4,5},{5,4},{6,7},{7,6},{8,9},{9,8},{10,11... | collective-permute-start | bytes 393224 | tf_op jit(solution)/shard_map/ppermute | solution.py:57
  77.4 26.3 %collective-permute-start.8 = (bf16[8,32,768]{2,1,0:T(8,128)(2,1)}, bf16[8,32,768]{2,1,0:T(8,128)(2,1)}, u32[]{:S(2)}, u32[]{:S(2)}) collective-permute-start(bf16[8,32,768]{2,1,0:T(8,128)(2,1)} %get-tuple-element.12), channel_id=1, source_target_pairs={{0,8},{8,16},{16,24},{24,0},{1,9},{9,17},{17,25},{25,1},{2,10},{10... | collective-permute-start | bytes 1179656 | tf_op jit(solution)/shard_map/ppermute | solution.py:53
  79.3 21.2 %copy-start.2 = (bf16[8,32,1152]{2,1,0:T(8,128)(2,1)}, bf16[8,32,1152]{2,1,0:T(8,128)(2,1)S(1)}, u32[]{:S(2)}) copy-start(bf16[8,32,1152]{2,1,0:T(8,128)(2,1)S(1)} %collective-permute-done.17) | copy-start | bytes 1769476
  79.3 28.3 %collective-permute-start.9 = (bf16[8,32,768]{2,1,0:T(8,128)(2,1)}, bf16[8,32,768]{2,1,0:T(8,128)(2,1)}, u32[]{:S(2)}, u32[]{:S(2)}) collective-permute-start(bf16[8,32,768]{2,1,0:T(8,128)(2,1)} %get-tuple-element.12), channel_id=1, source_target_pairs={{0,16},{8,24},{16,0},{24,8},{1,17},{9,25},{17,1},{25,9},{2,18},{10... | collective-permute-start | bytes 1179656 | tf_op jit(solution)/shard_map/ppermute | solution.py:53
  84.7 29.0 %collective-permute-start.10 = (bf16[8,32,768]{2,1,0:T(8,128)(2,1)}, bf16[8,32,768]{2,1,0:T(8,128)(2,1)}, u32[]{:S(2)}, u32[]{:S(2)}) collective-permute-start(bf16[8,32,768]{2,1,0:T(8,128)(2,1)} %get-tuple-element.12), channel_id=1, source_target_pairs={{0,24},{8,0},{16,8},{24,16},{1,25},{9,1},{17,9},{25,17},{2,26},{10... | collective-permute-start | bytes 1179656 | tf_op jit(solution)/shard_map/ppermute | solution.py:53
  98.6 9.1 %copy-start.11 = (bf16[8,32,512]{2,1,0:T(8,128)(2,1)}, bf16[8,32,512]{2,1,0:T(8,128)(2,1)S(1)}, u32[]{:S(2)}) copy-start(bf16[8,32,512]{2,1,0:T(8,128)(2,1)S(1)} %constant_dynamic-update-slice_fusion) | copy-start | bytes 786436
  98.6 25.9 %collective-permute-start.13 = (bf16[8,32,512]{2,1,0:T(8,128)(2,1)S(1)}, bf16[8,32,512]{2,1,0:T(8,128)(2,1)S(1)}, u32[]{:S(2)}, u32[]{:S(2)}) collective-permute-start(bf16[8,32,512]{2,1,0:T(8,128)(2,1)S(1)} %constant_dynamic-update-slice_fusion), channel_id=1, source_target_pairs={{0,8},{8,16},{16,24},{24,0},{1,9},{9,17},{17,25},{25,1},{2,10},{10... | collective-permute-start | bytes 786440 | tf_op jit(solution)/shard_map/ppermute | solution.py:53
  103.7 20.8 %collective-permute-start.14 = (bf16[8,32,512]{2,1,0:T(8,128)(2,1)S(1)}, bf16[8,32,512]{2,1,0:T(8,128)(2,1)S(1)}, u32[]{:S(2)}, u32[]{:S(2)}) collective-permute-start(bf16[8,32,512]{2,1,0:T(8,128)(2,1)S(1)} %constant_dynamic-update-slice_fusion), channel_id=1, source_target_pairs={{0,16},{8,24},{16,0},{24,8},{1,17},{9,25},{17,1},{25,9},{2,18},{10... | collective-permute-start | bytes 786440 | tf_op jit(solution)/shard_map/ppermute | solution.py:53
  107.7 16.8 %collective-permute-start.15 = (bf16[8,32,512]{2,1,0:T(8,128)(2,1)S(1)}, bf16[8,32,512]{2,1,0:T(8,128)(2,1)S(1)}, u32[]{:S(2)}, u32[]{:S(2)}) collective-permute-start(bf16[8,32,512]{2,1,0:T(8,128)(2,1)S(1)} %constant_dynamic-update-slice_fusion), channel_id=1, source_target_pairs={{0,24},{8,0},{16,8},{24,16},{1,25},{9,1},{17,9},{25,17},{2,26},{10... | collective-permute-start | bytes 786440 | tf_op jit(solution)/shard_map/ppermute | solution.py:53
  113.7 66.4 %collective-permute-start.20 = (bf16[1024,1152]{1,0:T(8,128)(2,1)}, bf16[1024,1152]{1,0:T(8,128)(2,1)}, u32[]{:S(2)}, u32[]{:S(2)}) collective-permute-start(bf16[1024,1152]{1,0:T(8,128)(2,1)} %bitcast.39), channel_id=1, source_target_pairs={{0,1},{1,0},{2,3},{3,2},{4,5},{5,4},{6,7},{7,6},{8,9},{9,8},{10,11... | collective-permute-start | bytes 7077896 | tf_op jit(solution)/shard_map/ppermute | solution.py:57
  122.0 3.7 %collective-permute-start.11 = (bf16[512,256]{1,0:T(8,128)(2,1)}, bf16[512,256]{1,0:T(8,128)(2,1)S(1)}, u32[]{:S(2)}, u32[]{:S(2)}) collective-permute-start(bf16[512,256]{1,0:T(8,128)(2,1)} %get-tuple-element.14), channel_id=1, source_target_pairs={{0,1},{1,0},{2,3},{3,2},{4,5},{5,4},{6,7},{7,6},{8,9},{9,8},{10,11... | collective-permute-start | bytes 786440 | tf_op jit(solution)/shard_map/ppermute | solution.py:57
  124.4 1.3 copy-start.14
  124.5 1.3 copy-start.15
  124.5 1.3 copy-start.16
  125.8 0.7 copy-start.17
  129.6 44.6 %copy-start.12 = (f32[352]{0:T(512)S(1)}, f32[352]{0:T(512)}, u32[]{:S(2)}) copy-start(f32[352]{0:T(512)} %param.32) | copy-start | bytes 4228
  129.6 45.2 %copy-start.13 = (f32[352]{0:T(512)S(1)}, f32[352]{0:T(512)}, u32[]{:S(2)}) copy-start(f32[352]{0:T(512)} %param.33) | copy-start | bytes 4228
  172.2 7.9 %copy-start = (bf16[4,128,1024]{2,1,0:T(8,128)(2,1)}, bf16[4,128,1024]{2,1,0:T(8,128)(2,1)S(1)}, u32[]{:S(2)}) copy-start(bf16[4,128,1024]{2,1,0:T(8,128)(2,1)S(1)} %all_to_all.21) | copy-start | bytes 3145732
  172.3 7.8 %collective-permute-start.16 = (bf16[8,1024]{1,0:T(8,128)(2,1)S(1)}, bf16[8,1024]{1,0:T(8,128)(2,1)S(1)}, u32[]{:S(2)}, u32[]{:S(2)}) collective-permute-start(bf16[8,1024]{1,0:T(8,128)(2,1)S(1)} %pad_maximum_fusion.2), channel_id=1, source_target_pairs={{0,1},{1,0},{2,3},{3,2},{4,5},{5,4},{6,7},{7,6},{8,9},{9,8},{10,11... | collective-permute-start | bytes 49160 | tf_op jit(solution)/shard_map/ppermute | solution.py:57
  176.6 3.4 %collective-permute-start.21 = (f32[8,384]{1,0:T(8,128)}, f32[8,384]{1,0:T(8,128)S(1)}, u32[]{:S(2)}, u32[]{:S(2)}) collective-permute-start(f32[8,384]{1,0:T(8,128)} %shard_map.179.my_taps), channel_id=1, source_target_pairs={{0,1},{1,0},{2,3},{3,2},{4,5},{5,4},{6,7},{7,6},{8,9},{9,8},{10,11... | collective-permute-start | bytes 36872 | tf_op jit(solution)/shard_map/ppermute | solution.py:57
  180.0 0.6 copy-start.19
  180.1 0.6 copy-start.18

commit v2 on v1

--- a/solution.py
+++ b/solution.py
@@ -2,6 +2,7 @@
 
 import jax
 import jax.numpy as jnp
+import numpy as np
 from jax import lax
 from jax.experimental import pallas as pl
 from jax.experimental.pallas import tpu as pltpu
@@ -65,20 +66,6 @@
     return values * lax.rsqrt(jnp.mean(values * values, axis=-1, keepdims=True) + epsilon) * gain
 
 
-def to_pieces(values):
-    return jnp.concatenate(
-        [values[:, z * 128 + y * 32 : z * 128 + y * 32 + 32] for y in range(4) for z in range(8)],
-        axis=1,
-    )
-
-
-def from_pieces(values):
-    return jnp.concatenate(
-        [values[:, y * 256 + z * 32 : y * 256 + z * 32 + 32] for z in range(8) for y in range(4)],
-        axis=1,
-    )
-
-
 def pack_body(width, q, k, v, g, mo, ge, li, dn, out):
     out[:, :DK] = q[...]
     out[:, DK : 2 * DK] = k[...]
@@ -100,7 +87,7 @@
 
 
 def first_norm_body(tokens, gain, out):
-    rows = to_pieces(rms_rows(tokens[...].astype(f32), gain[...])).astype(bf16)
+    rows = rms_rows(tokens[...].astype(f32), gain[...]).astype(bf16)
     for k in range(out.shape[0]):
         out[k] = rows
 
@@ -117,21 +104,22 @@
 def line_order_body(index, *refs):
     pieces, out = refs[:4], refs[4]
     for shift, piece in zip(Y_SHIFTS, pieces):
-        out[lax.rem(index[0] - shift + 4, 4)] = piece[...]
+        at = lax.rem(index[0] - shift + 4, 4)
+        for z in range(8):
+            out[z, at] = piece[z * 32 : z * 32 + 32, :]
 
 
 def summed(pieces):
     total = pieces[0].astype(f32)
     for k in range(1, pieces.shape[0]):
         total = total + pieces[k].astype(f32)
-    inverse = lax.rsqrt(jnp.mean(total * total, axis=-1, keepdims=True) + epsilon)
-    return from_pieces(total * inverse)
+    return total * lax.rsqrt(jnp.mean(total * total, axis=-1, keepdims=True) + epsilon)
 
 
 def middle_body(pieces, tokens, out_gain, in_gain, after_mix, channel_in):
     mix = (tokens[...].astype(f32) + summed(pieces) * out_gain[...]).astype(bf16)
     after_mix[...] = mix
-    rows = to_pieces(rms_rows(mix.astype(f32), in_gain[...])).astype(bf16)
+    rows = rms_rows(mix.astype(f32), in_gain[...]).astype(bf16)
     for k in range(channel_in.shape[0]):
         channel_in[k] = rows
 
@@ -147,17 +135,34 @@
 
 
 def attend_body(
-    index, logits, own, other, p0, p1, p2, p3, cosine, sine, out_own, out_other, w, qs, ks, vs, gs
+    index, logits, own, other, p0, p1, p2, p3, frequency, out_own, out_other, w, qs, ks, vs, gs
 ):
     y, core = index[0], index[1]
     for shift, piece in zip(Y_SHIFTS, (p0, p1, p2, p3)):
-        at = lax.rem(y - shift + 4, 4) * 256
-        w[pl.ds(pl.multiple_of(at, 256), 256), :] = piece[...]
+        at = lax.rem(y - shift + 4, 4) * 32
+        for z in range(8):
+            place = pl.ds(pl.multiple_of(z * 128 + at, 32), 32)
+            w[place, :] = piece[z * 32 : z * 32 + 32, :]
+    inside = lax.broadcasted_iota(jnp.int32, (128, DK), 0).astype(f32) * frequency[...]
+    cos_in, sin_in = jnp.cos(inside), jnp.sin(inside)
+    block = lax.broadcasted_iota(jnp.int32, (8, DK), 0)
+    base = (block % 4) * 256 + jnp.where(block < 4, core, 1 - core) * 128
+    start = base.astype(f32) * frequency[...]
+    cos_at, sin_at = jnp.cos(start), jnp.sin(start)
+    sign = jnp.where(lax.broadcasted_iota(jnp.int32, (128, DK), 1) < DK // 2, -1.0, 1.0)
+    cos_turn, sin_turn = cos_in * sign, sin_in * sign
+
+    def tables(r):
+        c, s = cos_at[r : r + 1, :], sin_at[r : r + 1, :]
+        return c * cos_in - s * sin_in, s * cos_turn + c * sin_turn
+
     step = 256
     for r in range(0, 1024, step):
         rows = own[r : r + step, :] if r < 512 else other[r - 512 : r - 512 + step, :]
         projected = dot(rows, w[...])
-        cos, sin = cosine[r : r + step, :], sine[r : r + step, :]
+        pair = [tables(b) for b in range(r // 128, (r + step) // 128)]
+        cos = jnp.concatenate([p[0] for p in pair], axis=0)
+        sin = jnp.concatenate([p[1] for p in pair], axis=0)
         q = projected[:, :DK]
         k = projected[:, DK : 2 * DK]
         qs[r : r + step, :] = (q * cos + pltpu.roll(q, DK // 2, 1) * sin).astype(bf16)
@@ -195,11 +200,21 @@
             out_other[r * 128 - 512 : r * 128 - 384, :] = gated
 
 
-def output_body(index, mine, theirs, p0, p1, p2, p3, out):
-    for shift, piece in zip(Y_SHIFTS, (p0, p1, p2, p3)):
-        at = lax.rem(index[0] - shift + 4, 4) * 256
-        part = dot_nt(mine[...], piece[:, :DV]) + dot_nt(theirs[...], piece[:, DV:])
-        out[:, pl.ds(pl.multiple_of(at, 256), 256)] = part.astype(bf16)
+def spread_body(mine, theirs, out):
+    for y in range(out.shape[0]):
+        out[y, :, :, :DV] = mine[...]
+        out[y, :, :, DV:] = theirs[...]
+
+
+def output_body(mine, theirs, pieces, out, w):
+    for y in range(4):
+        for z in range(8):
+            at = z * 128 + y * 32
+            w[at : at + 32, :] = pieces[y, z]
+    step = 256
+    for d in range(0, 1024, step):
+        part = dot_nt(mine[...], w[d : d + step, :DV]) + dot_nt(theirs[...], w[d : d + step, DV:])
+        out[:, d : d + step] = part.astype(bf16)
 
 
 def feed_body(index, rows, edges, mine, theirs, my_taps, their_taps, out, hidden):
@@ -257,17 +272,10 @@
     return [got[s].reshape(256, piece.shape[-1]) for s in Y_SHIFTS]
 
 
-def rope_tables(core, chips, own):
-    block = jnp.arange(chips, dtype=jnp.int32)[:, None] * (2 * own)
-    inside = jnp.arange(own, dtype=jnp.int32)[None, :]
-    positions = jnp.concatenate(
-        [(block + inside + side * own).reshape(-1) for side in (core, 1 - core)]
-    )
+def rope_frequency():
     half = DK // 2
-    frequency = 1.0 / rope_base ** (jnp.arange(half, dtype=f32) / half)
-    angles = positions.astype(f32)[:, None] * frequency[None, :]
-    cosine, sine = jnp.cos(angles), jnp.sin(angles)
-    return jnp.concatenate([cosine, cosine], axis=1), jnp.concatenate([-sine, sine], axis=1)
+    frequency = 1.0 / rope_base ** (np.arange(half, dtype=np.float32) / half)
+    return jnp.asarray(np.tile(frequency.astype(np.float32), 2)[None])
 
 
 def layer(
@@ -328,10 +336,9 @@
         smem=1,
     )
     first_pieces = line_gather(first_z)
-    second_both = jnp.concatenate([second_z, swap(second_z)], axis=2)
-    second_pieces = line_gather(second_both)
+    second_spread = call(spread_body, shape((4, 8, 32, 2 * SECOND)), second_z, swap(second_z))
+    second_pieces = lax.all_to_all(second_spread, "y", 0, 0, tiled=True)
     third_pieces = line_gather(third_z)
-    cosine, sine = rope_tables(core, chips, own)
     gated_own, gated_other = call(
         attend_body,
         [shape((half, DV)), shape((half, DV))],
@@ -340,8 +347,7 @@
         normed_own,
         normed_other,
         *first_pieces,
-        cosine,
-        sine,
+        rope_frequency(),
         flops=1 << 32,
         smem=2,
         scratch=[
@@ -356,12 +362,11 @@
     mixed = call(
         output_body,
         shape((half, model)),
-        y_index[None],
         gated_own,
         gated_partner,
-        *second_pieces,
+        second_pieces,
         flops=1 << 30,
-        smem=1,
+        scratch=[pltpu.VMEM((model, 2 * SECOND), bf16)],
     )
     mix_pieces = exchanged(mixed.reshape(chips, own, model))
     taps = call(
@@ -383,7 +388,7 @@
     )
     channel_rows = exchanged(channel_spread)
     third_own = call(
-        line_order_body, shape((4, 256, THIRD)), y_index[None], *third_pieces, smem=1
+        line_order_body, shape((8, 4, 32, THIRD)), y_index[None], *third_pieces, smem=1
     ).reshape(model, THIRD)
     third_other = swap(third_own)
     edges = jnp.concatenate([channel_rows[:, 0], channel_rows[:, own - 1]], axis=0)

time: 213 us -> 238 us (1.12)
  the two profiles are of different devices: /device:TPU:8 before, /device:TPU:104 now
where the time goes in v2:
time: 238 us; the launch traced here: 237 us
  blocking collectives  78.4 us (33%)
  starting transfers between devices  74.4 us (31%)
  waiting for transfers between devices  44.3 us (19%)
  Pallas kernels  34.6 us (15%)
  local copies, waits for them, and re-layouts  4.14 us (2%)
    all_to_all x4, blocking collectives, exchanged(): return lax.all_to_all(value, 'x', 0, 0, tiled=True)  78.4 us
    ppermute x13, starting transfers between devices, permuted(): lax.ppermute(value, axes, [(i, (i + shift) % size) for i in range(size)])  57.6 us
    ppermute x13, waiting for transfers between devices, permuted(): lax.ppermute(value, axes, [(i, (i + shift) % size) for i in range(size)])  41.7 us
    pallas_call x11, Pallas kernels, call(): pl.pallas_call(body, out_shape=out_shapes, in_specs=specs, out_specs=VMEM...  34.6 us
    ppermute x6, starting transfers between devices, swap(): return lax.ppermute(value, 'c', SWAP)  12 us
    all_to_all x1, starting transfers between devices, layer(): second_pieces = lax.all_to_all(second_spread, 'y', 0, 0, tiled=True)  4.83 us
  transfers between devices with their start and end apart: 20, of which 9 were waited for; matrix products, arithmetic and copies ran while one was open for 1% of the time, Pallas kernels for 10%

profile of v2, /device:TPU:104, one launch (start us, length us, event | category | flops | bytes accessed | tf_op | source)
XLA Modules:
  0.0 236.9 jit_solution(7259579633156953140)
XLA Ops:
  0.0 2.1 shard_map.181
  2.1 19.4 %all_to_all.25 = bf16[4,128,1024]{2,1,0:T(8,128)(2,1)S(1)} all-to-all(bf16[4,128,1024]{2,1,0:T(8,128)(2,1)} %shard_map.181), channel_id=1, replica_groups=mesh['rep'=2,'z'=8,'y'=4,'x'=4,'c'=2] {'x'}, dimensions={0} | all-to-all | bytes 2097152 | tf_op jit(solution)/shard_map/all_to_all | solution.py:62
  21.5 1.9 collective-permute-start
  23.4 1.5 shard_map.182.refs_4_
  24.9 9.1 %collective-permute-start.1 = (bf16[32,2176]{1,0:T(8,128)(2,1)}, bf16[32,2176]{1,0:T(8,128)(2,1)S(1)}, u32[]{:S(2)}, u32[]{:S(2)}) collective-permute-start(bf16[32,2176]{1,0:T(8,128)(2,1)} %shard_map.182.refs_4_), channel_id=1, source_target_pairs={{0,128},{32,160},{64,192},{96,224},{128,256},{160,288},{192,320},{... | collective-permute-start | bytes 417800 | tf_op jit(solution)/shard_map/ppermute | solution.py:54
  34.0 5.9 %collective-permute-start.2 = (bf16[32,2176]{1,0:T(8,128)(2,1)}, bf16[32,2176]{1,0:T(8,128)(2,1)S(1)}, u32[]{:S(2)}, u32[]{:S(2)}) collective-permute-start(bf16[32,2176]{1,0:T(8,128)(2,1)} %shard_map.182.refs_4_), channel_id=1, source_target_pairs={{0,96},{32,128},{64,160},{96,192},{128,224},{160,256},{192,288},{2... | collective-permute-start | bytes 417800 | tf_op jit(solution)/shard_map/ppermute | solution.py:54
  40.0 3.4 %collective-permute-start.3 = (bf16[32,2176]{1,0:T(8,128)(2,1)}, bf16[32,2176]{1,0:T(8,128)(2,1)S(1)}, u32[]{:S(2)}, u32[]{:S(2)}) collective-permute-start(bf16[32,2176]{1,0:T(8,128)(2,1)} %shard_map.182.refs_4_), channel_id=1, source_target_pairs={{0,64},{32,96},{64,128},{96,160},{128,192},{160,224},{192,256},{22... | collective-permute-start | bytes 417800 | tf_op jit(solution)/shard_map/ppermute | solution.py:54
  43.4 2.9 %collective-permute-start.4 = (bf16[32,2176]{1,0:T(8,128)(2,1)}, bf16[32,2176]{1,0:T(8,128)(2,1)S(1)}, u32[]{:S(2)}, u32[]{:S(2)}) collective-permute-start(bf16[32,2176]{1,0:T(8,128)(2,1)} %shard_map.182.refs_4_), channel_id=1, source_target_pairs={{0,32},{32,64},{64,96},{96,128},{128,160},{160,192},{192,224},{224... | collective-permute-start | bytes 417800 | tf_op jit(solution)/shard_map/ppermute | solution.py:54
  46.3 8.9 %collective-permute-start.5 = (bf16[32,2176]{1,0:T(8,128)(2,1)}, bf16[32,2176]{1,0:T(8,128)(2,1)S(1)}, u32[]{:S(2)}, u32[]{:S(2)}) collective-permute-start(bf16[32,2176]{1,0:T(8,128)(2,1)} %shard_map.182.refs_4_), channel_id=1, source_target_pairs={{0,480},{32,0},{64,32},{96,64},{128,96},{160,128},{192,160},{224,1... | collective-permute-start | bytes 417800 | tf_op jit(solution)/shard_map/ppermute | solution.py:54
  55.2 2.7 %collective-permute-done.2.refs_1_ = bf16[32,2176]{1,0:T(8,128)(2,1)S(1)} collective-permute-done((bf16[32,2176]{1,0:T(8,128)(2,1)}, bf16[32,2176]{1,0:T(8,128)(2,1)S(1)}, u32[]{:S(2)}, u32[]{:S(2)}) %collective-permute-start.2) | collective-permute-done | bytes 139296 | tf_op jit(solution)/shard_map/ppermute | solution.py:54
  58.0 1.9 collective-permute-start.6
  59.9 1.5 collective-permute-done.3.refs_2_
  61.4 4.3 %collective-permute-start.7 = (bf16[32,2176]{1,0:T(8,128)(2,1)}, bf16[32,2176]{1,0:T(8,128)(2,1)S(1)}, u32[]{:S(2)}, u32[]{:S(2)}) collective-permute-start(bf16[32,2176]{1,0:T(8,128)(2,1)} %shard_map.182.refs_4_), channel_id=1, source_target_pairs={{0,416},{32,448},{64,480},{96,0},{128,32},{160,64},{192,96},{224,1... | collective-permute-start | bytes 417800 | tf_op jit(solution)/shard_map/ppermute | solution.py:54
  65.8 5.3 %collective-permute-done.6.refs_6_ = bf16[32,2176]{1,0:T(8,128)(2,1)S(1)} collective-permute-done((bf16[32,2176]{1,0:T(8,128)(2,1)}, bf16[32,2176]{1,0:T(8,128)(2,1)S(1)}, u32[]{:S(2)}, u32[]{:S(2)}) %collective-permute-start.6) | collective-permute-done | bytes 139296 | tf_op jit(solution)/shard_map/ppermute | solution.py:54
  71.0 10.1 %collective-permute-done.7.refs_7_ = bf16[32,2176]{1,0:T(8,128)(2,1)S(1)} collective-permute-done((bf16[32,2176]{1,0:T(8,128)(2,1)}, bf16[32,2176]{1,0:T(8,128)(2,1)S(1)}, u32[]{:S(2)}, u32[]{:S(2)}) %collective-permute-start.7) | collective-permute-done | bytes 139296 | tf_op jit(solution)/shard_map/ppermute | solution.py:54
  81.2 0.6 copy-done.11
  81.8 2.4 %shard_map.183 = (bf16[8,32,768]{2,1,0:T(8,128)(2,1)}, bf16[8,32,256]{2,1,0:T(8,128)(2,1)}, bf16[8,32,1152]{2,1,0:T(8,128)(2,1)}) custom-call(s32[1]{0:T(128)} %bitcast.6.index, bf16[32,2176]{1,0:T(8,128)(2,1)} %copy-done.5, bf16[32,2176]{1,0:T(8,128)(2,1)} %copy-done.6, bf16[32,2176]{1,0:T(8,128)(2,1)} %copy-done.7, bf16[32,2176]{1,0:T(8,128)(2,1)} %copy-done.8, ...), custom_call_target="tpu_custom_call" | custom-call | flops 16777216 | bytes 2097152 | tf_op jit(solution)/shard_map/pallas_call | solution.py:37
  84.2 3.6 %collective-permute-start.8 = (bf16[8,32,768]{2,1,0:T(8,128)(2,1)}, bf16[8,32,768]{2,1,0:T(8,128)(2,1)}, u32[]{:S(2)}, u32[]{:S(2)}) collective-permute-start(bf16[8,32,768]{2,1,0:T(8,128)(2,1)} %get-tuple-element.12), channel_id=1, source_target_pairs={{0,8},{8,16},{16,24},{24,0},{1,9},{9,17},{17,25},{25,1},{2,10},{10... | collective-permute-start | bytes 1179656 | tf_op jit(solution)/shard_map/ppermute | solution.py:54
  87.8 2.9 %collective-permute-start.9 = (bf16[8,32,768]{2,1,0:T(8,128)(2,1)}, bf16[8,32,768]{2,1,0:T(8,128)(2,1)}, u32[]{:S(2)}, u32[]{:S(2)}) collective-permute-start(bf16[8,32,768]{2,1,0:T(8,128)(2,1)} %get-tuple-element.12), channel_id=1, source_target_pairs={{0,16},{8,24},{16,0},{24,8},{1,17},{9,25},{17,1},{25,9},{2,18},{10... | collective-permute-start | bytes 1179656 | tf_op jit(solution)/shard_map/ppermute | solution.py:54
  90.7 4.3 %collective-permute-start.10 = (bf16[8,32,768]{2,1,0:T(8,128)(2,1)}, bf16[8,32,768]{2,1,0:T(8,128)(2,1)}, u32[]{:S(2)}, u32[]{:S(2)}) collective-permute-start(bf16[8,32,768]{2,1,0:T(8,128)(2,1)} %get-tuple-element.12), channel_id=1, source_target_pairs={{0,24},{8,0},{16,8},{24,16},{1,25},{9,1},{17,9},{25,17},{2,26},{10... | collective-permute-start | bytes 1179656 | tf_op jit(solution)/shard_map/ppermute | solution.py:54
  95.0 1.9 collective-permute-start.12
  96.9 1.5 collective-permute-done.12.theirs
  98.5 0.7 copy-done.12
  99.1 2.0 shard_map.185
  101.2 4.8 %all-to-all-start.1 = ((bf16[4,8,32,512]{3,2,1,0:T(8,128)(2,1)}), bf16[4,8,32,512]{3,2,1,0:T(8,128)(2,1)S(1)}, u32[]{:S(2)}, u32[]{:S(2)}) async-start(bf16[4,8,32,512]{3,2,1,0:T(8,128)(2,1)} %shard_map.185), calls=%async_computation.1 | async-start | bytes 2097152 | tf_op jit(solution)/shard_map/all_to_all | solution.py:340
  106.0 3.4 %collective-permute-start.14 = (bf16[8,32,1152]{2,1,0:T(8,128)(2,1)S(1)}, bf16[8,32,1152]{2,1,0:T(8,128)(2,1)S(1)}, u32[]{:S(2)}, u32[]{:S(2)}) collective-permute-start(bf16[8,32,1152]{2,1,0:T(8,128)(2,1)S(1)} %copy-done.3), channel_id=1, source_target_pairs={{0,8},{8,16},{16,24},{24,0},{1,9},{9,17},{17,25},{25,1},{2,10},{10... | collective-permute-start | bytes 1769480 | tf_op jit(solution)/shard_map/ppermute | solution.py:54
  109.4 2.6 %collective-permute-start.15 = (bf16[8,32,1152]{2,1,0:T(8,128)(2,1)S(1)}, bf16[8,32,1152]{2,1,0:T(8,128)(2,1)}, u32[]{:S(2)}, u32[]{:S(2)}) collective-permute-start(bf16[8,32,1152]{2,1,0:T(8,128)(2,1)S(1)} %copy-done.3), channel_id=1, source_target_pairs={{0,16},{8,24},{16,0},{24,8},{1,17},{9,25},{17,1},{25,9},{2,18},{10... | collective-permute-start | bytes 1769480 | tf_op jit(solution)/shard_map/ppermute | solution.py:54
  112.0 4.5 %collective-permute-start.16 = (bf16[8,32,1152]{2,1,0:T(8,128)(2,1)S(1)}, bf16[8,32,1152]{2,1,0:T(8,128)(2,1)}, u32[]{:S(2)}, u32[]{:S(2)}) collective-permute-start(bf16[8,32,1152]{2,1,0:T(8,128)(2,1)S(1)} %copy-done.3), channel_id=1, source_target_pairs={{0,24},{8,0},{16,8},{24,16},{1,25},{9,1},{17,9},{25,17},{2,26},{10... | collective-permute-start | bytes 1769480 | tf_op jit(solution)/shard_map/ppermute | solution.py:54
  116.5 0.6 pad_add_fusion.index
  117.1 6.2 %shard_map.184 = (bf16[512,256]{1,0:T(8,128)(2,1)}, bf16[512,256]{1,0:T(8,128)(2,1)}) custom-call(s32[2]{0:T(128)} %pad_add_fusion.index, f32[2]{0:T(128)} %bitcast.47, bf16[512,1024]{1,0:T(8,128)(2,1)} %bitcast.35, bf16[512,1024]{1,0:T(8,128)(2,1)} %collective-permute-done.other, bf16[256,768]{1,0:T(8,128)(2,1)} %bitcast.46, bf16[256,768]{1,0:T(8,128)(2,1)} %bitcast.10.p1, ...), custom_call_target="tpu_custom_call" | custom-call | flops 4294967296 | bytes 2097152 | tf_op jit(solution)/shard_map/pallas_call | solution.py:37
  123.3 1.9 collective-permute-start.11
  125.2 6.5 %collective-permute-done.14 = bf16[8,32,1152]{2,1,0:T(8,128)(2,1)S(1)} collective-permute-done((bf16[8,32,1152]{2,1,0:T(8,128)(2,1)S(1)}, bf16[8,32,1152]{2,1,0:T(8,128)(2,1)S(1)}, u32[]{:S(2)}, u32[]{:S(2)}) %collective-permute-start.14) | collective-permute-done | bytes 589856 | tf_op jit(solution)/shard_map/ppermute | solution.py:54
  131.7 4.2 %collective-permute-done.15 = bf16[8,32,1152]{2,1,0:T(8,128)(2,1)} collective-permute-done((bf16[8,32,1152]{2,1,0:T(8,128)(2,1)S(1)}, bf16[8,32,1152]{2,1,0:T(8,128)(2,1)}, u32[]{:S(2)}, u32[]{:S(2)}) %collective-permute-start.15) | collective-permute-done | bytes 589856 | tf_op jit(solution)/shard_map/ppermute | solution.py:54
  135.9 11.3 %collective-permute-done.16 = bf16[8,32,1152]{2,1,0:T(8,128)(2,1)} collective-permute-done((bf16[8,32,1152]{2,1,0:T(8,128)(2,1)S(1)}, bf16[8,32,1152]{2,1,0:T(8,128)(2,1)}, u32[]{:S(2)}, u32[]{:S(2)}) %collective-permute-start.16) | collective-permute-done | bytes 589856 | tf_op jit(solution)/shard_map/ppermute | solution.py:54
  147.2 3.2 %shard_map.188 = bf16[8,4,32,1152]{3,2,1,0:T(8,128)(2,1)} custom-call(s32[1]{0:T(128)} %bitcast.1.index, bf16[256,1152]{1,0:T(8,128)(2,1)} %bitcast.38, bf16[256,1152]{1,0:T(8,128)(2,1)} %bitcast.39, bf16[256,1152]{1,0:T(8,128)(2,1)} %bitcast.21.refs_2_, bf16[256,1152]{1,0:T(8,128)(2,1)} %bitcast.22.refs_3_), custom_call_target="tpu_custom_call" | custom-call | flops 16777216 | bytes 2097152 | tf_op jit(solution)/shard_map/pallas_call | solution.py:37
  150.4 1.9 collective-permute-start.17
  152.4 1.0 copy-done.2
  153.5 3.1 %shard_map.186 = bf16[512,1024]{1,0:T(8,128)(2,1)} custom-call(bf16[512,256]{1,0:T(8,128)(2,1)} %get-tuple-element.13.mine, bf16[512,256]{1,0:T(8,128)(2,1)} %copy-done.15, bf16[4,8,32,512]{3,2,1,0:T(8,128)(2,1)} %copy-done.2), custom_call_target="tpu_custom_call" | custom-call | flops 1073741824 | bytes 2097152 | tf_op jit(solution)/shard_map/pallas_call | solution.py:37
  156.6 20.5 %all_to_all.26.pieces = bf16[4,128,1024]{2,1,0:T(8,128)(2,1)} all-to-all(bf16[4,128,1024]{2,1,0:T(8,128)(2,1)} %bitcast.37), channel_id=1, replica_groups=mesh['rep'=2,'z'=8,'y'=4,'x'=4,'c'=2] {'x'}, dimensions={0} | all-to-all | bytes 2097152 | tf_op jit(solution)/shard_map/all_to_all | solution.py:62
  177.1 2.7 %shard_map.187 = (bf16[128,1024]{1,0:T(8,128)(2,1)}, bf16[4,128,1024]{2,1,0:T(8,128)(2,1)}) custom-call(bf16[4,128,1024]{2,1,0:T(8,128)(2,1)} %all_to_all.26.pieces, bf16[128,1024]{1,0:T(8,128)(2,1)} %bitcast.33, f32[1,1024]{1,0:T(1,128)} %bitcast.43, f32[1,1024]{1,0:T(1,128)} %bitcast.44), custom_call_target="tpu_custom_call" | custom-call | flops 16777216 | bytes 2097152 | tf_op jit(solution)/shard_map/pallas_call | solution.py:37
  179.8 18.4 %all_to_all.27 = bf16[4,128,1024]{2,1,0:T(8,128)(2,1)S(1)} all-to-all(bf16[4,128,1024]{2,1,0:T(8,128)(2,1)} %get-tuple-element.16), channel_id=1, replica_groups=mesh['rep'=2,'z'=8,'y'=4,'x'=4,'c'=2] {'x'}, dimensions={0} | all-to-all | bytes 2097152 | tf_op jit(solution)/shard_map/all_to_all | solution.py:62
  198.2 1.9 collective-permute-start.13
  201.3 1.3 shard_map.189.my_taps
  202.6 2.4 %collective-permute-start.18 = (f32[8,384]{1,0:T(8,128)}, f32[8,384]{1,0:T(8,128)S(1)}, u32[]{:S(2)}, u32[]{:S(2)}) collective-permute-start(f32[8,384]{1,0:T(8,128)} %shard_map.189.my_taps), channel_id=1, source_target_pairs={{0,1},{1,0},{2,3},{3,2},{4,5},{5,4},{6,7},{7,6},{8,9},{9,8},{10,11... | collective-permute-start | bytes 36872 | tf_op jit(solution)/shard_map/ppermute | solution.py:58
  205.0 1.0 collective-permute-done.18.their_taps
  206.7 7.7 %shard_map.190 = bf16[512,1024]{1,0:T(8,128)(2,1)} custom-call(s32[1]{0:T(128)} %bitcast.index, bf16[512,1024]{1,0:T(8,128)(2,1)} %bitcast.31, bf16[8,1024]{1,0:T(8,128)(2,1)} %copy-done.16, bf16[1024,1152]{1,0:T(8,128)(2,1)} %bitcast.30, bf16[1024,1152]{1,0:T(8,128)(2,1)} %collective-permute-done.17.theirs, f32[8,384]{1,0:T(8,128)} %shard_map.189.my_taps, ...), custom_call_target="tpu_custom_call" | custom-call | flops 4294967296 | bytes 2097152 | tf_op jit(solution)/shard_map/pallas_call | solution.py:37
  214.4 20.2 %all_to_all.28.pieces = bf16[4,128,1024]{2,1,0:T(8,128)(2,1)} all-to-all(bf16[4,128,1024]{2,1,0:T(8,128)(2,1)} %bitcast.36), channel_id=1, replica_groups=mesh['rep'=2,'z'=8,'y'=4,'x'=4,'c'=2] {'x'}, dimensions={0} | all-to-all | bytes 2097152 | tf_op jit(solution)/shard_map/all_to_all | solution.py:62
  234.6 2.3 shard_map.191
  (49 shorter events, 2.0 us)
Async XLA Ops:
  21.5 79.7 %copy-start.1 = (bf16[4,128,1024]{2,1,0:T(8,128)(2,1)}, bf16[4,128,1024]{2,1,0:T(8,128)(2,1)S(1)}, u32[]{:S(2)}) copy-start(bf16[4,128,1024]{2,1,0:T(8,128)(2,1)S(1)} %all_to_all.25) | copy-start | bytes 3145732
  21.5 95.6 %collective-permute-start = (bf16[512,1024]{1,0:T(8,128)(2,1)S(1)}, bf16[512,1024]{1,0:T(8,128)(2,1)}, u32[]{:S(2)}, u32[]{:S(2)}) collective-permute-start(bf16[512,1024]{1,0:T(8,128)(2,1)S(1)} %bitcast.34), channel_id=1, source_target_pairs={{0,1},{1,0},{2,3},{3,2},{4,5},{5,4},{6,7},{7,6},{8,9},{9,8},{10,11... | collective-permute-start | bytes 3145736 | tf_op jit(solution)/shard_map/ppermute | solution.py:58
  24.9 21.4 %collective-permute-start.1 = (bf16[32,2176]{1,0:T(8,128)(2,1)}, bf16[32,2176]{1,0:T(8,128)(2,1)S(1)}, u32[]{:S(2)}, u32[]{:S(2)}) collective-permute-start(bf16[32,2176]{1,0:T(8,128)(2,1)} %shard_map.182.refs_4_), channel_id=1, source_target_pairs={{0,128},{32,160},{64,192},{96,224},{128,256},{160,288},{192,320},{... | collective-permute-start | bytes 417800 | tf_op jit(solution)/shard_map/ppermute | solution.py:54
  34.0 23.9 %collective-permute-start.2 = (bf16[32,2176]{1,0:T(8,128)(2,1)}, bf16[32,2176]{1,0:T(8,128)(2,1)S(1)}, u32[]{:S(2)}, u32[]{:S(2)}) collective-permute-start(bf16[32,2176]{1,0:T(8,128)(2,1)} %shard_map.182.refs_4_), channel_id=1, source_target_pairs={{0,96},{32,128},{64,160},{96,192},{128,224},{160,256},{192,288},{2... | collective-permute-start | bytes 417800 | tf_op jit(solution)/shard_map/ppermute | solution.py:54
  40.0 21.4 %collective-permute-start.3 = (bf16[32,2176]{1,0:T(8,128)(2,1)}, bf16[32,2176]{1,0:T(8,128)(2,1)S(1)}, u32[]{:S(2)}, u32[]{:S(2)}) collective-permute-start(bf16[32,2176]{1,0:T(8,128)(2,1)} %shard_map.182.refs_4_), channel_id=1, source_target_pairs={{0,64},{32,96},{64,128},{96,160},{128,192},{160,224},{192,256},{22... | collective-permute-start | bytes 417800 | tf_op jit(solution)/shard_map/ppermute | solution.py:54
  43.4 22.3 %collective-permute-start.4 = (bf16[32,2176]{1,0:T(8,128)(2,1)}, bf16[32,2176]{1,0:T(8,128)(2,1)S(1)}, u32[]{:S(2)}, u32[]{:S(2)}) collective-permute-start(bf16[32,2176]{1,0:T(8,128)(2,1)} %shard_map.182.refs_4_), channel_id=1, source_target_pairs={{0,32},{32,64},{64,96},{96,128},{128,160},{160,192},{192,224},{224... | collective-permute-start | bytes 417800 | tf_op jit(solution)/shard_map/ppermute | solution.py:54
  46.3 34.8 %copy-start.5 = (bf16[32,2176]{1,0:T(8,128)(2,1)}, bf16[32,2176]{1,0:T(8,128)(2,1)S(1)}, u32[]{:S(2)}) copy-start(bf16[32,2176]{1,0:T(8,128)(2,1)S(1)} %collective-permute-done.1.refs_0_) | copy-start | bytes 417796
  46.3 19.4 %collective-permute-start.5 = (bf16[32,2176]{1,0:T(8,128)(2,1)}, bf16[32,2176]{1,0:T(8,128)(2,1)S(1)}, u32[]{:S(2)}, u32[]{:S(2)}) collective-permute-start(bf16[32,2176]{1,0:T(8,128)(2,1)} %shard_map.182.refs_4_), channel_id=1, source_target_pairs={{0,480},{32,0},{64,32},{96,64},{128,96},{160,128},{192,160},{224,1... | collective-permute-start | bytes 417800 | tf_op jit(solution)/shard_map/ppermute | solution.py:54
  58.0 23.2 %copy-start.6 = (bf16[32,2176]{1,0:T(8,128)(2,1)}, bf16[32,2176]{1,0:T(8,128)(2,1)S(1)}, u32[]{:S(2)}) copy-start(bf16[32,2176]{1,0:T(8,128)(2,1)S(1)} %collective-permute-done.2.refs_1_) | copy-start | bytes 417796
  58.0 13.1 %collective-permute-start.6 = (bf16[32,2176]{1,0:T(8,128)(2,1)}, bf16[32,2176]{1,0:T(8,128)(2,1)S(1)}, u32[]{:S(2)}, u32[]{:S(2)}) collective-permute-start(bf16[32,2176]{1,0:T(8,128)(2,1)} %shard_map.182.refs_4_), channel_id=1, source_target_pairs={{0,448},{32,480},{64,0},{96,32},{128,64},{160,96},{192,128},{224,1... | collective-permute-start | bytes 417800 | tf_op jit(solution)/shard_map/ppermute | solution.py:54
  61.4 19.8 %copy-start.7 = (bf16[32,2176]{1,0:T(8,128)(2,1)}, bf16[32,2176]{1,0:T(8,128)(2,1)S(1)}, u32[]{:S(2)}) copy-start(bf16[32,2176]{1,0:T(8,128)(2,1)S(1)} %collective-permute-done.3.refs_2_) | copy-start | bytes 417796
  61.4 19.8 %collective-permute-start.7 = (bf16[32,2176]{1,0:T(8,128)(2,1)}, bf16[32,2176]{1,0:T(8,128)(2,1)S(1)}, u32[]{:S(2)}, u32[]{:S(2)}) collective-permute-start(bf16[32,2176]{1,0:T(8,128)(2,1)} %shard_map.182.refs_4_), channel_id=1, source_target_pairs={{0,416},{32,448},{64,480},{96,0},{128,32},{160,64},{192,96},{224,1... | collective-permute-start | bytes 417800 | tf_op jit(solution)/shard_map/ppermute | solution.py:54
  65.7 15.4 %copy-start.8 = (bf16[32,2176]{1,0:T(8,128)(2,1)}, bf16[32,2176]{1,0:T(8,128)(2,1)S(1)}, u32[]{:S(2)}) copy-start(bf16[32,2176]{1,0:T(8,128)(2,1)S(1)} %collective-permute-done.4.refs_3_) | copy-start | bytes 417796
  65.7 15.4 %copy-start.9 = (bf16[32,2176]{1,0:T(8,128)(2,1)}, bf16[32,2176]{1,0:T(8,128)(2,1)S(1)}, u32[]{:S(2)}) copy-start(bf16[32,2176]{1,0:T(8,128)(2,1)S(1)} %collective-permute-done.5.refs_5_) | copy-start | bytes 417796
  71.0 10.2 %copy-start.10 = (bf16[32,2176]{1,0:T(8,128)(2,1)}, bf16[32,2176]{1,0:T(8,128)(2,1)S(1)}, u32[]{:S(2)}) copy-start(bf16[32,2176]{1,0:T(8,128)(2,1)S(1)} %collective-permute-done.6.refs_6_) | copy-start | bytes 417796
  81.2 0.7 copy-start.11
  84.2 21.8 %copy-start.3 = (bf16[8,32,1152]{2,1,0:T(8,128)(2,1)S(1)}, bf16[8,32,1152]{2,1,0:T(8,128)(2,1)}, u32[]{:S(2)}) copy-start(bf16[8,32,1152]{2,1,0:T(8,128)(2,1)} %get-tuple-element.17) | copy-start | bytes 1769476
  84.2 25.2 %collective-permute-start.8 = (bf16[8,32,768]{2,1,0:T(8,128)(2,1)}, bf16[8,32,768]{2,1,0:T(8,128)(2,1)}, u32[]{:S(2)}, u32[]{:S(2)}) collective-permute-start(bf16[8,32,768]{2,1,0:T(8,128)(2,1)} %get-tuple-element.12), channel_id=1, source_target_pairs={{0,8},{8,16},{16,24},{24,0},{1,9},{9,17},{17,25},{25,1},{2,10},{10... | collective-permute-start | bytes 1179656 | tf_op jit(solution)/shard_map/ppermute | solution.py:54
  87.8 24.1 %collective-permute-start.9 = (bf16[8,32,768]{2,1,0:T(8,128)(2,1)}, bf16[8,32,768]{2,1,0:T(8,128)(2,1)}, u32[]{:S(2)}, u32[]{:S(2)}) collective-permute-start(bf16[8,32,768]{2,1,0:T(8,128)(2,1)} %get-tuple-element.12), channel_id=1, source_target_pairs={{0,16},{8,24},{16,0},{24,8},{1,17},{9,25},{17,1},{25,9},{2,18},{10... | collective-permute-start | bytes 1179656 | tf_op jit(solution)/shard_map/ppermute | solution.py:54
  90.7 26.4 %collective-permute-start.10 = (bf16[8,32,768]{2,1,0:T(8,128)(2,1)}, bf16[8,32,768]{2,1,0:T(8,128)(2,1)}, u32[]{:S(2)}, u32[]{:S(2)}) collective-permute-start(bf16[8,32,768]{2,1,0:T(8,128)(2,1)} %get-tuple-element.12), channel_id=1, source_target_pairs={{0,24},{8,0},{16,8},{24,16},{1,25},{9,1},{17,9},{25,17},{2,26},{10... | collective-permute-start | bytes 1179656 | tf_op jit(solution)/shard_map/ppermute | solution.py:54
  95.0 3.5 %collective-permute-start.12 = (bf16[8,32,256]{2,1,0:T(8,128)(2,1)}, bf16[8,32,256]{2,1,0:T(8,128)(2,1)S(1)}, u32[]{:S(2)}, u32[]{:S(2)}) collective-permute-start(bf16[8,32,256]{2,1,0:T(8,128)(2,1)} %get-tuple-element.15.mine), channel_id=1, source_target_pairs={{0,1},{1,0},{2,3},{3,2},{4,5},{5,4},{6,7},{7,6},{8,9},{9,8},{10,11... | collective-permute-start | bytes 393224 | tf_op jit(solution)/shard_map/ppermute | solution.py:58
  98.5 0.7 copy-start.12
  101.2 51.2 %all-to-all-start.1 = ((bf16[4,8,32,512]{3,2,1,0:T(8,128)(2,1)}), bf16[4,8,32,512]{3,2,1,0:T(8,128)(2,1)S(1)}, u32[]{:S(2)}, u32[]{:S(2)}) async-start(bf16[4,8,32,512]{3,2,1,0:T(8,128)(2,1)} %shard_map.185), calls=%async_computation.1 | async-start | bytes 2097152 | tf_op jit(solution)/shard_map/all_to_all | solution.py:340
  106.0 25.7 %collective-permute-start.14 = (bf16[8,32,1152]{2,1,0:T(8,128)(2,1)S(1)}, bf16[8,32,1152]{2,1,0:T(8,128)(2,1)S(1)}, u32[]{:S(2)}, u32[]{:S(2)}) collective-permute-start(bf16[8,32,1152]{2,1,0:T(8,128)(2,1)S(1)} %copy-done.3), channel_id=1, source_target_pairs={{0,8},{8,16},{16,24},{24,0},{1,9},{9,17},{17,25},{25,1},{2,10},{10... | collective-permute-start | bytes 1769480 | tf_op jit(solution)/shard_map/ppermute | solution.py:54
  109.4 26.5 %collective-permute-start.15 = (bf16[8,32,1152]{2,1,0:T(8,128)(2,1)S(1)}, bf16[8,32,1152]{2,1,0:T(8,128)(2,1)}, u32[]{:S(2)}, u32[]{:S(2)}) collective-permute-start(bf16[8,32,1152]{2,1,0:T(8,128)(2,1)S(1)} %copy-done.3), channel_id=1, source_target_pairs={{0,16},{8,24},{16,0},{24,8},{1,17},{9,25},{17,1},{25,9},{2,18},{10... | collective-permute-start | bytes 1769480 | tf_op jit(solution)/shard_map/ppermute | solution.py:54
  112.0 35.3 %collective-permute-start.16 = (bf16[8,32,1152]{2,1,0:T(8,128)(2,1)S(1)}, bf16[8,32,1152]{2,1,0:T(8,128)(2,1)}, u32[]{:S(2)}, u32[]{:S(2)}) collective-permute-start(bf16[8,32,1152]{2,1,0:T(8,128)(2,1)S(1)} %copy-done.3), channel_id=1, source_target_pairs={{0,24},{8,0},{16,8},{24,16},{1,25},{9,1},{17,9},{25,17},{2,26},{10... | collective-permute-start | bytes 1769480 | tf_op jit(solution)/shard_map/ppermute | solution.py:54
  123.3 29.1 %collective-permute-start.11 = (bf16[512,256]{1,0:T(8,128)(2,1)}, bf16[512,256]{1,0:T(8,128)(2,1)S(1)}, u32[]{:S(2)}, u32[]{:S(2)}) collective-permute-start(bf16[512,256]{1,0:T(8,128)(2,1)} %get-tuple-element.14), channel_id=1, source_target_pairs={{0,1},{1,0},{2,3},{3,2},{4,5},{5,4},{6,7},{7,6},{8,9},{9,8},{10,11... | collective-permute-start | bytes 786440 | tf_op jit(solution)/shard_map/ppermute | solution.py:58
  131.7 15.6 %copy-start.4 = (bf16[8,32,1152]{2,1,0:T(8,128)(2,1)}, bf16[8,32,1152]{2,1,0:T(8,128)(2,1)S(1)}, u32[]{:S(2)}) copy-start(bf16[8,32,1152]{2,1,0:T(8,128)(2,1)S(1)} %collective-permute-done.14) | copy-start | bytes 1769476
  150.4 55.6 %collective-permute-start.17 = (bf16[1024,1152]{1,0:T(8,128)(2,1)}, bf16[1024,1152]{1,0:T(8,128)(2,1)}, u32[]{:S(2)}, u32[]{:S(2)}) collective-permute-start(bf16[1024,1152]{1,0:T(8,128)(2,1)} %bitcast.29), channel_id=1, source_target_pairs={{0,1},{1,0},{2,3},{3,2},{4,5},{5,4},{6,7},{7,6},{8,9},{9,8},{10,11... | collective-permute-start | bytes 7077896 | tf_op jit(solution)/shard_map/ppermute | solution.py:58
  152.4 1.0 copy-start.2
  152.4 1.1 copy-start.15
  156.6 43.6 %copy-start.13 = (f32[352]{0:T(512)S(1)}, f32[352]{0:T(512)}, u32[]{:S(2)}) copy-start(f32[352]{0:T(512)} %param.33) | copy-start | bytes 4228
  156.6 44.1 %copy-start.14 = (f32[352]{0:T(512)S(1)}, f32[352]{0:T(512)}, u32[]{:S(2)}) copy-start(f32[352]{0:T(512)} %param.34) | copy-start | bytes 4228
  198.1 7.9 %copy-start = (bf16[4,128,1024]{2,1,0:T(8,128)(2,1)}, bf16[4,128,1024]{2,1,0:T(8,128)(2,1)S(1)}, u32[]{:S(2)}) copy-start(bf16[4,128,1024]{2,1,0:T(8,128)(2,1)S(1)} %all_to_all.27) | copy-start | bytes 3145732
  198.2 7.8 %collective-permute-start.13 = (bf16[8,1024]{1,0:T(8,128)(2,1)S(1)}, bf16[8,1024]{1,0:T(8,128)(2,1)S(1)}, u32[]{:S(2)}, u32[]{:S(2)}) collective-permute-start(bf16[8,1024]{1,0:T(8,128)(2,1)S(1)} %pad_maximum_fusion), channel_id=1, source_target_pairs={{0,1},{1,0},{2,3},{3,2},{4,5},{5,4},{6,7},{7,6},{8,9},{9,8},{10,11... | collective-permute-start | bytes 49160 | tf_op jit(solution)/shard_map/ppermute | solution.py:58
  202.6 3.4 %collective-permute-start.18 = (f32[8,384]{1,0:T(8,128)}, f32[8,384]{1,0:T(8,128)S(1)}, u32[]{:S(2)}, u32[]{:S(2)}) collective-permute-start(f32[8,384]{1,0:T(8,128)} %shard_map.189.my_taps), channel_id=1, source_target_pairs={{0,1},{1,0},{2,3},{3,2},{4,5},{5,4},{6,7},{7,6},{8,9},{9,8},{10,11... | collective-permute-start | bytes 36872 | tf_op jit(solution)/shard_map/ppermute | solution.py:58
  206.0 0.6 copy-start.17
  206.1 0.6 copy-start.16

commit v3 on v2

--- a/solution.py
+++ b/solution.py
@@ -97,7 +97,8 @@
     for shift, piece in zip(Z_SHIFTS, pieces):
         at = lax.rem(index[0] - shift + 8, 8)
         one[at] = piece[:, :FIRST]
-        two[at] = piece[:, FIRST : FIRST + SECOND]
+        for y in range(two.shape[0]):
+            two[y, at] = piece[:, FIRST : FIRST + SECOND]
         three[at] = piece[:, FIRST + SECOND :]
 
 
@@ -111,21 +112,21 @@
 
 def summed(pieces):
     total = pieces[0].astype(f32)
-    for k in range(1, pieces.shape[0]):
-        total = total + pieces[k].astype(f32)
+    for piece in pieces[1:]:
+        total = total + piece.astype(f32)
     return total * lax.rsqrt(jnp.mean(total * total, axis=-1, keepdims=True) + epsilon)
 
 
 def middle_body(pieces, tokens, out_gain, in_gain, after_mix, channel_in):
-    mix = (tokens[...].astype(f32) + summed(pieces) * out_gain[...]).astype(bf16)
+    mix = (tokens[...].astype(f32) + summed([pieces[k] for k in range(4)]) * out_gain[...]).astype(bf16)
     after_mix[...] = mix
     rows = rms_rows(mix.astype(f32), in_gain[...]).astype(bf16)
     for k in range(channel_in.shape[0]):
         channel_in[k] = rows
 
 
-def final_body(pieces, after_mix, gain, out):
-    out[...] = (after_mix[...].astype(f32) + summed(pieces) * gain[...]).astype(bf16)
+def final_body(here, right, left, far, after_mix, gain, out):
+    out[...] = (after_mix[...].astype(f32) + summed([here[...], right[...], left[...], far[...]]) * gain[...]).astype(bf16)
 
 
 def log_sigmoid_tile(logit):
@@ -135,9 +136,9 @@
 
 
 def attend_body(
-    index, logits, own, other, p0, p1, p2, p3, frequency, out_own, out_other, w, qs, ks, vs, gs
+    y_ref, core_ref, logits, own, other, p0, p1, p2, p3, frequency, out_own, out_other, w, qs, ks, vs, gs
 ):
-    y, core = index[0], index[1]
+    y, core = y_ref[0], core_ref[0]
     for shift, piece in zip(Y_SHIFTS, (p0, p1, p2, p3)):
         at = lax.rem(y - shift + 4, 4) * 32
         for z in range(8):
@@ -200,56 +201,94 @@
             out_other[r * 128 - 512 : r * 128 - 384, :] = gated
 
 
-def spread_body(mine, theirs, out):
-    for y in range(out.shape[0]):
-        out[y, :, :, :DV] = mine[...]
-        out[y, :, :, DV:] = theirs[...]
-
-
-def output_body(mine, theirs, pieces, out, w):
+def output_body(mine, theirs, my_pieces, their_pieces, out, w):
     for y in range(4):
         for z in range(8):
             at = z * 128 + y * 32
-            w[at : at + 32, :] = pieces[y, z]
+            w[at : at + 32, :DV] = my_pieces[y, z]
+            w[at : at + 32, DV:] = their_pieces[y, z]
     step = 256
     for d in range(0, 1024, step):
         part = dot_nt(mine[...], w[d : d + step, :DV]) + dot_nt(theirs[...], w[d : d + step, DV:])
         out[:, d : d + step] = part.astype(bf16)
 
 
-def feed_body(index, rows, edges, mine, theirs, my_taps, their_taps, out, hidden):
-    core = index[0]
+def feed_block(main, before, after, taps):
     line = lax.broadcasted_iota(jnp.int32, (128, 1), 0)
-    for part, (weights, taps) in enumerate(((mine, my_taps), (theirs, their_taps))):
-        kernel = [
-            jnp.concatenate([taps[t : t + 1, :], taps[t + 3 : t + 4, :]], axis=1) for t in range(3)
-        ]
-        bias = jnp.concatenate([taps[6:7, :], taps[7:8, :]], axis=1)
-        edge = dot(edges[...], weights[:, : 2 * PAD])
-        none = jnp.zeros((1, 2 * PAD), f32)
-        for x in range(4):
-            main = dot(rows[x * 128 : x * 128 + 128, :], weights[:, : 2 * PAD])
-            last = edge[4 + x : 5 + x, :]
-            sooner = edge[3 + x : 4 + x, :] if x else none
-            first = edge[x : x + 1, :]
-            later = edge[x + 1 : x + 2, :] if x < 3 else none
-            before = jnp.where(core == 0, sooner, last)
-            after = jnp.where(core == 0, first, later)
-            prev = jnp.where(line == 0, before, pltpu.roll(main, 1, 0))
-            nxt = jnp.where(line == 127, after, pltpu.roll(main, 127, 0))
-            conv = kernel[0] * prev + kernel[1] * main + kernel[2] * nxt + bias
-            value = conv[:, :PAD]
-            bent = value * (
-                0.5 + 0.5 * jnp.tanh(0.7978845608028654 * (value + 0.044715 * value**3))
-            )
-            hidden[x * 128 : x * 128 + 128, part * PAD : part * PAD + PAD] = (
-                bent * conv[:, PAD:]
-            ).astype(bf16)
+    prev = jnp.where(line == 0, before, pltpu.roll(main, 1, 0))
+    nxt = jnp.where(line == 127, after, pltpu.roll(main, 127, 0))
+    kernel = [
+        jnp.concatenate([taps[t : t + 1, :], taps[t + 3 : t + 4, :]], axis=1) for t in range(3)
+    ]
+    bias = jnp.concatenate([taps[6:7, :], taps[7:8, :]], axis=1)
+    conv = kernel[0] * prev + kernel[1] * main + kernel[2] * nxt + bias
+    value = conv[:, :PAD]
+    bent = value * (0.5 + 0.5 * jnp.tanh(0.7978845608028654 * (value + 0.044715 * value**3)))
+    return (bent * conv[:, PAD:]).astype(bf16)
+
+
+def feed_down(hidden, mine, theirs, outs):
     for d in range(0, 1024, 256):
         total = dot_nt(hidden[:, :PAD], mine[d : d + 256, 2 * PAD :]) + dot_nt(
             hidden[:, PAD:], theirs[d : d + 256, 2 * PAD :]
         )
-        out[:, d : d + 256] = total.astype(bf16)
+        for place, out in enumerate(outs):
+            out[:, d : d + 256] = total[place * 128 : place * 128 + 128, :].astype(bf16)
+
+
+def feed_far_body(
+    x_ref, core_ref, rows, edges, mine, theirs, my_taps, their_taps, out, outer, lines, hidden
+):
+    core = core_ref[0]
+    block = lax.rem(x_ref[0] + 2, 4)
+    lines[:128, :] = rows[pl.ds(pl.multiple_of(block * 128, 128), 128), :]
+    lines[128:136, :] = edges[...]
+    lines[136:144, :] = jnp.zeros((8, 1024), bf16)
+    outer[...] = jnp.zeros(outer.shape, f32)
+    for part, (weights, taps) in enumerate(((mine, my_taps), (theirs, their_taps))):
+        columns = slice(part * 2 * PAD, part * 2 * PAD + 2 * PAD)
+        main = dot(lines[...], weights[:, : 2 * PAD])
+        for x in range(4):
+            outer[8 + x : 9 + x, columns] = main[128 + 2 * x : 129 + 2 * x, :]
+            outer[1 + x : 2 + x, columns] = main[129 + 2 * x : 130 + 2 * x, :]
+        before = outer[pl.ds(block + core, 1), columns]
+        after = outer[pl.ds(8 + block + core, 1), columns]
+        hidden[:, part * PAD : part * PAD + PAD] = feed_block(main[:128, :], before, after, taps)
+    feed_down(hidden, mine, theirs, (out,))
+
+
+def feed_near_body(
+    x_ref,
+    core_ref,
+    rows,
+    outer,
+    mine,
+    theirs,
+    my_taps,
+    their_taps,
+    right,
+    left,
+    here,
+    lines,
+    hidden,
+):
+    core = core_ref[0]
+    blocks = [lax.rem(x_ref[0] + k, 4) for k in (1, 3, 0)]
+    for place, block in enumerate(blocks):
+        lines[place * 128 : place * 128 + 128, :] = rows[
+            pl.ds(pl.multiple_of(block * 128, 128), 128), :
+        ]
+    for part, (weights, taps) in enumerate(((mine, my_taps), (theirs, their_taps))):
+        columns = slice(part * 2 * PAD, part * 2 * PAD + 2 * PAD)
+        main = dot(lines[...], weights[:, : 2 * PAD])
+        for place, block in enumerate(blocks):
+            inner = slice(place * 128, place * 128 + 128)
+            before = outer[pl.ds(block + core, 1), columns]
+            after = outer[pl.ds(8 + block + core, 1), columns]
+            hidden[inner, part * PAD : part * PAD + PAD] = feed_block(
+                main[inner, :], before, after, taps
+            )
+    feed_down(hidden, mine, theirs, (right, left, here))
 
 
 def head_norm(values):
@@ -330,26 +369,26 @@
     normed_other = swap(normed_own)
     first_z, second_z, third_z = call(
         ring_order_body,
-        [shape((8, 32, FIRST)), shape((8, 32, SECOND)), shape((8, 32, THIRD))],
+        [shape((8, 32, FIRST)), shape((4, 8, 32, SECOND)), shape((8, 32, THIRD))],
         z_index[None],
         *[got[s] for s in Z_SHIFTS],
         smem=1,
     )
     first_pieces = line_gather(first_z)
-    second_spread = call(spread_body, shape((4, 8, 32, 2 * SECOND)), second_z, swap(second_z))
-    second_pieces = lax.all_to_all(second_spread, "y", 0, 0, tiled=True)
+    second_own = lax.all_to_all(second_z, "y", 0, 0, tiled=True)
     third_pieces = line_gather(third_z)
     gated_own, gated_other = call(
         attend_body,
         [shape((half, DV)), shape((half, DV))],
-        jnp.stack([y_index, core]),
+        y_index[None],
+        core[None],
         decay_logits[:, 0],
         normed_own,
         normed_other,
         *first_pieces,
         rope_frequency(),
         flops=1 << 32,
-        smem=2,
+        smem=3,
         scratch=[
             pltpu.VMEM((model, FIRST), bf16),
             pltpu.VMEM((2 * half, DK), bf16),
@@ -364,7 +403,8 @@
         shape((half, model)),
         gated_own,
         gated_partner,
-        second_pieces,
+        second_own,
+        swap(second_own),
         flops=1 << 30,
         scratch=[pltpu.VMEM((model, 2 * SECOND), bf16)],
     )
@@ -391,24 +431,55 @@
         line_order_body, shape((8, 4, 32, THIRD)), y_index[None], *third_pieces, smem=1
     ).reshape(model, THIRD)
     third_other = swap(third_own)
-    edges = jnp.concatenate([channel_rows[:, 0], channel_rows[:, own - 1]], axis=0)
+    edges = lax.slice(
+        channel_rows, (0, 0, 0), (chips, own, model), (1, own - 1, 1)
+    ).reshape(2 * chips, model)
     edges_other = swap(edges)
-    channel = call(
-        feed_body,
-        shape((half, model)),
+    flat_rows = channel_rows.reshape(half, model)
+    x_index = lax.axis_index("x").astype(jnp.int32)[None]
+    far, outer = call(
+        feed_far_body,
+        [shape((own, model)), shape((16, 4 * PAD), f32)],
+        x_index,
         core[None],
-        channel_rows.reshape(half, model),
+        flat_rows,
         edges_other,
         third_own,
         third_other,
         taps,
         taps_other,
+        flops=1 << 31,
+        smem=2,
+        scratch=[pltpu.VMEM((own + 16, model), bf16), pltpu.VMEM((own, 2 * PAD), bf16)],
+    )
+    far_got = permuted(far, "x", 2, 4)
+    right, left, here = call(
+        feed_near_body,
+        [shape((own, model))] * 3,
+        x_index,
+        core[None],
+        flat_rows,
+        outer,
+        third_own,
+        third_other,
+        taps,
+        taps_other,
         flops=1 << 32,
-        smem=1,
-        scratch=[pltpu.VMEM((half, 2 * PAD), bf16)],
-    )
-    channel_pieces = exchanged(channel.reshape(chips, own, model))
-    result = call(final_body, shape((own, model)), channel_pieces, after_mix, row(channel_out_gain))
+        smem=2,
+        scratch=[pltpu.VMEM((3 * own, model), bf16), pltpu.VMEM((3 * own, 2 * PAD), bf16)],
+    )
+    right_got = permuted(right, "x", 1, 4)
+    left_got = permuted(left, "x", -1, 4)
+    result = call(
+        final_body,
+        shape((own, model)),
+        here,
+        right_got,
+        left_got,
+        far_got,
+        after_mix,
+        row(channel_out_gain),
+    )
     return result[None]
 
 

time: 238 us -> 216 us (0.908)
  the two profiles are of different devices: /device:TPU:104 before, /device:TPU:14 now
where the time goes in v3:
time: 216 us; the launch traced here: 214 us
  starting transfers between devices  91.5 us (42%)
  waiting for transfers between devices  45.2 us (21%)
  Pallas kernels  36.3 us (17%)
  blocking collectives  36.1 us (17%)
  local copies, waits for them, and re-layouts  4.81 us (2%)
    ppermute x16, starting transfers between devices, permuted(): lax.ppermute(value, axes, [(i, (i + shift) % size) for i in range(size)])  68.4 us
    ppermute x16, waiting for transfers between devices, permuted(): lax.ppermute(value, axes, [(i, (i + shift) % size) for i in range(size)])  42.4 us
    pallas_call x11, Pallas kernels, call(): pl.pallas_call(body, out_shape=out_shapes, in_specs=specs, out_specs=VMEM...  36.3 us
    all_to_all x2, blocking collectives, exchanged(): return lax.all_to_all(value, 'x', 0, 0, tiled=True)  36.1 us
    ppermute x6, starting transfers between devices, swap(): return lax.ppermute(value, 'c', SWAP)  12.5 us
    all_to_all x1, starting transfers between devices, layer(): second_own = lax.all_to_all(second_z, 'y', 0, 0, tiled=True)  5.85 us
    all_to_all x1, starting transfers between devices, exchanged(): return lax.all_to_all(value, 'x', 0, 0, tiled=True)  4.77 us
  transfers between devices with their start and end apart: 24, of which 9 were waited for; matrix products, arithmetic and copies ran while one was open for 1% of the time, Pallas kernels for 10%

profile of v3, /device:TPU:14, one launch (start us, length us, event | category | flops | bytes accessed | tf_op | source)
XLA Modules:
  0.0 214.3 jit_solution(12169352618556416626)
XLA Ops:
  0.0 2.1 shard_map.181
  2.1 4.8 %all-to-all-start = ((bf16[4,128,1024]{2,1,0:T(8,128)(2,1)}), bf16[4,128,1024]{2,1,0:T(8,128)(2,1)S(1)}, u32[]{:S(2)}, u32[]{:S(2)}) async-start(bf16[4,128,1024]{2,1,0:T(8,128)(2,1)} %shard_map.181), calls=%async_computation | async-start | bytes 2097152 | tf_op jit(solution)/shard_map/all_to_all | solution.py:62
  6.9 1.5 shard_map.182.refs_4_
  8.4 9.1 %collective-permute-start.1 = (bf16[32,2176]{1,0:T(8,128)(2,1)}, bf16[32,2176]{1,0:T(8,128)(2,1)S(1)}, u32[]{:S(2)}, u32[]{:S(2)}) collective-permute-start(bf16[32,2176]{1,0:T(8,128)(2,1)} %shard_map.182.refs_4_), channel_id=1, source_target_pairs={{0,128},{32,160},{64,192},{96,224},{128,256},{160,288},{192,320},{... | collective-permute-start | bytes 417800 | tf_op jit(solution)/shard_map/ppermute | solution.py:54
  17.5 6.5 %collective-permute-start.2 = (bf16[32,2176]{1,0:T(8,128)(2,1)}, bf16[32,2176]{1,0:T(8,128)(2,1)S(1)}, u32[]{:S(2)}, u32[]{:S(2)}) collective-permute-start(bf16[32,2176]{1,0:T(8,128)(2,1)} %shard_map.182.refs_4_), channel_id=1, source_target_pairs={{0,96},{32,128},{64,160},{96,192},{128,224},{160,256},{192,288},{2... | collective-permute-start | bytes 417800 | tf_op jit(solution)/shard_map/ppermute | solution.py:54
  24.0 5.5 %collective-permute-start.3 = (bf16[32,2176]{1,0:T(8,128)(2,1)}, bf16[32,2176]{1,0:T(8,128)(2,1)S(1)}, u32[]{:S(2)}, u32[]{:S(2)}) collective-permute-start(bf16[32,2176]{1,0:T(8,128)(2,1)} %shard_map.182.refs_4_), channel_id=1, source_target_pairs={{0,64},{32,96},{64,128},{96,160},{128,192},{160,224},{192,256},{22... | collective-permute-start | bytes 417800 | tf_op jit(solution)/shard_map/ppermute | solution.py:54
  29.5 2.9 %collective-permute-start.4 = (bf16[32,2176]{1,0:T(8,128)(2,1)}, bf16[32,2176]{1,0:T(8,128)(2,1)S(1)}, u32[]{:S(2)}, u32[]{:S(2)}) collective-permute-start(bf16[32,2176]{1,0:T(8,128)(2,1)} %shard_map.182.refs_4_), channel_id=1, source_target_pairs={{0,32},{32,64},{64,96},{96,128},{128,160},{160,192},{192,224},{224... | collective-permute-start | bytes 417800 | tf_op jit(solution)/shard_map/ppermute | solution.py:54
  32.5 4.1 %collective-permute-start.5 = (bf16[32,2176]{1,0:T(8,128)(2,1)}, bf16[32,2176]{1,0:T(8,128)(2,1)S(1)}, u32[]{:S(2)}, u32[]{:S(2)}) collective-permute-start(bf16[32,2176]{1,0:T(8,128)(2,1)} %shard_map.182.refs_4_), channel_id=1, source_target_pairs={{0,480},{32,0},{64,32},{96,64},{128,96},{160,128},{192,160},{224,1... | collective-permute-start | bytes 417800 | tf_op jit(solution)/shard_map/ppermute | solution.py:54
  36.6 5.1 %collective-permute-start.6 = (bf16[32,2176]{1,0:T(8,128)(2,1)}, bf16[32,2176]{1,0:T(8,128)(2,1)S(1)}, u32[]{:S(2)}, u32[]{:S(2)}) collective-permute-start(bf16[32,2176]{1,0:T(8,128)(2,1)} %shard_map.182.refs_4_), channel_id=1, source_target_pairs={{0,448},{32,480},{64,0},{96,32},{128,64},{160,96},{192,128},{224,1... | collective-permute-start | bytes 417800 | tf_op jit(solution)/shard_map/ppermute | solution.py:54
  41.7 3.0 %collective-permute-done.2.refs_1_ = bf16[32,2176]{1,0:T(8,128)(2,1)S(1)} collective-permute-done((bf16[32,2176]{1,0:T(8,128)(2,1)}, bf16[32,2176]{1,0:T(8,128)(2,1)S(1)}, u32[]{:S(2)}, u32[]{:S(2)}) %collective-permute-start.2) | collective-permute-done | bytes 139296 | tf_op jit(solution)/shard_map/ppermute | solution.py:54
  44.7 4.1 %collective-permute-start.7 = (bf16[32,2176]{1,0:T(8,128)(2,1)}, bf16[32,2176]{1,0:T(8,128)(2,1)S(1)}, u32[]{:S(2)}, u32[]{:S(2)}) collective-permute-start(bf16[32,2176]{1,0:T(8,128)(2,1)} %shard_map.182.refs_4_), channel_id=1, source_target_pairs={{0,416},{32,448},{64,480},{96,0},{128,32},{160,64},{192,96},{224,1... | collective-permute-start | bytes 417800 | tf_op jit(solution)/shard_map/ppermute | solution.py:54
  48.8 1.9 collective-permute-start
  50.8 7.0 %collective-permute-done.7.refs_7_ = bf16[32,2176]{1,0:T(8,128)(2,1)S(1)} collective-permute-done((bf16[32,2176]{1,0:T(8,128)(2,1)}, bf16[32,2176]{1,0:T(8,128)(2,1)S(1)}, u32[]{:S(2)}, u32[]{:S(2)}) %collective-permute-start.7) | collective-permute-done | bytes 139296 | tf_op jit(solution)/shard_map/ppermute | solution.py:54
  58.4 2.5 %shard_map.183 = (bf16[8,32,768]{2,1,0:T(8,128)(2,1)}, bf16[4,8,32,256]{3,2,1,0:T(8,128)(2,1)}, bf16[8,32,1152]{2,1,0:T(8,128)(2,1)}) custom-call(s32[1]{0:T(128)} %bitcast.7.index, bf16[32,2176]{1,0:T(8,128)(2,1)} %copy-done.9, bf16[32,2176]{1,0:T(8,128)(2,1)} %copy-done.10, bf16[32,2176]{1,0:T(8,128)(2,1)} %copy-done.11, bf16[32,2176]{1,0:T(8,128)(2,1)} %copy-done.12, ...), custom_call_target="tpu_custom_call" | custom-call | flops 16777216 | bytes 2097152 | tf_op jit(solution)/shard_map/pallas_call | solution.py:37
  61.0 3.5 %collective-permute-start.14 = (bf16[8,32,1152]{2,1,0:T(8,128)(2,1)}, bf16[8,32,1152]{2,1,0:T(8,128)(2,1)S(1)}, u32[]{:S(2)}, u32[]{:S(2)}) collective-permute-start(bf16[8,32,1152]{2,1,0:T(8,128)(2,1)} %get-tuple-element.22), channel_id=1, source_target_pairs={{0,8},{8,16},{16,24},{24,0},{1,9},{9,17},{17,25},{25,1},{2,10},{10... | collective-permute-start | bytes 1769480 | tf_op jit(solution)/shard_map/ppermute | solution.py:54
  64.5 2.8 %collective-permute-start.15 = (bf16[8,32,1152]{2,1,0:T(8,128)(2,1)}, bf16[8,32,1152]{2,1,0:T(8,128)(2,1)S(1)}, u32[]{:S(2)}, u32[]{:S(2)}) collective-permute-start(bf16[8,32,1152]{2,1,0:T(8,128)(2,1)} %get-tuple-element.22), channel_id=1, source_target_pairs={{0,16},{8,24},{16,0},{24,8},{1,17},{9,25},{17,1},{25,9},{2,18},{10... | collective-permute-start | bytes 1769480 | tf_op jit(solution)/shard_map/ppermute | solution.py:54
  67.3 4.3 %collective-permute-start.16 = (bf16[8,32,1152]{2,1,0:T(8,128)(2,1)}, bf16[8,32,1152]{2,1,0:T(8,128)(2,1)S(1)}, u32[]{:S(2)}, u32[]{:S(2)}) collective-permute-start(bf16[8,32,1152]{2,1,0:T(8,128)(2,1)} %get-tuple-element.22), channel_id=1, source_target_pairs={{0,24},{8,0},{16,8},{24,16},{1,25},{9,1},{17,9},{25,17},{2,26},{10... | collective-permute-start | bytes 1769480 | tf_op jit(solution)/shard_map/ppermute | solution.py:54
  71.7 1.9 collective-permute-start.8
  73.6 5.9 %all-to-all-start.1 = ((bf16[4,8,32,256]{3,2,1,0:T(8,128)(2,1)}), bf16[4,8,32,256]{3,2,1,0:T(8,128)(2,1)S(1)}, u32[]{:S(2)}, u32[]{:S(2)}) async-start(bf16[4,8,32,256]{3,2,1,0:T(8,128)(2,1)} %get-tuple-element.20), calls=%async_computation.1 | async-start | bytes 1048576 | tf_op jit(solution)/shard_map/all_to_all | solution.py:378
  79.4 11.3 %collective-permute-done.14 = bf16[8,32,1152]{2,1,0:T(8,128)(2,1)S(1)} collective-permute-done((bf16[8,32,1152]{2,1,0:T(8,128)(2,1)}, bf16[8,32,1152]{2,1,0:T(8,128)(2,1)S(1)}, u32[]{:S(2)}, u32[]{:S(2)}) %collective-permute-start.14) | collective-permute-done | bytes 589856 | tf_op jit(solution)/shard_map/ppermute | solution.py:54
  90.7 1.9 collective-permute-start.9
  92.6 6.8 %collective-permute-start.10 = (bf16[8,32,768]{2,1,0:T(8,128)(2,1)}, bf16[8,32,768]{2,1,0:T(8,128)(2,1)}, u32[]{:S(2)}, u32[]{:S(2)}) collective-permute-start(bf16[8,32,768]{2,1,0:T(8,128)(2,1)} %get-tuple-element.17), channel_id=1, source_target_pairs={{0,24},{8,0},{16,8},{24,16},{1,25},{9,1},{17,9},{25,17},{2,26},{10... | collective-permute-start | bytes 1179656 | tf_op jit(solution)/shard_map/ppermute | solution.py:54
  99.5 0.8 copy-done.4
  100.2 3.2 %shard_map.187 = bf16[8,4,32,1152]{3,2,1,0:T(8,128)(2,1)} custom-call(s32[1]{0:T(128)} %bitcast.2.y_ref.index, bf16[256,1152]{1,0:T(8,128)(2,1)} %bitcast.35, bf16[256,1152]{1,0:T(8,128)(2,1)} %bitcast.36, bf16[256,1152]{1,0:T(8,128)(2,1)} %bitcast.37, bf16[256,1152]{1,0:T(8,128)(2,1)} %bitcast.38), custom_call_target="tpu_custom_call" | custom-call | flops 16777216 | bytes 2097152 | tf_op jit(solution)/shard_map/pallas_call | solution.py:37
  103.4 1.9 collective-permute-start.17
  105.4 2.4 %collective-permute-start.12 = (bf16[4,8,32,256]{3,2,1,0:T(8,128)(2,1)S(1)}, bf16[4,8,32,256]{3,2,1,0:T(8,128)(2,1)S(1)}, u32[]{:S(2)}, u32[]{:S(2)}) collective-permute-start(bf16[4,8,32,256]{3,2,1,0:T(8,128)(2,1)S(1)} %all-to-all-done.1.my_pieces), channel_id=1, source_target_pairs={{0,1},{1,0},{2,3},{3,2},{4,5},{5,4},{6,7},{7,6},{8,9},{9,8},{10,11... | collective-permute-start | bytes 1572872 | tf_op jit(solution)/shard_map/ppermute | solution.py:58
  107.8 3.4 %collective-permute-done.9 = bf16[8,32,768]{2,1,0:T(8,128)(2,1)} collective-permute-done((bf16[8,32,768]{2,1,0:T(8,128)(2,1)}, bf16[8,32,768]{2,1,0:T(8,128)(2,1)}, u32[]{:S(2)}, u32[]{:S(2)}) %collective-permute-start.9) | collective-permute-done | bytes 393248 | tf_op jit(solution)/shard_map/ppermute | solution.py:54
  111.2 6.5 %collective-permute-done.10 = bf16[8,32,768]{2,1,0:T(8,128)(2,1)} collective-permute-done((bf16[8,32,768]{2,1,0:T(8,128)(2,1)}, bf16[8,32,768]{2,1,0:T(8,128)(2,1)}, u32[]{:S(2)}, u32[]{:S(2)}) %collective-permute-start.10) | collective-permute-done | bytes 393248 | tf_op jit(solution)/shard_map/ppermute | solution.py:54
  117.7 6.2 %shard_map.184 = (bf16[512,256]{1,0:T(8,128)(2,1)}, bf16[512,256]{1,0:T(8,128)(2,1)}) custom-call(s32[1]{0:T(128)} %bitcast.2.y_ref.index, s32[1]{0:T(128)} %bitcast.1.core_ref, f32[2]{0:T(128)} %bitcast.46, bf16[512,1024]{1,0:T(8,128)(2,1)} %bitcast.33, bf16[512,1024]{1,0:T(8,128)(2,1)} %collective-permute-done.other, bf16[256,768]{1,0:T(8,128)(2,1)} %bitcast.45, ...), custom_call_target="tpu_custom_call" | custom-call | flops 4294967296 | bytes 2097152 | tf_op jit(solution)/shard_map/pallas_call | solution.py:37
  123.9 1.9 collective-permute-start.11
  125.8 1.7 collective-permute-done.11.theirs
  127.5 0.7 copy-done.20
  128.2 3.1 %shard_map.185 = bf16[512,1024]{1,0:T(8,128)(2,1)} custom-call(bf16[512,256]{1,0:T(8,128)(2,1)} %get-tuple-element.18.mine, bf16[512,256]{1,0:T(8,128)(2,1)} %copy-done.20, bf16[4,8,32,256]{3,2,1,0:T(8,128)(2,1)} %copy-done.5, bf16[4,8,32,256]{3,2,1,0:T(8,128)(2,1)} %copy-done.18), custom_call_target="tpu_custom_call" | custom-call | flops 1073741824 | bytes 2097152 | tf_op jit(solution)/shard_map/pallas_call | solution.py:37
  131.3 18.4 %all_to_all.20.pieces = bf16[4,128,1024]{2,1,0:T(8,128)(2,1)} all-to-all(bf16[4,128,1024]{2,1,0:T(8,128)(2,1)} %bitcast.34), channel_id=1, replica_groups=mesh['rep'=2,'z'=8,'y'=4,'x'=4,'c'=2] {'x'}, dimensions={0} | all-to-all | bytes 2097152 | tf_op jit(solution)/shard_map/all_to_all | solution.py:62
  149.6 2.7 %shard_map.186 = (bf16[128,1024]{1,0:T(8,128)(2,1)}, bf16[4,128,1024]{2,1,0:T(8,128)(2,1)}) custom-call(bf16[4,128,1024]{2,1,0:T(8,128)(2,1)} %all_to_all.20.pieces, bf16[128,1024]{1,0:T(8,128)(2,1)} %bitcast.31, f32[1,1024]{1,0:T(1,128)} %bitcast.42, f32[1,1024]{1,0:T(1,128)} %bitcast.43), custom_call_target="tpu_custom_call" | custom-call | flops 16777216 | bytes 2097152 | tf_op jit(solution)/shard_map/pallas_call | solution.py:37
  152.3 17.7 %all_to_all.21 = bf16[4,128,1024]{2,1,0:T(8,128)(2,1)S(1)} all-to-all(bf16[4,128,1024]{2,1,0:T(8,128)(2,1)} %get-tuple-element.21), channel_id=1, replica_groups=mesh['rep'=2,'z'=8,'y'=4,'x'=4,'c'=2] {'x'}, dimensions={0} | all-to-all | bytes 2097152 | tf_op jit(solution)/shard_map/all_to_all | solution.py:62
  170.2 1.9 collective-permute-start.13
  173.3 1.3 shard_map.188.my_taps
  174.6 2.4 %collective-permute-start.18 = (f32[8,384]{1,0:T(8,128)}, f32[8,384]{1,0:T(8,128)S(1)}, u32[]{:S(2)}, u32[]{:S(2)}) collective-permute-start(f32[8,384]{1,0:T(8,128)} %shard_map.188.my_taps), channel_id=1, source_target_pairs={{0,1},{1,0},{2,3},{3,2},{4,5},{5,4},{6,7},{7,6},{8,9},{9,8},{10,11... | collective-permute-start | bytes 36872 | tf_op jit(solution)/shard_map/ppermute | solution.py:58
  177.0 1.0 collective-permute-done.18.their_taps
  178.6 4.8 %shard_map.189 = (bf16[128,1024]{1,0:T(8,128)(2,1)}, f32[16,1536]{1,0:T(8,128)}) custom-call(s32[1]{0:T(128)} %bitcast.x_ref, s32[1]{0:T(128)} %bitcast.1.core_ref, bf16[512,1024]{1,0:T(8,128)(2,1)} %bitcast.28, bf16[8,1024]{1,0:T(8,128)(2,1)} %copy-done.21, bf16[1024,1152]{1,0:T(8,128)(2,1)} %bitcast.26, bf16[1024,1152]{1,0:T(8,128)(2,1)} %collective-permute-done.17.theirs, ...), custom_call_target="tpu_custom_call" | custom-call | flops 2147483648 | bytes 2097152 | tf_op jit(solution)/shard_map/pallas_call | solution.py:37
  183.5 6.6 %shard_map.190 = (bf16[128,1024]{1,0:T(8,128)(2,1)}, bf16[128,1024]{1,0:T(8,128)(2,1)}, bf16[128,1024]{1,0:T(8,128)(2,1)}) custom-call(s32[1]{0:T(128)} %bitcast.x_ref, s32[1]{0:T(128)} %bitcast.1.core_ref, bf16[512,1024]{1,0:T(8,128)(2,1)} %bitcast.29, f32[16,1536]{1,0:T(8,128)} %get-tuple-element.23.outer, bf16[1024,1152]{1,0:T(8,128)(2,1)} %bitcast.27, ...), custom_call_target="tpu_custom_call" | custom-call | flops 4294967296 | bytes 2097152 | tf_op jit(solution)/shard_map/pallas_call | solution.py:37
  190.0 4.0 %collective-permute-start.19 = (bf16[128,1024]{1,0:T(8,128)(2,1)}, bf16[128,1024]{1,0:T(8,128)(2,1)S(1)}, u32[]{:S(2)}, u32[]{:S(2)}) collective-permute-start(bf16[128,1024]{1,0:T(8,128)(2,1)} %get-tuple-element.25), channel_id=1, source_target_pairs={{0,2},{2,4},{4,6},{6,0},{1,3},{3,5},{5,7},{7,1},{8,10},{10,12},{12... | collective-permute-start | bytes 786440 | tf_op jit(solution)/shard_map/ppermute | solution.py:54
  194.0 1.9 collective-permute-start.20
  195.9 3.9 %collective-permute-start.21 = (bf16[128,1024]{1,0:T(8,128)(2,1)S(1)}, bf16[128,1024]{1,0:T(8,128)(2,1)S(1)}, u32[]{:S(2)}, u32[]{:S(2)}) collective-permute-start(bf16[128,1024]{1,0:T(8,128)(2,1)S(1)} %copy-done.19), channel_id=1, source_target_pairs={{0,4},{2,6},{4,0},{6,2},{1,5},{3,7},{5,1},{7,3},{8,12},{10,14},{12... | collective-permute-start | bytes 786440 | tf_op jit(solution)/shard_map/ppermute | solution.py:54
  199.9 0.8 collective-permute-done.19.right
  200.7 10.5 %collective-permute-done.20.left = bf16[128,1024]{1,0:T(8,128)(2,1)S(1)} collective-permute-done((bf16[128,1024]{1,0:T(8,128)(2,1)}, bf16[128,1024]{1,0:T(8,128)(2,1)S(1)}, u32[]{:S(2)}, u32[]{:S(2)}) %collective-permute-start.20) | collective-permute-done | bytes 262176 | tf_op jit(solution)/shard_map/ppermute | solution.py:54
  212.0 2.2 %shard_map.191 = bf16[128,1024]{1,0:T(8,128)(2,1)} custom-call(bf16[128,1024]{1,0:T(8,128)(2,1)} %get-tuple-element.24.here, bf16[128,1024]{1,0:T(8,128)(2,1)} %copy-done.6, bf16[128,1024]{1,0:T(8,128)(2,1)} %copy-done.7, bf16[128,1024]{1,0:T(8,128)(2,1)} %copy-done.8, bf16[128,1024]{1,0:T(8,128)(2,1)} %get-tuple-element.28.after_mix, f32[1,1024]{1,0:T(1,128)} %bitcast.44), custom_call_target="tpu_custom_call" | custom-call | flops 16777216 | bytes 2097152 | tf_op jit(solution)/shard_map/pallas_call | solution.py:37
  (63 shorter events, 3.4 us)
Async XLA Ops:
  2.1 46.7 %all-to-all-start = ((bf16[4,128,1024]{2,1,0:T(8,128)(2,1)}), bf16[4,128,1024]{2,1,0:T(8,128)(2,1)S(1)}, u32[]{:S(2)}, u32[]{:S(2)}) async-start(bf16[4,128,1024]{2,1,0:T(8,128)(2,1)} %shard_map.181), calls=%async_computation | async-start | bytes 2097152 | tf_op jit(solution)/shard_map/all_to_all | solution.py:62
  8.4 28.2 %collective-permute-start.1 = (bf16[32,2176]{1,0:T(8,128)(2,1)}, bf16[32,2176]{1,0:T(8,128)(2,1)S(1)}, u32[]{:S(2)}, u32[]{:S(2)}) collective-permute-start(bf16[32,2176]{1,0:T(8,128)(2,1)} %shard_map.182.refs_4_), channel_id=1, source_target_pairs={{0,128},{32,160},{64,192},{96,224},{128,256},{160,288},{192,320},{... | collective-permute-start | bytes 417800 | tf_op jit(solution)/shard_map/ppermute | solution.py:54
  17.5 27.2 %collective-permute-start.2 = (bf16[32,2176]{1,0:T(8,128)(2,1)}, bf16[32,2176]{1,0:T(8,128)(2,1)S(1)}, u32[]{:S(2)}, u32[]{:S(2)}) collective-permute-start(bf16[32,2176]{1,0:T(8,128)(2,1)} %shard_map.182.refs_4_), channel_id=1, source_target_pairs={{0,96},{32,128},{64,160},{96,192},{128,224},{160,256},{192,288},{2... | collective-permute-start | bytes 417800 | tf_op jit(solution)/shard_map/ppermute | solution.py:54
  24.0 24.8 %collective-permute-start.3 = (bf16[32,2176]{1,0:T(8,128)(2,1)}, bf16[32,2176]{1,0:T(8,128)(2,1)S(1)}, u32[]{:S(2)}, u32[]{:S(2)}) collective-permute-start(bf16[32,2176]{1,0:T(8,128)(2,1)} %shard_map.182.refs_4_), channel_id=1, source_target_pairs={{0,64},{32,96},{64,128},{96,160},{128,192},{160,224},{192,256},{22... | collective-permute-start | bytes 417800 | tf_op jit(solution)/shard_map/ppermute | solution.py:54
  29.5 21.2 %collective-permute-start.4 = (bf16[32,2176]{1,0:T(8,128)(2,1)}, bf16[32,2176]{1,0:T(8,128)(2,1)S(1)}, u32[]{:S(2)}, u32[]{:S(2)}) collective-permute-start(bf16[32,2176]{1,0:T(8,128)(2,1)} %shard_map.182.refs_4_), channel_id=1, source_target_pairs={{0,32},{32,64},{64,96},{96,128},{128,160},{160,192},{192,224},{224... | collective-permute-start | bytes 417800 | tf_op jit(solution)/shard_map/ppermute | solution.py:54
  32.5 18.3 %collective-permute-start.5 = (bf16[32,2176]{1,0:T(8,128)(2,1)}, bf16[32,2176]{1,0:T(8,128)(2,1)S(1)}, u32[]{:S(2)}, u32[]{:S(2)}) collective-permute-start(bf16[32,2176]{1,0:T(8,128)(2,1)} %shard_map.182.refs_4_), channel_id=1, source_target_pairs={{0,480},{32,0},{64,32},{96,64},{128,96},{160,128},{192,160},{224,1... | collective-permute-start | bytes 417800 | tf_op jit(solution)/shard_map/ppermute | solution.py:54
  36.6 21.2 %copy-start.9 = (bf16[32,2176]{1,0:T(8,128)(2,1)}, bf16[32,2176]{1,0:T(8,128)(2,1)S(1)}, u32[]{:S(2)}) copy-start(bf16[32,2176]{1,0:T(8,128)(2,1)S(1)} %collective-permute-done.1.refs_0_) | copy-start | bytes 417796
  36.6 14.2 %collective-permute-start.6 = (bf16[32,2176]{1,0:T(8,128)(2,1)}, bf16[32,2176]{1,0:T(8,128)(2,1)S(1)}, u32[]{:S(2)}, u32[]{:S(2)}) collective-permute-start(bf16[32,2176]{1,0:T(8,128)(2,1)} %shard_map.182.refs_4_), channel_id=1, source_target_pairs={{0,448},{32,480},{64,0},{96,32},{128,64},{160,96},{192,128},{224,1... | collective-permute-start | bytes 417800 | tf_op jit(solution)/shard_map/ppermute | solution.py:54
  44.7 13.1 %copy-start.10 = (bf16[32,2176]{1,0:T(8,128)(2,1)}, bf16[32,2176]{1,0:T(8,128)(2,1)S(1)}, u32[]{:S(2)}) copy-start(bf16[32,2176]{1,0:T(8,128)(2,1)S(1)} %collective-permute-done.2.refs_1_) | copy-start | bytes 417796
  44.7 13.1 %collective-permute-start.7 = (bf16[32,2176]{1,0:T(8,128)(2,1)}, bf16[32,2176]{1,0:T(8,128)(2,1)S(1)}, u32[]{:S(2)}, u32[]{:S(2)}) collective-permute-start(bf16[32,2176]{1,0:T(8,128)(2,1)} %shard_map.182.refs_4_), channel_id=1, source_target_pairs={{0,416},{32,448},{64,480},{96,0},{128,32},{160,64},{192,96},{224,1... | collective-permute-start | bytes 417800 | tf_op jit(solution)/shard_map/ppermute | solution.py:54
  48.8 9.0 %copy-start.11 = (bf16[32,2176]{1,0:T(8,128)(2,1)}, bf16[32,2176]{1,0:T(8,128)(2,1)S(1)}, u32[]{:S(2)}) copy-start(bf16[32,2176]{1,0:T(8,128)(2,1)S(1)} %collective-permute-done.3.refs_2_) | copy-start | bytes 417796
  48.8 54.6 %copy-start.1 = (bf16[4,128,1024]{2,1,0:T(8,128)(2,1)}, bf16[4,128,1024]{2,1,0:T(8,128)(2,1)S(1)}, u32[]{:S(2)}) copy-start(bf16[4,128,1024]{2,1,0:T(8,128)(2,1)S(1)} %all-to-all-done) | copy-start | bytes 3145732
  48.8 68.8 %collective-permute-start = (bf16[512,1024]{1,0:T(8,128)(2,1)S(1)}, bf16[512,1024]{1,0:T(8,128)(2,1)}, u32[]{:S(2)}, u32[]{:S(2)}) collective-permute-start(bf16[512,1024]{1,0:T(8,128)(2,1)S(1)} %bitcast.32), channel_id=1, source_target_pairs={{0,1},{1,0},{2,3},{3,2},{4,5},{5,4},{6,7},{7,6},{8,9},{9,8},{10,11... | collective-permute-start | bytes 3145736 | tf_op jit(solution)/shard_map/ppermute | solution.py:58
  50.8 7.0 %copy-start.12 = (bf16[32,2176]{1,0:T(8,128)(2,1)}, bf16[32,2176]{1,0:T(8,128)(2,1)S(1)}, u32[]{:S(2)}) copy-start(bf16[32,2176]{1,0:T(8,128)(2,1)S(1)} %collective-permute-done.4.refs_3_) | copy-start | bytes 417796
  50.8 7.0 %copy-start.13 = (bf16[32,2176]{1,0:T(8,128)(2,1)}, bf16[32,2176]{1,0:T(8,128)(2,1)S(1)}, u32[]{:S(2)}) copy-start(bf16[32,2176]{1,0:T(8,128)(2,1)S(1)} %collective-permute-done.5.refs_5_) | copy-start | bytes 417796
  50.8 7.0 %copy-start.14 = (bf16[32,2176]{1,0:T(8,128)(2,1)}, bf16[32,2176]{1,0:T(8,128)(2,1)S(1)}, u32[]{:S(2)}) copy-start(bf16[32,2176]{1,0:T(8,128)(2,1)S(1)} %collective-permute-done.6.refs_6_) | copy-start | bytes 417796
  57.8 0.7 copy-start.15
  61.0 29.7 %collective-permute-start.14 = (bf16[8,32,1152]{2,1,0:T(8,128)(2,1)}, bf16[8,32,1152]{2,1,0:T(8,128)(2,1)S(1)}, u32[]{:S(2)}, u32[]{:S(2)}) collective-permute-start(bf16[8,32,1152]{2,1,0:T(8,128)(2,1)} %get-tuple-element.22), channel_id=1, source_target_pairs={{0,8},{8,16},{16,24},{24,0},{1,9},{9,17},{17,25},{25,1},{2,10},{10... | collective-permute-start | bytes 1769480 | tf_op jit(solution)/shard_map/ppermute | solution.py:54
  64.5 28.1 %collective-permute-start.15 = (bf16[8,32,1152]{2,1,0:T(8,128)(2,1)}, bf16[8,32,1152]{2,1,0:T(8,128)(2,1)S(1)}, u32[]{:S(2)}, u32[]{:S(2)}) collective-permute-start(bf16[8,32,1152]{2,1,0:T(8,128)(2,1)} %get-tuple-element.22), channel_id=1, source_target_pairs={{0,16},{8,24},{16,0},{24,8},{1,17},{9,25},{17,1},{25,9},{2,18},{10... | collective-permute-start | bytes 1769480 | tf_op jit(solution)/shard_map/ppermute | solution.py:54
  67.3 32.1 %collective-permute-start.16 = (bf16[8,32,1152]{2,1,0:T(8,128)(2,1)}, bf16[8,32,1152]{2,1,0:T(8,128)(2,1)S(1)}, u32[]{:S(2)}, u32[]{:S(2)}) collective-permute-start(bf16[8,32,1152]{2,1,0:T(8,128)(2,1)} %get-tuple-element.22), channel_id=1, source_target_pairs={{0,24},{8,0},{16,8},{24,16},{1,25},{9,1},{17,9},{25,17},{2,26},{10... | collective-permute-start | bytes 1769480 | tf_op jit(solution)/shard_map/ppermute | solution.py:54
  71.7 33.7 %collective-permute-start.8 = (bf16[8,32,768]{2,1,0:T(8,128)(2,1)}, bf16[8,32,768]{2,1,0:T(8,128)(2,1)}, u32[]{:S(2)}, u32[]{:S(2)}) collective-permute-start(bf16[8,32,768]{2,1,0:T(8,128)(2,1)} %get-tuple-element.17), channel_id=1, source_target_pairs={{0,8},{8,16},{16,24},{24,0},{1,9},{9,17},{17,25},{25,1},{2,10},{10... | collective-permute-start | bytes 1179656 | tf_op jit(solution)/shard_map/ppermute | solution.py:54
  73.6 31.8 %all-to-all-start.1 = ((bf16[4,8,32,256]{3,2,1,0:T(8,128)(2,1)}), bf16[4,8,32,256]{3,2,1,0:T(8,128)(2,1)S(1)}, u32[]{:S(2)}, u32[]{:S(2)}) async-start(bf16[4,8,32,256]{3,2,1,0:T(8,128)(2,1)} %get-tuple-element.20), calls=%async_computation.1 | async-start | bytes 1048576 | tf_op jit(solution)/shard_map/all_to_all | solution.py:378
  90.7 8.7 %copy-start.2 = (bf16[8,32,1152]{2,1,0:T(8,128)(2,1)}, bf16[8,32,1152]{2,1,0:T(8,128)(2,1)S(1)}, u32[]{:S(2)}) copy-start(bf16[8,32,1152]{2,1,0:T(8,128)(2,1)S(1)} %collective-permute-done.14) | copy-start | bytes 1769476
  90.7 20.5 %collective-permute-start.9 = (bf16[8,32,768]{2,1,0:T(8,128)(2,1)}, bf16[8,32,768]{2,1,0:T(8,128)(2,1)}, u32[]{:S(2)}, u32[]{:S(2)}) collective-permute-start(bf16[8,32,768]{2,1,0:T(8,128)(2,1)} %get-tuple-element.17), channel_id=1, source_target_pairs={{0,16},{8,24},{16,0},{24,8},{1,17},{9,25},{17,1},{25,9},{2,18},{10... | collective-permute-start | bytes 1179656 | tf_op jit(solution)/shard_map/ppermute | solution.py:54
  92.6 6.8 %copy-start.3 = (bf16[8,32,1152]{2,1,0:T(8,128)(2,1)}, bf16[8,32,1152]{2,1,0:T(8,128)(2,1)S(1)}, u32[]{:S(2)}) copy-start(bf16[8,32,1152]{2,1,0:T(8,128)(2,1)S(1)} %collective-permute-done.15) | copy-start | bytes 1769476
  92.6 25.0 %collective-permute-start.10 = (bf16[8,32,768]{2,1,0:T(8,128)(2,1)}, bf16[8,32,768]{2,1,0:T(8,128)(2,1)}, u32[]{:S(2)}, u32[]{:S(2)}) collective-permute-start(bf16[8,32,768]{2,1,0:T(8,128)(2,1)} %get-tuple-element.17), channel_id=1, source_target_pairs={{0,24},{8,0},{16,8},{24,16},{1,25},{9,1},{17,9},{25,17},{2,26},{10... | collective-permute-start | bytes 1179656 | tf_op jit(solution)/shard_map/ppermute | solution.py:54
  99.4 0.8 copy-start.4
  103.4 74.6 %collective-permute-start.17 = (bf16[1024,1152]{1,0:T(8,128)(2,1)}, bf16[1024,1152]{1,0:T(8,128)(2,1)}, u32[]{:S(2)}, u32[]{:S(2)}) collective-permute-start(bf16[1024,1152]{1,0:T(8,128)(2,1)} %bitcast.25), channel_id=1, source_target_pairs={{0,1},{1,0},{2,3},{3,2},{4,5},{5,4},{6,7},{7,6},{8,9},{9,8},{10,11... | collective-permute-start | bytes 7077896 | tf_op jit(solution)/shard_map/ppermute | solution.py:58
  105.4 18.5 %copy-start.5 = (bf16[4,8,32,256]{3,2,1,0:T(8,128)(2,1)}, bf16[4,8,32,256]{3,2,1,0:T(8,128)(2,1)S(1)}, u32[]{:S(2)}) copy-start(bf16[4,8,32,256]{3,2,1,0:T(8,128)(2,1)S(1)} %all-to-all-done.1.my_pieces) | copy-start | bytes 1572868
  105.4 20.4 %collective-permute-start.12 = (bf16[4,8,32,256]{3,2,1,0:T(8,128)(2,1)S(1)}, bf16[4,8,32,256]{3,2,1,0:T(8,128)(2,1)S(1)}, u32[]{:S(2)}, u32[]{:S(2)}) collective-permute-start(bf16[4,8,32,256]{3,2,1,0:T(8,128)(2,1)S(1)} %all-to-all-done.1.my_pieces), channel_id=1, source_target_pairs={{0,1},{1,0},{2,3},{3,2},{4,5},{5,4},{6,7},{7,6},{8,9},{9,8},{10,11... | collective-permute-start | bytes 1572872 | tf_op jit(solution)/shard_map/ppermute | solution.py:58
  123.9 3.6 %collective-permute-start.11 = (bf16[512,256]{1,0:T(8,128)(2,1)}, bf16[512,256]{1,0:T(8,128)(2,1)S(1)}, u32[]{:S(2)}, u32[]{:S(2)}) collective-permute-start(bf16[512,256]{1,0:T(8,128)(2,1)} %get-tuple-element.19), channel_id=1, source_target_pairs={{0,1},{1,0},{2,3},{3,2},{4,5},{5,4},{6,7},{7,6},{8,9},{9,8},{10,11... | collective-permute-start | bytes 786440 | tf_op jit(solution)/shard_map/ppermute | solution.py:58
  125.8 1.7 copy-start.18
  127.5 0.7 copy-start.20
  131.3 40.8 %copy-start.16 = (f32[352]{0:T(512)S(1)}, f32[352]{0:T(512)}, u32[]{:S(2)}) copy-start(f32[352]{0:T(512)} %param.33) | copy-start | bytes 4228
  131.3 41.4 %copy-start.17 = (f32[352]{0:T(512)S(1)}, f32[352]{0:T(512)}, u32[]{:S(2)}) copy-start(f32[352]{0:T(512)} %param.34) | copy-start | bytes 4228
  170.1 8.0 %copy-start = (bf16[4,128,1024]{2,1,0:T(8,128)(2,1)}, bf16[4,128,1024]{2,1,0:T(8,128)(2,1)S(1)}, u32[]{:S(2)}) copy-start(bf16[4,128,1024]{2,1,0:T(8,128)(2,1)S(1)} %all_to_all.21) | copy-start | bytes 3145732
  170.2 7.9 %collective-permute-start.13 = (bf16[8,1024]{1,0:T(8,128)(2,1)S(1)}, bf16[8,1024]{1,0:T(8,128)(2,1)S(1)}, u32[]{:S(2)}, u32[]{:S(2)}) collective-permute-start(bf16[8,1024]{1,0:T(8,128)(2,1)S(1)} %reshape.67), channel_id=1, source_target_pairs={{0,1},{1,0},{2,3},{3,2},{4,5},{5,4},{6,7},{7,6},{8,9},{9,8},{10,11... | collective-permute-start | bytes 49160 | tf_op jit(solution)/shard_map/ppermute | solution.py:58
  174.6 3.4 %collective-permute-start.18 = (f32[8,384]{1,0:T(8,128)}, f32[8,384]{1,0:T(8,128)S(1)}, u32[]{:S(2)}, u32[]{:S(2)}) collective-permute-start(f32[8,384]{1,0:T(8,128)} %shard_map.188.my_taps), channel_id=1, source_target_pairs={{0,1},{1,0},{2,3},{3,2},{4,5},{5,4},{6,7},{7,6},{8,9},{9,8},{10,11... | collective-permute-start | bytes 36872 | tf_op jit(solution)/shard_map/ppermute | solution.py:58
  178.0 0.6 copy-start.22
  178.0 0.6 copy-start.21
  183.5 12.5 %copy-start.19 = (bf16[128,1024]{1,0:T(8,128)(2,1)S(1)}, bf16[128,1024]{1,0:T(8,128)(2,1)}, u32[]{:S(2)}) copy-start(bf16[128,1024]{1,0:T(8,128)(2,1)} %get-tuple-element.27) | copy-start | bytes 786436
  190.0 10.7 %collective-permute-start.19 = (bf16[128,1024]{1,0:T(8,128)(2,1)}, bf16[128,1024]{1,0:T(8,128)(2,1)S(1)}, u32[]{:S(2)}, u32[]{:S(2)}) collective-permute-start(bf16[128,1024]{1,0:T(8,128)(2,1)} %get-tuple-element.25), channel_id=1, source_target_pairs={{0,2},{2,4},{4,6},{6,0},{1,3},{3,5},{5,7},{7,1},{8,10},{10,12},{12... | collective-permute-start | bytes 786440 | tf_op jit(solution)/shard_map/ppermute | solution.py:54
  194.0 17.2 %collective-permute-start.20 = (bf16[128,1024]{1,0:T(8,128)(2,1)}, bf16[128,1024]{1,0:T(8,128)(2,1)S(1)}, u32[]{:S(2)}, u32[]{:S(2)}) collective-permute-start(bf16[128,1024]{1,0:T(8,128)(2,1)} %get-tuple-element.26), channel_id=1, source_target_pairs={{0,6},{2,0},{4,2},{6,4},{1,7},{3,1},{5,3},{7,5},{8,14},{10,8},{12,... | collective-permute-start | bytes 786440 | tf_op jit(solution)/shard_map/ppermute | solution.py:54
  195.9 15.3 %collective-permute-start.21 = (bf16[128,1024]{1,0:T(8,128)(2,1)S(1)}, bf16[128,1024]{1,0:T(8,128)(2,1)S(1)}, u32[]{:S(2)}, u32[]{:S(2)}) collective-permute-start(bf16[128,1024]{1,0:T(8,128)(2,1)S(1)} %copy-done.19), channel_id=1, source_target_pairs={{0,4},{2,6},{4,0},{6,2},{1,5},{3,7},{5,1},{7,3},{8,12},{10,14},{12... | collective-permute-start | bytes 786440 | tf_op jit(solution)/shard_map/ppermute | solution.py:54
  200.7 10.5 %copy-start.6 = (bf16[128,1024]{1,0:T(8,128)(2,1)}, bf16[128,1024]{1,0:T(8,128)(2,1)S(1)}, u32[]{:S(2)}) copy-start(bf16[128,1024]{1,0:T(8,128)(2,1)S(1)} %collective-permute-done.19.right) | copy-start | bytes 786436
  211.2 0.7 copy-start.7
  211.2 0.8 copy-start.8

commit v4 on v3

--- a/solution.py
+++ b/solution.py
@@ -17,7 +17,7 @@
 RING = ("rep", "z")
 SWAP = ((0, 1), (1, 0))
 PAD = 384
-FIRST, SECOND, THIRD = 2 * DK + 2 * DV, DV, 3 * PAD
+PROJECT, FIRST, THIRD = 2 * DK + 2 * DV, 2 * DK + 3 * DV, 3 * PAD
 Z_SHIFTS = (4, 3, 2, 1, 0, -1, -2, -3)
 Z_ISSUE = (4, -3, 3, -2, 2, -1, 1)
 Y_SHIFTS = (0, 1, 2, -1)
@@ -70,11 +70,11 @@
     out[:, :DK] = q[...]
     out[:, DK : 2 * DK] = k[...]
     out[:, 2 * DK : 2 * DK + DV] = v[...]
-    out[:, 2 * DK + DV : FIRST] = g[...]
-    out[:, FIRST : FIRST + SECOND] = mo[...]
+    out[:, 2 * DK + DV : PROJECT] = g[...]
+    out[:, PROJECT:FIRST] = mo[...]
     gap = jnp.zeros((out.shape[0], PAD - width), bf16)
     for place, piece in enumerate((ge, li, dn)):
-        at = FIRST + SECOND + place * PAD
+        at = FIRST + place * PAD
         out[:, at : at + PAD] = jnp.concatenate([piece[...], gap], axis=1)
 
 
@@ -93,40 +93,31 @@
 
 
 def ring_order_body(index, *refs):
-    pieces, (one, two, three) = refs[:8], refs[8:]
+    pieces, (one, three) = refs[:8], refs[8:]
     for shift, piece in zip(Z_SHIFTS, pieces):
         at = lax.rem(index[0] - shift + 8, 8)
         one[at] = piece[:, :FIRST]
-        for y in range(two.shape[0]):
-            two[y, at] = piece[:, FIRST : FIRST + SECOND]
-        three[at] = piece[:, FIRST + SECOND :]
-
-
-def line_order_body(index, *refs):
-    pieces, out = refs[:4], refs[4]
-    for shift, piece in zip(Y_SHIFTS, pieces):
-        at = lax.rem(index[0] - shift + 4, 4)
-        for z in range(8):
-            out[z, at] = piece[z * 32 : z * 32 + 32, :]
+        for y in range(three.shape[0]):
+            three[y, at] = piece[:, FIRST:]
 
 
 def summed(pieces):
-    total = pieces[0].astype(f32)
+    total = pieces[0][...].astype(f32)
     for piece in pieces[1:]:
-        total = total + piece.astype(f32)
+        total = total + piece[...].astype(f32)
     return total * lax.rsqrt(jnp.mean(total * total, axis=-1, keepdims=True) + epsilon)
 
 
-def middle_body(pieces, tokens, out_gain, in_gain, after_mix, channel_in):
-    mix = (tokens[...].astype(f32) + summed([pieces[k] for k in range(4)]) * out_gain[...]).astype(bf16)
+def middle_body(far, right, left, here, tokens, out_gain, in_gain, after_mix, channel_in):
+    total = summed((here, right, left, far))
+    mix = (tokens[...].astype(f32) + total * out_gain[...]).astype(bf16)
     after_mix[...] = mix
-    rows = rms_rows(mix.astype(f32), in_gain[...]).astype(bf16)
-    for k in range(channel_in.shape[0]):
-        channel_in[k] = rows
-
-
-def final_body(here, right, left, far, after_mix, gain, out):
-    out[...] = (after_mix[...].astype(f32) + summed([here[...], right[...], left[...], far[...]]) * gain[...]).astype(bf16)
+    channel_in[...] = rms_rows(mix.astype(f32), in_gain[...]).astype(bf16)
+
+
+def final_body(far, right, left, here, after_mix, gain, out):
+    total = summed((here, right, left, far))
+    out[...] = (after_mix[...].astype(f32) + total * gain[...]).astype(bf16)
 
 
 def log_sigmoid_tile(logit):
@@ -136,14 +127,15 @@
 
 
 def attend_body(
-    y_ref, core_ref, logits, own, other, p0, p1, p2, p3, frequency, out_own, out_other, w, qs, ks, vs, gs
+    y_ref, core_ref, logits, own, other, p0, p1, p2, p3, frequency, out_own, out_other, mo, w, qs, ks, vs, gs
 ):
     y, core = y_ref[0], core_ref[0]
     for shift, piece in zip(Y_SHIFTS, (p0, p1, p2, p3)):
         at = lax.rem(y - shift + 4, 4) * 32
         for z in range(8):
             place = pl.ds(pl.multiple_of(z * 128 + at, 32), 32)
-            w[place, :] = piece[z * 32 : z * 32 + 32, :]
+            w[place, :] = piece[z * 32 : z * 32 + 32, :PROJECT]
+            mo[place, :] = piece[z * 32 : z * 32 + 32, PROJECT:]
     inside = lax.broadcasted_iota(jnp.int32, (128, DK), 0).astype(f32) * frequency[...]
     cos_in, sin_in = jnp.cos(inside), jnp.sin(inside)
     block = lax.broadcasted_iota(jnp.int32, (8, DK), 0)
@@ -201,16 +193,19 @@
             out_other[r * 128 - 512 : r * 128 - 384, :] = gated
 
 
-def output_body(mine, theirs, my_pieces, their_pieces, out, w):
-    for y in range(4):
-        for z in range(8):
-            at = z * 128 + y * 32
-            w[at : at + 32, :DV] = my_pieces[y, z]
-            w[at : at + 32, DV:] = their_pieces[y, z]
-    step = 256
-    for d in range(0, 1024, step):
-        part = dot_nt(mine[...], w[d : d + step, :DV]) + dot_nt(theirs[...], w[d : d + step, DV:])
-        out[:, d : d + step] = part.astype(bf16)
+def output_body(x_ref, mine, theirs, my_weights, their_weights, far, right, left, here, lines):
+    for place, ahead in enumerate((2, 1, 3, 0)):
+        block = lax.rem(x_ref[0] + ahead, 4)
+        rows = pl.ds(pl.multiple_of(block * 128, 128), 128)
+        lines[place * 128 : place * 128 + 128, :DV] = mine[rows, :]
+        lines[place * 128 : place * 128 + 128, DV:] = theirs[rows, :]
+    for d in range(0, 1024, 256):
+        columns = slice(d, d + 256)
+        total = dot_nt(lines[:, :DV], my_weights[columns, :]) + dot_nt(
+            lines[:, DV:], their_weights[columns, :]
+        )
+        for place, out in enumerate((far, right, left, here)):
+            out[:, columns] = total[place * 128 : place * 128 + 128, :].astype(bf16)
 
 
 def feed_block(main, before, after, taps):
@@ -227,68 +222,60 @@
     return (bent * conv[:, PAD:]).astype(bf16)
 
 
-def feed_down(hidden, mine, theirs, outs):
-    for d in range(0, 1024, 256):
-        total = dot_nt(hidden[:, :PAD], mine[d : d + 256, 2 * PAD :]) + dot_nt(
-            hidden[:, PAD:], theirs[d : d + 256, 2 * PAD :]
-        )
-        for place, out in enumerate(outs):
-            out[:, d : d + 256] = total[place * 128 : place * 128 + 128, :].astype(bf16)
-
-
-def feed_far_body(
-    x_ref, core_ref, rows, edges, mine, theirs, my_taps, their_taps, out, outer, lines, hidden
-):
-    core = core_ref[0]
-    block = lax.rem(x_ref[0] + 2, 4)
-    lines[:128, :] = rows[pl.ds(pl.multiple_of(block * 128, 128), 128), :]
-    lines[128:136, :] = edges[...]
-    lines[136:144, :] = jnp.zeros((8, 1024), bf16)
-    outer[...] = jnp.zeros(outer.shape, f32)
-    for part, (weights, taps) in enumerate(((mine, my_taps), (theirs, their_taps))):
-        columns = slice(part * 2 * PAD, part * 2 * PAD + 2 * PAD)
-        main = dot(lines[...], weights[:, : 2 * PAD])
-        for x in range(4):
-            outer[8 + x : 9 + x, columns] = main[128 + 2 * x : 129 + 2 * x, :]
-            outer[1 + x : 2 + x, columns] = main[129 + 2 * x : 130 + 2 * x, :]
-        before = outer[pl.ds(block + core, 1), columns]
-        after = outer[pl.ds(8 + block + core, 1), columns]
-        hidden[:, part * PAD : part * PAD + PAD] = feed_block(main[:128, :], before, after, taps)
-    feed_down(hidden, mine, theirs, (out,))
-
-
-def feed_near_body(
+def feed_body(
     x_ref,
     core_ref,
-    rows,
-    outer,
+    got_far,
+    got_next,
+    got_prev,
+    own,
+    edges,
     mine,
     theirs,
     my_taps,
     their_taps,
+    far,
     right,
     left,
     here,
     lines,
+    outer,
     hidden,
+    my_weights,
+    their_weights,
 ):
     core = core_ref[0]
-    blocks = [lax.rem(x_ref[0] + k, 4) for k in (1, 3, 0)]
-    for place, block in enumerate(blocks):
-        lines[place * 128 : place * 128 + 128, :] = rows[
-            pl.ds(pl.multiple_of(block * 128, 128), 128), :
-        ]
-    for part, (weights, taps) in enumerate(((mine, my_taps), (theirs, their_taps))):
-        columns = slice(part * 2 * PAD, part * 2 * PAD + 2 * PAD)
+    blocks = [lax.rem(x_ref[0] + k, 4) for k in (2, 1, 3, 0)]
+    for place, piece in enumerate((got_far, got_next, got_prev, own)):
+        lines[place * 128 : place * 128 + 128, :] = piece[...]
+    lines[512:520, :] = edges[...]
+    lines[520:528, :] = jnp.zeros((8, 1024), bf16)
+    outer[...] = jnp.zeros(outer.shape, f32)
+    for part, (raw, weights, taps) in enumerate(
+        ((mine, my_weights, my_taps), (theirs, their_weights, their_taps))
+    ):
+        for z in range(8):
+            for y in range(4):
+                at = z * 128 + y * 32
+                weights[at : at + 32, :] = raw[y, z]
         main = dot(lines[...], weights[:, : 2 * PAD])
         for place, block in enumerate(blocks):
+            outer[pl.ds(8 + block, 1), :] = main[512 + 2 * place : 513 + 2 * place, :]
+            outer[pl.ds(1 + block, 1), :] = main[513 + 2 * place : 514 + 2 * place, :]
+        for place, block in enumerate(blocks):
             inner = slice(place * 128, place * 128 + 128)
-            before = outer[pl.ds(block + core, 1), columns]
-            after = outer[pl.ds(8 + block + core, 1), columns]
+            before = outer[pl.ds(block + core, 1), :]
+            after = outer[pl.ds(8 + block + core, 1), :]
             hidden[inner, part * PAD : part * PAD + PAD] = feed_block(
                 main[inner, :], before, after, taps
             )
-    feed_down(hidden, mine, theirs, (right, left, here))
+    for d in range(0, 1024, 256):
+        columns = slice(d, d + 256)
+        total = dot_nt(hidden[:, :PAD], my_weights[columns, 2 * PAD :]) + dot_nt(
+            hidden[:, PAD:], their_weights[columns, 2 * PAD :]
+        )
+        for place, out in enumerate((far, right, left, here)):
+            out[:, columns] = total[place * 128 : place * 128 + 128, :].astype(bf16)
 
 
 def head_norm(values):
@@ -309,6 +296,10 @@
     for shift in Y_ISSUE:
         got[shift] = permuted(piece, "y", shift, 4)
     return [got[s].reshape(256, piece.shape[-1]) for s in Y_SHIFTS]
+
+
+def sent(far, right, left):
+    return (permuted(far, "x", 2, 4), permuted(right, "x", 1, 4), permuted(left, "x", -1, 4))
 
 
 def rope_frequency():
@@ -351,7 +342,7 @@
 
     packed = call(
         functools.partial(pack_body, width),
-        shape((32, FIRST + SECOND + THIRD)),
+        shape((32, FIRST + THIRD)),
         query_weight,
         key_weight,
         value_weight,
@@ -367,19 +358,27 @@
     spread = call(first_norm_body, shape((chips, own, model)), token_rows, row(mixer_in_gain))
     normed_own = exchanged(spread).reshape(half, model)
     normed_other = swap(normed_own)
-    first_z, second_z, third_z = call(
+    first_z, third_z = call(
         ring_order_body,
-        [shape((8, 32, FIRST)), shape((4, 8, 32, SECOND)), shape((8, 32, THIRD))],
+        [shape((8, 32, FIRST)), shape((4, 8, 32, THIRD))],
         z_index[None],
         *[got[s] for s in Z_SHIFTS],
         smem=1,
     )
     first_pieces = line_gather(first_z)
-    second_own = lax.all_to_all(second_z, "y", 0, 0, tiled=True)
-    third_pieces = line_gather(third_z)
-    gated_own, gated_other = call(
+    third_own = lax.all_to_all(third_z, "y", 0, 0, tiled=True)
+    taps = call(
+        functools.partial(taps_body, width),
+        shape((8, PAD), f32),
+        gelu_kernel,
+        linear_kernel,
+        row(gelu_bias),
+        row(linear_bias),
+    )
+    taps_other = swap(taps)
+    gated_own, gated_other, out_own = call(
         attend_body,
-        [shape((half, DV)), shape((half, DV))],
+        [shape((half, DV)), shape((half, DV)), shape((model, DV))],
         y_index[None],
         core[None],
         decay_logits[:, 0],
@@ -390,7 +389,7 @@
         flops=1 << 32,
         smem=3,
         scratch=[
-            pltpu.VMEM((model, FIRST), bf16),
+            pltpu.VMEM((model, PROJECT), bf16),
             pltpu.VMEM((2 * half, DK), bf16),
             pltpu.VMEM((2 * half, DK), bf16),
             pltpu.VMEM((2 * half, DV), bf16),
@@ -398,85 +397,58 @@
         ],
     )
     gated_partner = swap(gated_other)
-    mixed = call(
+    x_index = lax.axis_index("x").astype(jnp.int32)[None]
+    far, right, left, here = call(
         output_body,
-        shape((half, model)),
+        [shape((own, model))] * 4,
+        x_index,
         gated_own,
         gated_partner,
-        second_own,
-        swap(second_own),
+        out_own,
+        swap(out_own),
         flops=1 << 30,
-        scratch=[pltpu.VMEM((model, 2 * SECOND), bf16)],
-    )
-    mix_pieces = exchanged(mixed.reshape(chips, own, model))
-    taps = call(
-        functools.partial(taps_body, width),
-        shape((8, PAD), f32),
-        gelu_kernel,
-        linear_kernel,
-        row(gelu_bias),
-        row(linear_bias),
-    )
-    taps_other = swap(taps)
-    after_mix, channel_spread = call(
+        smem=1,
+        scratch=[pltpu.VMEM((half, 2 * DV), bf16)],
+    )
+    after_mix, channel_in = call(
         middle_body,
-        [shape((own, model)), shape((chips, own, model))],
-        mix_pieces,
+        [shape((own, model)), shape((own, model))],
+        *sent(far, right, left),
+        here,
         token_rows,
         row(mixer_out_gain),
         row(channel_in_gain),
     )
-    channel_rows = exchanged(channel_spread)
-    third_own = call(
-        line_order_body, shape((8, 4, 32, THIRD)), y_index[None], *third_pieces, smem=1
-    ).reshape(model, THIRD)
     third_other = swap(third_own)
-    edges = lax.slice(
-        channel_rows, (0, 0, 0), (chips, own, model), (1, own - 1, 1)
-    ).reshape(2 * chips, model)
-    edges_other = swap(edges)
-    flat_rows = channel_rows.reshape(half, model)
-    x_index = lax.axis_index("x").astype(jnp.int32)[None]
-    far, outer = call(
-        feed_far_body,
-        [shape((own, model)), shape((16, 4 * PAD), f32)],
+    got_far, got_prev, got_next = sent(channel_in, channel_in, channel_in)
+    blocks = (got_far, got_next, got_prev, channel_in)
+    edges = jnp.concatenate([b[k : k + 1] for b in blocks for k in (0, own - 1)], axis=0)
+    far, right, left, here = call(
+        feed_body,
+        [shape((own, model))] * 4,
         x_index,
         core[None],
-        flat_rows,
-        edges_other,
-        third_own,
-        third_other,
-        taps,
-        taps_other,
-        flops=1 << 31,
-        smem=2,
-        scratch=[pltpu.VMEM((own + 16, model), bf16), pltpu.VMEM((own, 2 * PAD), bf16)],
-    )
-    far_got = permuted(far, "x", 2, 4)
-    right, left, here = call(
-        feed_near_body,
-        [shape((own, model))] * 3,
-        x_index,
-        core[None],
-        flat_rows,
-        outer,
+        *blocks,
+        swap(edges),
         third_own,
         third_other,
         taps,
         taps_other,
         flops=1 << 32,
         smem=2,
-        scratch=[pltpu.VMEM((3 * own, model), bf16), pltpu.VMEM((3 * own, 2 * PAD), bf16)],
-    )
-    right_got = permuted(right, "x", 1, 4)
-    left_got = permuted(left, "x", -1, 4)
+        scratch=[
+            pltpu.VMEM((half + 16, model), bf16),
+            pltpu.VMEM((16, 2 * PAD), f32),
+            pltpu.VMEM((half, 2 * PAD), bf16),
+            pltpu.VMEM((model, THIRD), bf16),
+            pltpu.VMEM((model, THIRD), bf16),
+        ],
+    )
     result = call(
         final_body,
         shape((own, model)),
+        *sent(far, right, left),
         here,
-        right_got,
-        left_got,
-        far_got,
         after_mix,
         row(channel_out_gain),
     )

time: 216 us -> 213 us (0.986)
  the two profiles are of different devices: /device:TPU:14 before, /device:TPU:3 now
where the time goes in v4:
time: 213 us; the launch traced here: 211 us
  starting transfers between devices  105 us (49%)
  waiting for transfers between devices  70.6 us (33%)
  Pallas kernels  30.2 us (14%)
  local copies, waits for them, and re-layouts  5.49 us (3%)
    ppermute x19, starting transfers between devices, permuted(): lax.ppermute(value, axes, [(i, (i + shift) % size) for i in range(size)])  74.4 us
    ppermute x19, waiting for transfers between devices, permuted(): lax.ppermute(value, axes, [(i, (i + shift) % size) for i in range(size)])  54 us
    pallas_call x9, Pallas kernels, call(): pl.pallas_call(body, out_shape=out_shapes, in_specs=specs, out_specs=VMEM...  30.2 us
    ppermute x6, starting transfers between devices, swap(): return lax.ppermute(value, 'c', SWAP)  21.7 us
    all_to_all x1, waiting for transfers between devices, layer(): third_own = lax.all_to_all(third_z, 'y', 0, 0, tiled=True)  13.6 us
    all_to_all x1, starting transfers between devices, exchanged(): return lax.all_to_all(value, 'x', 0, 0, tiled=True)  4.26 us
  transfers between devices with their start and end apart: 27, of which 16 were waited for; matrix products, arithmetic and copies ran while one was open for 1% of the time, Pallas kernels for 8%

profile of v4, /device:TPU:3, one launch (start us, length us, event | category | flops | bytes accessed | tf_op | source)
XLA Modules:
  0.0 211.3 jit_solution(15327504884655576141)
XLA Ops:
  0.0 2.1 shard_map.181
  2.1 4.3 %all-to-all-start = ((bf16[4,128,1024]{2,1,0:T(8,128)(2,1)}), bf16[4,128,1024]{2,1,0:T(8,128)(2,1)S(1)}, u32[]{:S(2)}, u32[]{:S(2)}) async-start(bf16[4,128,1024]{2,1,0:T(8,128)(2,1)} %shard_map.181), calls=%async_computation | async-start | bytes 2097152 | tf_op jit(solution)/shard_map/all_to_all | solution.py:62
  7.9 8.8 %collective-permute-start.1 = (bf16[32,2176]{1,0:T(8,128)(2,1)}, bf16[32,2176]{1,0:T(8,128)(2,1)S(1)}, u32[]{:S(2)}, u32[]{:S(2)}) collective-permute-start(bf16[32,2176]{1,0:T(8,128)(2,1)} %shard_map.182.refs_4_), channel_id=1, source_target_pairs={{0,128},{32,160},{64,192},{96,224},{128,256},{160,288},{192,320},{... | collective-permute-start | bytes 417800 | tf_op jit(solution)/shard_map/ppermute | solution.py:54
  16.7 6.3 %collective-permute-start.2 = (bf16[32,2176]{1,0:T(8,128)(2,1)}, bf16[32,2176]{1,0:T(8,128)(2,1)S(1)}, u32[]{:S(2)}, u32[]{:S(2)}) collective-permute-start(bf16[32,2176]{1,0:T(8,128)(2,1)} %shard_map.182.refs_4_), channel_id=1, source_target_pairs={{0,96},{32,128},{64,160},{96,192},{128,224},{160,256},{192,288},{2... | collective-permute-start | bytes 417800 | tf_op jit(solution)/shard_map/ppermute | solution.py:54
  23.0 5.2 %collective-permute-start.3 = (bf16[32,2176]{1,0:T(8,128)(2,1)}, bf16[32,2176]{1,0:T(8,128)(2,1)S(1)}, u32[]{:S(2)}, u32[]{:S(2)}) collective-permute-start(bf16[32,2176]{1,0:T(8,128)(2,1)} %shard_map.182.refs_4_), channel_id=1, source_target_pairs={{0,64},{32,96},{64,128},{96,160},{128,192},{160,224},{192,256},{22... | collective-permute-start | bytes 417800 | tf_op jit(solution)/shard_map/ppermute | solution.py:54
  28.2 2.6 %collective-permute-start.4 = (bf16[32,2176]{1,0:T(8,128)(2,1)}, bf16[32,2176]{1,0:T(8,128)(2,1)S(1)}, u32[]{:S(2)}, u32[]{:S(2)}) collective-permute-start(bf16[32,2176]{1,0:T(8,128)(2,1)} %shard_map.182.refs_4_), channel_id=1, source_target_pairs={{0,32},{32,64},{64,96},{96,128},{128,160},{160,192},{192,224},{224... | collective-permute-start | bytes 417800 | tf_op jit(solution)/shard_map/ppermute | solution.py:54
  30.9 3.8 %collective-permute-start.5 = (bf16[32,2176]{1,0:T(8,128)(2,1)}, bf16[32,2176]{1,0:T(8,128)(2,1)S(1)}, u32[]{:S(2)}, u32[]{:S(2)}) collective-permute-start(bf16[32,2176]{1,0:T(8,128)(2,1)} %shard_map.182.refs_4_), channel_id=1, source_target_pairs={{0,480},{32,0},{64,32},{96,64},{128,96},{160,128},{192,160},{224,1... | collective-permute-start | bytes 417800 | tf_op jit(solution)/shard_map/ppermute | solution.py:54
  34.7 5.7 %collective-permute-start.6 = (bf16[32,2176]{1,0:T(8,128)(2,1)}, bf16[32,2176]{1,0:T(8,128)(2,1)S(1)}, u32[]{:S(2)}, u32[]{:S(2)}) collective-permute-start(bf16[32,2176]{1,0:T(8,128)(2,1)} %shard_map.182.refs_4_), channel_id=1, source_target_pairs={{0,448},{32,480},{64,0},{96,32},{128,64},{160,96},{192,128},{224,1... | collective-permute-start | bytes 417800 | tf_op jit(solution)/shard_map/ppermute | solution.py:54
  40.4 2.8 %collective-permute-done.2.refs_1_ = bf16[32,2176]{1,0:T(8,128)(2,1)S(1)} collective-permute-done((bf16[32,2176]{1,0:T(8,128)(2,1)}, bf16[32,2176]{1,0:T(8,128)(2,1)S(1)}, u32[]{:S(2)}, u32[]{:S(2)}) %collective-permute-start.2) | collective-permute-done | bytes 139296 | tf_op jit(solution)/shard_map/ppermute | solution.py:54
  43.2 4.4 %collective-permute-start.7 = (bf16[32,2176]{1,0:T(8,128)(2,1)}, bf16[32,2176]{1,0:T(8,128)(2,1)S(1)}, u32[]{:S(2)}, u32[]{:S(2)}) collective-permute-start(bf16[32,2176]{1,0:T(8,128)(2,1)} %shard_map.182.refs_4_), channel_id=1, source_target_pairs={{0,416},{32,448},{64,480},{96,0},{128,32},{160,64},{192,96},{224,1... | collective-permute-start | bytes 417800 | tf_op jit(solution)/shard_map/ppermute | solution.py:54
  47.6 2.2 %collective-permute-done.4.refs_3_ = bf16[32,2176]{1,0:T(8,128)(2,1)S(1)} collective-permute-done((bf16[32,2176]{1,0:T(8,128)(2,1)}, bf16[32,2176]{1,0:T(8,128)(2,1)S(1)}, u32[]{:S(2)}, u32[]{:S(2)}) %collective-permute-start.4) | collective-permute-done | bytes 139296 | tf_op jit(solution)/shard_map/ppermute | solution.py:54
  49.9 7.6 %collective-permute-done.7.refs_7_ = bf16[32,2176]{1,0:T(8,128)(2,1)S(1)} collective-permute-done((bf16[32,2176]{1,0:T(8,128)(2,1)}, bf16[32,2176]{1,0:T(8,128)(2,1)S(1)}, u32[]{:S(2)}, u32[]{:S(2)}) %collective-permute-start.7) | collective-permute-done | bytes 139296 | tf_op jit(solution)/shard_map/ppermute | solution.py:54
  58.1 3.1 %shard_map.183 = (bf16[8,32,1024]{2,1,0:T(8,128)(2,1)}, bf16[4,8,32,1152]{3,2,1,0:T(8,128)(2,1)}) custom-call(s32[1]{0:T(128)} %bitcast.7.index, bf16[32,2176]{1,0:T(8,128)(2,1)} %copy-done.8, bf16[32,2176]{1,0:T(8,128)(2,1)} %copy-done.9, bf16[32,2176]{1,0:T(8,128)(2,1)} %copy-done.10, bf16[32,2176]{1,0:T(8,128)(2,1)} %copy-done.11, ...), custom_call_target="tpu_custom_call" | custom-call | flops 16777216 | bytes 2097152 | tf_op jit(solution)/shard_map/pallas_call | solution.py:37
  61.1 4.2 %all-to-all-start.1 = ((bf16[4,8,32,1152]{3,2,1,0:T(8,128)(2,1)}), bf16[4,8,32,1152]{3,2,1,0:T(8,128)(2,1)S(1)}, u32[]{:S(2)}, u32[]{:S(2)}) async-start(bf16[4,8,32,1152]{3,2,1,0:T(8,128)(2,1)} %get-tuple-element.29), calls=%async_computation.1 | async-start | bytes 4718592 | tf_op jit(solution)/shard_map/all_to_all | solution.py:369
  65.3 3.3 %collective-permute-start = (bf16[512,1024]{1,0:T(8,128)(2,1)S(1)}, bf16[512,1024]{1,0:T(8,128)(2,1)}, u32[]{:S(2)}, u32[]{:S(2)}) collective-permute-start(bf16[512,1024]{1,0:T(8,128)(2,1)S(1)} %bitcast.20), channel_id=1, source_target_pairs={{0,1},{1,0},{2,3},{3,2},{4,5},{5,4},{6,7},{7,6},{8,9},{9,8},{10,11... | collective-permute-start | bytes 3145736 | tf_op jit(solution)/shard_map/ppermute | solution.py:58
  68.6 3.7 %collective-permute-start.8 = (bf16[8,32,1024]{2,1,0:T(8,128)(2,1)}, bf16[8,32,1024]{2,1,0:T(8,128)(2,1)}, u32[]{:S(2)}, u32[]{:S(2)}) collective-permute-start(bf16[8,32,1024]{2,1,0:T(8,128)(2,1)} %get-tuple-element.20), channel_id=1, source_target_pairs={{0,8},{8,16},{16,24},{24,0},{1,9},{9,17},{17,25},{25,1},{2,10},{10... | collective-permute-start | bytes 1572872 | tf_op jit(solution)/shard_map/ppermute | solution.py:54
  72.3 4.3 %collective-permute-start.9 = (bf16[8,32,1024]{2,1,0:T(8,128)(2,1)}, bf16[8,32,1024]{2,1,0:T(8,128)(2,1)}, u32[]{:S(2)}, u32[]{:S(2)}) collective-permute-start(bf16[8,32,1024]{2,1,0:T(8,128)(2,1)} %get-tuple-element.20), channel_id=1, source_target_pairs={{0,16},{8,24},{16,0},{24,8},{1,17},{9,25},{17,1},{25,9},{2,18},{10... | collective-permute-start | bytes 1572872 | tf_op jit(solution)/shard_map/ppermute | solution.py:54
  76.6 3.1 %collective-permute-start.10 = (bf16[8,32,1024]{2,1,0:T(8,128)(2,1)}, bf16[8,32,1024]{2,1,0:T(8,128)(2,1)}, u32[]{:S(2)}, u32[]{:S(2)}) collective-permute-start(bf16[8,32,1024]{2,1,0:T(8,128)(2,1)} %get-tuple-element.20), channel_id=1, source_target_pairs={{0,24},{8,0},{16,8},{24,16},{1,25},{9,1},{17,9},{25,17},{2,26},{10... | collective-permute-start | bytes 1572872 | tf_op jit(solution)/shard_map/ppermute | solution.py:54
  79.7 13.6 %all-to-all-done.1.mine = bf16[4,8,32,1152]{3,2,1,0:T(8,128)(2,1)S(1)} async-done(((bf16[4,8,32,1152]{3,2,1,0:T(8,128)(2,1)}), bf16[4,8,32,1152]{3,2,1,0:T(8,128)(2,1)S(1)}, u32[]{:S(2)}, u32[]{:S(2)}) %all-to-all-start.1) | async-done | bytes 2359328 | tf_op jit(solution)/shard_map/all_to_all | solution.py:369
  93.3 5.9 %collective-permute-start.20 = (bf16[4,8,32,1152]{3,2,1,0:T(8,128)(2,1)S(1)}, bf16[4,8,32,1152]{3,2,1,0:T(8,128)(2,1)}, u32[]{:S(2)}, u32[]{:S(2)}) collective-permute-start(bf16[4,8,32,1152]{3,2,1,0:T(8,128)(2,1)S(1)} %all-to-all-done.1.mine), channel_id=1, source_target_pairs={{0,1},{1,0},{2,3},{3,2},{4,5},{5,4},{6,7},{7,6},{8,9},{9,8},{10,11... | collective-permute-start | bytes 7077896 | tf_op jit(solution)/shard_map/ppermute | solution.py:58
  99.2 5.1 %collective-permute-done.8 = bf16[8,32,1024]{2,1,0:T(8,128)(2,1)} collective-permute-done((bf16[8,32,1024]{2,1,0:T(8,128)(2,1)}, bf16[8,32,1024]{2,1,0:T(8,128)(2,1)}, u32[]{:S(2)}, u32[]{:S(2)}) %collective-permute-start.8) | collective-permute-done | bytes 524320 | tf_op jit(solution)/shard_map/ppermute | solution.py:54
  104.3 11.6 %collective-permute-done.9 = bf16[8,32,1024]{2,1,0:T(8,128)(2,1)} collective-permute-done((bf16[8,32,1024]{2,1,0:T(8,128)(2,1)}, bf16[8,32,1024]{2,1,0:T(8,128)(2,1)}, u32[]{:S(2)}, u32[]{:S(2)}) %collective-permute-start.9) | collective-permute-done | bytes 524320 | tf_op jit(solution)/shard_map/ppermute | solution.py:54
  115.9 6.7 %shard_map.184 = (bf16[512,256]{1,0:T(8,128)(2,1)}, bf16[512,256]{1,0:T(8,128)(2,1)}, bf16[1024,256]{1,0:T(8,128)(2,1)}) custom-call(s32[1]{0:T(128)} %bitcast.2.y_ref, s32[1]{0:T(128)} %bitcast.1.core_ref, f32[2]{0:T(128)} %bitcast.29, bf16[512,1024]{1,0:T(8,128)(2,1)} %bitcast.21, bf16[512,1024]{1,0:T(8,128)(2,1)} %collective-permute-done.other, ...), custom_call_target="tpu_custom_call" | custom-call | flops 4294967296 | bytes 2097152 | tf_op jit(solution)/shard_map/pallas_call | solution.py:37
  122.5 4.1 %collective-permute-start.12 = (bf16[1024,256]{1,0:T(8,128)(2,1)}, bf16[1024,256]{1,0:T(8,128)(2,1)S(1)}, u32[]{:S(2)}, u32[]{:S(2)}) collective-permute-start(bf16[1024,256]{1,0:T(8,128)(2,1)} %get-tuple-element.23.my_weights), channel_id=1, source_target_pairs={{0,1},{1,0},{2,3},{3,2},{4,5},{5,4},{6,7},{7,6},{8,9},{9,8},{10,11... | collective-permute-start | bytes 1572872 | tf_op jit(solution)/shard_map/ppermute | solution.py:58
  126.6 1.9 collective-permute-start.11
  128.6 1.7 collective-permute-done.11.theirs
  131.2 3.0 %shard_map.185 = (bf16[128,1024]{1,0:T(8,128)(2,1)}, bf16[128,1024]{1,0:T(8,128)(2,1)}, bf16[128,1024]{1,0:T(8,128)(2,1)}, bf16[128,1024]{1,0:T(8,128)(2,1)}) custom-call(s32[1]{0:T(128)} %bitcast.x_ref, bf16[512,256]{1,0:T(8,128)(2,1)} %get-tuple-element.21.mine, bf16[512,256]{1,0:T(8,128)(2,1)} %copy-done.21, ...), custom_call_target="tpu_custom_call" | custom-call | flops 1073741824 | bytes 2097152 | tf_op jit(solution)/shard_map/pallas_call | solution.py:37
  134.2 3.7 %collective-permute-start.13 = (bf16[128,1024]{1,0:T(8,128)(2,1)}, bf16[128,1024]{1,0:T(8,128)(2,1)S(1)}, u32[]{:S(2)}, u32[]{:S(2)}) collective-permute-start(bf16[128,1024]{1,0:T(8,128)(2,1)} %get-tuple-element.24), channel_id=1, source_target_pairs={{0,4},{2,6},{4,0},{6,2},{1,5},{3,7},{5,1},{7,3},{8,12},{10,14},{12... | collective-permute-start | bytes 786440 | tf_op jit(solution)/shard_map/ppermute | solution.py:54
  137.9 1.9 collective-permute-start.14
  139.8 3.4 %collective-permute-start.15 = (bf16[128,1024]{1,0:T(8,128)(2,1)}, bf16[128,1024]{1,0:T(8,128)(2,1)S(1)}, u32[]{:S(2)}, u32[]{:S(2)}) collective-permute-start(bf16[128,1024]{1,0:T(8,128)(2,1)} %get-tuple-element.26), channel_id=1, source_target_pairs={{0,6},{2,0},{4,2},{6,4},{1,7},{3,1},{5,3},{7,5},{8,14},{10,8},{12,... | collective-permute-start | bytes 786440 | tf_op jit(solution)/shard_map/ppermute | solution.py:54
  143.2 2.3 %collective-permute-done.13.far = bf16[128,1024]{1,0:T(8,128)(2,1)S(1)} collective-permute-done((bf16[128,1024]{1,0:T(8,128)(2,1)}, bf16[128,1024]{1,0:T(8,128)(2,1)S(1)}, u32[]{:S(2)}, u32[]{:S(2)}) %collective-permute-start.13) | collective-permute-done | bytes 262176 | tf_op jit(solution)/shard_map/ppermute | solution.py:54
  145.5 5.7 %collective-permute-done.14.right = bf16[128,1024]{1,0:T(8,128)(2,1)S(1)} collective-permute-done((bf16[128,1024]{1,0:T(8,128)(2,1)}, bf16[128,1024]{1,0:T(8,128)(2,1)S(1)}, u32[]{:S(2)}, u32[]{:S(2)}) %collective-permute-start.14) | collective-permute-done | bytes 262176 | tf_op jit(solution)/shard_map/ppermute | solution.py:54
  152.3 2.4 %shard_map.186 = (bf16[128,1024]{1,0:T(8,128)(2,1)}, bf16[128,1024]{1,0:T(8,128)(2,1)}) custom-call(bf16[128,1024]{1,0:T(8,128)(2,1)} %copy-done.2, bf16[128,1024]{1,0:T(8,128)(2,1)} %copy-done.3, bf16[128,1024]{1,0:T(8,128)(2,1)} %copy-done.4, bf16[128,1024]{1,0:T(8,128)(2,1)} %get-tuple-element.27.here, bf16[128,1024]{1,0:T(8,128)(2,1)} %bitcast.19, ...), custom_call_target="tpu_custom_call" | custom-call | flops 16777216 | bytes 2097152 | tf_op jit(solution)/shard_map/pallas_call | solution.py:37
  154.7 3.2 %collective-permute-start.18 = (bf16[128,1024]{1,0:T(8,128)(2,1)}, bf16[128,1024]{1,0:T(8,128)(2,1)S(1)}, u32[]{:S(2)}, u32[]{:S(2)}) collective-permute-start(bf16[128,1024]{1,0:T(8,128)(2,1)} %get-tuple-element.28.own), channel_id=1, source_target_pairs={{0,2},{2,4},{4,6},{6,0},{1,3},{3,5},{5,7},{7,1},{8,10},{10,12},{12... | collective-permute-start | bytes 786440 | tf_op jit(solution)/shard_map/ppermute | solution.py:54
  157.9 2.1 collective-permute-start.17
  160.0 3.5 %collective-permute-start.16 = (bf16[128,1024]{1,0:T(8,128)(2,1)}, bf16[128,1024]{1,0:T(8,128)(2,1)S(1)}, u32[]{:S(2)}, u32[]{:S(2)}) collective-permute-start(bf16[128,1024]{1,0:T(8,128)(2,1)} %get-tuple-element.28.own), channel_id=1, source_target_pairs={{0,4},{2,6},{4,0},{6,2},{1,5},{3,7},{5,1},{7,3},{8,12},{10,14},{12... | collective-permute-start | bytes 786440 | tf_op jit(solution)/shard_map/ppermute | solution.py:54
  164.3 3.6 %collective-permute-done.17.got_next = bf16[128,1024]{1,0:T(8,128)(2,1)S(1)} collective-permute-done((bf16[128,1024]{1,0:T(8,128)(2,1)}, bf16[128,1024]{1,0:T(8,128)(2,1)S(1)}, u32[]{:S(2)}, u32[]{:S(2)}) %collective-permute-start.17) | collective-permute-done | bytes 262176 | tf_op jit(solution)/shard_map/ppermute | solution.py:54
  168.0 4.0 %collective-permute-done.16.got_far = bf16[128,1024]{1,0:T(8,128)(2,1)S(1)} collective-permute-done((bf16[128,1024]{1,0:T(8,128)(2,1)}, bf16[128,1024]{1,0:T(8,128)(2,1)S(1)}, u32[]{:S(2)}, u32[]{:S(2)}) %collective-permute-start.16) | collective-permute-done | bytes 262176 | tf_op jit(solution)/shard_map/ppermute | solution.py:54
  172.1 4.6 %collective-permute-start.19 = (bf16[8,1024]{1,0:T(8,128)(2,1)S(1)}, bf16[8,1024]{1,0:T(8,128)(2,1)S(1)}, u32[]{:S(2)}, u32[]{:S(2)}) collective-permute-start(bf16[8,1024]{1,0:T(8,128)(2,1)S(1)} %concatenate.3), channel_id=1, source_target_pairs={{0,1},{1,0},{2,3},{3,2},{4,5},{5,4},{6,7},{7,6},{8,9},{9,8},{10,11... | collective-permute-start | bytes 49160 | tf_op jit(solution)/shard_map/ppermute | solution.py:58
  179.1 1.9 collective-permute-start.21
  183.0 7.9 %shard_map.188 = (bf16[128,1024]{1,0:T(8,128)(2,1)}, bf16[128,1024]{1,0:T(8,128)(2,1)}, bf16[128,1024]{1,0:T(8,128)(2,1)}, bf16[128,1024]{1,0:T(8,128)(2,1)}) custom-call(s32[1]{0:T(128)} %bitcast.x_ref, s32[1]{0:T(128)} %bitcast.1.core_ref, bf16[128,1024]{1,0:T(8,128)(2,1)} %copy-done.19, bf16[128,1024]{1,0:T(8,128)(2,1)} %copy-done.18, ...), custom_call_target="tpu_custom_call" | custom-call | flops 4294967296 | bytes 2097152 | tf_op jit(solution)/shard_map/pallas_call | solution.py:37
  190.9 3.4 %collective-permute-start.22 = (bf16[128,1024]{1,0:T(8,128)(2,1)}, bf16[128,1024]{1,0:T(8,128)(2,1)S(1)}, u32[]{:S(2)}, u32[]{:S(2)}) collective-permute-start(bf16[128,1024]{1,0:T(8,128)(2,1)} %get-tuple-element.30), channel_id=1, source_target_pairs={{0,4},{2,6},{4,0},{6,2},{1,5},{3,7},{5,1},{7,3},{8,12},{10,14},{12... | collective-permute-start | bytes 786440 | tf_op jit(solution)/shard_map/ppermute | solution.py:54
  194.4 1.9 collective-permute-start.23
  196.3 3.4 %collective-permute-start.24 = (bf16[128,1024]{1,0:T(8,128)(2,1)}, bf16[128,1024]{1,0:T(8,128)(2,1)S(1)}, u32[]{:S(2)}, u32[]{:S(2)}) collective-permute-start(bf16[128,1024]{1,0:T(8,128)(2,1)} %get-tuple-element.32), channel_id=1, source_target_pairs={{0,6},{2,0},{4,2},{6,4},{1,7},{3,1},{5,3},{7,5},{8,14},{10,8},{12,... | collective-permute-start | bytes 786440 | tf_op jit(solution)/shard_map/ppermute | solution.py:54
  199.7 2.5 %collective-permute-done.22.far = bf16[128,1024]{1,0:T(8,128)(2,1)S(1)} collective-permute-done((bf16[128,1024]{1,0:T(8,128)(2,1)}, bf16[128,1024]{1,0:T(8,128)(2,1)S(1)}, u32[]{:S(2)}, u32[]{:S(2)}) %collective-permute-start.22) | collective-permute-done | bytes 262176 | tf_op jit(solution)/shard_map/ppermute | solution.py:54
  202.2 3.5 %collective-permute-done.23.right = bf16[128,1024]{1,0:T(8,128)(2,1)S(1)} collective-permute-done((bf16[128,1024]{1,0:T(8,128)(2,1)}, bf16[128,1024]{1,0:T(8,128)(2,1)S(1)}, u32[]{:S(2)}, u32[]{:S(2)}) %collective-permute-start.23) | collective-permute-done | bytes 262176 | tf_op jit(solution)/shard_map/ppermute | solution.py:54
  205.7 2.7 %collective-permute-done.24.left = bf16[128,1024]{1,0:T(8,128)(2,1)S(1)} collective-permute-done((bf16[128,1024]{1,0:T(8,128)(2,1)}, bf16[128,1024]{1,0:T(8,128)(2,1)S(1)}, u32[]{:S(2)}, u32[]{:S(2)}) %collective-permute-start.24) | collective-permute-done | bytes 262176 | tf_op jit(solution)/shard_map/ppermute | solution.py:54
  209.1 2.2 %shard_map.189 = bf16[128,1024]{1,0:T(8,128)(2,1)} custom-call(bf16[128,1024]{1,0:T(8,128)(2,1)} %copy-done.5, bf16[128,1024]{1,0:T(8,128)(2,1)} %copy-done.6, bf16[128,1024]{1,0:T(8,128)(2,1)} %copy-done.7, bf16[128,1024]{1,0:T(8,128)(2,1)} %get-tuple-element.33.here, bf16[128,1024]{1,0:T(8,128)(2,1)} %get-tuple-element.34.after_mix, f32[1,1024]{1,0:T(1,128)} %bitcast.27), custom_call_target="tpu_custom_call" | custom-call | flops 16777216 | bytes 2097152 | tf_op jit(solution)/shard_map/pallas_call | solution.py:37
  (70 shorter events, 10.2 us)
Async XLA Ops:
  2.1 59.0 %all-to-all-start = ((bf16[4,128,1024]{2,1,0:T(8,128)(2,1)}), bf16[4,128,1024]{2,1,0:T(8,128)(2,1)S(1)}, u32[]{:S(2)}, u32[]{:S(2)}) async-start(bf16[4,128,1024]{2,1,0:T(8,128)(2,1)} %shard_map.181), calls=%async_computation | async-start | bytes 2097152 | tf_op jit(solution)/shard_map/all_to_all | solution.py:62
  7.9 26.8 %collective-permute-start.1 = (bf16[32,2176]{1,0:T(8,128)(2,1)}, bf16[32,2176]{1,0:T(8,128)(2,1)S(1)}, u32[]{:S(2)}, u32[]{:S(2)}) collective-permute-start(bf16[32,2176]{1,0:T(8,128)(2,1)} %shard_map.182.refs_4_), channel_id=1, source_target_pairs={{0,128},{32,160},{64,192},{96,224},{128,256},{160,288},{192,320},{... | collective-permute-start | bytes 417800 | tf_op jit(solution)/shard_map/ppermute | solution.py:54
  16.7 26.4 %collective-permute-start.2 = (bf16[32,2176]{1,0:T(8,128)(2,1)}, bf16[32,2176]{1,0:T(8,128)(2,1)S(1)}, u32[]{:S(2)}, u32[]{:S(2)}) collective-permute-start(bf16[32,2176]{1,0:T(8,128)(2,1)} %shard_map.182.refs_4_), channel_id=1, source_target_pairs={{0,96},{32,128},{64,160},{96,192},{128,224},{160,256},{192,288},{2... | collective-permute-start | bytes 417800 | tf_op jit(solution)/shard_map/ppermute | solution.py:54
  23.0 24.6 %collective-permute-start.3 = (bf16[32,2176]{1,0:T(8,128)(2,1)}, bf16[32,2176]{1,0:T(8,128)(2,1)S(1)}, u32[]{:S(2)}, u32[]{:S(2)}) collective-permute-start(bf16[32,2176]{1,0:T(8,128)(2,1)} %shard_map.182.refs_4_), channel_id=1, source_target_pairs={{0,64},{32,96},{64,128},{96,160},{128,192},{160,224},{192,256},{22... | collective-permute-start | bytes 417800 | tf_op jit(solution)/shard_map/ppermute | solution.py:54
  28.2 21.7 %collective-permute-start.4 = (bf16[32,2176]{1,0:T(8,128)(2,1)}, bf16[32,2176]{1,0:T(8,128)(2,1)S(1)}, u32[]{:S(2)}, u32[]{:S(2)}) collective-permute-start(bf16[32,2176]{1,0:T(8,128)(2,1)} %shard_map.182.refs_4_), channel_id=1, source_target_pairs={{0,32},{32,64},{64,96},{96,128},{128,160},{160,192},{192,224},{224... | collective-permute-start | bytes 417800 | tf_op jit(solution)/shard_map/ppermute | solution.py:54
  30.9 19.0 %collective-permute-start.5 = (bf16[32,2176]{1,0:T(8,128)(2,1)}, bf16[32,2176]{1,0:T(8,128)(2,1)S(1)}, u32[]{:S(2)}, u32[]{:S(2)}) collective-permute-start(bf16[32,2176]{1,0:T(8,128)(2,1)} %shard_map.182.refs_4_), channel_id=1, source_target_pairs={{0,480},{32,0},{64,32},{96,64},{128,96},{160,128},{192,160},{224,1... | collective-permute-start | bytes 417800 | tf_op jit(solution)/shard_map/ppermute | solution.py:54
  34.7 22.7 %copy-start.8 = (bf16[32,2176]{1,0:T(8,128)(2,1)}, bf16[32,2176]{1,0:T(8,128)(2,1)S(1)}, u32[]{:S(2)}) copy-start(bf16[32,2176]{1,0:T(8,128)(2,1)S(1)} %collective-permute-done.1.refs_0_) | copy-start | bytes 417796
  34.7 15.1 %collective-permute-start.6 = (bf16[32,2176]{1,0:T(8,128)(2,1)}, bf16[32,2176]{1,0:T(8,128)(2,1)S(1)}, u32[]{:S(2)}, u32[]{:S(2)}) collective-permute-start(bf16[32,2176]{1,0:T(8,128)(2,1)} %shard_map.182.refs_4_), channel_id=1, source_target_pairs={{0,448},{32,480},{64,0},{96,32},{128,64},{160,96},{192,128},{224,1... | collective-permute-start | bytes 417800 | tf_op jit(solution)/shard_map/ppermute | solution.py:54
  43.2 14.3 %copy-start.9 = (bf16[32,2176]{1,0:T(8,128)(2,1)}, bf16[32,2176]{1,0:T(8,128)(2,1)S(1)}, u32[]{:S(2)}) copy-start(bf16[32,2176]{1,0:T(8,128)(2,1)S(1)} %collective-permute-done.2.refs_1_) | copy-start | bytes 417796
  43.2 14.3 %collective-permute-start.7 = (bf16[32,2176]{1,0:T(8,128)(2,1)}, bf16[32,2176]{1,0:T(8,128)(2,1)S(1)}, u32[]{:S(2)}, u32[]{:S(2)}) collective-permute-start(bf16[32,2176]{1,0:T(8,128)(2,1)} %shard_map.182.refs_4_), channel_id=1, source_target_pairs={{0,416},{32,448},{64,480},{96,0},{128,32},{160,64},{192,96},{224,1... | collective-permute-start | bytes 417800 | tf_op jit(solution)/shard_map/ppermute | solution.py:54
  47.6 9.8 %copy-start.10 = (bf16[32,2176]{1,0:T(8,128)(2,1)}, bf16[32,2176]{1,0:T(8,128)(2,1)S(1)}, u32[]{:S(2)}) copy-start(bf16[32,2176]{1,0:T(8,128)(2,1)S(1)} %collective-permute-done.3.refs_2_) | copy-start | bytes 417796
  49.9 7.6 %copy-start.11 = (bf16[32,2176]{1,0:T(8,128)(2,1)}, bf16[32,2176]{1,0:T(8,128)(2,1)S(1)}, u32[]{:S(2)}) copy-start(bf16[32,2176]{1,0:T(8,128)(2,1)S(1)} %collective-permute-done.4.refs_3_) | copy-start | bytes 417796
  49.9 7.6 %copy-start.12 = (bf16[32,2176]{1,0:T(8,128)(2,1)}, bf16[32,2176]{1,0:T(8,128)(2,1)S(1)}, u32[]{:S(2)}) copy-start(bf16[32,2176]{1,0:T(8,128)(2,1)S(1)} %collective-permute-done.5.refs_5_) | copy-start | bytes 417796
  49.9 7.6 %copy-start.13 = (bf16[32,2176]{1,0:T(8,128)(2,1)}, bf16[32,2176]{1,0:T(8,128)(2,1)S(1)}, u32[]{:S(2)}) copy-start(bf16[32,2176]{1,0:T(8,128)(2,1)S(1)} %collective-permute-done.6.refs_6_) | copy-start | bytes 417796
  61.1 4.2 %copy-start.1 = (bf16[4,128,1024]{2,1,0:T(8,128)(2,1)}, bf16[4,128,1024]{2,1,0:T(8,128)(2,1)S(1)}, u32[]{:S(2)}) copy-start(bf16[4,128,1024]{2,1,0:T(8,128)(2,1)S(1)} %all-to-all-done) | copy-start | bytes 3145732
  61.1 32.1 %all-to-all-start.1 = ((bf16[4,8,32,1152]{3,2,1,0:T(8,128)(2,1)}), bf16[4,8,32,1152]{3,2,1,0:T(8,128)(2,1)S(1)}, u32[]{:S(2)}, u32[]{:S(2)}) async-start(bf16[4,8,32,1152]{3,2,1,0:T(8,128)(2,1)} %get-tuple-element.29), calls=%async_computation.1 | async-start | bytes 4718592 | tf_op jit(solution)/shard_map/all_to_all | solution.py:369
  65.3 50.5 %collective-permute-start = (bf16[512,1024]{1,0:T(8,128)(2,1)S(1)}, bf16[512,1024]{1,0:T(8,128)(2,1)}, u32[]{:S(2)}, u32[]{:S(2)}) collective-permute-start(bf16[512,1024]{1,0:T(8,128)(2,1)S(1)} %bitcast.20), channel_id=1, source_target_pairs={{0,1},{1,0},{2,3},{3,2},{4,5},{5,4},{6,7},{7,6},{8,9},{9,8},{10,11... | collective-permute-start | bytes 3145736 | tf_op jit(solution)/shard_map/ppermute | solution.py:58
  68.6 35.7 %collective-permute-start.8 = (bf16[8,32,1024]{2,1,0:T(8,128)(2,1)}, bf16[8,32,1024]{2,1,0:T(8,128)(2,1)}, u32[]{:S(2)}, u32[]{:S(2)}) collective-permute-start(bf16[8,32,1024]{2,1,0:T(8,128)(2,1)} %get-tuple-element.20), channel_id=1, source_target_pairs={{0,8},{8,16},{16,24},{24,0},{1,9},{9,17},{17,25},{25,1},{2,10},{10... | collective-permute-start | bytes 1572872 | tf_op jit(solution)/shard_map/ppermute | solution.py:54
  72.3 43.6 %collective-permute-start.9 = (bf16[8,32,1024]{2,1,0:T(8,128)(2,1)}, bf16[8,32,1024]{2,1,0:T(8,128)(2,1)}, u32[]{:S(2)}, u32[]{:S(2)}) collective-permute-start(bf16[8,32,1024]{2,1,0:T(8,128)(2,1)} %get-tuple-element.20), channel_id=1, source_target_pairs={{0,16},{8,24},{16,0},{24,8},{1,17},{9,25},{17,1},{25,9},{2,18},{10... | collective-permute-start | bytes 1572872 | tf_op jit(solution)/shard_map/ppermute | solution.py:54
  76.6 39.3 %collective-permute-start.10 = (bf16[8,32,1024]{2,1,0:T(8,128)(2,1)}, bf16[8,32,1024]{2,1,0:T(8,128)(2,1)}, u32[]{:S(2)}, u32[]{:S(2)}) collective-permute-start(bf16[8,32,1024]{2,1,0:T(8,128)(2,1)} %get-tuple-element.20), channel_id=1, source_target_pairs={{0,24},{8,0},{16,8},{24,16},{1,25},{9,1},{17,9},{25,17},{2,26},{10... | collective-permute-start | bytes 1572872 | tf_op jit(solution)/shard_map/ppermute | solution.py:54
  93.3 29.3 %copy-start = (bf16[4,8,32,1152]{3,2,1,0:T(8,128)(2,1)}, bf16[4,8,32,1152]{3,2,1,0:T(8,128)(2,1)S(1)}, u32[]{:S(2)}) copy-start(bf16[4,8,32,1152]{3,2,1,0:T(8,128)(2,1)S(1)} %all-to-all-done.1.mine) | copy-start | bytes 7077892
  93.3 89.1 %collective-permute-start.20 = (bf16[4,8,32,1152]{3,2,1,0:T(8,128)(2,1)S(1)}, bf16[4,8,32,1152]{3,2,1,0:T(8,128)(2,1)}, u32[]{:S(2)}, u32[]{:S(2)}) collective-permute-start(bf16[4,8,32,1152]{3,2,1,0:T(8,128)(2,1)S(1)} %all-to-all-done.1.mine), channel_id=1, source_target_pairs={{0,1},{1,0},{2,3},{3,2},{4,5},{5,4},{6,7},{7,6},{8,9},{9,8},{10,11... | collective-permute-start | bytes 7077896 | tf_op jit(solution)/shard_map/ppermute | solution.py:58
  122.5 7.8 %collective-permute-start.12 = (bf16[1024,256]{1,0:T(8,128)(2,1)}, bf16[1024,256]{1,0:T(8,128)(2,1)S(1)}, u32[]{:S(2)}, u32[]{:S(2)}) collective-permute-start(bf16[1024,256]{1,0:T(8,128)(2,1)} %get-tuple-element.23.my_weights), channel_id=1, source_target_pairs={{0,1},{1,0},{2,3},{3,2},{4,5},{5,4},{6,7},{7,6},{8,9},{9,8},{10,11... | collective-permute-start | bytes 1572872 | tf_op jit(solution)/shard_map/ppermute | solution.py:58
  126.6 3.6 %collective-permute-start.11 = (bf16[512,256]{1,0:T(8,128)(2,1)}, bf16[512,256]{1,0:T(8,128)(2,1)S(1)}, u32[]{:S(2)}, u32[]{:S(2)}) collective-permute-start(bf16[512,256]{1,0:T(8,128)(2,1)} %get-tuple-element.22), channel_id=1, source_target_pairs={{0,1},{1,0},{2,3},{3,2},{4,5},{5,4},{6,7},{7,6},{8,9},{9,8},{10,11... | collective-permute-start | bytes 786440 | tf_op jit(solution)/shard_map/ppermute | solution.py:58
  130.3 0.7 copy-start.21
  130.3 0.9 copy-start.20
  131.2 45.5 %copy-start.15 = (f32[352]{0:T(512)S(1)}, f32[352]{0:T(512)}, u32[]{:S(2)}) copy-start(f32[352]{0:T(512)} %param.33) | copy-start | bytes 4228
  131.2 46.0 %copy-start.16 = (f32[352]{0:T(512)S(1)}, f32[352]{0:T(512)}, u32[]{:S(2)}) copy-start(f32[352]{0:T(512)} %param.34) | copy-start | bytes 4228
  134.2 11.3 %collective-permute-start.13 = (bf16[128,1024]{1,0:T(8,128)(2,1)}, bf16[128,1024]{1,0:T(8,128)(2,1)S(1)}, u32[]{:S(2)}, u32[]{:S(2)}) collective-permute-start(bf16[128,1024]{1,0:T(8,128)(2,1)} %get-tuple-element.24), channel_id=1, source_target_pairs={{0,4},{2,6},{4,0},{6,2},{1,5},{3,7},{5,1},{7,3},{8,12},{10,14},{12... | collective-permute-start | bytes 786440 | tf_op jit(solution)/shard_map/ppermute | solution.py:54
  137.9 13.3 %collective-permute-start.14 = (bf16[128,1024]{1,0:T(8,128)(2,1)}, bf16[128,1024]{1,0:T(8,128)(2,1)S(1)}, u32[]{:S(2)}, u32[]{:S(2)}) collective-permute-start(bf16[128,1024]{1,0:T(8,128)(2,1)} %get-tuple-element.25), channel_id=1, source_target_pairs={{0,2},{2,4},{4,6},{6,0},{1,3},{3,5},{5,7},{7,1},{8,10},{10,12},{12... | collective-permute-start | bytes 786440 | tf_op jit(solution)/shard_map/ppermute | solution.py:54
  139.8 11.8 %collective-permute-start.15 = (bf16[128,1024]{1,0:T(8,128)(2,1)}, bf16[128,1024]{1,0:T(8,128)(2,1)S(1)}, u32[]{:S(2)}, u32[]{:S(2)}) collective-permute-start(bf16[128,1024]{1,0:T(8,128)(2,1)} %get-tuple-element.26), channel_id=1, source_target_pairs={{0,6},{2,0},{4,2},{6,4},{1,7},{3,1},{5,3},{7,5},{8,14},{10,8},{12,... | collective-permute-start | bytes 786440 | tf_op jit(solution)/shard_map/ppermute | solution.py:54
  145.5 6.1 %copy-start.2 = (bf16[128,1024]{1,0:T(8,128)(2,1)}, bf16[128,1024]{1,0:T(8,128)(2,1)S(1)}, u32[]{:S(2)}) copy-start(bf16[128,1024]{1,0:T(8,128)(2,1)S(1)} %collective-permute-done.13.far) | copy-start | bytes 786436
  151.2 0.7 copy-start.3
  151.6 0.7 copy-start.4
  154.7 9.6 %collective-permute-start.18 = (bf16[128,1024]{1,0:T(8,128)(2,1)}, bf16[128,1024]{1,0:T(8,128)(2,1)S(1)}, u32[]{:S(2)}, u32[]{:S(2)}) collective-permute-start(bf16[128,1024]{1,0:T(8,128)(2,1)} %get-tuple-element.28.own), channel_id=1, source_target_pairs={{0,2},{2,4},{4,6},{6,0},{1,3},{3,5},{5,7},{7,1},{8,10},{10,12},{12... | collective-permute-start | bytes 786440 | tf_op jit(solution)/shard_map/ppermute | solution.py:54
  157.9 10.0 %collective-permute-start.17 = (bf16[128,1024]{1,0:T(8,128)(2,1)}, bf16[128,1024]{1,0:T(8,128)(2,1)S(1)}, u32[]{:S(2)}, u32[]{:S(2)}) collective-permute-start(bf16[128,1024]{1,0:T(8,128)(2,1)} %get-tuple-element.28.own), channel_id=1, source_target_pairs={{0,6},{2,0},{4,2},{6,4},{1,7},{3,1},{5,3},{7,5},{8,14},{10,8},{12,... | collective-permute-start | bytes 786440 | tf_op jit(solution)/shard_map/ppermute | solution.py:54
  160.0 12.0 %collective-permute-start.16 = (bf16[128,1024]{1,0:T(8,128)(2,1)}, bf16[128,1024]{1,0:T(8,128)(2,1)S(1)}, u32[]{:S(2)}, u32[]{:S(2)}) collective-permute-start(bf16[128,1024]{1,0:T(8,128)(2,1)} %get-tuple-element.28.own), channel_id=1, source_target_pairs={{0,4},{2,6},{4,0},{6,2},{1,5},{3,7},{5,1},{7,3},{8,12},{10,14},{12... | collective-permute-start | bytes 786440 | tf_op jit(solution)/shard_map/ppermute | solution.py:54
  164.3 18.1 %copy-start.17 = (bf16[128,1024]{1,0:T(8,128)(2,1)}, bf16[128,1024]{1,0:T(8,128)(2,1)S(1)}, u32[]{:S(2)}) copy-start(bf16[128,1024]{1,0:T(8,128)(2,1)S(1)} %collective-permute-done.18.got_prev) | copy-start | bytes 786436
  168.0 14.4 %copy-start.18 = (bf16[128,1024]{1,0:T(8,128)(2,1)}, bf16[128,1024]{1,0:T(8,128)(2,1)S(1)}, u32[]{:S(2)}) copy-start(bf16[128,1024]{1,0:T(8,128)(2,1)S(1)} %collective-permute-done.17.got_next) | copy-start | bytes 786436
  172.0 10.4 %copy-start.19 = (bf16[128,1024]{1,0:T(8,128)(2,1)}, bf16[128,1024]{1,0:T(8,128)(2,1)S(1)}, u32[]{:S(2)}) copy-start(bf16[128,1024]{1,0:T(8,128)(2,1)S(1)} %collective-permute-done.16.got_far) | copy-start | bytes 786436
  172.1 10.3 %collective-permute-start.19 = (bf16[8,1024]{1,0:T(8,128)(2,1)S(1)}, bf16[8,1024]{1,0:T(8,128)(2,1)S(1)}, u32[]{:S(2)}, u32[]{:S(2)}) collective-permute-start(bf16[8,1024]{1,0:T(8,128)(2,1)S(1)} %concatenate.3), channel_id=1, source_target_pairs={{0,1},{1,0},{2,3},{3,2},{4,5},{5,4},{6,7},{7,6},{8,9},{9,8},{10,11... | collective-permute-start | bytes 49160 | tf_op jit(solution)/shard_map/ppermute | solution.py:58
  179.1 3.3 %collective-permute-start.21 = (f32[8,384]{1,0:T(8,128)}, f32[8,384]{1,0:T(8,128)S(1)}, u32[]{:S(2)}, u32[]{:S(2)}) collective-permute-start(f32[8,384]{1,0:T(8,128)} %shard_map.187.my_taps), channel_id=1, source_target_pairs={{0,1},{1,0},{2,3},{3,2},{4,5},{5,4},{6,7},{7,6},{8,9},{9,8},{10,11... | collective-permute-start | bytes 36872 | tf_op jit(solution)/shard_map/ppermute | solution.py:58
  190.9 11.3 %collective-permute-start.22 = (bf16[128,1024]{1,0:T(8,128)(2,1)}, bf16[128,1024]{1,0:T(8,128)(2,1)S(1)}, u32[]{:S(2)}, u32[]{:S(2)}) collective-permute-start(bf16[128,1024]{1,0:T(8,128)(2,1)} %get-tuple-element.30), channel_id=1, source_target_pairs={{0,4},{2,6},{4,0},{6,2},{1,5},{3,7},{5,1},{7,3},{8,12},{10,14},{12... | collective-permute-start | bytes 786440 | tf_op jit(solution)/shard_map/ppermute | solution.py:54
  194.4 11.3 %collective-permute-start.23 = (bf16[128,1024]{1,0:T(8,128)(2,1)}, bf16[128,1024]{1,0:T(8,128)(2,1)S(1)}, u32[]{:S(2)}, u32[]{:S(2)}) collective-permute-start(bf16[128,1024]{1,0:T(8,128)(2,1)} %get-tuple-element.31), channel_id=1, source_target_pairs={{0,2},{2,4},{4,6},{6,0},{1,3},{3,5},{5,7},{7,1},{8,10},{10,12},{12... | collective-permute-start | bytes 786440 | tf_op jit(solution)/shard_map/ppermute | solution.py:54
  196.3 12.1 %collective-permute-start.24 = (bf16[128,1024]{1,0:T(8,128)(2,1)}, bf16[128,1024]{1,0:T(8,128)(2,1)S(1)}, u32[]{:S(2)}, u32[]{:S(2)}) collective-permute-start(bf16[128,1024]{1,0:T(8,128)(2,1)} %get-tuple-element.32), channel_id=1, source_target_pairs={{0,6},{2,0},{4,2},{6,4},{1,7},{3,1},{5,3},{7,5},{8,14},{10,8},{12,... | collective-permute-start | bytes 786440 | tf_op jit(solution)/shard_map/ppermute | solution.py:54
  202.2 6.2 %copy-start.5 = (bf16[128,1024]{1,0:T(8,128)(2,1)}, bf16[128,1024]{1,0:T(8,128)(2,1)S(1)}, u32[]{:S(2)}) copy-start(bf16[128,1024]{1,0:T(8,128)(2,1)S(1)} %collective-permute-done.22.far) | copy-start | bytes 786436
  205.7 2.7 %copy-start.6 = (bf16[128,1024]{1,0:T(8,128)(2,1)}, bf16[128,1024]{1,0:T(8,128)(2,1)S(1)}, u32[]{:S(2)}) copy-start(bf16[128,1024]{1,0:T(8,128)(2,1)S(1)} %collective-permute-done.23.right) | copy-start | bytes 786436
  208.4 0.7 copy-start.7
  (3 other events, 1.8 us)

commit v5 on v4

--- a/solution.py
+++ b/solution.py
@@ -31,7 +31,7 @@
 SMEM = pl.BlockSpec(memory_space=pltpu.SMEM)
 
 
-def call(body, out_shapes, *args, flops=0, smem=0, scratch=()):
+def call(body, out_shapes, *args, flops=0, smem=0, scratch=(), limit=6):
     specs = [SMEM] * smem + [VMEM] * (len(args) - smem)
     single = not isinstance(out_shapes, (list, tuple))
     return pl.pallas_call(
@@ -40,6 +40,7 @@
         in_specs=specs,
         out_specs=VMEM if single else [VMEM] * len(out_shapes),
         scratch_shapes=list(scratch),
+        compiler_params=pltpu.CompilerParams(vmem_limit_bytes=limit << 20),
         cost_estimate=pl.CostEstimate(
             flops=max(flops, 1 << 24), bytes_accessed=1 << 21, transcendentals=0
         ),
@@ -388,6 +389,7 @@
         rope_frequency(),
         flops=1 << 32,
         smem=3,
+        limit=14,
         scratch=[
             pltpu.VMEM((model, PROJECT), bf16),
             pltpu.VMEM((2 * half, DK), bf16),
@@ -436,6 +438,7 @@
         taps_other,
         flops=1 << 32,
         smem=2,
+        limit=18,
         scratch=[
             pltpu.VMEM((half + 16, model), bf16),
             pltpu.VMEM((16, 2 * PAD), f32),

time: 213 us -> 205 us (0.962)
  Pallas kernels: 30.2 us -> 16.5 us
  local copies, waits for them, and re-layouts: 5.49 us -> 11.8 us
    pallas_call x9, Pallas kernels: 30.2 us -> 16.5 us  [call(): pl.pallas_call(body, out_shape=out_shapes, in_specs=specs, out_specs=VMEM...]
    unnamed x48 -> x62, local copies, waits for them, and re-layouts: 3.5 us -> 11.7 us
  transfers between devices with their start and end apart: 27 -> 27, of which waited for: 16 -> 17; matrix products, arithmetic and copies ran while one was open for 1% -> 0% of each run, Pallas kernels for 8% -> 4%
where the time goes in v5:
time: 205 us; the launch traced here: 203 us
  starting transfers between devices  105 us (51%)
  waiting for transfers between devices  70 us (34%)
  Pallas kernels  16.5 us (8%)
  local copies, waits for them, and re-layouts  11.8 us (6%)
    ppermute x19, starting transfers between devices, permuted(): lax.ppermute(value, axes, [(i, (i + shift) % size) for i in range(size)])  74.1 us
    ppermute x19, waiting for transfers between devices, permuted(): lax.ppermute(value, axes, [(i, (i + shift) % size) for i in range(size)])  53.5 us
    ppermute x6, starting transfers between devices, swap(): return lax.ppermute(value, 'c', SWAP)  21.9 us
    pallas_call x9, Pallas kernels, call(): pl.pallas_call(body, out_shape=out_shapes, in_specs=specs, out_specs=VMEM...  16.5 us
    all_to_all x1, waiting for transfers between devices, layer(): third_own = lax.all_to_all(third_z, 'y', 0, 0, tiled=True)  13.6 us
    unnamed x62, local copies, waits for them, and re-layouts  11.7 us
    all_to_all x1, starting transfers between devices, layer(): third_own = lax.all_to_all(third_z, 'y', 0, 0, tiled=True)  4.32 us
    all_to_all x1, starting transfers between devices, exchanged(): return lax.all_to_all(value, 'x', 0, 0, tiled=True)  4.26 us
  transfers between devices with their start and end apart: 27, of which 17 were waited for; matrix products, arithmetic and copies ran while one was open for 0% of the time, Pallas kernels for 4%

profile of v5, /device:TPU:3, one launch (start us, length us, event | category | flops | bytes accessed | tf_op | source)
XLA Modules:
  0.0 203.4 jit_solution(5696744962992070810)
XLA Ops:
  1.7 1.2 shard_map.181
  2.8 4.3 %all-to-all-start = ((bf16[4,128,1024]{2,1,0:T(8,128)(2,1)}), bf16[4,128,1024]{2,1,0:T(8,128)(2,1)S(1)}, u32[]{:S(2)}, u32[]{:S(2)}) async-start(bf16[4,128,1024]{2,1,0:T(8,128)(2,1)} %shard_map.181), calls=%async_computation | async-start | bytes 2097152 | tf_op jit(solution)/shard_map/all_to_all | solution.py:63
  7.2 8.8 %collective-permute-start.1 = (bf16[32,2176]{1,0:T(8,128)(2,1)S(1)}, bf16[32,2176]{1,0:T(8,128)(2,1)S(1)}, u32[]{:S(2)}, u32[]{:S(2)}) collective-permute-start(bf16[32,2176]{1,0:T(8,128)(2,1)S(1)} %shard_map.182.refs_4_), channel_id=1, source_target_pairs={{0,128},{32,160},{64,192},{96,224},{128,256},{160,288},{192,320},{... | collective-permute-start | bytes 417800 | tf_op jit(solution)/shard_map/ppermute | solution.py:55
  16.0 6.3 %collective-permute-start.2 = (bf16[32,2176]{1,0:T(8,128)(2,1)S(1)}, bf16[32,2176]{1,0:T(8,128)(2,1)S(1)}, u32[]{:S(2)}, u32[]{:S(2)}) collective-permute-start(bf16[32,2176]{1,0:T(8,128)(2,1)S(1)} %shard_map.182.refs_4_), channel_id=1, source_target_pairs={{0,96},{32,128},{64,160},{96,192},{128,224},{160,256},{192,288},{2... | collective-permute-start | bytes 417800 | tf_op jit(solution)/shard_map/ppermute | solution.py:55
  22.3 5.2 %collective-permute-start.3 = (bf16[32,2176]{1,0:T(8,128)(2,1)S(1)}, bf16[32,2176]{1,0:T(8,128)(2,1)S(1)}, u32[]{:S(2)}, u32[]{:S(2)}) collective-permute-start(bf16[32,2176]{1,0:T(8,128)(2,1)S(1)} %shard_map.182.refs_4_), channel_id=1, source_target_pairs={{0,64},{32,96},{64,128},{96,160},{128,192},{160,224},{192,256},{22... | collective-permute-start | bytes 417800 | tf_op jit(solution)/shard_map/ppermute | solution.py:55
  27.5 2.6 %collective-permute-start.4 = (bf16[32,2176]{1,0:T(8,128)(2,1)S(1)}, bf16[32,2176]{1,0:T(8,128)(2,1)S(1)}, u32[]{:S(2)}, u32[]{:S(2)}) collective-permute-start(bf16[32,2176]{1,0:T(8,128)(2,1)S(1)} %shard_map.182.refs_4_), channel_id=1, source_target_pairs={{0,32},{32,64},{64,96},{96,128},{128,160},{160,192},{192,224},{224... | collective-permute-start | bytes 417800 | tf_op jit(solution)/shard_map/ppermute | solution.py:55
  30.2 3.8 %collective-permute-start.5 = (bf16[32,2176]{1,0:T(8,128)(2,1)S(1)}, bf16[32,2176]{1,0:T(8,128)(2,1)S(1)}, u32[]{:S(2)}, u32[]{:S(2)}) collective-permute-start(bf16[32,2176]{1,0:T(8,128)(2,1)S(1)} %shard_map.182.refs_4_), channel_id=1, source_target_pairs={{0,480},{32,0},{64,32},{96,64},{128,96},{160,128},{192,160},{224,1... | collective-permute-start | bytes 417800 | tf_op jit(solution)/shard_map/ppermute | solution.py:55
  34.0 5.4 %collective-permute-start.6 = (bf16[32,2176]{1,0:T(8,128)(2,1)S(1)}, bf16[32,2176]{1,0:T(8,128)(2,1)S(1)}, u32[]{:S(2)}, u32[]{:S(2)}) collective-permute-start(bf16[32,2176]{1,0:T(8,128)(2,1)S(1)} %shard_map.182.refs_4_), channel_id=1, source_target_pairs={{0,448},{32,480},{64,0},{96,32},{128,64},{160,96},{192,128},{224,1... | collective-permute-start | bytes 417800 | tf_op jit(solution)/shard_map/ppermute | solution.py:55
  39.5 2.8 %collective-permute-done.2.refs_1_ = bf16[32,2176]{1,0:T(8,128)(2,1)S(1)} collective-permute-done((bf16[32,2176]{1,0:T(8,128)(2,1)S(1)}, bf16[32,2176]{1,0:T(8,128)(2,1)S(1)}, u32[]{:S(2)}, u32[]{:S(2)}) %collective-permute-start.2) | collective-permute-done | bytes 139296 | tf_op jit(solution)/shard_map/ppermute | solution.py:55
  42.3 4.4 %collective-permute-start.7 = (bf16[32,2176]{1,0:T(8,128)(2,1)S(1)}, bf16[32,2176]{1,0:T(8,128)(2,1)S(1)}, u32[]{:S(2)}, u32[]{:S(2)}) collective-permute-start(bf16[32,2176]{1,0:T(8,128)(2,1)S(1)} %shard_map.182.refs_4_), channel_id=1, source_target_pairs={{0,416},{32,448},{64,480},{96,0},{128,32},{160,64},{192,96},{224,1... | collective-permute-start | bytes 417800 | tf_op jit(solution)/shard_map/ppermute | solution.py:55
  46.7 2.2 %collective-permute-done.4.refs_3_ = bf16[32,2176]{1,0:T(8,128)(2,1)S(1)} collective-permute-done((bf16[32,2176]{1,0:T(8,128)(2,1)S(1)}, bf16[32,2176]{1,0:T(8,128)(2,1)S(1)}, u32[]{:S(2)}, u32[]{:S(2)}) %collective-permute-start.4) | collective-permute-done | bytes 139296 | tf_op jit(solution)/shard_map/ppermute | solution.py:55
  49.0 7.5 %collective-permute-done.7.refs_7_ = bf16[32,2176]{1,0:T(8,128)(2,1)S(1)} collective-permute-done((bf16[32,2176]{1,0:T(8,128)(2,1)S(1)}, bf16[32,2176]{1,0:T(8,128)(2,1)S(1)}, u32[]{:S(2)}, u32[]{:S(2)}) %collective-permute-start.7) | collective-permute-done | bytes 139296 | tf_op jit(solution)/shard_map/ppermute | solution.py:55
  56.7 1.4 copy-done
  58.9 4.3 %all-to-all-start.1 = ((bf16[4,8,32,1152]{3,2,1,0:T(8,128)(2,1)}), bf16[4,8,32,1152]{3,2,1,0:T(8,128)(2,1)S(1)}, u32[]{:S(2)}, u32[]{:S(2)}) async-start(bf16[4,8,32,1152]{3,2,1,0:T(8,128)(2,1)} %copy-done), calls=%async_computation.1 | async-start | bytes 4718592 | tf_op jit(solution)/shard_map/all_to_all | solution.py:370
  63.2 3.3 %collective-permute-start = (bf16[512,1024]{1,0:T(8,128)(2,1)S(1)}, bf16[512,1024]{1,0:T(8,128)(2,1)}, u32[]{:S(2)}, u32[]{:S(2)}) collective-permute-start(bf16[512,1024]{1,0:T(8,128)(2,1)S(1)} %bitcast.20), channel_id=1, source_target_pairs={{0,1},{1,0},{2,3},{3,2},{4,5},{5,4},{6,7},{7,6},{8,9},{9,8},{10,11... | collective-permute-start | bytes 3145736 | tf_op jit(solution)/shard_map/ppermute | solution.py:59
  66.5 3.7 %collective-permute-start.8 = (bf16[8,32,1024]{2,1,0:T(8,128)(2,1)}, bf16[8,32,1024]{2,1,0:T(8,128)(2,1)}, u32[]{:S(2)}, u32[]{:S(2)}) collective-permute-start(bf16[8,32,1024]{2,1,0:T(8,128)(2,1)} %copy-done.19), channel_id=1, source_target_pairs={{0,8},{8,16},{16,24},{24,0},{1,9},{9,17},{17,25},{25,1},{2,10},{10... | collective-permute-start | bytes 1572872 | tf_op jit(solution)/shard_map/ppermute | solution.py:55
  70.1 4.3 %collective-permute-start.9 = (bf16[8,32,1024]{2,1,0:T(8,128)(2,1)}, bf16[8,32,1024]{2,1,0:T(8,128)(2,1)}, u32[]{:S(2)}, u32[]{:S(2)}) collective-permute-start(bf16[8,32,1024]{2,1,0:T(8,128)(2,1)} %copy-done.19), channel_id=1, source_target_pairs={{0,16},{8,24},{16,0},{24,8},{1,17},{9,25},{17,1},{25,9},{2,18},{10... | collective-permute-start | bytes 1572872 | tf_op jit(solution)/shard_map/ppermute | solution.py:55
  74.5 3.1 %collective-permute-start.10 = (bf16[8,32,1024]{2,1,0:T(8,128)(2,1)}, bf16[8,32,1024]{2,1,0:T(8,128)(2,1)}, u32[]{:S(2)}, u32[]{:S(2)}) collective-permute-start(bf16[8,32,1024]{2,1,0:T(8,128)(2,1)} %copy-done.19), channel_id=1, source_target_pairs={{0,24},{8,0},{16,8},{24,16},{1,25},{9,1},{17,9},{25,17},{2,26},{10... | collective-permute-start | bytes 1572872 | tf_op jit(solution)/shard_map/ppermute | solution.py:55
  77.6 13.6 %all-to-all-done.1.mine = bf16[4,8,32,1152]{3,2,1,0:T(8,128)(2,1)S(1)} async-done(((bf16[4,8,32,1152]{3,2,1,0:T(8,128)(2,1)}), bf16[4,8,32,1152]{3,2,1,0:T(8,128)(2,1)S(1)}, u32[]{:S(2)}, u32[]{:S(2)}) %all-to-all-start.1) | async-done | bytes 2359328 | tf_op jit(solution)/shard_map/all_to_all | solution.py:370
  91.1 5.9 %collective-permute-start.20 = (bf16[4,8,32,1152]{3,2,1,0:T(8,128)(2,1)S(1)}, bf16[4,8,32,1152]{3,2,1,0:T(8,128)(2,1)}, u32[]{:S(2)}, u32[]{:S(2)}) collective-permute-start(bf16[4,8,32,1152]{3,2,1,0:T(8,128)(2,1)S(1)} %all-to-all-done.1.mine), channel_id=1, source_target_pairs={{0,1},{1,0},{2,3},{3,2},{4,5},{5,4},{6,7},{7,6},{8,9},{9,8},{10,11... | collective-permute-start | bytes 7077896 | tf_op jit(solution)/shard_map/ppermute | solution.py:59
  97.1 5.1 %collective-permute-done.8 = bf16[8,32,1024]{2,1,0:T(8,128)(2,1)} collective-permute-done((bf16[8,32,1024]{2,1,0:T(8,128)(2,1)}, bf16[8,32,1024]{2,1,0:T(8,128)(2,1)}, u32[]{:S(2)}, u32[]{:S(2)}) %collective-permute-start.8) | collective-permute-done | bytes 524320 | tf_op jit(solution)/shard_map/ppermute | solution.py:55
  102.1 11.6 %collective-permute-done.9 = bf16[8,32,1024]{2,1,0:T(8,128)(2,1)} collective-permute-done((bf16[8,32,1024]{2,1,0:T(8,128)(2,1)}, bf16[8,32,1024]{2,1,0:T(8,128)(2,1)}, u32[]{:S(2)}, u32[]{:S(2)}) %collective-permute-start.9) | collective-permute-done | bytes 524320 | tf_op jit(solution)/shard_map/ppermute | solution.py:55
  114.8 5.9 %shard_map.184 = (bf16[512,256]{1,0:T(8,128)(2,1)S(1)}, bf16[512,256]{1,0:T(8,128)(2,1)}, bf16[1024,256]{1,0:T(8,128)(2,1)}) custom-call(s32[1]{0:T(128)} %bitcast.2.y_ref, s32[1]{0:T(128)} %bitcast.1.core_ref, f32[2]{0:T(128)S(1)} %bitcast.29, bf16[512,1024]{1,0:T(8,128)(2,1)S(1)} %bitcast.21, bf16[512,1024]{1,0:T(8,128)(2,1)} %collective-permute-done.other, ...), custom_call_target="tpu_custom_call" | custom-call | flops 4294967296 | bytes 2097152 | tf_op jit(solution)/shard_map/pallas_call | solution.py:37
  121.4 4.2 %collective-permute-start.12 = (bf16[1024,256]{1,0:T(8,128)(2,1)}, bf16[1024,256]{1,0:T(8,128)(2,1)S(1)}, u32[]{:S(2)}, u32[]{:S(2)}) collective-permute-start(bf16[1024,256]{1,0:T(8,128)(2,1)} %get-tuple-element.23.my_weights), channel_id=1, source_target_pairs={{0,1},{1,0},{2,3},{3,2},{4,5},{5,4},{6,7},{7,6},{8,9},{9,8},{10,11... | collective-permute-start | bytes 1572872 | tf_op jit(solution)/shard_map/ppermute | solution.py:59
  125.7 1.9 collective-permute-start.11
  127.6 1.7 collective-permute-done.11.theirs
  130.1 1.0 copy-done.22
  132.1 1.8 shard_map.185
  134.0 3.7 %collective-permute-start.13 = (bf16[128,1024]{1,0:T(8,128)(2,1)S(1)}, bf16[128,1024]{1,0:T(8,128)(2,1)S(1)}, u32[]{:S(2)}, u32[]{:S(2)}) collective-permute-start(bf16[128,1024]{1,0:T(8,128)(2,1)S(1)} %get-tuple-element.24), channel_id=1, source_target_pairs={{0,4},{2,6},{4,0},{6,2},{1,5},{3,7},{5,1},{7,3},{8,12},{10,14},{12... | collective-permute-start | bytes 786440 | tf_op jit(solution)/shard_map/ppermute | solution.py:55
  137.7 1.9 collective-permute-start.14
  139.6 3.4 %collective-permute-start.15 = (bf16[128,1024]{1,0:T(8,128)(2,1)S(1)}, bf16[128,1024]{1,0:T(8,128)(2,1)S(1)}, u32[]{:S(2)}, u32[]{:S(2)}) collective-permute-start(bf16[128,1024]{1,0:T(8,128)(2,1)S(1)} %get-tuple-element.26), channel_id=1, source_target_pairs={{0,6},{2,0},{4,2},{6,4},{1,7},{3,1},{5,3},{7,5},{8,14},{10,8},{12,... | collective-permute-start | bytes 786440 | tf_op jit(solution)/shard_map/ppermute | solution.py:55
  143.0 2.1 %collective-permute-done.13.far = bf16[128,1024]{1,0:T(8,128)(2,1)S(1)} collective-permute-done((bf16[128,1024]{1,0:T(8,128)(2,1)S(1)}, bf16[128,1024]{1,0:T(8,128)(2,1)S(1)}, u32[]{:S(2)}, u32[]{:S(2)}) %collective-permute-start.13) | collective-permute-done | bytes 262176 | tf_op jit(solution)/shard_map/ppermute | solution.py:55
  145.1 5.7 %collective-permute-done.14.right = bf16[128,1024]{1,0:T(8,128)(2,1)S(1)} collective-permute-done((bf16[128,1024]{1,0:T(8,128)(2,1)S(1)}, bf16[128,1024]{1,0:T(8,128)(2,1)S(1)}, u32[]{:S(2)}, u32[]{:S(2)}) %collective-permute-start.14) | collective-permute-done | bytes 262176 | tf_op jit(solution)/shard_map/ppermute | solution.py:55
  151.6 3.1 %collective-permute-start.18 = (bf16[128,1024]{1,0:T(8,128)(2,1)S(1)}, bf16[128,1024]{1,0:T(8,128)(2,1)S(1)}, u32[]{:S(2)}, u32[]{:S(2)}) collective-permute-start(bf16[128,1024]{1,0:T(8,128)(2,1)S(1)} %get-tuple-element.28.own), channel_id=1, source_target_pairs={{0,2},{2,4},{4,6},{6,0},{1,3},{3,5},{5,7},{7,1},{8,10},{10,12},{12... | collective-permute-start | bytes 786440 | tf_op jit(solution)/shard_map/ppermute | solution.py:55
  154.8 2.2 %collective-permute-start.17 = (bf16[128,1024]{1,0:T(8,128)(2,1)S(1)}, bf16[128,1024]{1,0:T(8,128)(2,1)S(1)}, u32[]{:S(2)}, u32[]{:S(2)}) collective-permute-start(bf16[128,1024]{1,0:T(8,128)(2,1)S(1)} %get-tuple-element.28.own), channel_id=1, source_target_pairs={{0,6},{2,0},{4,2},{6,4},{1,7},{3,1},{5,3},{7,5},{8,14},{10,8},{12,... | collective-permute-start | bytes 786440 | tf_op jit(solution)/shard_map/ppermute | solution.py:55
  156.9 3.5 %collective-permute-start.16 = (bf16[128,1024]{1,0:T(8,128)(2,1)S(1)}, bf16[128,1024]{1,0:T(8,128)(2,1)S(1)}, u32[]{:S(2)}, u32[]{:S(2)}) collective-permute-start(bf16[128,1024]{1,0:T(8,128)(2,1)S(1)} %get-tuple-element.28.own), channel_id=1, source_target_pairs={{0,4},{2,6},{4,0},{6,2},{1,5},{3,7},{5,1},{7,3},{8,12},{10,14},{12... | collective-permute-start | bytes 786440 | tf_op jit(solution)/shard_map/ppermute | solution.py:55
  160.9 3.6 %collective-permute-done.17.got_next = bf16[128,1024]{1,0:T(8,128)(2,1)S(1)} collective-permute-done((bf16[128,1024]{1,0:T(8,128)(2,1)S(1)}, bf16[128,1024]{1,0:T(8,128)(2,1)S(1)}, u32[]{:S(2)}, u32[]{:S(2)}) %collective-permute-start.17) | collective-permute-done | bytes 262176 | tf_op jit(solution)/shard_map/ppermute | solution.py:55
  165.1 3.5 %collective-permute-done.16.got_far = bf16[128,1024]{1,0:T(8,128)(2,1)S(1)} collective-permute-done((bf16[128,1024]{1,0:T(8,128)(2,1)S(1)}, bf16[128,1024]{1,0:T(8,128)(2,1)S(1)}, u32[]{:S(2)}, u32[]{:S(2)}) %collective-permute-start.16) | collective-permute-done | bytes 262176 | tf_op jit(solution)/shard_map/ppermute | solution.py:55
  169.5 4.6 %collective-permute-start.19 = (bf16[8,1024]{1,0:T(8,128)(2,1)S(1)}, bf16[8,1024]{1,0:T(8,128)(2,1)S(1)}, u32[]{:S(2)}, u32[]{:S(2)}) collective-permute-start(bf16[8,1024]{1,0:T(8,128)(2,1)S(1)} %concatenate.3), channel_id=1, source_target_pairs={{0,1},{1,0},{2,3},{3,2},{4,5},{5,4},{6,7},{7,6},{8,9},{9,8},{10,11... | collective-permute-start | bytes 49160 | tf_op jit(solution)/shard_map/ppermute | solution.py:59
  174.2 1.9 collective-permute-start.21
  176.1 1.1 collective-permute-done.21.their_taps
  179.1 6.0 %shard_map.188 = (bf16[128,1024]{1,0:T(8,128)(2,1)S(1)}, bf16[128,1024]{1,0:T(8,128)(2,1)S(1)}, bf16[128,1024]{1,0:T(8,128)(2,1)S(1)}, bf16[128,1024]{1,0:T(8,128)(2,1)S(1)}) custom-call(s32[1]{0:T(128)} %bitcast.x_ref, s32[1]{0:T(128)} %bitcast.1.core_ref, bf16[128,1024]{1,0:T(8,128)(2,1)S(1)} %copy-done.18, bf16[128,1024]{1,0:T(8,128)(2,1)S(1)} %copy-done.16, ...), custom_call_target="tpu_custom_call" | custom-call | flops 4294967296 | bytes 2097152 | tf_op jit(solution)/shard_map/pallas_call | solution.py:37
  185.1 3.3 %collective-permute-start.22 = (bf16[128,1024]{1,0:T(8,128)(2,1)S(1)}, bf16[128,1024]{1,0:T(8,128)(2,1)S(1)}, u32[]{:S(2)}, u32[]{:S(2)}) collective-permute-start(bf16[128,1024]{1,0:T(8,128)(2,1)S(1)} %get-tuple-element.30), channel_id=1, source_target_pairs={{0,4},{2,6},{4,0},{6,2},{1,5},{3,7},{5,1},{7,3},{8,12},{10,14},{12... | collective-permute-start | bytes 786440 | tf_op jit(solution)/shard_map/ppermute | solution.py:55
  188.5 1.9 collective-permute-start.23
  190.4 3.4 %collective-permute-start.24 = (bf16[128,1024]{1,0:T(8,128)(2,1)S(1)}, bf16[128,1024]{1,0:T(8,128)(2,1)S(1)}, u32[]{:S(2)}, u32[]{:S(2)}) collective-permute-start(bf16[128,1024]{1,0:T(8,128)(2,1)S(1)} %get-tuple-element.32), channel_id=1, source_target_pairs={{0,6},{2,0},{4,2},{6,4},{1,7},{3,1},{5,3},{7,5},{8,14},{10,8},{12,... | collective-permute-start | bytes 786440 | tf_op jit(solution)/shard_map/ppermute | solution.py:55
  193.8 2.5 %collective-permute-done.22.far = bf16[128,1024]{1,0:T(8,128)(2,1)S(1)} collective-permute-done((bf16[128,1024]{1,0:T(8,128)(2,1)S(1)}, bf16[128,1024]{1,0:T(8,128)(2,1)S(1)}, u32[]{:S(2)}, u32[]{:S(2)}) %collective-permute-start.22) | collective-permute-done | bytes 262176 | tf_op jit(solution)/shard_map/ppermute | solution.py:55
  196.2 3.4 %collective-permute-done.23.right = bf16[128,1024]{1,0:T(8,128)(2,1)S(1)} collective-permute-done((bf16[128,1024]{1,0:T(8,128)(2,1)S(1)}, bf16[128,1024]{1,0:T(8,128)(2,1)S(1)}, u32[]{:S(2)}, u32[]{:S(2)}) %collective-permute-start.23) | collective-permute-done | bytes 262176 | tf_op jit(solution)/shard_map/ppermute | solution.py:55
  199.6 2.8 %collective-permute-done.24.left = bf16[128,1024]{1,0:T(8,128)(2,1)S(1)} collective-permute-done((bf16[128,1024]{1,0:T(8,128)(2,1)S(1)}, bf16[128,1024]{1,0:T(8,128)(2,1)S(1)}, u32[]{:S(2)}, u32[]{:S(2)}) %collective-permute-start.24) | collective-permute-done | bytes 262176 | tf_op jit(solution)/shard_map/ppermute | solution.py:55
  (84 shorter events, 11.9 us)
Async XLA Ops:
  1.6 5.5 %copy-start.3 = (bf16[32,352]{1,0:T(8,128)(2,1)S(1)}, bf16[32,352]{1,0:T(8,128)(2,1)}, u32[]{:S(2)}) copy-start(bf16[32,352]{1,0:T(8,128)(2,1)} %ge.1) | copy-start | bytes 67588
  1.6 5.5 %copy-start.4 = (bf16[32,352]{1,0:T(8,128)(2,1)S(1)}, bf16[32,352]{1,0:T(8,128)(2,1)}, u32[]{:S(2)}) copy-start(bf16[32,352]{1,0:T(8,128)(2,1)} %li.1) | copy-start | bytes 67588
  1.6 5.5 %copy-start.5 = (bf16[352,32]{0,1:T(8,128)(2,1)S(1)}, bf16[352,32]{0,1:T(8,128)(2,1)}, u32[]{:S(2)}) copy-start(bf16[352,32]{0,1:T(8,128)(2,1)} %param.35) | copy-start | bytes 67588
  1.6 5.5 %copy-start.6 = (bf16[32,256]{1,0:T(8,128)(2,1)S(1)}, bf16[32,256]{1,0:T(8,128)(2,1)}, u32[]{:S(2)}) copy-start(bf16[32,256]{1,0:T(8,128)(2,1)} %v.1) | copy-start | bytes 49156
  1.6 5.5 %copy-start.7 = (bf16[32,256]{1,0:T(8,128)(2,1)S(1)}, bf16[32,256]{1,0:T(8,128)(2,1)}, u32[]{:S(2)}) copy-start(bf16[32,256]{1,0:T(8,128)(2,1)} %g.1) | copy-start | bytes 49156
  1.7 5.5 %copy-start.8 = (bf16[256,32]{0,1:T(8,128)(2,1)S(1)}, bf16[256,32]{0,1:T(8,128)(2,1)}, u32[]{:S(2)}) copy-start(bf16[256,32]{0,1:T(8,128)(2,1)} %param.26) | copy-start | bytes 49156
  1.7 5.5 %copy-start.9 = (bf16[32,128]{1,0:T(8,128)(2,1)S(1)}, bf16[32,128]{1,0:T(8,128)(2,1)}, u32[]{:S(2)}) copy-start(bf16[32,128]{1,0:T(8,128)(2,1)} %q.1) | copy-start | bytes 24580
  1.7 5.5 %copy-start.10 = (bf16[32,128]{1,0:T(8,128)(2,1)S(1)}, bf16[32,128]{1,0:T(8,128)(2,1)}, u32[]{:S(2)}) copy-start(bf16[32,128]{1,0:T(8,128)(2,1)} %k.1) | copy-start | bytes 24580
  2.8 56.1 %all-to-all-start = ((bf16[4,128,1024]{2,1,0:T(8,128)(2,1)}), bf16[4,128,1024]{2,1,0:T(8,128)(2,1)S(1)}, u32[]{:S(2)}, u32[]{:S(2)}) async-start(bf16[4,128,1024]{2,1,0:T(8,128)(2,1)} %shard_map.181), calls=%async_computation | async-start | bytes 2097152 | tf_op jit(solution)/shard_map/all_to_all | solution.py:63
  7.2 26.8 %collective-permute-start.1 = (bf16[32,2176]{1,0:T(8,128)(2,1)S(1)}, bf16[32,2176]{1,0:T(8,128)(2,1)S(1)}, u32[]{:S(2)}, u32[]{:S(2)}) collective-permute-start(bf16[32,2176]{1,0:T(8,128)(2,1)S(1)} %shard_map.182.refs_4_), channel_id=1, source_target_pairs={{0,128},{32,160},{64,192},{96,224},{128,256},{160,288},{192,320},{... | collective-permute-start | bytes 417800 | tf_op jit(solution)/shard_map/ppermute | solution.py:55
  16.0 26.2 %collective-permute-start.2 = (bf16[32,2176]{1,0:T(8,128)(2,1)S(1)}, bf16[32,2176]{1,0:T(8,128)(2,1)S(1)}, u32[]{:S(2)}, u32[]{:S(2)}) collective-permute-start(bf16[32,2176]{1,0:T(8,128)(2,1)S(1)} %shard_map.182.refs_4_), channel_id=1, source_target_pairs={{0,96},{32,128},{64,160},{96,192},{128,224},{160,256},{192,288},{2... | collective-permute-start | bytes 417800 | tf_op jit(solution)/shard_map/ppermute | solution.py:55
  22.3 24.4 %collective-permute-start.3 = (bf16[32,2176]{1,0:T(8,128)(2,1)S(1)}, bf16[32,2176]{1,0:T(8,128)(2,1)S(1)}, u32[]{:S(2)}, u32[]{:S(2)}) collective-permute-start(bf16[32,2176]{1,0:T(8,128)(2,1)S(1)} %shard_map.182.refs_4_), channel_id=1, source_target_pairs={{0,64},{32,96},{64,128},{96,160},{128,192},{160,224},{192,256},{22... | collective-permute-start | bytes 417800 | tf_op jit(solution)/shard_map/ppermute | solution.py:55
  27.5 21.4 %collective-permute-start.4 = (bf16[32,2176]{1,0:T(8,128)(2,1)S(1)}, bf16[32,2176]{1,0:T(8,128)(2,1)S(1)}, u32[]{:S(2)}, u32[]{:S(2)}) collective-permute-start(bf16[32,2176]{1,0:T(8,128)(2,1)S(1)} %shard_map.182.refs_4_), channel_id=1, source_target_pairs={{0,32},{32,64},{64,96},{96,128},{128,160},{160,192},{192,224},{224... | collective-permute-start | bytes 417800 | tf_op jit(solution)/shard_map/ppermute | solution.py:55
  30.2 18.8 %collective-permute-start.5 = (bf16[32,2176]{1,0:T(8,128)(2,1)S(1)}, bf16[32,2176]{1,0:T(8,128)(2,1)S(1)}, u32[]{:S(2)}, u32[]{:S(2)}) collective-permute-start(bf16[32,2176]{1,0:T(8,128)(2,1)S(1)} %shard_map.182.refs_4_), channel_id=1, source_target_pairs={{0,480},{32,0},{64,32},{96,64},{128,96},{160,128},{192,160},{224,1... | collective-permute-start | bytes 417800 | tf_op jit(solution)/shard_map/ppermute | solution.py:55
  34.0 14.9 %collective-permute-start.6 = (bf16[32,2176]{1,0:T(8,128)(2,1)S(1)}, bf16[32,2176]{1,0:T(8,128)(2,1)S(1)}, u32[]{:S(2)}, u32[]{:S(2)}) collective-permute-start(bf16[32,2176]{1,0:T(8,128)(2,1)S(1)} %shard_map.182.refs_4_), channel_id=1, source_target_pairs={{0,448},{32,480},{64,0},{96,32},{128,64},{160,96},{192,128},{224,1... | collective-permute-start | bytes 417800 | tf_op jit(solution)/shard_map/ppermute | solution.py:55
  42.3 14.2 %collective-permute-start.7 = (bf16[32,2176]{1,0:T(8,128)(2,1)S(1)}, bf16[32,2176]{1,0:T(8,128)(2,1)S(1)}, u32[]{:S(2)}, u32[]{:S(2)}) collective-permute-start(bf16[32,2176]{1,0:T(8,128)(2,1)S(1)} %shard_map.182.refs_4_), channel_id=1, source_target_pairs={{0,416},{32,448},{64,480},{96,0},{128,32},{160,64},{192,96},{224,1... | collective-permute-start | bytes 417800 | tf_op jit(solution)/shard_map/ppermute | solution.py:55
  56.7 1.4 copy-start
  58.9 54.8 %copy-start.25 = (f32[2,1]{0,1:T(1,128)S(1)}, f32[2,1]{0,1:T(1,128)}, u32[]{:S(2)}) copy-start(f32[2,1]{0,1:T(1,128)} %param.25) | copy-start | bytes 28
  58.9 54.8 %copy-start.26 = (f32[1,128]{1,0:T(1,128)S(1)}, f32[1,128]{1,0:T(1,128)}, u32[]{:S(2)}) copy-start(f32[1,128]{1,0:T(1,128)} %constant.18.clone.frequency) | copy-start | bytes 1540
  58.9 32.2 %all-to-all-start.1 = ((bf16[4,8,32,1152]{3,2,1,0:T(8,128)(2,1)}), bf16[4,8,32,1152]{3,2,1,0:T(8,128)(2,1)S(1)}, u32[]{:S(2)}, u32[]{:S(2)}) async-start(bf16[4,8,32,1152]{3,2,1,0:T(8,128)(2,1)} %copy-done), calls=%async_computation.1 | async-start | bytes 4718592 | tf_op jit(solution)/shard_map/all_to_all | solution.py:370
  63.2 50.5 %collective-permute-start = (bf16[512,1024]{1,0:T(8,128)(2,1)S(1)}, bf16[512,1024]{1,0:T(8,128)(2,1)}, u32[]{:S(2)}, u32[]{:S(2)}) collective-permute-start(bf16[512,1024]{1,0:T(8,128)(2,1)S(1)} %bitcast.20), channel_id=1, source_target_pairs={{0,1},{1,0},{2,3},{3,2},{4,5},{5,4},{6,7},{7,6},{8,9},{9,8},{10,11... | collective-permute-start | bytes 3145736 | tf_op jit(solution)/shard_map/ppermute | solution.py:59
  66.5 35.7 %collective-permute-start.8 = (bf16[8,32,1024]{2,1,0:T(8,128)(2,1)}, bf16[8,32,1024]{2,1,0:T(8,128)(2,1)}, u32[]{:S(2)}, u32[]{:S(2)}) collective-permute-start(bf16[8,32,1024]{2,1,0:T(8,128)(2,1)} %copy-done.19), channel_id=1, source_target_pairs={{0,8},{8,16},{16,24},{24,0},{1,9},{9,17},{17,25},{25,1},{2,10},{10... | collective-permute-start | bytes 1572872 | tf_op jit(solution)/shard_map/ppermute | solution.py:55
  70.1 43.6 %collective-permute-start.9 = (bf16[8,32,1024]{2,1,0:T(8,128)(2,1)}, bf16[8,32,1024]{2,1,0:T(8,128)(2,1)}, u32[]{:S(2)}, u32[]{:S(2)}) collective-permute-start(bf16[8,32,1024]{2,1,0:T(8,128)(2,1)} %copy-done.19), channel_id=1, source_target_pairs={{0,16},{8,24},{16,0},{24,8},{1,17},{9,25},{17,1},{25,9},{2,18},{10... | collective-permute-start | bytes 1572872 | tf_op jit(solution)/shard_map/ppermute | solution.py:55
  74.5 39.3 %collective-permute-start.10 = (bf16[8,32,1024]{2,1,0:T(8,128)(2,1)}, bf16[8,32,1024]{2,1,0:T(8,128)(2,1)}, u32[]{:S(2)}, u32[]{:S(2)}) collective-permute-start(bf16[8,32,1024]{2,1,0:T(8,128)(2,1)} %copy-done.19), channel_id=1, source_target_pairs={{0,24},{8,0},{16,8},{24,16},{1,25},{9,1},{17,9},{25,17},{2,26},{10... | collective-permute-start | bytes 1572872 | tf_op jit(solution)/shard_map/ppermute | solution.py:55
  91.1 86.1 %collective-permute-start.20 = (bf16[4,8,32,1152]{3,2,1,0:T(8,128)(2,1)S(1)}, bf16[4,8,32,1152]{3,2,1,0:T(8,128)(2,1)}, u32[]{:S(2)}, u32[]{:S(2)}) collective-permute-start(bf16[4,8,32,1152]{3,2,1,0:T(8,128)(2,1)S(1)} %all-to-all-done.1.mine), channel_id=1, source_target_pairs={{0,1},{1,0},{2,3},{3,2},{4,5},{5,4},{6,7},{7,6},{8,9},{9,8},{10,11... | collective-permute-start | bytes 7077896 | tf_op jit(solution)/shard_map/ppermute | solution.py:59
  113.7 1.0 copy-start.20
  121.4 29.8 %copy-start.2 = (bf16[1,128,1024]{2,1,0:T(8,128)(2,1)S(1)}, bf16[1,128,1024]{2,1,0:T(8,128)(2,1)}, u32[]{:S(2)}) copy-start(bf16[1,128,1024]{2,1,0:T(8,128)(2,1)} %param.19) | copy-start | bytes 786436
  121.4 29.8 %copy-start.12 = (f32[1024]{0:T(1024)S(1)}, f32[1024]{0:T(1024)}, u32[]{:S(2)}) copy-start(f32[1024]{0:T(1024)} %param.27) | copy-start | bytes 12292
  121.4 29.8 %copy-start.13 = (f32[1024]{0:T(1024)S(1)}, f32[1024]{0:T(1024)}, u32[]{:S(2)}) copy-start(f32[1024]{0:T(1024)} %param.28) | copy-start | bytes 12292
  121.4 7.9 %collective-permute-start.12 = (bf16[1024,256]{1,0:T(8,128)(2,1)}, bf16[1024,256]{1,0:T(8,128)(2,1)S(1)}, u32[]{:S(2)}, u32[]{:S(2)}) collective-permute-start(bf16[1024,256]{1,0:T(8,128)(2,1)} %get-tuple-element.23.my_weights), channel_id=1, source_target_pairs={{0,1},{1,0},{2,3},{3,2},{4,5},{5,4},{6,7},{7,6},{8,9},{9,8},{10,11... | collective-permute-start | bytes 1572872 | tf_op jit(solution)/shard_map/ppermute | solution.py:59
  125.7 3.6 %collective-permute-start.11 = (bf16[512,256]{1,0:T(8,128)(2,1)}, bf16[512,256]{1,0:T(8,128)(2,1)S(1)}, u32[]{:S(2)}, u32[]{:S(2)}) collective-permute-start(bf16[512,256]{1,0:T(8,128)(2,1)} %get-tuple-element.22), channel_id=1, source_target_pairs={{0,1},{1,0},{2,3},{3,2},{4,5},{5,4},{6,7},{7,6},{8,9},{9,8},{10,11... | collective-permute-start | bytes 786440 | tf_op jit(solution)/shard_map/ppermute | solution.py:59
  130.1 1.0 copy-start.22
  132.1 42.0 %copy-start.29 = (f32[352]{0:T(512)S(1)}, f32[352]{0:T(512)}, u32[]{:S(2)}) copy-start(f32[352]{0:T(512)} %param.33) | copy-start | bytes 4228
  132.1 42.0 %copy-start.30 = (f32[352]{0:T(512)S(1)}, f32[352]{0:T(512)}, u32[]{:S(2)}) copy-start(f32[352]{0:T(512)} %param.34) | copy-start | bytes 4228
  132.1 42.0 %copy-start.23 = (f32[3,352]{1,0:T(4,128)S(1)}, f32[3,352]{1,0:T(4,128)}, u32[]{:S(2)}) copy-start(f32[3,352]{1,0:T(4,128)} %ge_kernel.1) | copy-start | bytes 12676
  132.1 42.0 %copy-start.24 = (f32[3,352]{1,0:T(4,128)S(1)}, f32[3,352]{1,0:T(4,128)}, u32[]{:S(2)}) copy-start(f32[3,352]{1,0:T(4,128)} %li_kernel.1) | copy-start | bytes 12676
  134.0 11.1 %collective-permute-start.13 = (bf16[128,1024]{1,0:T(8,128)(2,1)S(1)}, bf16[128,1024]{1,0:T(8,128)(2,1)S(1)}, u32[]{:S(2)}, u32[]{:S(2)}) collective-permute-start(bf16[128,1024]{1,0:T(8,128)(2,1)S(1)} %get-tuple-element.24), channel_id=1, source_target_pairs={{0,4},{2,6},{4,0},{6,2},{1,5},{3,7},{5,1},{7,3},{8,12},{10,14},{12... | collective-permute-start | bytes 786440 | tf_op jit(solution)/shard_map/ppermute | solution.py:55
  137.7 13.1 %collective-permute-start.14 = (bf16[128,1024]{1,0:T(8,128)(2,1)S(1)}, bf16[128,1024]{1,0:T(8,128)(2,1)S(1)}, u32[]{:S(2)}, u32[]{:S(2)}) collective-permute-start(bf16[128,1024]{1,0:T(8,128)(2,1)S(1)} %get-tuple-element.25), channel_id=1, source_target_pairs={{0,2},{2,4},{4,6},{6,0},{1,3},{3,5},{5,7},{7,1},{8,10},{10,12},{12... | collective-permute-start | bytes 786440 | tf_op jit(solution)/shard_map/ppermute | solution.py:55
  139.6 11.6 %collective-permute-start.15 = (bf16[128,1024]{1,0:T(8,128)(2,1)S(1)}, bf16[128,1024]{1,0:T(8,128)(2,1)S(1)}, u32[]{:S(2)}, u32[]{:S(2)}) collective-permute-start(bf16[128,1024]{1,0:T(8,128)(2,1)S(1)} %get-tuple-element.26), channel_id=1, source_target_pairs={{0,6},{2,0},{4,2},{6,4},{1,7},{3,1},{5,3},{7,5},{8,14},{10,8},{12,... | collective-permute-start | bytes 786440 | tf_op jit(solution)/shard_map/ppermute | solution.py:55
  151.6 9.2 %collective-permute-start.18 = (bf16[128,1024]{1,0:T(8,128)(2,1)S(1)}, bf16[128,1024]{1,0:T(8,128)(2,1)S(1)}, u32[]{:S(2)}, u32[]{:S(2)}) collective-permute-start(bf16[128,1024]{1,0:T(8,128)(2,1)S(1)} %get-tuple-element.28.own), channel_id=1, source_target_pairs={{0,2},{2,4},{4,6},{6,0},{1,3},{3,5},{5,7},{7,1},{8,10},{10,12},{12... | collective-permute-start | bytes 786440 | tf_op jit(solution)/shard_map/ppermute | solution.py:55
  154.8 9.7 %collective-permute-start.17 = (bf16[128,1024]{1,0:T(8,128)(2,1)S(1)}, bf16[128,1024]{1,0:T(8,128)(2,1)S(1)}, u32[]{:S(2)}, u32[]{:S(2)}) collective-permute-start(bf16[128,1024]{1,0:T(8,128)(2,1)S(1)} %get-tuple-element.28.own), channel_id=1, source_target_pairs={{0,6},{2,0},{4,2},{6,4},{1,7},{3,1},{5,3},{7,5},{8,14},{10,8},{12,... | collective-permute-start | bytes 786440 | tf_op jit(solution)/shard_map/ppermute | solution.py:55
  156.9 11.8 %collective-permute-start.16 = (bf16[128,1024]{1,0:T(8,128)(2,1)S(1)}, bf16[128,1024]{1,0:T(8,128)(2,1)S(1)}, u32[]{:S(2)}, u32[]{:S(2)}) collective-permute-start(bf16[128,1024]{1,0:T(8,128)(2,1)S(1)} %get-tuple-element.28.own), channel_id=1, source_target_pairs={{0,4},{2,6},{4,0},{6,2},{1,5},{3,7},{5,1},{7,3},{8,12},{10,14},{12... | collective-permute-start | bytes 786440 | tf_op jit(solution)/shard_map/ppermute | solution.py:55
  169.5 7.8 %collective-permute-start.19 = (bf16[8,1024]{1,0:T(8,128)(2,1)S(1)}, bf16[8,1024]{1,0:T(8,128)(2,1)S(1)}, u32[]{:S(2)}, u32[]{:S(2)}) collective-permute-start(bf16[8,1024]{1,0:T(8,128)(2,1)S(1)} %concatenate.3), channel_id=1, source_target_pairs={{0,1},{1,0},{2,3},{3,2},{4,5},{5,4},{6,7},{7,6},{8,9},{9,8},{10,11... | collective-permute-start | bytes 49160 | tf_op jit(solution)/shard_map/ppermute | solution.py:59
  174.1 28.3 %copy-start.14 = (f32[1024]{0:T(1024)S(1)}, f32[1024]{0:T(1024)}, u32[]{:S(2)}) copy-start(f32[1024]{0:T(1024)} %param.36) | copy-start | bytes 12292
  174.2 3.1 %collective-permute-start.21 = (f32[8,384]{1,0:T(8,128)S(1)}, f32[8,384]{1,0:T(8,128)S(1)}, u32[]{:S(2)}, u32[]{:S(2)}) collective-permute-start(f32[8,384]{1,0:T(8,128)S(1)} %shard_map.187.my_taps), channel_id=1, source_target_pairs={{0,1},{1,0},{2,3},{3,2},{4,5},{5,4},{6,7},{7,6},{8,9},{9,8},{10,11... | collective-permute-start | bytes 36872 | tf_op jit(solution)/shard_map/ppermute | solution.py:59
  185.1 11.1 %collective-permute-start.22 = (bf16[128,1024]{1,0:T(8,128)(2,1)S(1)}, bf16[128,1024]{1,0:T(8,128)(2,1)S(1)}, u32[]{:S(2)}, u32[]{:S(2)}) collective-permute-start(bf16[128,1024]{1,0:T(8,128)(2,1)S(1)} %get-tuple-element.30), channel_id=1, source_target_pairs={{0,4},{2,6},{4,0},{6,2},{1,5},{3,7},{5,1},{7,3},{8,12},{10,14},{12... | collective-permute-start | bytes 786440 | tf_op jit(solution)/shard_map/ppermute | solution.py:55
  188.5 11.1 %collective-permute-start.23 = (bf16[128,1024]{1,0:T(8,128)(2,1)S(1)}, bf16[128,1024]{1,0:T(8,128)(2,1)S(1)}, u32[]{:S(2)}, u32[]{:S(2)}) collective-permute-start(bf16[128,1024]{1,0:T(8,128)(2,1)S(1)} %get-tuple-element.31), channel_id=1, source_target_pairs={{0,2},{2,4},{4,6},{6,0},{1,3},{3,5},{5,7},{7,1},{8,10},{10,12},{12... | collective-permute-start | bytes 786440 | tf_op jit(solution)/shard_map/ppermute | solution.py:55
  190.4 12.0 %collective-permute-start.24 = (bf16[128,1024]{1,0:T(8,128)(2,1)S(1)}, bf16[128,1024]{1,0:T(8,128)(2,1)S(1)}, u32[]{:S(2)}, u32[]{:S(2)}) collective-permute-start(bf16[128,1024]{1,0:T(8,128)(2,1)S(1)} %get-tuple-element.32), channel_id=1, source_target_pairs={{0,6},{2,0},{4,2},{6,4},{1,7},{3,1},{5,3},{7,5},{8,14},{10,8},{12,... | collective-permute-start | bytes 786440 | tf_op jit(solution)/shard_map/ppermute | solution.py:55
  (10 other events, 8.2 us)

commit v6 on v5

--- a/solution.py
+++ b/solution.py
@@ -29,11 +29,16 @@
 
 VMEM = pl.BlockSpec(memory_space=pltpu.VMEM)
 SMEM = pl.BlockSpec(memory_space=pltpu.SMEM)
-
-
-def call(body, out_shapes, *args, flops=0, smem=0, scratch=(), limit=6):
-    specs = [SMEM] * smem + [VMEM] * (len(args) - smem)
+HBM = pl.BlockSpec(memory_space=pltpu.HBM)
+
+
+def call(body, out_shapes, *args, flops=0, smem=0, hbm=0, scratch=(), limit=6):
+    specs = [SMEM] * smem + [HBM] * hbm + [VMEM] * (len(args) - smem - hbm)
     single = not isinstance(out_shapes, (list, tuple))
+    args = [
+        pltpu.with_memory_space_constraint(a, pltpu.HBM) if smem <= k < smem + hbm else a
+        for k, a in enumerate(args)
+    ]
     return pl.pallas_call(
         body,
         out_shape=out_shapes,
@@ -67,24 +72,32 @@
     return values * lax.rsqrt(jnp.mean(values * values, axis=-1, keepdims=True) + epsilon) * gain
 
 
-def pack_body(width, q, k, v, g, mo, ge, li, dn, out):
-    out[:, :DK] = q[...]
-    out[:, DK : 2 * DK] = k[...]
-    out[:, 2 * DK : 2 * DK + DV] = v[...]
-    out[:, 2 * DK + DV : PROJECT] = g[...]
-    out[:, PROJECT:FIRST] = mo[...]
+def pack_body(width, *refs):
+    sources, out, places, arrived = refs[:8], refs[8], refs[9:17], refs[17]
+    copies = [
+        pltpu.make_async_copy(source, place, arrived.at[k])
+        for k, (source, place) in enumerate(zip(sources, places))
+    ]
+    for copy in copies:
+        copy.start()
+    for copy in copies:
+        copy.wait()
+    at = 0
+    for place in places[:5]:
+        out[:, at : at + place.shape[1]] = place[...]
+        at += place.shape[1]
     gap = jnp.zeros((out.shape[0], PAD - width), bf16)
-    for place, piece in enumerate((ge, li, dn)):
-        at = FIRST + place * PAD
-        out[:, at : at + PAD] = jnp.concatenate([piece[...], gap], axis=1)
+    for place in places[5:]:
+        out[:, at : at + PAD] = jnp.concatenate([place[...], gap], axis=1)
+        at += PAD
 
 
 def taps_body(width, ge_kernel, li_kernel, ge_bias, li_bias, out):
     out[...] = jnp.zeros(out.shape, f32)
     out[0:3, :width] = ge_kernel[...]
     out[3:6, :width] = li_kernel[...]
-    out[6:7, :width] = ge_bias[...]
-    out[7:8, :width] = li_bias[...]
+    out[6:7, :width] = ge_bias[...].reshape(1, width)
+    out[7:8, :width] = li_bias[...].reshape(1, width)
 
 
 def first_norm_body(tokens, gain, out):
@@ -96,10 +109,22 @@
 def ring_order_body(index, *refs):
     pieces, (one, three) = refs[:8], refs[8:]
     for shift, piece in zip(Z_SHIFTS, pieces):
-        at = lax.rem(index[0] - shift + 8, 8)
+        at = lax.rem(index[2] - shift + 8, 8)
         one[at] = piece[:, :FIRST]
-        for y in range(three.shape[0]):
-            three[y, at] = piece[:, FIRST:]
+        three[at] = piece[:, FIRST:]
+
+
+def line_order_body(index, *refs):
+    pieces, out = refs[:4], refs[4]
+    for shift, piece in zip(Y_SHIFTS, pieces):
+        at = lax.rem(index[1] - shift + 4, 4)
+        for z in range(8):
+            out[z, at] = piece[z * 32 : z * 32 + 32, :]
+
+
+def edges_body(far, after, before, own, out):
+    rows = [p[k : k + 1, :].astype(f32) for p in (far, after, before, own) for k in (0, 127)]
+    out[...] = jnp.concatenate(rows, axis=0).astype(bf16)
 
 
 def summed(pieces):
@@ -128,9 +153,9 @@
 
 
 def attend_body(
-    y_ref, core_ref, logits, own, other, p0, p1, p2, p3, frequency, out_own, out_other, mo, w, qs, ks, vs, gs
+    index, logits, own, other, p0, p1, p2, p3, frequency, out_own, out_other, mo, w, qs, ks, vs, gs
 ):
-    y, core = y_ref[0], core_ref[0]
+    y, core = index[1], index[3]
     for shift, piece in zip(Y_SHIFTS, (p0, p1, p2, p3)):
         at = lax.rem(y - shift + 4, 4) * 32
         for z in range(8):
@@ -194,9 +219,9 @@
             out_other[r * 128 - 512 : r * 128 - 384, :] = gated
 
 
-def output_body(x_ref, mine, theirs, my_weights, their_weights, far, right, left, here, lines):
+def output_body(index, mine, theirs, my_weights, their_weights, far, right, left, here, lines):
     for place, ahead in enumerate((2, 1, 3, 0)):
-        block = lax.rem(x_ref[0] + ahead, 4)
+        block = lax.rem(index[0] + ahead, 4)
         rows = pl.ds(pl.multiple_of(block * 128, 128), 128)
         lines[place * 128 : place * 128 + 128, :DV] = mine[rows, :]
         lines[place * 128 : place * 128 + 128, DV:] = theirs[rows, :]
@@ -224,8 +249,7 @@
 
 
 def feed_body(
-    x_ref,
-    core_ref,
+    index,
     got_far,
     got_next,
     got_prev,
@@ -242,23 +266,15 @@
     lines,
     outer,
     hidden,
-    my_weights,
-    their_weights,
 ):
-    core = core_ref[0]
-    blocks = [lax.rem(x_ref[0] + k, 4) for k in (2, 1, 3, 0)]
+    core = index[3]
+    blocks = [lax.rem(index[0] + k, 4) for k in (2, 1, 3, 0)]
     for place, piece in enumerate((got_far, got_next, got_prev, own)):
         lines[place * 128 : place * 128 + 128, :] = piece[...]
     lines[512:520, :] = edges[...]
     lines[520:528, :] = jnp.zeros((8, 1024), bf16)
     outer[...] = jnp.zeros(outer.shape, f32)
-    for part, (raw, weights, taps) in enumerate(
-        ((mine, my_weights, my_taps), (theirs, their_weights, their_taps))
-    ):
-        for z in range(8):
-            for y in range(4):
-                at = z * 128 + y * 32
-                weights[at : at + 32, :] = raw[y, z]
+    for part, (weights, taps) in enumerate(((mine, my_taps), (theirs, their_taps))):
         main = dot(lines[...], weights[:, : 2 * PAD])
         for place, block in enumerate(blocks):
             outer[pl.ds(8 + block, 1), :] = main[512 + 2 * place : 513 + 2 * place, :]
@@ -272,8 +288,8 @@
             )
     for d in range(0, 1024, 256):
         columns = slice(d, d + 256)
-        total = dot_nt(hidden[:, :PAD], my_weights[columns, 2 * PAD :]) + dot_nt(
-            hidden[:, PAD:], their_weights[columns, 2 * PAD :]
+        total = dot_nt(hidden[:, :PAD], mine[columns, 2 * PAD :]) + dot_nt(
+            hidden[:, PAD:], theirs[columns, 2 * PAD :]
         )
         for place, out in enumerate((far, right, left, here)):
             out[:, columns] = total[place * 128 : place * 128 + 128, :].astype(bf16)
@@ -329,9 +345,8 @@
     down_weight,
     channel_out_gain,
 ):
-    core = lax.axis_index("c").astype(jnp.int32)
-    y_index = lax.axis_index("y").astype(jnp.int32)
-    z_index = lax.axis_index("z").astype(jnp.int32)
+    place = jnp.stack([lax.axis_index(a).astype(jnp.int32) for a in ("x", "y", "z", "c")])
+    place, query_weight = lax.optimization_barrier((place, query_weight))
     token_rows = tokens[0]
     own, model = token_rows.shape
     chips = lax.axis_size("x")
@@ -341,9 +356,7 @@
     def row(vector):
         return vector.reshape(1, -1)
 
-    packed = call(
-        functools.partial(pack_body, width),
-        shape((32, FIRST + THIRD)),
+    parts = (
         query_weight,
         key_weight,
         value_weight,
@@ -353,43 +366,52 @@
         linear_weight,
         down_weight.T,
     )
+    packed = call(
+        functools.partial(pack_body, width),
+        shape((32, FIRST + THIRD)),
+        *parts,
+        hbm=8,
+        scratch=[pltpu.VMEM(part.shape, bf16) for part in parts]
+        + [pltpu.SemaphoreType.DMA((8,))],
+    )
     got = {0: packed}
     for shift in Z_ISSUE:
         got[shift] = permuted(packed, RING, shift, 16)
-    spread = call(first_norm_body, shape((chips, own, model)), token_rows, row(mixer_in_gain))
+    spread = call(
+        first_norm_body, shape((chips, own, model)), token_rows, row(mixer_in_gain), limit=60
+    )
     normed_own = exchanged(spread).reshape(half, model)
     normed_other = swap(normed_own)
     first_z, third_z = call(
         ring_order_body,
-        [shape((8, 32, FIRST)), shape((4, 8, 32, THIRD))],
-        z_index[None],
+        [shape((8, 32, FIRST)), shape((8, 32, THIRD))],
+        place,
         *[got[s] for s in Z_SHIFTS],
         smem=1,
     )
     first_pieces = line_gather(first_z)
-    third_own = lax.all_to_all(third_z, "y", 0, 0, tiled=True)
+    third_pieces = line_gather(third_z)
     taps = call(
         functools.partial(taps_body, width),
         shape((8, PAD), f32),
         gelu_kernel,
         linear_kernel,
-        row(gelu_bias),
-        row(linear_bias),
+        gelu_bias,
+        linear_bias,
     )
     taps_other = swap(taps)
     gated_own, gated_other, out_own = call(
         attend_body,
         [shape((half, DV)), shape((half, DV)), shape((model, DV))],
-        y_index[None],
-        core[None],
+        place,
         decay_logits[:, 0],
         normed_own,
         normed_other,
         *first_pieces,
         rope_frequency(),
         flops=1 << 32,
-        smem=3,
-        limit=14,
+        smem=2,
+        limit=10,
         scratch=[
             pltpu.VMEM((model, PROJECT), bf16),
             pltpu.VMEM((2 * half, DK), bf16),
@@ -399,11 +421,10 @@
         ],
     )
     gated_partner = swap(gated_other)
-    x_index = lax.axis_index("x").astype(jnp.int32)[None]
     far, right, left, here = call(
         output_body,
         [shape((own, model))] * 4,
-        x_index,
+        place,
         gated_own,
         gated_partner,
         out_own,
@@ -421,15 +442,17 @@
         row(mixer_out_gain),
         row(channel_in_gain),
     )
+    third_own = call(
+        line_order_body, shape((8, 4, 32, THIRD)), place, *third_pieces, smem=1
+    ).reshape(model, THIRD)
     third_other = swap(third_own)
     got_far, got_prev, got_next = sent(channel_in, channel_in, channel_in)
     blocks = (got_far, got_next, got_prev, channel_in)
-    edges = jnp.concatenate([b[k : k + 1] for b in blocks for k in (0, own - 1)], axis=0)
+    edges = call(edges_body, shape((8, model)), *blocks)
     far, right, left, here = call(
         feed_body,
         [shape((own, model))] * 4,
-        x_index,
-        core[None],
+        place,
         *blocks,
         swap(edges),
         third_own,
@@ -437,14 +460,12 @@
         taps,
         taps_other,
         flops=1 << 32,
-        smem=2,
+        smem=1,
         limit=18,
         scratch=[
             pltpu.VMEM((half + 16, model), bf16),
             pltpu.VMEM((16, 2 * PAD), f32),
             pltpu.VMEM((half, 2 * PAD), bf16),
-            pltpu.VMEM((model, THIRD), bf16),
-            pltpu.VMEM((model, THIRD), bf16),
         ],
     )
     result = call(

time: 205 us -> 204 us (level)
  the two profiles are of different devices: /device:TPU:3 before, /device:TPU:8 now
where the time goes in v6:
time: 204 us; the launch traced here: 203 us
  starting transfers between devices  109 us (53%)
  waiting for transfers between devices  76.5 us (38%)
  Pallas kernels  16 us (8%)
    ppermute x22, starting transfers between devices, permuted(): lax.ppermute(value, axes, [(i, (i + shift) % size) for i in range(size)])  92 us
    ppermute x22, waiting for transfers between devices, permuted(): lax.ppermute(value, axes, [(i, (i + shift) % size) for i in range(size)])  74.5 us
    pallas_call x11, Pallas kernels, call(): pl.pallas_call(body, out_shape=out_shapes, in_specs=specs, out_specs=VMEM...  16 us
    ppermute x6, starting transfers between devices, swap(): return lax.ppermute(value, 'c', SWAP)  12.6 us
    all_to_all x1, starting transfers between devices, exchanged(): return lax.all_to_all(value, 'x', 0, 0, tiled=True)  4.29 us
  transfers between devices with their start and end apart: 29, of which 19 were waited for; matrix products, arithmetic and copies ran while one was open for 0% of the time, Pallas kernels for 4%

profile of v6, /device:TPU:8, one launch (start us, length us, event | category | flops | bytes accessed | tf_op | source)
XLA Modules:
  0.0 202.8 jit_solution(13321880289446351852)
XLA Ops:
  0.0 2.1 %shard_map.181 = bf16[4,128,1024]{2,1,0:T(8,128)(2,1)} custom-call(bf16[128,1024]{1,0:T(8,128)(2,1)} %bitcast.25, f32[1,1024]{1,0:T(1,128)} %bitcast.43), custom_call_target="tpu_custom_call" | custom-call | flops 16777216 | bytes 2097152 | tf_op jit(solution)/shard_map/pallas_call | solution.py:42
  2.1 4.3 %all-to-all-start = ((bf16[4,128,1024]{2,1,0:T(8,128)(2,1)}), bf16[4,128,1024]{2,1,0:T(8,128)(2,1)S(1)}, u32[]{:S(2)}, u32[]{:S(2)}) async-start(bf16[4,128,1024]{2,1,0:T(8,128)(2,1)} %shard_map.181), calls=%async_computation | async-start | bytes 2097152 | tf_op jit(solution)/shard_map/all_to_all | solution.py:68
  7.4 9.1 %collective-permute-start.1 = (bf16[32,2176]{1,0:T(8,128)(2,1)S(1)}, bf16[32,2176]{1,0:T(8,128)(2,1)S(1)}, u32[]{:S(2)}, u32[]{:S(2)}) collective-permute-start(bf16[32,2176]{1,0:T(8,128)(2,1)S(1)} %shard_map.182.refs_4_), channel_id=1, source_target_pairs={{0,128},{32,160},{64,192},{96,224},{128,256},{160,288},{192,320},{... | collective-permute-start | bytes 417800 | tf_op jit(solution)/shard_map/ppermute | solution.py:60
  16.6 6.5 %collective-permute-start.2 = (bf16[32,2176]{1,0:T(8,128)(2,1)S(1)}, bf16[32,2176]{1,0:T(8,128)(2,1)S(1)}, u32[]{:S(2)}, u32[]{:S(2)}) collective-permute-start(bf16[32,2176]{1,0:T(8,128)(2,1)S(1)} %shard_map.182.refs_4_), channel_id=1, source_target_pairs={{0,96},{32,128},{64,160},{96,192},{128,224},{160,256},{192,288},{2... | collective-permute-start | bytes 417800 | tf_op jit(solution)/shard_map/ppermute | solution.py:60
  23.1 5.5 %collective-permute-start.3 = (bf16[32,2176]{1,0:T(8,128)(2,1)S(1)}, bf16[32,2176]{1,0:T(8,128)(2,1)S(1)}, u32[]{:S(2)}, u32[]{:S(2)}) collective-permute-start(bf16[32,2176]{1,0:T(8,128)(2,1)S(1)} %shard_map.182.refs_4_), channel_id=1, source_target_pairs={{0,64},{32,96},{64,128},{96,160},{128,192},{160,224},{192,256},{22... | collective-permute-start | bytes 417800 | tf_op jit(solution)/shard_map/ppermute | solution.py:60
  28.6 2.9 %collective-permute-start.4 = (bf16[32,2176]{1,0:T(8,128)(2,1)S(1)}, bf16[32,2176]{1,0:T(8,128)(2,1)S(1)}, u32[]{:S(2)}, u32[]{:S(2)}) collective-permute-start(bf16[32,2176]{1,0:T(8,128)(2,1)S(1)} %shard_map.182.refs_4_), channel_id=1, source_target_pairs={{0,32},{32,64},{64,96},{96,128},{128,160},{160,192},{192,224},{224... | collective-permute-start | bytes 417800 | tf_op jit(solution)/shard_map/ppermute | solution.py:60
  31.5 4.1 %collective-permute-start.5 = (bf16[32,2176]{1,0:T(8,128)(2,1)S(1)}, bf16[32,2176]{1,0:T(8,128)(2,1)S(1)}, u32[]{:S(2)}, u32[]{:S(2)}) collective-permute-start(bf16[32,2176]{1,0:T(8,128)(2,1)S(1)} %shard_map.182.refs_4_), channel_id=1, source_target_pairs={{0,480},{32,0},{64,32},{96,64},{128,96},{160,128},{192,160},{224,1... | collective-permute-start | bytes 417800 | tf_op jit(solution)/shard_map/ppermute | solution.py:60
  35.7 5.1 %collective-permute-start.6 = (bf16[32,2176]{1,0:T(8,128)(2,1)S(1)}, bf16[32,2176]{1,0:T(8,128)(2,1)S(1)}, u32[]{:S(2)}, u32[]{:S(2)}) collective-permute-start(bf16[32,2176]{1,0:T(8,128)(2,1)S(1)} %shard_map.182.refs_4_), channel_id=1, source_target_pairs={{0,448},{32,480},{64,0},{96,32},{128,64},{160,96},{192,128},{224,1... | collective-permute-start | bytes 417800 | tf_op jit(solution)/shard_map/ppermute | solution.py:60
  40.8 2.9 %collective-permute-done.2.refs_1_ = bf16[32,2176]{1,0:T(8,128)(2,1)S(1)} collective-permute-done((bf16[32,2176]{1,0:T(8,128)(2,1)S(1)}, bf16[32,2176]{1,0:T(8,128)(2,1)S(1)}, u32[]{:S(2)}, u32[]{:S(2)}) %collective-permute-start.2) | collective-permute-done | bytes 139296 | tf_op jit(solution)/shard_map/ppermute | solution.py:60
  43.7 4.2 %collective-permute-start.7 = (bf16[32,2176]{1,0:T(8,128)(2,1)S(1)}, bf16[32,2176]{1,0:T(8,128)(2,1)S(1)}, u32[]{:S(2)}, u32[]{:S(2)}) collective-permute-start(bf16[32,2176]{1,0:T(8,128)(2,1)S(1)} %shard_map.182.refs_4_), channel_id=1, source_target_pairs={{0,416},{32,448},{64,480},{96,0},{128,32},{160,64},{192,96},{224,1... | collective-permute-start | bytes 417800 | tf_op jit(solution)/shard_map/ppermute | solution.py:60
  47.9 1.3 collective-permute-done.4.refs_3_
  49.2 7.0 %collective-permute-done.7.refs_7_ = bf16[32,2176]{1,0:T(8,128)(2,1)S(1)} collective-permute-done((bf16[32,2176]{1,0:T(8,128)(2,1)S(1)}, bf16[32,2176]{1,0:T(8,128)(2,1)S(1)}, u32[]{:S(2)}, u32[]{:S(2)}) %collective-permute-start.7) | collective-permute-done | bytes 139296 | tf_op jit(solution)/shard_map/ppermute | solution.py:60
  57.7 3.5 %collective-permute-start.20 = (bf16[8,32,1152]{2,1,0:T(8,128)(2,1)S(1)}, bf16[8,32,1152]{2,1,0:T(8,128)(2,1)S(1)}, u32[]{:S(2)}, u32[]{:S(2)}) collective-permute-start(bf16[8,32,1152]{2,1,0:T(8,128)(2,1)S(1)} %get-tuple-element.33), channel_id=1, source_target_pairs={{0,8},{8,16},{16,24},{24,0},{1,9},{9,17},{17,25},{25,1},{2,10},{10... | collective-permute-start | bytes 1769480 | tf_op jit(solution)/shard_map/ppermute | solution.py:60
  61.1 2.8 %collective-permute-start.21 = (bf16[8,32,1152]{2,1,0:T(8,128)(2,1)S(1)}, bf16[8,32,1152]{2,1,0:T(8,128)(2,1)S(1)}, u32[]{:S(2)}, u32[]{:S(2)}) collective-permute-start(bf16[8,32,1152]{2,1,0:T(8,128)(2,1)S(1)} %get-tuple-element.33), channel_id=1, source_target_pairs={{0,16},{8,24},{16,0},{24,8},{1,17},{9,25},{17,1},{25,9},{2,18},{10... | collective-permute-start | bytes 1769480 | tf_op jit(solution)/shard_map/ppermute | solution.py:60
  64.0 4.3 %collective-permute-start.22 = (bf16[8,32,1152]{2,1,0:T(8,128)(2,1)S(1)}, bf16[8,32,1152]{2,1,0:T(8,128)(2,1)S(1)}, u32[]{:S(2)}, u32[]{:S(2)}) collective-permute-start(bf16[8,32,1152]{2,1,0:T(8,128)(2,1)S(1)} %get-tuple-element.33), channel_id=1, source_target_pairs={{0,24},{8,0},{16,8},{24,16},{1,25},{9,1},{17,9},{25,17},{2,26},{10... | collective-permute-start | bytes 1769480 | tf_op jit(solution)/shard_map/ppermute | solution.py:60
  68.3 1.9 collective-permute-start
  70.3 5.5 %collective-permute-done.20 = bf16[8,32,1152]{2,1,0:T(8,128)(2,1)S(1)} collective-permute-done((bf16[8,32,1152]{2,1,0:T(8,128)(2,1)S(1)}, bf16[8,32,1152]{2,1,0:T(8,128)(2,1)S(1)}, u32[]{:S(2)}, u32[]{:S(2)}) %collective-permute-start.20) | collective-permute-done | bytes 589856 | tf_op jit(solution)/shard_map/ppermute | solution.py:60
  75.7 5.0 %collective-permute-done.21 = bf16[8,32,1152]{2,1,0:T(8,128)(2,1)S(1)} collective-permute-done((bf16[8,32,1152]{2,1,0:T(8,128)(2,1)S(1)}, bf16[8,32,1152]{2,1,0:T(8,128)(2,1)S(1)}, u32[]{:S(2)}, u32[]{:S(2)}) %collective-permute-start.21) | collective-permute-done | bytes 589856 | tf_op jit(solution)/shard_map/ppermute | solution.py:60
  80.8 10.2 %collective-permute-done.22 = bf16[8,32,1152]{2,1,0:T(8,128)(2,1)S(1)} collective-permute-done((bf16[8,32,1152]{2,1,0:T(8,128)(2,1)S(1)}, bf16[8,32,1152]{2,1,0:T(8,128)(2,1)S(1)}, u32[]{:S(2)}, u32[]{:S(2)}) %collective-permute-start.22) | collective-permute-done | bytes 589856 | tf_op jit(solution)/shard_map/ppermute | solution.py:60
  91.8 1.9 collective-permute-start.23
  93.7 2.5 %collective-permute-start.8 = (bf16[8,32,1024]{2,1,0:T(8,128)(2,1)S(1)}, bf16[8,32,1024]{2,1,0:T(8,128)(2,1)S(1)}, u32[]{:S(2)}, u32[]{:S(2)}) collective-permute-start(bf16[8,32,1024]{2,1,0:T(8,128)(2,1)S(1)} %copy-done.5), channel_id=1, source_target_pairs={{0,8},{8,16},{16,24},{24,0},{1,9},{9,17},{17,25},{25,1},{2,10},{10... | collective-permute-start | bytes 1572872 | tf_op jit(solution)/shard_map/ppermute | solution.py:60
  96.2 2.9 %collective-permute-start.9 = (bf16[8,32,1024]{2,1,0:T(8,128)(2,1)S(1)}, bf16[8,32,1024]{2,1,0:T(8,128)(2,1)S(1)}, u32[]{:S(2)}, u32[]{:S(2)}) collective-permute-start(bf16[8,32,1024]{2,1,0:T(8,128)(2,1)S(1)} %copy-done.5), channel_id=1, source_target_pairs={{0,16},{8,24},{16,0},{24,8},{1,17},{9,25},{17,1},{25,9},{2,18},{10... | collective-permute-start | bytes 1572872 | tf_op jit(solution)/shard_map/ppermute | solution.py:60
  99.1 3.9 %collective-permute-start.10 = (bf16[8,32,1024]{2,1,0:T(8,128)(2,1)S(1)}, bf16[8,32,1024]{2,1,0:T(8,128)(2,1)S(1)}, u32[]{:S(2)}, u32[]{:S(2)}) collective-permute-start(bf16[8,32,1024]{2,1,0:T(8,128)(2,1)S(1)} %copy-done.5), channel_id=1, source_target_pairs={{0,24},{8,0},{16,8},{24,16},{1,25},{9,1},{17,9},{25,17},{2,26},{10... | collective-permute-start | bytes 1572872 | tf_op jit(solution)/shard_map/ppermute | solution.py:60
  103.1 7.3 %collective-permute-done.8 = bf16[8,32,1024]{2,1,0:T(8,128)(2,1)S(1)} collective-permute-done((bf16[8,32,1024]{2,1,0:T(8,128)(2,1)S(1)}, bf16[8,32,1024]{2,1,0:T(8,128)(2,1)S(1)}, u32[]{:S(2)}, u32[]{:S(2)}) %collective-permute-start.8) | collective-permute-done | bytes 524320 | tf_op jit(solution)/shard_map/ppermute | solution.py:60
  110.4 4.1 %collective-permute-done.9 = bf16[8,32,1024]{2,1,0:T(8,128)(2,1)S(1)} collective-permute-done((bf16[8,32,1024]{2,1,0:T(8,128)(2,1)S(1)}, bf16[8,32,1024]{2,1,0:T(8,128)(2,1)S(1)}, u32[]{:S(2)}, u32[]{:S(2)}) %collective-permute-start.9) | collective-permute-done | bytes 524320 | tf_op jit(solution)/shard_map/ppermute | solution.py:60
  114.5 10.4 %collective-permute-done.10 = bf16[8,32,1024]{2,1,0:T(8,128)(2,1)S(1)} collective-permute-done((bf16[8,32,1024]{2,1,0:T(8,128)(2,1)S(1)}, bf16[8,32,1024]{2,1,0:T(8,128)(2,1)S(1)}, u32[]{:S(2)}, u32[]{:S(2)}) %collective-permute-start.10) | collective-permute-done | bytes 524320 | tf_op jit(solution)/shard_map/ppermute | solution.py:60
  124.9 4.2 %shard_map.184 = (bf16[512,256]{1,0:T(8,128)(2,1)S(1)}, bf16[512,256]{1,0:T(8,128)(2,1)S(1)}, bf16[1024,256]{1,0:T(8,128)(2,1)S(1)}) custom-call(s32[4]{0:T(128)S(1)} %pad_add_fusion.index, f32[2]{0:T(128)S(1)} %bitcast.40, bf16[512,1024]{1,0:T(8,128)(2,1)S(1)} %bitcast.28, bf16[512,1024]{1,0:T(8,128)(2,1)S(1)} %collective-permute-done.other, ...), custom_call_target="tpu_custom_call" | custom-call | flops 4294967296 | bytes 2097152 | tf_op jit(solution)/shard_map/pallas_call | solution.py:42
  129.1 2.1 %collective-permute-start.12 = (bf16[1024,256]{1,0:T(8,128)(2,1)S(1)}, bf16[1024,256]{1,0:T(8,128)(2,1)S(1)}, u32[]{:S(2)}, u32[]{:S(2)}) collective-permute-start(bf16[1024,256]{1,0:T(8,128)(2,1)S(1)} %get-tuple-element.27.my_weights), channel_id=1, source_target_pairs={{0,1},{1,0},{2,3},{3,2},{4,5},{5,4},{6,7},{7,6},{8,9},{9,8},{10,11... | collective-permute-start | bytes 1572872 | tf_op jit(solution)/shard_map/ppermute | solution.py:64
  131.2 2.4 %collective-permute-start.11 = (bf16[512,256]{1,0:T(8,128)(2,1)S(1)}, bf16[512,256]{1,0:T(8,128)(2,1)S(1)}, u32[]{:S(2)}, u32[]{:S(2)}) collective-permute-start(bf16[512,256]{1,0:T(8,128)(2,1)S(1)} %get-tuple-element.26), channel_id=1, source_target_pairs={{0,1},{1,0},{2,3},{3,2},{4,5},{5,4},{6,7},{7,6},{8,9},{9,8},{10,11... | collective-permute-start | bytes 786440 | tf_op jit(solution)/shard_map/ppermute | solution.py:64
  133.6 1.1 collective-permute-done.11.theirs
  134.7 1.3 shard_map.185
  136.0 6.3 %collective-permute-start.13 = (bf16[128,1024]{1,0:T(8,128)(2,1)S(1)}, bf16[128,1024]{1,0:T(8,128)(2,1)S(1)}, u32[]{:S(2)}, u32[]{:S(2)}) collective-permute-start(bf16[128,1024]{1,0:T(8,128)(2,1)S(1)} %get-tuple-element.28), channel_id=1, source_target_pairs={{0,4},{2,6},{4,0},{6,2},{1,5},{3,7},{5,1},{7,3},{8,12},{10,14},{12... | collective-permute-start | bytes 786440 | tf_op jit(solution)/shard_map/ppermute | solution.py:60
  142.3 2.5 %collective-permute-start.14 = (bf16[128,1024]{1,0:T(8,128)(2,1)S(1)}, bf16[128,1024]{1,0:T(8,128)(2,1)S(1)}, u32[]{:S(2)}, u32[]{:S(2)}) collective-permute-start(bf16[128,1024]{1,0:T(8,128)(2,1)S(1)} %get-tuple-element.29), channel_id=1, source_target_pairs={{0,2},{2,4},{4,6},{6,0},{1,3},{3,5},{5,7},{7,1},{8,10},{10,12},{12... | collective-permute-start | bytes 786440 | tf_op jit(solution)/shard_map/ppermute | solution.py:60
  144.8 4.6 %collective-permute-start.15 = (bf16[128,1024]{1,0:T(8,128)(2,1)S(1)}, bf16[128,1024]{1,0:T(8,128)(2,1)S(1)}, u32[]{:S(2)}, u32[]{:S(2)}) collective-permute-start(bf16[128,1024]{1,0:T(8,128)(2,1)S(1)} %get-tuple-element.30), channel_id=1, source_target_pairs={{0,6},{2,0},{4,2},{6,4},{1,7},{3,1},{5,3},{7,5},{8,14},{10,8},{12,... | collective-permute-start | bytes 786440 | tf_op jit(solution)/shard_map/ppermute | solution.py:60
  149.5 5.3 %collective-permute-done.14.right = bf16[128,1024]{1,0:T(8,128)(2,1)S(1)} collective-permute-done((bf16[128,1024]{1,0:T(8,128)(2,1)S(1)}, bf16[128,1024]{1,0:T(8,128)(2,1)S(1)}, u32[]{:S(2)}, u32[]{:S(2)}) %collective-permute-start.14) | collective-permute-done | bytes 262176 | tf_op jit(solution)/shard_map/ppermute | solution.py:60
  155.4 4.9 %collective-permute-start.16 = (bf16[128,1024]{1,0:T(8,128)(2,1)S(1)}, bf16[128,1024]{1,0:T(8,128)(2,1)S(1)}, u32[]{:S(2)}, u32[]{:S(2)}) collective-permute-start(bf16[128,1024]{1,0:T(8,128)(2,1)S(1)} %get-tuple-element.32.own), channel_id=1, source_target_pairs={{0,4},{2,6},{4,0},{6,2},{1,5},{3,7},{5,1},{7,3},{8,12},{10,14},{12... | collective-permute-start | bytes 786440 | tf_op jit(solution)/shard_map/ppermute | solution.py:60
  160.3 3.1 %collective-permute-start.17 = (bf16[128,1024]{1,0:T(8,128)(2,1)S(1)}, bf16[128,1024]{1,0:T(8,128)(2,1)S(1)}, u32[]{:S(2)}, u32[]{:S(2)}) collective-permute-start(bf16[128,1024]{1,0:T(8,128)(2,1)S(1)} %get-tuple-element.32.own), channel_id=1, source_target_pairs={{0,6},{2,0},{4,2},{6,4},{1,7},{3,1},{5,3},{7,5},{8,14},{10,8},{12,... | collective-permute-start | bytes 786440 | tf_op jit(solution)/shard_map/ppermute | solution.py:60
  163.5 2.7 %collective-permute-start.18 = (bf16[128,1024]{1,0:T(8,128)(2,1)S(1)}, bf16[128,1024]{1,0:T(8,128)(2,1)S(1)}, u32[]{:S(2)}, u32[]{:S(2)}) collective-permute-start(bf16[128,1024]{1,0:T(8,128)(2,1)S(1)} %get-tuple-element.32.own), channel_id=1, source_target_pairs={{0,2},{2,4},{4,6},{6,0},{1,3},{3,5},{5,7},{7,1},{8,10},{10,12},{12... | collective-permute-start | bytes 786440 | tf_op jit(solution)/shard_map/ppermute | solution.py:60
  166.9 5.7 %collective-permute-done.17.after.got_next = bf16[128,1024]{1,0:T(8,128)(2,1)S(1)} collective-permute-done((bf16[128,1024]{1,0:T(8,128)(2,1)S(1)}, bf16[128,1024]{1,0:T(8,128)(2,1)S(1)}, u32[]{:S(2)}, u32[]{:S(2)}) %collective-permute-start.17) | collective-permute-done | bytes 262176 | tf_op jit(solution)/shard_map/ppermute | solution.py:60
  172.5 1.7 collective-permute-done.18.before.got_prev
  174.2 1.9 collective-permute-start.19
  176.2 2.4 %collective-permute-start.24 = (f32[8,384]{1,0:T(8,128)S(1)}, f32[8,384]{1,0:T(8,128)S(1)}, u32[]{:S(2)}, u32[]{:S(2)}) collective-permute-start(f32[8,384]{1,0:T(8,128)S(1)} %shard_map.189.my_taps), channel_id=1, source_target_pairs={{0,1},{1,0},{2,3},{3,2},{4,5},{5,4},{6,7},{7,6},{8,9},{9,8},{10,11... | collective-permute-start | bytes 36872 | tf_op jit(solution)/shard_map/ppermute | solution.py:64
  179.5 4.8 %shard_map.190 = (bf16[128,1024]{1,0:T(8,128)(2,1)S(1)}, bf16[128,1024]{1,0:T(8,128)(2,1)S(1)}, bf16[128,1024]{1,0:T(8,128)(2,1)S(1)}, bf16[128,1024]{1,0:T(8,128)(2,1)S(1)}) custom-call(s32[4]{0:T(128)S(1)} %pad_add_fusion.index, bf16[128,1024]{1,0:T(8,128)(2,1)S(1)} %collective-permute-done.16.far.got_far, ...), custom_call_target="tpu_custom_call" | custom-call | flops 4294967296 | bytes 2097152 | tf_op jit(solution)/shard_map/pallas_call | solution.py:42
  184.2 3.4 %collective-permute-start.25 = (bf16[128,1024]{1,0:T(8,128)(2,1)S(1)}, bf16[128,1024]{1,0:T(8,128)(2,1)S(1)}, u32[]{:S(2)}, u32[]{:S(2)}) collective-permute-start(bf16[128,1024]{1,0:T(8,128)(2,1)S(1)} %get-tuple-element.34), channel_id=1, source_target_pairs={{0,4},{2,6},{4,0},{6,2},{1,5},{3,7},{5,1},{7,3},{8,12},{10,14},{12... | collective-permute-start | bytes 786440 | tf_op jit(solution)/shard_map/ppermute | solution.py:60
  187.7 2.2 %collective-permute-start.26 = (bf16[128,1024]{1,0:T(8,128)(2,1)S(1)}, bf16[128,1024]{1,0:T(8,128)(2,1)S(1)}, u32[]{:S(2)}, u32[]{:S(2)}) collective-permute-start(bf16[128,1024]{1,0:T(8,128)(2,1)S(1)} %get-tuple-element.35), channel_id=1, source_target_pairs={{0,2},{2,4},{4,6},{6,0},{1,3},{3,5},{5,7},{7,1},{8,10},{10,12},{12... | collective-permute-start | bytes 786440 | tf_op jit(solution)/shard_map/ppermute | solution.py:60
  189.9 4.8 %collective-permute-start.27 = (bf16[128,1024]{1,0:T(8,128)(2,1)S(1)}, bf16[128,1024]{1,0:T(8,128)(2,1)S(1)}, u32[]{:S(2)}, u32[]{:S(2)}) collective-permute-start(bf16[128,1024]{1,0:T(8,128)(2,1)S(1)} %get-tuple-element.36), channel_id=1, source_target_pairs={{0,6},{2,0},{4,2},{6,4},{1,7},{3,1},{5,3},{7,5},{8,14},{10,8},{12,... | collective-permute-start | bytes 786440 | tf_op jit(solution)/shard_map/ppermute | solution.py:60
  194.7 2.1 %collective-permute-done.25.far = bf16[128,1024]{1,0:T(8,128)(2,1)S(1)} collective-permute-done((bf16[128,1024]{1,0:T(8,128)(2,1)S(1)}, bf16[128,1024]{1,0:T(8,128)(2,1)S(1)}, u32[]{:S(2)}, u32[]{:S(2)}) %collective-permute-start.25) | collective-permute-done | bytes 262176 | tf_op jit(solution)/shard_map/ppermute | solution.py:60
  196.8 4.9 %collective-permute-done.26.right = bf16[128,1024]{1,0:T(8,128)(2,1)S(1)} collective-permute-done((bf16[128,1024]{1,0:T(8,128)(2,1)S(1)}, bf16[128,1024]{1,0:T(8,128)(2,1)S(1)}, u32[]{:S(2)}, u32[]{:S(2)}) %collective-permute-start.26) | collective-permute-done | bytes 262176 | tf_op jit(solution)/shard_map/ppermute | solution.py:60
  (46 shorter events, 6.4 us)
Async XLA Ops:
  2.1 66.2 %all-to-all-start = ((bf16[4,128,1024]{2,1,0:T(8,128)(2,1)}), bf16[4,128,1024]{2,1,0:T(8,128)(2,1)S(1)}, u32[]{:S(2)}, u32[]{:S(2)}) async-start(bf16[4,128,1024]{2,1,0:T(8,128)(2,1)} %shard_map.181), calls=%async_computation | async-start | bytes 2097152 | tf_op jit(solution)/shard_map/all_to_all | solution.py:68
  7.4 28.2 %collective-permute-start.1 = (bf16[32,2176]{1,0:T(8,128)(2,1)S(1)}, bf16[32,2176]{1,0:T(8,128)(2,1)S(1)}, u32[]{:S(2)}, u32[]{:S(2)}) collective-permute-start(bf16[32,2176]{1,0:T(8,128)(2,1)S(1)} %shard_map.182.refs_4_), channel_id=1, source_target_pairs={{0,128},{32,160},{64,192},{96,224},{128,256},{160,288},{192,320},{... | collective-permute-start | bytes 417800 | tf_op jit(solution)/shard_map/ppermute | solution.py:60
  16.6 27.2 %collective-permute-start.2 = (bf16[32,2176]{1,0:T(8,128)(2,1)S(1)}, bf16[32,2176]{1,0:T(8,128)(2,1)S(1)}, u32[]{:S(2)}, u32[]{:S(2)}) collective-permute-start(bf16[32,2176]{1,0:T(8,128)(2,1)S(1)} %shard_map.182.refs_4_), channel_id=1, source_target_pairs={{0,96},{32,128},{64,160},{96,192},{128,224},{160,256},{192,288},{2... | collective-permute-start | bytes 417800 | tf_op jit(solution)/shard_map/ppermute | solution.py:60
  23.1 24.8 %collective-permute-start.3 = (bf16[32,2176]{1,0:T(8,128)(2,1)S(1)}, bf16[32,2176]{1,0:T(8,128)(2,1)S(1)}, u32[]{:S(2)}, u32[]{:S(2)}) collective-permute-start(bf16[32,2176]{1,0:T(8,128)(2,1)S(1)} %shard_map.182.refs_4_), channel_id=1, source_target_pairs={{0,64},{32,96},{64,128},{96,160},{128,192},{160,224},{192,256},{22... | collective-permute-start | bytes 417800 | tf_op jit(solution)/shard_map/ppermute | solution.py:60
  28.6 20.6 %collective-permute-start.4 = (bf16[32,2176]{1,0:T(8,128)(2,1)S(1)}, bf16[32,2176]{1,0:T(8,128)(2,1)S(1)}, u32[]{:S(2)}, u32[]{:S(2)}) collective-permute-start(bf16[32,2176]{1,0:T(8,128)(2,1)S(1)} %shard_map.182.refs_4_), channel_id=1, source_target_pairs={{0,32},{32,64},{64,96},{96,128},{128,160},{160,192},{192,224},{224... | collective-permute-start | bytes 417800 | tf_op jit(solution)/shard_map/ppermute | solution.py:60
  31.5 17.7 %collective-permute-start.5 = (bf16[32,2176]{1,0:T(8,128)(2,1)S(1)}, bf16[32,2176]{1,0:T(8,128)(2,1)S(1)}, u32[]{:S(2)}, u32[]{:S(2)}) collective-permute-start(bf16[32,2176]{1,0:T(8,128)(2,1)S(1)} %shard_map.182.refs_4_), channel_id=1, source_target_pairs={{0,480},{32,0},{64,32},{96,64},{128,96},{160,128},{192,160},{224,1... | collective-permute-start | bytes 417800 | tf_op jit(solution)/shard_map/ppermute | solution.py:60
  35.7 13.5 %collective-permute-start.6 = (bf16[32,2176]{1,0:T(8,128)(2,1)S(1)}, bf16[32,2176]{1,0:T(8,128)(2,1)S(1)}, u32[]{:S(2)}, u32[]{:S(2)}) collective-permute-start(bf16[32,2176]{1,0:T(8,128)(2,1)S(1)} %shard_map.182.refs_4_), channel_id=1, source_target_pairs={{0,448},{32,480},{64,0},{96,32},{128,64},{160,96},{192,128},{224,1... | collective-permute-start | bytes 417800 | tf_op jit(solution)/shard_map/ppermute | solution.py:60
  43.7 12.5 %collective-permute-start.7 = (bf16[32,2176]{1,0:T(8,128)(2,1)S(1)}, bf16[32,2176]{1,0:T(8,128)(2,1)S(1)}, u32[]{:S(2)}, u32[]{:S(2)}) collective-permute-start(bf16[32,2176]{1,0:T(8,128)(2,1)S(1)} %shard_map.182.refs_4_), channel_id=1, source_target_pairs={{0,416},{32,448},{64,480},{96,0},{128,32},{160,64},{192,96},{224,1... | collective-permute-start | bytes 417800 | tf_op jit(solution)/shard_map/ppermute | solution.py:60
  56.9 0.8 copy-start.4
  57.7 18.1 %collective-permute-start.20 = (bf16[8,32,1152]{2,1,0:T(8,128)(2,1)S(1)}, bf16[8,32,1152]{2,1,0:T(8,128)(2,1)S(1)}, u32[]{:S(2)}, u32[]{:S(2)}) collective-permute-start(bf16[8,32,1152]{2,1,0:T(8,128)(2,1)S(1)} %get-tuple-element.33), channel_id=1, source_target_pairs={{0,8},{8,16},{16,24},{24,0},{1,9},{9,17},{17,25},{25,1},{2,10},{10... | collective-permute-start | bytes 1769480 | tf_op jit(solution)/shard_map/ppermute | solution.py:60
  61.1 19.6 %collective-permute-start.21 = (bf16[8,32,1152]{2,1,0:T(8,128)(2,1)S(1)}, bf16[8,32,1152]{2,1,0:T(8,128)(2,1)S(1)}, u32[]{:S(2)}, u32[]{:S(2)}) collective-permute-start(bf16[8,32,1152]{2,1,0:T(8,128)(2,1)S(1)} %get-tuple-element.33), channel_id=1, source_target_pairs={{0,16},{8,24},{16,0},{24,8},{1,17},{9,25},{17,1},{25,9},{2,18},{10... | collective-permute-start | bytes 1769480 | tf_op jit(solution)/shard_map/ppermute | solution.py:60
  64.0 27.0 %collective-permute-start.22 = (bf16[8,32,1152]{2,1,0:T(8,128)(2,1)S(1)}, bf16[8,32,1152]{2,1,0:T(8,128)(2,1)S(1)}, u32[]{:S(2)}, u32[]{:S(2)}) collective-permute-start(bf16[8,32,1152]{2,1,0:T(8,128)(2,1)S(1)} %get-tuple-element.33), channel_id=1, source_target_pairs={{0,24},{8,0},{16,8},{24,16},{1,25},{9,1},{17,9},{25,17},{2,26},{10... | collective-permute-start | bytes 1769480 | tf_op jit(solution)/shard_map/ppermute | solution.py:60
  68.3 56.6 %collective-permute-start = (bf16[512,1024]{1,0:T(8,128)(2,1)S(1)}, bf16[512,1024]{1,0:T(8,128)(2,1)S(1)}, u32[]{:S(2)}, u32[]{:S(2)}) collective-permute-start(bf16[512,1024]{1,0:T(8,128)(2,1)S(1)} %bitcast.27), channel_id=1, source_target_pairs={{0,1},{1,0},{2,3},{3,2},{4,5},{5,4},{6,7},{7,6},{8,9},{9,8},{10,11... | collective-permute-start | bytes 3145736 | tf_op jit(solution)/shard_map/ppermute | solution.py:64
  91.0 2.7 %copy-start.5 = (bf16[8,32,1024]{2,1,0:T(8,128)(2,1)S(1)}, bf16[8,32,1024]{2,1,0:T(8,128)(2,1)}, u32[]{:S(2)}) copy-start(bf16[8,32,1024]{2,1,0:T(8,128)(2,1)} %copy-done.4) | copy-start | bytes 1572868
  91.0 33.9 %copy-start.10 = (f32[2,1]{0,1:T(1,128)S(1)}, f32[2,1]{0,1:T(1,128)}, u32[]{:S(2)}) copy-start(f32[2,1]{0,1:T(1,128)} %param.25) | copy-start | bytes 28
  91.0 33.9 %copy-start.11 = (f32[1,128]{1,0:T(1,128)S(1)}, f32[1,128]{1,0:T(1,128)}, u32[]{:S(2)}) copy-start(f32[1,128]{1,0:T(1,128)} %constant.18.clone.frequency) | copy-start | bytes 1540
  91.8 87.7 %collective-permute-start.23 = (bf16[1024,1152]{1,0:T(8,128)(2,1)S(1)}, bf16[1024,1152]{1,0:T(8,128)(2,1)S(1)}, u32[]{:S(2)}, u32[]{:S(2)}) collective-permute-start(bf16[1024,1152]{1,0:T(8,128)(2,1)S(1)} %bitcast.23), channel_id=1, source_target_pairs={{0,1},{1,0},{2,3},{3,2},{4,5},{5,4},{6,7},{7,6},{8,9},{9,8},{10,11... | collective-permute-start | bytes 7077896 | tf_op jit(solution)/shard_map/ppermute | solution.py:64
  93.7 16.7 %collective-permute-start.8 = (bf16[8,32,1024]{2,1,0:T(8,128)(2,1)S(1)}, bf16[8,32,1024]{2,1,0:T(8,128)(2,1)S(1)}, u32[]{:S(2)}, u32[]{:S(2)}) collective-permute-start(bf16[8,32,1024]{2,1,0:T(8,128)(2,1)S(1)} %copy-done.5), channel_id=1, source_target_pairs={{0,8},{8,16},{16,24},{24,0},{1,9},{9,17},{17,25},{25,1},{2,10},{10... | collective-permute-start | bytes 1572872 | tf_op jit(solution)/shard_map/ppermute | solution.py:60
  96.2 18.2 %collective-permute-start.9 = (bf16[8,32,1024]{2,1,0:T(8,128)(2,1)S(1)}, bf16[8,32,1024]{2,1,0:T(8,128)(2,1)S(1)}, u32[]{:S(2)}, u32[]{:S(2)}) collective-permute-start(bf16[8,32,1024]{2,1,0:T(8,128)(2,1)S(1)} %copy-done.5), channel_id=1, source_target_pairs={{0,16},{8,24},{16,0},{24,8},{1,17},{9,25},{17,1},{25,9},{2,18},{10... | collective-permute-start | bytes 1572872 | tf_op jit(solution)/shard_map/ppermute | solution.py:60
  99.1 25.8 %collective-permute-start.10 = (bf16[8,32,1024]{2,1,0:T(8,128)(2,1)S(1)}, bf16[8,32,1024]{2,1,0:T(8,128)(2,1)S(1)}, u32[]{:S(2)}, u32[]{:S(2)}) collective-permute-start(bf16[8,32,1024]{2,1,0:T(8,128)(2,1)S(1)} %copy-done.5), channel_id=1, source_target_pairs={{0,24},{8,0},{16,8},{24,16},{1,25},{9,1},{17,9},{25,17},{2,26},{10... | collective-permute-start | bytes 1572872 | tf_op jit(solution)/shard_map/ppermute | solution.py:60
  129.1 26.0 %copy-start = (bf16[1,128,1024]{2,1,0:T(8,128)(2,1)S(1)}, bf16[1,128,1024]{2,1,0:T(8,128)(2,1)}, u32[]{:S(2)}) copy-start(bf16[1,128,1024]{2,1,0:T(8,128)(2,1)} %param.19) | copy-start | bytes 786436
  129.1 26.0 %copy-start.1 = (f32[1024]{0:T(1024)S(1)}, f32[1024]{0:T(1024)}, u32[]{:S(2)}) copy-start(f32[1024]{0:T(1024)} %param.27) | copy-start | bytes 12292
  129.1 26.0 %copy-start.2 = (f32[1024]{0:T(1024)S(1)}, f32[1024]{0:T(1024)}, u32[]{:S(2)}) copy-start(f32[1024]{0:T(1024)} %param.28) | copy-start | bytes 12292
  129.1 5.6 %collective-permute-start.12 = (bf16[1024,256]{1,0:T(8,128)(2,1)S(1)}, bf16[1024,256]{1,0:T(8,128)(2,1)S(1)}, u32[]{:S(2)}, u32[]{:S(2)}) collective-permute-start(bf16[1024,256]{1,0:T(8,128)(2,1)S(1)} %get-tuple-element.27.my_weights), channel_id=1, source_target_pairs={{0,1},{1,0},{2,3},{3,2},{4,5},{5,4},{6,7},{7,6},{8,9},{9,8},{10,11... | collective-permute-start | bytes 1572872 | tf_op jit(solution)/shard_map/ppermute | solution.py:64
  131.2 3.5 %collective-permute-start.11 = (bf16[512,256]{1,0:T(8,128)(2,1)S(1)}, bf16[512,256]{1,0:T(8,128)(2,1)S(1)}, u32[]{:S(2)}, u32[]{:S(2)}) collective-permute-start(bf16[512,256]{1,0:T(8,128)(2,1)S(1)} %get-tuple-element.26), channel_id=1, source_target_pairs={{0,1},{1,0},{2,3},{3,2},{4,5},{5,4},{6,7},{7,6},{8,9},{9,8},{10,11... | collective-permute-start | bytes 786440 | tf_op jit(solution)/shard_map/ppermute | solution.py:64
  134.7 41.4 %copy-start.6 = (f32[3,352]{1,0:T(4,128)S(1)}, f32[3,352]{1,0:T(4,128)}, u32[]{:S(2)}) copy-start(f32[3,352]{1,0:T(4,128)} %ge_kernel.1) | copy-start | bytes 12676
  134.7 41.4 %copy-start.7 = (f32[3,352]{1,0:T(4,128)S(1)}, f32[3,352]{1,0:T(4,128)}, u32[]{:S(2)}) copy-start(f32[3,352]{1,0:T(4,128)} %li_kernel.1) | copy-start | bytes 12676
  134.7 41.5 %copy-start.8 = (f32[352]{0:T(512)S(1)}, f32[352]{0:T(512)}, u32[]{:S(2)}) copy-start(f32[352]{0:T(512)} %ge_bias.1) | copy-start | bytes 4228
  134.7 41.5 %copy-start.9 = (f32[352]{0:T(512)S(1)}, f32[352]{0:T(512)}, u32[]{:S(2)}) copy-start(f32[352]{0:T(512)} %li_bias.1) | copy-start | bytes 4228
  136.0 13.4 %collective-permute-start.13 = (bf16[128,1024]{1,0:T(8,128)(2,1)S(1)}, bf16[128,1024]{1,0:T(8,128)(2,1)S(1)}, u32[]{:S(2)}, u32[]{:S(2)}) collective-permute-start(bf16[128,1024]{1,0:T(8,128)(2,1)S(1)} %get-tuple-element.28), channel_id=1, source_target_pairs={{0,4},{2,6},{4,0},{6,2},{1,5},{3,7},{5,1},{7,3},{8,12},{10,14},{12... | collective-permute-start | bytes 786440 | tf_op jit(solution)/shard_map/ppermute | solution.py:60
  142.3 12.4 %collective-permute-start.14 = (bf16[128,1024]{1,0:T(8,128)(2,1)S(1)}, bf16[128,1024]{1,0:T(8,128)(2,1)S(1)}, u32[]{:S(2)}, u32[]{:S(2)}) collective-permute-start(bf16[128,1024]{1,0:T(8,128)(2,1)S(1)} %get-tuple-element.29), channel_id=1, source_target_pairs={{0,2},{2,4},{4,6},{6,0},{1,3},{3,5},{5,7},{7,1},{8,10},{10,12},{12... | collective-permute-start | bytes 786440 | tf_op jit(solution)/shard_map/ppermute | solution.py:60
  144.8 10.2 %collective-permute-start.15 = (bf16[128,1024]{1,0:T(8,128)(2,1)S(1)}, bf16[128,1024]{1,0:T(8,128)(2,1)S(1)}, u32[]{:S(2)}, u32[]{:S(2)}) collective-permute-start(bf16[128,1024]{1,0:T(8,128)(2,1)S(1)} %get-tuple-element.30), channel_id=1, source_target_pairs={{0,6},{2,0},{4,2},{6,4},{1,7},{3,1},{5,3},{7,5},{8,14},{10,8},{12,... | collective-permute-start | bytes 786440 | tf_op jit(solution)/shard_map/ppermute | solution.py:60
  155.4 11.4 %collective-permute-start.16 = (bf16[128,1024]{1,0:T(8,128)(2,1)S(1)}, bf16[128,1024]{1,0:T(8,128)(2,1)S(1)}, u32[]{:S(2)}, u32[]{:S(2)}) collective-permute-start(bf16[128,1024]{1,0:T(8,128)(2,1)S(1)} %get-tuple-element.32.own), channel_id=1, source_target_pairs={{0,4},{2,6},{4,0},{6,2},{1,5},{3,7},{5,1},{7,3},{8,12},{10,14},{12... | collective-permute-start | bytes 786440 | tf_op jit(solution)/shard_map/ppermute | solution.py:60
  160.3 12.2 %collective-permute-start.17 = (bf16[128,1024]{1,0:T(8,128)(2,1)S(1)}, bf16[128,1024]{1,0:T(8,128)(2,1)S(1)}, u32[]{:S(2)}, u32[]{:S(2)}) collective-permute-start(bf16[128,1024]{1,0:T(8,128)(2,1)S(1)} %get-tuple-element.32.own), channel_id=1, source_target_pairs={{0,6},{2,0},{4,2},{6,4},{1,7},{3,1},{5,3},{7,5},{8,14},{10,8},{12,... | collective-permute-start | bytes 786440 | tf_op jit(solution)/shard_map/ppermute | solution.py:60
  163.5 10.7 %collective-permute-start.18 = (bf16[128,1024]{1,0:T(8,128)(2,1)S(1)}, bf16[128,1024]{1,0:T(8,128)(2,1)S(1)}, u32[]{:S(2)}, u32[]{:S(2)}) collective-permute-start(bf16[128,1024]{1,0:T(8,128)(2,1)S(1)} %get-tuple-element.32.own), channel_id=1, source_target_pairs={{0,2},{2,4},{4,6},{6,0},{1,3},{3,5},{5,7},{7,1},{8,10},{10,12},{12... | collective-permute-start | bytes 786440 | tf_op jit(solution)/shard_map/ppermute | solution.py:60
  174.2 5.2 %collective-permute-start.19 = (bf16[8,1024]{1,0:T(8,128)(2,1)S(1)}, bf16[8,1024]{1,0:T(8,128)(2,1)S(1)}, u32[]{:S(2)}, u32[]{:S(2)}) collective-permute-start(bf16[8,1024]{1,0:T(8,128)(2,1)S(1)} %shard_map.187), channel_id=1, source_target_pairs={{0,1},{1,0},{2,3},{3,2},{4,5},{5,4},{6,7},{7,6},{8,9},{9,8},{10,11... | collective-permute-start | bytes 49160 | tf_op jit(solution)/shard_map/ppermute | solution.py:64
  176.2 25.6 %copy-start.3 = (f32[1024]{0:T(1024)S(1)}, f32[1024]{0:T(1024)}, u32[]{:S(2)}) copy-start(f32[1024]{0:T(1024)} %param.36) | copy-start | bytes 12292
  176.2 3.2 %collective-permute-start.24 = (f32[8,384]{1,0:T(8,128)S(1)}, f32[8,384]{1,0:T(8,128)S(1)}, u32[]{:S(2)}, u32[]{:S(2)}) collective-permute-start(f32[8,384]{1,0:T(8,128)S(1)} %shard_map.189.my_taps), channel_id=1, source_target_pairs={{0,1},{1,0},{2,3},{3,2},{4,5},{5,4},{6,7},{7,6},{8,9},{9,8},{10,11... | collective-permute-start | bytes 36872 | tf_op jit(solution)/shard_map/ppermute | solution.py:64
  184.2 12.6 %collective-permute-start.25 = (bf16[128,1024]{1,0:T(8,128)(2,1)S(1)}, bf16[128,1024]{1,0:T(8,128)(2,1)S(1)}, u32[]{:S(2)}, u32[]{:S(2)}) collective-permute-start(bf16[128,1024]{1,0:T(8,128)(2,1)S(1)} %get-tuple-element.34), channel_id=1, source_target_pairs={{0,4},{2,6},{4,0},{6,2},{1,5},{3,7},{5,1},{7,3},{8,12},{10,14},{12... | collective-permute-start | bytes 786440 | tf_op jit(solution)/shard_map/ppermute | solution.py:60
  187.7 14.1 %collective-permute-start.26 = (bf16[128,1024]{1,0:T(8,128)(2,1)S(1)}, bf16[128,1024]{1,0:T(8,128)(2,1)S(1)}, u32[]{:S(2)}, u32[]{:S(2)}) collective-permute-start(bf16[128,1024]{1,0:T(8,128)(2,1)S(1)} %get-tuple-element.35), channel_id=1, source_target_pairs={{0,2},{2,4},{4,6},{6,0},{1,3},{3,5},{5,7},{7,1},{8,10},{10,12},{12... | collective-permute-start | bytes 786440 | tf_op jit(solution)/shard_map/ppermute | solution.py:60
  189.9 11.9 %collective-permute-start.27 = (bf16[128,1024]{1,0:T(8,128)(2,1)S(1)}, bf16[128,1024]{1,0:T(8,128)(2,1)S(1)}, u32[]{:S(2)}, u32[]{:S(2)}) collective-permute-start(bf16[128,1024]{1,0:T(8,128)(2,1)S(1)} %get-tuple-element.36), channel_id=1, source_target_pairs={{0,6},{2,0},{4,2},{6,4},{1,7},{3,1},{5,3},{7,5},{8,14},{10,8},{12,... | collective-permute-start | bytes 786440 | tf_op jit(solution)/shard_map/ppermute | solution.py:60

commit v7 on v6

--- a/solution.py
+++ b/solution.py
@@ -18,10 +18,8 @@
 SWAP = ((0, 1), (1, 0))
 PAD = 384
 PROJECT, FIRST, THIRD = 2 * DK + 2 * DV, 2 * DK + 3 * DV, 3 * PAD
-Z_SHIFTS = (4, 3, 2, 1, 0, -1, -2, -3)
-Z_ISSUE = (4, -3, 3, -2, 2, -1, 1)
-Y_SHIFTS = (0, 1, 2, -1)
-Y_ISSUE = (2, 1, -1)
+Z_ISSUE = (4, 5, 6, 7, 3, 2, 1)
+PARTNERS = (2, 1, 3)
 epsilon = 1e-06
 rope_base = 10000.0
 bf16 = jnp.bfloat16
@@ -56,8 +54,18 @@
     return jax.ShapeDtypeStruct(dims, kind)
 
 
-def permuted(value, axes, shift, size):
-    return lax.ppermute(value, axes, [(i, (i + shift) % size) for i in range(size)])
+def line_pairs(k):
+    return [(i, i ^ k) for i in range(4)]
+
+
+def ring_pairs(k):
+    pairs = []
+    for i in range(16):
+        here = i // 8 * 8 + (i % 8 ^ k)
+        there = (here + 8) % 16
+        gap = min((here - i) % 16, (i - here) % 16)
+        pairs.append((i, here if gap <= 4 else there))
+    return pairs
 
 
 def swap(value):
@@ -108,16 +116,16 @@
 
 def ring_order_body(index, *refs):
     pieces, (one, three) = refs[:8], refs[8:]
-    for shift, piece in zip(Z_SHIFTS, pieces):
-        at = lax.rem(index[2] - shift + 8, 8)
+    for k, piece in enumerate(pieces):
+        at = index[2] ^ k
         one[at] = piece[:, :FIRST]
         three[at] = piece[:, FIRST:]
 
 
 def line_order_body(index, *refs):
     pieces, out = refs[:4], refs[4]
-    for shift, piece in zip(Y_SHIFTS, pieces):
-        at = lax.rem(index[1] - shift + 4, 4)
+    for k, piece in enumerate(pieces):
+        at = index[1] ^ k
         for z in range(8):
             out[z, at] = piece[z * 32 : z * 32 + 32, :]
 
@@ -156,8 +164,8 @@
     index, logits, own, other, p0, p1, p2, p3, frequency, out_own, out_other, mo, w, qs, ks, vs, gs
 ):
     y, core = index[1], index[3]
-    for shift, piece in zip(Y_SHIFTS, (p0, p1, p2, p3)):
-        at = lax.rem(y - shift + 4, 4) * 32
+    for k, piece in enumerate((p0, p1, p2, p3)):
+        at = (y ^ k) * 32
         for z in range(8):
             place = pl.ds(pl.multiple_of(z * 128 + at, 32), 32)
             w[place, :] = piece[z * 32 : z * 32 + 32, :PROJECT]
@@ -220,8 +228,8 @@
 
 
 def output_body(index, mine, theirs, my_weights, their_weights, far, right, left, here, lines):
-    for place, ahead in enumerate((2, 1, 3, 0)):
-        block = lax.rem(index[0] + ahead, 4)
+    for place, k in enumerate((2, 1, 3, 0)):
+        block = index[0] ^ k
         rows = pl.ds(pl.multiple_of(block * 128, 128), 128)
         lines[place * 128 : place * 128 + 128, :DV] = mine[rows, :]
         lines[place * 128 : place * 128 + 128, DV:] = theirs[rows, :]
@@ -268,7 +276,7 @@
     hidden,
 ):
     core = index[3]
-    blocks = [lax.rem(index[0] + k, 4) for k in (2, 1, 3, 0)]
+    blocks = [index[0] ^ k for k in (2, 1, 3, 0)]
     for place, piece in enumerate((got_far, got_next, got_prev, own)):
         lines[place * 128 : place * 128 + 128, :] = piece[...]
     lines[512:520, :] = edges[...]
@@ -310,13 +318,13 @@
 
 def line_gather(piece):
     got = {0: piece}
-    for shift in Y_ISSUE:
-        got[shift] = permuted(piece, "y", shift, 4)
-    return [got[s].reshape(256, piece.shape[-1]) for s in Y_SHIFTS]
-
-
-def sent(far, right, left):
-    return (permuted(far, "x", 2, 4), permuted(right, "x", 1, 4), permuted(left, "x", -1, 4))
+    for k in PARTNERS:
+        got[k] = lax.ppermute(piece, "y", line_pairs(k))
+    return [got[k].reshape(256, piece.shape[-1]) for k in range(4)]
+
+
+def sent(blocks):
+    return [lax.ppermute(block, "x", line_pairs(k)) for k, block in zip(PARTNERS, blocks)]
 
 
 def rope_frequency():
@@ -375,8 +383,8 @@
         + [pltpu.SemaphoreType.DMA((8,))],
     )
     got = {0: packed}
-    for shift in Z_ISSUE:
-        got[shift] = permuted(packed, RING, shift, 16)
+    for k in Z_ISSUE:
+        got[k] = lax.ppermute(packed, RING, ring_pairs(k))
     spread = call(
         first_norm_body, shape((chips, own, model)), token_rows, row(mixer_in_gain), limit=60
     )
@@ -386,7 +394,7 @@
         ring_order_body,
         [shape((8, 32, FIRST)), shape((8, 32, THIRD))],
         place,
-        *[got[s] for s in Z_SHIFTS],
+        *[got[k] for k in range(8)],
         smem=1,
     )
     first_pieces = line_gather(first_z)
@@ -436,7 +444,7 @@
     after_mix, channel_in = call(
         middle_body,
         [shape((own, model)), shape((own, model))],
-        *sent(far, right, left),
+        *sent((far, right, left)),
         here,
         token_rows,
         row(mixer_out_gain),
@@ -446,8 +454,7 @@
         line_order_body, shape((8, 4, 32, THIRD)), place, *third_pieces, smem=1
     ).reshape(model, THIRD)
     third_other = swap(third_own)
-    got_far, got_prev, got_next = sent(channel_in, channel_in, channel_in)
-    blocks = (got_far, got_next, got_prev, channel_in)
+    blocks = (*sent([channel_in] * 3), channel_in)
     edges = call(edges_body, shape((8, model)), *blocks)
     far, right, left, here = call(
         feed_body,
@@ -471,7 +478,7 @@
     result = call(
         final_body,
         shape((own, model)),
-        *sent(far, right, left),
+        *sent((far, right, left)),
         here,
         after_mix,
         row(channel_out_gain),

time: 204 us -> 209 us (1.025)
  the two profiles are of different devices: /device:TPU:8 before, /device:TPU:128 now
where the time goes in v7:
time: 209 us; the launch traced here: 208 us
  starting transfers between devices  98.1 us (47%)
  waiting for transfers between devices  92.3 us (44%)
  Pallas kernels  15.9 us (8%)
    ppermute x6, waiting for transfers between devices, line_gather(): got[k] = lax.ppermute(piece, 'y', line_pairs(k))  49.6 us
    ppermute x7, starting transfers between devices, layer(): got[k] = lax.ppermute(packed, RING, ring_pairs(k))  30.6 us
    ppermute x9, starting transfers between devices, sent(): lax.ppermute(block, 'x', line_pairs(k))  29.8 us
    ppermute x9, waiting for transfers between devices, sent(): lax.ppermute(block, 'x', line_pairs(k))  24.1 us
    ppermute x6, starting transfers between devices, line_gather(): got[k] = lax.ppermute(piece, 'y', line_pairs(k))  20.8 us
    ppermute x7, waiting for transfers between devices, layer(): got[k] = lax.ppermute(packed, RING, ring_pairs(k))  16.6 us
    pallas_call x11, Pallas kernels, call(): pl.pallas_call(body, out_shape=out_shapes, in_specs=specs, out_specs=VMEM...  15.9 us
    ppermute x6, starting transfers between devices, swap(): return lax.ppermute(value, 'c', SWAP)  12.6 us
  transfers between devices with their start and end apart: 29, of which 20 were waited for; matrix products, arithmetic and copies ran while one was open for 0% of the time, Pallas kernels for 4%

profile of v7, /device:TPU:128, one launch (start us, length us, event | category | flops | bytes accessed | tf_op | source)
XLA Modules:
  0.0 207.7 jit_solution(4579425597878295807)
XLA Ops:
  0.0 2.1 %shard_map.181 = bf16[4,128,1024]{2,1,0:T(8,128)(2,1)} custom-call(bf16[128,1024]{1,0:T(8,128)(2,1)} %bitcast.25, f32[1,1024]{1,0:T(1,128)} %bitcast.43), custom_call_target="tpu_custom_call" | custom-call | flops 16777216 | bytes 2097152 | tf_op jit(solution)/shard_map/pallas_call | solution.py:40
  2.1 4.3 %all-to-all-start = ((bf16[4,128,1024]{2,1,0:T(8,128)(2,1)}), bf16[4,128,1024]{2,1,0:T(8,128)(2,1)S(1)}, u32[]{:S(2)}, u32[]{:S(2)}) async-start(bf16[4,128,1024]{2,1,0:T(8,128)(2,1)} %shard_map.181), calls=%async_computation | async-start | bytes 2097152 | tf_op jit(solution)/shard_map/all_to_all | solution.py:76
  7.4 3.8 %collective-permute-start.1 = (bf16[32,2176]{1,0:T(8,128)(2,1)S(1)}, bf16[32,2176]{1,0:T(8,128)(2,1)S(1)}, u32[]{:S(2)}, u32[]{:S(2)}) collective-permute-start(bf16[32,2176]{1,0:T(8,128)(2,1)S(1)} %shard_map.182.refs_0_), channel_id=1, source_target_pairs={{0,32},{32,0},{64,96},{96,64},{128,160},{160,128},{192,224},{224,1... | collective-permute-start | bytes 417800 | tf_op jit(solution)/shard_map/ppermute | solution.py:387
  11.3 5.2 %collective-permute-start.2 = (bf16[32,2176]{1,0:T(8,128)(2,1)S(1)}, bf16[32,2176]{1,0:T(8,128)(2,1)S(1)}, u32[]{:S(2)}, u32[]{:S(2)}) collective-permute-start(bf16[32,2176]{1,0:T(8,128)(2,1)S(1)} %shard_map.182.refs_0_), channel_id=1, source_target_pairs={{0,64},{32,96},{64,0},{96,32},{128,192},{160,224},{192,128},{224,1... | collective-permute-start | bytes 417800 | tf_op jit(solution)/shard_map/ppermute | solution.py:387
  16.5 1.9 collective-permute-start.3
  18.4 4.4 %collective-permute-start.4 = (bf16[32,2176]{1,0:T(8,128)(2,1)S(1)}, bf16[32,2176]{1,0:T(8,128)(2,1)S(1)}, u32[]{:S(2)}, u32[]{:S(2)}) collective-permute-start(bf16[32,2176]{1,0:T(8,128)(2,1)S(1)} %shard_map.182.refs_0_), channel_id=1, source_target_pairs={{0,128},{32,160},{64,192},{96,224},{128,0},{160,32},{192,64},{224,... | collective-permute-start | bytes 417800 | tf_op jit(solution)/shard_map/ppermute | solution.py:387
  22.8 4.4 %collective-permute-start.5 = (bf16[32,2176]{1,0:T(8,128)(2,1)S(1)}, bf16[32,2176]{1,0:T(8,128)(2,1)S(1)}, u32[]{:S(2)}, u32[]{:S(2)}) collective-permute-start(bf16[32,2176]{1,0:T(8,128)(2,1)S(1)} %shard_map.182.refs_0_), channel_id=1, source_target_pairs={{0,416},{32,128},{64,480},{96,192},{128,32},{160,256},{192,96},{22... | collective-permute-start | bytes 417800 | tf_op jit(solution)/shard_map/ppermute | solution.py:387
  27.3 7.8 %collective-permute-start.6 = (bf16[32,2176]{1,0:T(8,128)(2,1)S(1)}, bf16[32,2176]{1,0:T(8,128)(2,1)S(1)}, u32[]{:S(2)}, u32[]{:S(2)}) collective-permute-start(bf16[32,2176]{1,0:T(8,128)(2,1)S(1)} %shard_map.182.refs_0_), channel_id=1, source_target_pairs={{0,448},{32,480},{64,128},{96,160},{128,64},{160,96},{192,256},{22... | collective-permute-start | bytes 417800 | tf_op jit(solution)/shard_map/ppermute | solution.py:387
  35.1 2.9 %collective-permute-start.7 = (bf16[32,2176]{1,0:T(8,128)(2,1)S(1)}, bf16[32,2176]{1,0:T(8,128)(2,1)S(1)}, u32[]{:S(2)}, u32[]{:S(2)}) collective-permute-start(bf16[32,2176]{1,0:T(8,128)(2,1)S(1)} %shard_map.182.refs_0_), channel_id=1, source_target_pairs={{0,480},{32,448},{64,160},{96,128},{128,96},{160,64},{192,288},{22... | collective-permute-start | bytes 417800 | tf_op jit(solution)/shard_map/ppermute | solution.py:387
  38.1 7.8 %collective-permute-done.5.refs_5_ = bf16[32,2176]{1,0:T(8,128)(2,1)S(1)} collective-permute-done((bf16[32,2176]{1,0:T(8,128)(2,1)S(1)}, bf16[32,2176]{1,0:T(8,128)(2,1)S(1)}, u32[]{:S(2)}, u32[]{:S(2)}) %collective-permute-start.5) | collective-permute-done | bytes 139296 | tf_op jit(solution)/shard_map/ppermute | solution.py:387
  45.9 3.0 %collective-permute-done.6.refs_6_ = bf16[32,2176]{1,0:T(8,128)(2,1)S(1)} collective-permute-done((bf16[32,2176]{1,0:T(8,128)(2,1)S(1)}, bf16[32,2176]{1,0:T(8,128)(2,1)S(1)}, u32[]{:S(2)}, u32[]{:S(2)}) %collective-permute-start.6) | collective-permute-done | bytes 139296 | tf_op jit(solution)/shard_map/ppermute | solution.py:387
  48.9 5.9 %collective-permute-done.7.refs_7_ = bf16[32,2176]{1,0:T(8,128)(2,1)S(1)} collective-permute-done((bf16[32,2176]{1,0:T(8,128)(2,1)S(1)}, bf16[32,2176]{1,0:T(8,128)(2,1)S(1)}, u32[]{:S(2)}, u32[]{:S(2)}) %collective-permute-start.7) | collective-permute-done | bytes 139296 | tf_op jit(solution)/shard_map/ppermute | solution.py:387
  56.2 3.5 %collective-permute-start.20 = (bf16[8,32,1152]{2,1,0:T(8,128)(2,1)S(1)}, bf16[8,32,1152]{2,1,0:T(8,128)(2,1)S(1)}, u32[]{:S(2)}, u32[]{:S(2)}) collective-permute-start(bf16[8,32,1152]{2,1,0:T(8,128)(2,1)S(1)} %get-tuple-element.33), channel_id=1, source_target_pairs={{0,8},{8,0},{16,24},{24,16},{1,9},{9,1},{17,25},{25,17},{2,10},{10... | collective-permute-start | bytes 1769480 | tf_op jit(solution)/shard_map/ppermute | solution.py:322
  59.6 4.8 %collective-permute-start.21 = (bf16[8,32,1152]{2,1,0:T(8,128)(2,1)S(1)}, bf16[8,32,1152]{2,1,0:T(8,128)(2,1)S(1)}, u32[]{:S(2)}, u32[]{:S(2)}) collective-permute-start(bf16[8,32,1152]{2,1,0:T(8,128)(2,1)S(1)} %get-tuple-element.33), channel_id=1, source_target_pairs={{0,16},{8,24},{16,0},{24,8},{1,17},{9,25},{17,1},{25,9},{2,18},{10... | collective-permute-start | bytes 1769480 | tf_op jit(solution)/shard_map/ppermute | solution.py:322
  64.5 2.1 %collective-permute-start.22 = (bf16[8,32,1152]{2,1,0:T(8,128)(2,1)S(1)}, bf16[8,32,1152]{2,1,0:T(8,128)(2,1)S(1)}, u32[]{:S(2)}, u32[]{:S(2)}) collective-permute-start(bf16[8,32,1152]{2,1,0:T(8,128)(2,1)S(1)} %get-tuple-element.33), channel_id=1, source_target_pairs={{0,24},{8,16},{16,8},{24,0},{1,25},{9,17},{17,9},{25,1},{2,26},{10... | collective-permute-start | bytes 1769480 | tf_op jit(solution)/shard_map/ppermute | solution.py:322
  66.6 1.9 collective-permute-start
  68.5 5.7 %collective-permute-done.20 = bf16[8,32,1152]{2,1,0:T(8,128)(2,1)S(1)} collective-permute-done((bf16[8,32,1152]{2,1,0:T(8,128)(2,1)S(1)}, bf16[8,32,1152]{2,1,0:T(8,128)(2,1)S(1)}, u32[]{:S(2)}, u32[]{:S(2)}) %collective-permute-start.20) | collective-permute-done | bytes 589856 | tf_op jit(solution)/shard_map/ppermute | solution.py:322
  74.2 14.2 %collective-permute-done.21 = bf16[8,32,1152]{2,1,0:T(8,128)(2,1)S(1)} collective-permute-done((bf16[8,32,1152]{2,1,0:T(8,128)(2,1)S(1)}, bf16[8,32,1152]{2,1,0:T(8,128)(2,1)S(1)}, u32[]{:S(2)}, u32[]{:S(2)}) %collective-permute-start.21) | collective-permute-done | bytes 589856 | tf_op jit(solution)/shard_map/ppermute | solution.py:322
  88.5 6.4 %collective-permute-done.22 = bf16[8,32,1152]{2,1,0:T(8,128)(2,1)S(1)} collective-permute-done((bf16[8,32,1152]{2,1,0:T(8,128)(2,1)S(1)}, bf16[8,32,1152]{2,1,0:T(8,128)(2,1)S(1)}, u32[]{:S(2)}, u32[]{:S(2)}) %collective-permute-start.22) | collective-permute-done | bytes 589856 | tf_op jit(solution)/shard_map/ppermute | solution.py:322
  95.6 1.9 collective-permute-start.23
  97.6 1.9 collective-permute-start.8
  99.5 3.7 %collective-permute-start.9 = (bf16[8,32,1024]{2,1,0:T(8,128)(2,1)S(1)}, bf16[8,32,1024]{2,1,0:T(8,128)(2,1)S(1)}, u32[]{:S(2)}, u32[]{:S(2)}) collective-permute-start(bf16[8,32,1024]{2,1,0:T(8,128)(2,1)S(1)} %copy-done.5), channel_id=1, source_target_pairs={{0,16},{8,24},{16,0},{24,8},{1,17},{9,25},{17,1},{25,9},{2,18},{10... | collective-permute-start | bytes 1572872 | tf_op jit(solution)/shard_map/ppermute | solution.py:322
  103.1 4.9 %collective-permute-start.10 = (bf16[8,32,1024]{2,1,0:T(8,128)(2,1)S(1)}, bf16[8,32,1024]{2,1,0:T(8,128)(2,1)S(1)}, u32[]{:S(2)}, u32[]{:S(2)}) collective-permute-start(bf16[8,32,1024]{2,1,0:T(8,128)(2,1)S(1)} %copy-done.5), channel_id=1, source_target_pairs={{0,24},{8,16},{16,8},{24,0},{1,25},{9,17},{17,9},{25,1},{2,26},{10... | collective-permute-start | bytes 1572872 | tf_op jit(solution)/shard_map/ppermute | solution.py:322
  108.0 6.2 %collective-permute-done.8 = bf16[8,32,1024]{2,1,0:T(8,128)(2,1)S(1)} collective-permute-done((bf16[8,32,1024]{2,1,0:T(8,128)(2,1)S(1)}, bf16[8,32,1024]{2,1,0:T(8,128)(2,1)S(1)}, u32[]{:S(2)}, u32[]{:S(2)}) %collective-permute-start.8) | collective-permute-done | bytes 524320 | tf_op jit(solution)/shard_map/ppermute | solution.py:322
  114.2 10.6 %collective-permute-done.9 = bf16[8,32,1024]{2,1,0:T(8,128)(2,1)S(1)} collective-permute-done((bf16[8,32,1024]{2,1,0:T(8,128)(2,1)S(1)}, bf16[8,32,1024]{2,1,0:T(8,128)(2,1)S(1)}, u32[]{:S(2)}, u32[]{:S(2)}) %collective-permute-start.9) | collective-permute-done | bytes 524320 | tf_op jit(solution)/shard_map/ppermute | solution.py:322
  124.8 6.4 %collective-permute-done.10 = bf16[8,32,1024]{2,1,0:T(8,128)(2,1)S(1)} collective-permute-done((bf16[8,32,1024]{2,1,0:T(8,128)(2,1)S(1)}, bf16[8,32,1024]{2,1,0:T(8,128)(2,1)S(1)}, u32[]{:S(2)}, u32[]{:S(2)}) %collective-permute-start.10) | collective-permute-done | bytes 524320 | tf_op jit(solution)/shard_map/ppermute | solution.py:322
  131.3 4.1 %shard_map.184 = (bf16[512,256]{1,0:T(8,128)(2,1)S(1)}, bf16[512,256]{1,0:T(8,128)(2,1)S(1)}, bf16[1024,256]{1,0:T(8,128)(2,1)S(1)}) custom-call(s32[4]{0:T(128)S(1)} %pad_add_fusion.index, f32[2]{0:T(128)S(1)} %bitcast.40, bf16[512,1024]{1,0:T(8,128)(2,1)S(1)} %bitcast.28, bf16[512,1024]{1,0:T(8,128)(2,1)S(1)} %collective-permute-done.other, ...), custom_call_target="tpu_custom_call" | custom-call | flops 4294967296 | bytes 2097152 | tf_op jit(solution)/shard_map/pallas_call | solution.py:40
  135.4 2.1 collective-permute-start.12
  137.5 2.4 %collective-permute-start.11 = (bf16[512,256]{1,0:T(8,128)(2,1)S(1)}, bf16[512,256]{1,0:T(8,128)(2,1)S(1)}, u32[]{:S(2)}, u32[]{:S(2)}) collective-permute-start(bf16[512,256]{1,0:T(8,128)(2,1)S(1)} %get-tuple-element.26), channel_id=1, source_target_pairs={{0,1},{1,0},{2,3},{3,2},{4,5},{5,4},{6,7},{7,6},{8,9},{9,8},{10,11... | collective-permute-start | bytes 786440 | tf_op jit(solution)/shard_map/ppermute | solution.py:72
  142.3 5.2 %collective-permute-start.13 = (bf16[128,1024]{1,0:T(8,128)(2,1)S(1)}, bf16[128,1024]{1,0:T(8,128)(2,1)S(1)}, u32[]{:S(2)}, u32[]{:S(2)}) collective-permute-start(bf16[128,1024]{1,0:T(8,128)(2,1)S(1)} %get-tuple-element.28), channel_id=1, source_target_pairs={{0,4},{2,6},{4,0},{6,2},{1,5},{3,7},{5,1},{7,3},{8,12},{10,14},{12... | collective-permute-start | bytes 786440 | tf_op jit(solution)/shard_map/ppermute | solution.py:327
  147.5 2.5 %collective-permute-start.14 = (bf16[128,1024]{1,0:T(8,128)(2,1)S(1)}, bf16[128,1024]{1,0:T(8,128)(2,1)S(1)}, u32[]{:S(2)}, u32[]{:S(2)}) collective-permute-start(bf16[128,1024]{1,0:T(8,128)(2,1)S(1)} %get-tuple-element.29), channel_id=1, source_target_pairs={{0,2},{2,0},{4,6},{6,4},{1,3},{3,1},{5,7},{7,5},{8,10},{10,8},{12,... | collective-permute-start | bytes 786440 | tf_op jit(solution)/shard_map/ppermute | solution.py:327
  150.0 2.5 %collective-permute-start.15 = (bf16[128,1024]{1,0:T(8,128)(2,1)S(1)}, bf16[128,1024]{1,0:T(8,128)(2,1)S(1)}, u32[]{:S(2)}, u32[]{:S(2)}) collective-permute-start(bf16[128,1024]{1,0:T(8,128)(2,1)S(1)} %get-tuple-element.30), channel_id=1, source_target_pairs={{0,6},{2,4},{4,2},{6,0},{1,7},{3,5},{5,3},{7,1},{8,14},{10,12},{12... | collective-permute-start | bytes 786440 | tf_op jit(solution)/shard_map/ppermute | solution.py:327
  152.5 2.4 %collective-permute-done.13.far = bf16[128,1024]{1,0:T(8,128)(2,1)S(1)} collective-permute-done((bf16[128,1024]{1,0:T(8,128)(2,1)S(1)}, bf16[128,1024]{1,0:T(8,128)(2,1)S(1)}, u32[]{:S(2)}, u32[]{:S(2)}) %collective-permute-start.13) | collective-permute-done | bytes 262176 | tf_op jit(solution)/shard_map/ppermute | solution.py:327
  154.9 5.3 %collective-permute-done.14.right = bf16[128,1024]{1,0:T(8,128)(2,1)S(1)} collective-permute-done((bf16[128,1024]{1,0:T(8,128)(2,1)S(1)}, bf16[128,1024]{1,0:T(8,128)(2,1)S(1)}, u32[]{:S(2)}, u32[]{:S(2)}) %collective-permute-start.14) | collective-permute-done | bytes 262176 | tf_op jit(solution)/shard_map/ppermute | solution.py:327
  161.5 4.0 %collective-permute-start.16 = (bf16[128,1024]{1,0:T(8,128)(2,1)S(1)}, bf16[128,1024]{1,0:T(8,128)(2,1)S(1)}, u32[]{:S(2)}, u32[]{:S(2)}) collective-permute-start(bf16[128,1024]{1,0:T(8,128)(2,1)S(1)} %get-tuple-element.32.own), channel_id=1, source_target_pairs={{0,4},{2,6},{4,0},{6,2},{1,5},{3,7},{5,1},{7,3},{8,12},{10,14},{12... | collective-permute-start | bytes 786440 | tf_op jit(solution)/shard_map/ppermute | solution.py:327
  165.5 2.5 %collective-permute-start.17 = (bf16[128,1024]{1,0:T(8,128)(2,1)S(1)}, bf16[128,1024]{1,0:T(8,128)(2,1)S(1)}, u32[]{:S(2)}, u32[]{:S(2)}) collective-permute-start(bf16[128,1024]{1,0:T(8,128)(2,1)S(1)} %get-tuple-element.32.own), channel_id=1, source_target_pairs={{0,2},{2,0},{4,6},{6,4},{1,3},{3,1},{5,7},{7,5},{8,10},{10,8},{12,... | collective-permute-start | bytes 786440 | tf_op jit(solution)/shard_map/ppermute | solution.py:327
  168.0 3.4 %collective-permute-start.18 = (bf16[128,1024]{1,0:T(8,128)(2,1)S(1)}, bf16[128,1024]{1,0:T(8,128)(2,1)S(1)}, u32[]{:S(2)}, u32[]{:S(2)}) collective-permute-start(bf16[128,1024]{1,0:T(8,128)(2,1)S(1)} %get-tuple-element.32.own), channel_id=1, source_target_pairs={{0,6},{2,4},{4,2},{6,0},{1,7},{3,5},{5,3},{7,1},{8,14},{10,12},{12... | collective-permute-start | bytes 786440 | tf_op jit(solution)/shard_map/ppermute | solution.py:327
  171.4 2.7 %collective-permute-done.16.far.got_far = bf16[128,1024]{1,0:T(8,128)(2,1)S(1)} collective-permute-done((bf16[128,1024]{1,0:T(8,128)(2,1)S(1)}, bf16[128,1024]{1,0:T(8,128)(2,1)S(1)}, u32[]{:S(2)}, u32[]{:S(2)}) %collective-permute-start.16) | collective-permute-done | bytes 262176 | tf_op jit(solution)/shard_map/ppermute | solution.py:327
  174.1 3.6 %collective-permute-done.17.after.got_next = bf16[128,1024]{1,0:T(8,128)(2,1)S(1)} collective-permute-done((bf16[128,1024]{1,0:T(8,128)(2,1)S(1)}, bf16[128,1024]{1,0:T(8,128)(2,1)S(1)}, u32[]{:S(2)}, u32[]{:S(2)}) %collective-permute-start.17) | collective-permute-done | bytes 262176 | tf_op jit(solution)/shard_map/ppermute | solution.py:327
  179.2 1.9 collective-permute-start.19
  181.2 2.4 %collective-permute-start.24 = (f32[8,384]{1,0:T(8,128)S(1)}, f32[8,384]{1,0:T(8,128)S(1)}, u32[]{:S(2)}, u32[]{:S(2)}) collective-permute-start(f32[8,384]{1,0:T(8,128)S(1)} %shard_map.189.my_taps), channel_id=1, source_target_pairs={{0,1},{1,0},{2,3},{3,2},{4,5},{5,4},{6,7},{7,6},{8,9},{9,8},{10,11... | collective-permute-start | bytes 36872 | tf_op jit(solution)/shard_map/ppermute | solution.py:72
  184.4 4.8 %shard_map.190 = (bf16[128,1024]{1,0:T(8,128)(2,1)S(1)}, bf16[128,1024]{1,0:T(8,128)(2,1)S(1)}, bf16[128,1024]{1,0:T(8,128)(2,1)S(1)}, bf16[128,1024]{1,0:T(8,128)(2,1)S(1)}) custom-call(s32[4]{0:T(128)S(1)} %pad_add_fusion.index, bf16[128,1024]{1,0:T(8,128)(2,1)S(1)} %collective-permute-done.16.far.got_far, ...), custom_call_target="tpu_custom_call" | custom-call | flops 4294967296 | bytes 2097152 | tf_op jit(solution)/shard_map/pallas_call | solution.py:40
  189.2 3.4 %collective-permute-start.25 = (bf16[128,1024]{1,0:T(8,128)(2,1)S(1)}, bf16[128,1024]{1,0:T(8,128)(2,1)S(1)}, u32[]{:S(2)}, u32[]{:S(2)}) collective-permute-start(bf16[128,1024]{1,0:T(8,128)(2,1)S(1)} %get-tuple-element.34), channel_id=1, source_target_pairs={{0,4},{2,6},{4,0},{6,2},{1,5},{3,7},{5,1},{7,3},{8,12},{10,14},{12... | collective-permute-start | bytes 786440 | tf_op jit(solution)/shard_map/ppermute | solution.py:327
  192.6 2.5 %collective-permute-start.26 = (bf16[128,1024]{1,0:T(8,128)(2,1)S(1)}, bf16[128,1024]{1,0:T(8,128)(2,1)S(1)}, u32[]{:S(2)}, u32[]{:S(2)}) collective-permute-start(bf16[128,1024]{1,0:T(8,128)(2,1)S(1)} %get-tuple-element.35), channel_id=1, source_target_pairs={{0,2},{2,0},{4,6},{6,4},{1,3},{3,1},{5,7},{7,5},{8,10},{10,8},{12,... | collective-permute-start | bytes 786440 | tf_op jit(solution)/shard_map/ppermute | solution.py:327
  195.1 3.9 %collective-permute-start.27 = (bf16[128,1024]{1,0:T(8,128)(2,1)S(1)}, bf16[128,1024]{1,0:T(8,128)(2,1)S(1)}, u32[]{:S(2)}, u32[]{:S(2)}) collective-permute-start(bf16[128,1024]{1,0:T(8,128)(2,1)S(1)} %get-tuple-element.36), channel_id=1, source_target_pairs={{0,6},{2,4},{4,2},{6,0},{1,7},{3,5},{5,3},{7,1},{8,14},{10,12},{12... | collective-permute-start | bytes 786440 | tf_op jit(solution)/shard_map/ppermute | solution.py:327
  199.0 2.7 %collective-permute-done.25.far = bf16[128,1024]{1,0:T(8,128)(2,1)S(1)} collective-permute-done((bf16[128,1024]{1,0:T(8,128)(2,1)S(1)}, bf16[128,1024]{1,0:T(8,128)(2,1)S(1)}, u32[]{:S(2)}, u32[]{:S(2)}) %collective-permute-start.25) | collective-permute-done | bytes 262176 | tf_op jit(solution)/shard_map/ppermute | solution.py:327
  201.7 3.5 %collective-permute-done.26.right = bf16[128,1024]{1,0:T(8,128)(2,1)S(1)} collective-permute-done((bf16[128,1024]{1,0:T(8,128)(2,1)S(1)}, bf16[128,1024]{1,0:T(8,128)(2,1)S(1)}, u32[]{:S(2)}, u32[]{:S(2)}) %collective-permute-start.26) | collective-permute-done | bytes 262176 | tf_op jit(solution)/shard_map/ppermute | solution.py:327
  205.3 1.5 collective-permute-done.27.left
  (46 shorter events, 10.2 us)
Async XLA Ops:
  2.1 64.5 %all-to-all-start = ((bf16[4,128,1024]{2,1,0:T(8,128)(2,1)}), bf16[4,128,1024]{2,1,0:T(8,128)(2,1)S(1)}, u32[]{:S(2)}, u32[]{:S(2)}) async-start(bf16[4,128,1024]{2,1,0:T(8,128)(2,1)} %shard_map.181), calls=%async_computation | async-start | bytes 2097152 | tf_op jit(solution)/shard_map/all_to_all | solution.py:76
  7.4 19.8 %collective-permute-start.1 = (bf16[32,2176]{1,0:T(8,128)(2,1)S(1)}, bf16[32,2176]{1,0:T(8,128)(2,1)S(1)}, u32[]{:S(2)}, u32[]{:S(2)}) collective-permute-start(bf16[32,2176]{1,0:T(8,128)(2,1)S(1)} %shard_map.182.refs_0_), channel_id=1, source_target_pairs={{0,32},{32,0},{64,96},{96,64},{128,160},{160,128},{192,224},{224,1... | collective-permute-start | bytes 417800 | tf_op jit(solution)/shard_map/ppermute | solution.py:387
  11.3 23.9 %collective-permute-start.2 = (bf16[32,2176]{1,0:T(8,128)(2,1)S(1)}, bf16[32,2176]{1,0:T(8,128)(2,1)S(1)}, u32[]{:S(2)}, u32[]{:S(2)}) collective-permute-start(bf16[32,2176]{1,0:T(8,128)(2,1)S(1)} %shard_map.182.refs_0_), channel_id=1, source_target_pairs={{0,64},{32,96},{64,0},{96,32},{128,192},{160,224},{192,128},{224,1... | collective-permute-start | bytes 417800 | tf_op jit(solution)/shard_map/ppermute | solution.py:387
  16.5 21.6 %collective-permute-start.3 = (bf16[32,2176]{1,0:T(8,128)(2,1)S(1)}, bf16[32,2176]{1,0:T(8,128)(2,1)S(1)}, u32[]{:S(2)}, u32[]{:S(2)}) collective-permute-start(bf16[32,2176]{1,0:T(8,128)(2,1)S(1)} %shard_map.182.refs_0_), channel_id=1, source_target_pairs={{0,96},{32,64},{64,32},{96,0},{128,224},{160,192},{192,160},{224,1... | collective-permute-start | bytes 417800 | tf_op jit(solution)/shard_map/ppermute | solution.py:387
  18.4 19.7 %collective-permute-start.4 = (bf16[32,2176]{1,0:T(8,128)(2,1)S(1)}, bf16[32,2176]{1,0:T(8,128)(2,1)S(1)}, u32[]{:S(2)}, u32[]{:S(2)}) collective-permute-start(bf16[32,2176]{1,0:T(8,128)(2,1)S(1)} %shard_map.182.refs_0_), channel_id=1, source_target_pairs={{0,128},{32,160},{64,192},{96,224},{128,0},{160,32},{192,64},{224,... | collective-permute-start | bytes 417800 | tf_op jit(solution)/shard_map/ppermute | solution.py:387
  22.8 23.1 %collective-permute-start.5 = (bf16[32,2176]{1,0:T(8,128)(2,1)S(1)}, bf16[32,2176]{1,0:T(8,128)(2,1)S(1)}, u32[]{:S(2)}, u32[]{:S(2)}) collective-permute-start(bf16[32,2176]{1,0:T(8,128)(2,1)S(1)} %shard_map.182.refs_0_), channel_id=1, source_target_pairs={{0,416},{32,128},{64,480},{96,192},{128,32},{160,256},{192,96},{22... | collective-permute-start | bytes 417800 | tf_op jit(solution)/shard_map/ppermute | solution.py:387
  27.3 21.6 %collective-permute-start.6 = (bf16[32,2176]{1,0:T(8,128)(2,1)S(1)}, bf16[32,2176]{1,0:T(8,128)(2,1)S(1)}, u32[]{:S(2)}, u32[]{:S(2)}) collective-permute-start(bf16[32,2176]{1,0:T(8,128)(2,1)S(1)} %shard_map.182.refs_0_), channel_id=1, source_target_pairs={{0,448},{32,480},{64,128},{96,160},{128,64},{160,96},{192,256},{22... | collective-permute-start | bytes 417800 | tf_op jit(solution)/shard_map/ppermute | solution.py:387
  35.1 19.6 %collective-permute-start.7 = (bf16[32,2176]{1,0:T(8,128)(2,1)S(1)}, bf16[32,2176]{1,0:T(8,128)(2,1)S(1)}, u32[]{:S(2)}, u32[]{:S(2)}) collective-permute-start(bf16[32,2176]{1,0:T(8,128)(2,1)S(1)} %shard_map.182.refs_0_), channel_id=1, source_target_pairs={{0,480},{32,448},{64,160},{96,128},{128,96},{160,64},{192,288},{22... | collective-permute-start | bytes 417800 | tf_op jit(solution)/shard_map/ppermute | solution.py:387
  55.4 0.8 copy-start.4
  56.2 18.1 %collective-permute-start.20 = (bf16[8,32,1152]{2,1,0:T(8,128)(2,1)S(1)}, bf16[8,32,1152]{2,1,0:T(8,128)(2,1)S(1)}, u32[]{:S(2)}, u32[]{:S(2)}) collective-permute-start(bf16[8,32,1152]{2,1,0:T(8,128)(2,1)S(1)} %get-tuple-element.33), channel_id=1, source_target_pairs={{0,8},{8,0},{16,24},{24,16},{1,9},{9,1},{17,25},{25,17},{2,10},{10... | collective-permute-start | bytes 1769480 | tf_op jit(solution)/shard_map/ppermute | solution.py:322
  59.6 28.8 %collective-permute-start.21 = (bf16[8,32,1152]{2,1,0:T(8,128)(2,1)S(1)}, bf16[8,32,1152]{2,1,0:T(8,128)(2,1)S(1)}, u32[]{:S(2)}, u32[]{:S(2)}) collective-permute-start(bf16[8,32,1152]{2,1,0:T(8,128)(2,1)S(1)} %get-tuple-element.33), channel_id=1, source_target_pairs={{0,16},{8,24},{16,0},{24,8},{1,17},{9,25},{17,1},{25,9},{2,18},{10... | collective-permute-start | bytes 1769480 | tf_op jit(solution)/shard_map/ppermute | solution.py:322
  64.5 30.4 %collective-permute-start.22 = (bf16[8,32,1152]{2,1,0:T(8,128)(2,1)S(1)}, bf16[8,32,1152]{2,1,0:T(8,128)(2,1)S(1)}, u32[]{:S(2)}, u32[]{:S(2)}) collective-permute-start(bf16[8,32,1152]{2,1,0:T(8,128)(2,1)S(1)} %get-tuple-element.33), channel_id=1, source_target_pairs={{0,24},{8,16},{16,8},{24,0},{1,25},{9,17},{17,9},{25,1},{2,26},{10... | collective-permute-start | bytes 1769480 | tf_op jit(solution)/shard_map/ppermute | solution.py:322
  66.6 64.6 %collective-permute-start = (bf16[512,1024]{1,0:T(8,128)(2,1)S(1)}, bf16[512,1024]{1,0:T(8,128)(2,1)S(1)}, u32[]{:S(2)}, u32[]{:S(2)}) collective-permute-start(bf16[512,1024]{1,0:T(8,128)(2,1)S(1)} %bitcast.27), channel_id=1, source_target_pairs={{0,1},{1,0},{2,3},{3,2},{4,5},{5,4},{6,7},{7,6},{8,9},{9,8},{10,11... | collective-permute-start | bytes 3145736 | tf_op jit(solution)/shard_map/ppermute | solution.py:72
  94.9 2.7 %copy-start.5 = (bf16[8,32,1024]{2,1,0:T(8,128)(2,1)S(1)}, bf16[8,32,1024]{2,1,0:T(8,128)(2,1)}, u32[]{:S(2)}) copy-start(bf16[8,32,1024]{2,1,0:T(8,128)(2,1)} %copy-done.4) | copy-start | bytes 1572868
  94.9 36.4 %copy-start.10 = (f32[2,1]{0,1:T(1,128)S(1)}, f32[2,1]{0,1:T(1,128)}, u32[]{:S(2)}) copy-start(f32[2,1]{0,1:T(1,128)} %param.25) | copy-start | bytes 28
  94.9 36.4 %copy-start.11 = (f32[1,128]{1,0:T(1,128)S(1)}, f32[1,128]{1,0:T(1,128)}, u32[]{:S(2)}) copy-start(f32[1,128]{1,0:T(1,128)} %constant.18.clone.frequency) | copy-start | bytes 1540
  95.6 88.8 %collective-permute-start.23 = (bf16[1024,1152]{1,0:T(8,128)(2,1)S(1)}, bf16[1024,1152]{1,0:T(8,128)(2,1)S(1)}, u32[]{:S(2)}, u32[]{:S(2)}) collective-permute-start(bf16[1024,1152]{1,0:T(8,128)(2,1)S(1)} %bitcast.23), channel_id=1, source_target_pairs={{0,1},{1,0},{2,3},{3,2},{4,5},{5,4},{6,7},{7,6},{8,9},{9,8},{10,11... | collective-permute-start | bytes 7077896 | tf_op jit(solution)/shard_map/ppermute | solution.py:72
  97.6 16.7 %collective-permute-start.8 = (bf16[8,32,1024]{2,1,0:T(8,128)(2,1)S(1)}, bf16[8,32,1024]{2,1,0:T(8,128)(2,1)S(1)}, u32[]{:S(2)}, u32[]{:S(2)}) collective-permute-start(bf16[8,32,1024]{2,1,0:T(8,128)(2,1)S(1)} %copy-done.5), channel_id=1, source_target_pairs={{0,8},{8,0},{16,24},{24,16},{1,9},{9,1},{17,25},{25,17},{2,10},{10... | collective-permute-start | bytes 1572872 | tf_op jit(solution)/shard_map/ppermute | solution.py:322
  99.5 25.4 %collective-permute-start.9 = (bf16[8,32,1024]{2,1,0:T(8,128)(2,1)S(1)}, bf16[8,32,1024]{2,1,0:T(8,128)(2,1)S(1)}, u32[]{:S(2)}, u32[]{:S(2)}) collective-permute-start(bf16[8,32,1024]{2,1,0:T(8,128)(2,1)S(1)} %copy-done.5), channel_id=1, source_target_pairs={{0,16},{8,24},{16,0},{24,8},{1,17},{9,25},{17,1},{25,9},{2,18},{10... | collective-permute-start | bytes 1572872 | tf_op jit(solution)/shard_map/ppermute | solution.py:322
  103.1 28.1 %collective-permute-start.10 = (bf16[8,32,1024]{2,1,0:T(8,128)(2,1)S(1)}, bf16[8,32,1024]{2,1,0:T(8,128)(2,1)S(1)}, u32[]{:S(2)}, u32[]{:S(2)}) collective-permute-start(bf16[8,32,1024]{2,1,0:T(8,128)(2,1)S(1)} %copy-done.5), channel_id=1, source_target_pairs={{0,24},{8,16},{16,8},{24,0},{1,25},{9,17},{17,9},{25,1},{2,26},{10... | collective-permute-start | bytes 1572872 | tf_op jit(solution)/shard_map/ppermute | solution.py:322
  135.4 25.7 %copy-start = (bf16[1,128,1024]{2,1,0:T(8,128)(2,1)S(1)}, bf16[1,128,1024]{2,1,0:T(8,128)(2,1)}, u32[]{:S(2)}) copy-start(bf16[1,128,1024]{2,1,0:T(8,128)(2,1)} %param.19) | copy-start | bytes 786436
  135.4 25.7 %copy-start.1 = (f32[1024]{0:T(1024)S(1)}, f32[1024]{0:T(1024)}, u32[]{:S(2)}) copy-start(f32[1024]{0:T(1024)} %param.27) | copy-start | bytes 12292
  135.4 25.7 %copy-start.2 = (f32[1024]{0:T(1024)S(1)}, f32[1024]{0:T(1024)}, u32[]{:S(2)}) copy-start(f32[1024]{0:T(1024)} %param.28) | copy-start | bytes 12292
  135.4 5.6 %collective-permute-start.12 = (bf16[1024,256]{1,0:T(8,128)(2,1)S(1)}, bf16[1024,256]{1,0:T(8,128)(2,1)S(1)}, u32[]{:S(2)}, u32[]{:S(2)}) collective-permute-start(bf16[1024,256]{1,0:T(8,128)(2,1)S(1)} %get-tuple-element.27.my_weights), channel_id=1, source_target_pairs={{0,1},{1,0},{2,3},{3,2},{4,5},{5,4},{6,7},{7,6},{8,9},{9,8},{10,11... | collective-permute-start | bytes 1572872 | tf_op jit(solution)/shard_map/ppermute | solution.py:72
  137.5 3.6 %collective-permute-start.11 = (bf16[512,256]{1,0:T(8,128)(2,1)S(1)}, bf16[512,256]{1,0:T(8,128)(2,1)S(1)}, u32[]{:S(2)}, u32[]{:S(2)}) collective-permute-start(bf16[512,256]{1,0:T(8,128)(2,1)S(1)} %get-tuple-element.26), channel_id=1, source_target_pairs={{0,1},{1,0},{2,3},{3,2},{4,5},{5,4},{6,7},{7,6},{8,9},{9,8},{10,11... | collective-permute-start | bytes 786440 | tf_op jit(solution)/shard_map/ppermute | solution.py:72
  141.0 40.1 %copy-start.6 = (f32[3,352]{1,0:T(4,128)S(1)}, f32[3,352]{1,0:T(4,128)}, u32[]{:S(2)}) copy-start(f32[3,352]{1,0:T(4,128)} %ge_kernel.1) | copy-start | bytes 12676
  141.0 40.1 %copy-start.7 = (f32[3,352]{1,0:T(4,128)S(1)}, f32[3,352]{1,0:T(4,128)}, u32[]{:S(2)}) copy-start(f32[3,352]{1,0:T(4,128)} %li_kernel.1) | copy-start | bytes 12676
  141.0 40.1 %copy-start.8 = (f32[352]{0:T(512)S(1)}, f32[352]{0:T(512)}, u32[]{:S(2)}) copy-start(f32[352]{0:T(512)} %ge_bias.1) | copy-start | bytes 4228
  141.0 40.1 %copy-start.9 = (f32[352]{0:T(512)S(1)}, f32[352]{0:T(512)}, u32[]{:S(2)}) copy-start(f32[352]{0:T(512)} %li_bias.1) | copy-start | bytes 4228
  142.3 12.6 %collective-permute-start.13 = (bf16[128,1024]{1,0:T(8,128)(2,1)S(1)}, bf16[128,1024]{1,0:T(8,128)(2,1)S(1)}, u32[]{:S(2)}, u32[]{:S(2)}) collective-permute-start(bf16[128,1024]{1,0:T(8,128)(2,1)S(1)} %get-tuple-element.28), channel_id=1, source_target_pairs={{0,4},{2,6},{4,0},{6,2},{1,5},{3,7},{5,1},{7,3},{8,12},{10,14},{12... | collective-permute-start | bytes 786440 | tf_op jit(solution)/shard_map/ppermute | solution.py:327
  147.5 12.7 %collective-permute-start.14 = (bf16[128,1024]{1,0:T(8,128)(2,1)S(1)}, bf16[128,1024]{1,0:T(8,128)(2,1)S(1)}, u32[]{:S(2)}, u32[]{:S(2)}) collective-permute-start(bf16[128,1024]{1,0:T(8,128)(2,1)S(1)} %get-tuple-element.29), channel_id=1, source_target_pairs={{0,2},{2,0},{4,6},{6,4},{1,3},{3,1},{5,7},{7,5},{8,10},{10,8},{12,... | collective-permute-start | bytes 786440 | tf_op jit(solution)/shard_map/ppermute | solution.py:327
  150.0 11.1 %collective-permute-start.15 = (bf16[128,1024]{1,0:T(8,128)(2,1)S(1)}, bf16[128,1024]{1,0:T(8,128)(2,1)S(1)}, u32[]{:S(2)}, u32[]{:S(2)}) collective-permute-start(bf16[128,1024]{1,0:T(8,128)(2,1)S(1)} %get-tuple-element.30), channel_id=1, source_target_pairs={{0,6},{2,4},{4,2},{6,0},{1,7},{3,5},{5,3},{7,1},{8,14},{10,12},{12... | collective-permute-start | bytes 786440 | tf_op jit(solution)/shard_map/ppermute | solution.py:327
  161.5 12.6 %collective-permute-start.16 = (bf16[128,1024]{1,0:T(8,128)(2,1)S(1)}, bf16[128,1024]{1,0:T(8,128)(2,1)S(1)}, u32[]{:S(2)}, u32[]{:S(2)}) collective-permute-start(bf16[128,1024]{1,0:T(8,128)(2,1)S(1)} %get-tuple-element.32.own), channel_id=1, source_target_pairs={{0,4},{2,6},{4,0},{6,2},{1,5},{3,7},{5,1},{7,3},{8,12},{10,14},{12... | collective-permute-start | bytes 786440 | tf_op jit(solution)/shard_map/ppermute | solution.py:327
  165.5 12.2 %collective-permute-start.17 = (bf16[128,1024]{1,0:T(8,128)(2,1)S(1)}, bf16[128,1024]{1,0:T(8,128)(2,1)S(1)}, u32[]{:S(2)}, u32[]{:S(2)}) collective-permute-start(bf16[128,1024]{1,0:T(8,128)(2,1)S(1)} %get-tuple-element.32.own), channel_id=1, source_target_pairs={{0,2},{2,0},{4,6},{6,4},{1,3},{3,1},{5,7},{7,5},{8,10},{10,8},{12,... | collective-permute-start | bytes 786440 | tf_op jit(solution)/shard_map/ppermute | solution.py:327
  168.0 11.2 %collective-permute-start.18 = (bf16[128,1024]{1,0:T(8,128)(2,1)S(1)}, bf16[128,1024]{1,0:T(8,128)(2,1)S(1)}, u32[]{:S(2)}, u32[]{:S(2)}) collective-permute-start(bf16[128,1024]{1,0:T(8,128)(2,1)S(1)} %get-tuple-element.32.own), channel_id=1, source_target_pairs={{0,6},{2,4},{4,2},{6,0},{1,7},{3,5},{5,3},{7,1},{8,14},{10,12},{12... | collective-permute-start | bytes 786440 | tf_op jit(solution)/shard_map/ppermute | solution.py:327
  179.2 5.2 %collective-permute-start.19 = (bf16[8,1024]{1,0:T(8,128)(2,1)S(1)}, bf16[8,1024]{1,0:T(8,128)(2,1)S(1)}, u32[]{:S(2)}, u32[]{:S(2)}) collective-permute-start(bf16[8,1024]{1,0:T(8,128)(2,1)S(1)} %shard_map.187), channel_id=1, source_target_pairs={{0,1},{1,0},{2,3},{3,2},{4,5},{5,4},{6,7},{7,6},{8,9},{9,8},{10,11... | collective-permute-start | bytes 49160 | tf_op jit(solution)/shard_map/ppermute | solution.py:72
  181.1 25.6 %copy-start.3 = (f32[1024]{0:T(1024)S(1)}, f32[1024]{0:T(1024)}, u32[]{:S(2)}) copy-start(f32[1024]{0:T(1024)} %param.36) | copy-start | bytes 12292
  181.2 3.2 %collective-permute-start.24 = (f32[8,384]{1,0:T(8,128)S(1)}, f32[8,384]{1,0:T(8,128)S(1)}, u32[]{:S(2)}, u32[]{:S(2)}) collective-permute-start(f32[8,384]{1,0:T(8,128)S(1)} %shard_map.189.my_taps), channel_id=1, source_target_pairs={{0,1},{1,0},{2,3},{3,2},{4,5},{5,4},{6,7},{7,6},{8,9},{9,8},{10,11... | collective-permute-start | bytes 36872 | tf_op jit(solution)/shard_map/ppermute | solution.py:72
  189.2 12.6 %collective-permute-start.25 = (bf16[128,1024]{1,0:T(8,128)(2,1)S(1)}, bf16[128,1024]{1,0:T(8,128)(2,1)S(1)}, u32[]{:S(2)}, u32[]{:S(2)}) collective-permute-start(bf16[128,1024]{1,0:T(8,128)(2,1)S(1)} %get-tuple-element.34), channel_id=1, source_target_pairs={{0,4},{2,6},{4,0},{6,2},{1,5},{3,7},{5,1},{7,3},{8,12},{10,14},{12... | collective-permute-start | bytes 786440 | tf_op jit(solution)/shard_map/ppermute | solution.py:327
  192.6 12.7 %collective-permute-start.26 = (bf16[128,1024]{1,0:T(8,128)(2,1)S(1)}, bf16[128,1024]{1,0:T(8,128)(2,1)S(1)}, u32[]{:S(2)}, u32[]{:S(2)}) collective-permute-start(bf16[128,1024]{1,0:T(8,128)(2,1)S(1)} %get-tuple-element.35), channel_id=1, source_target_pairs={{0,2},{2,0},{4,6},{6,4},{1,3},{3,1},{5,7},{7,5},{8,10},{10,8},{12,... | collective-permute-start | bytes 786440 | tf_op jit(solution)/shard_map/ppermute | solution.py:327
  195.1 11.7 %collective-permute-start.27 = (bf16[128,1024]{1,0:T(8,128)(2,1)S(1)}, bf16[128,1024]{1,0:T(8,128)(2,1)S(1)}, u32[]{:S(2)}, u32[]{:S(2)}) collective-permute-start(bf16[128,1024]{1,0:T(8,128)(2,1)S(1)} %get-tuple-element.36), channel_id=1, source_target_pairs={{0,6},{2,4},{4,2},{6,0},{1,7},{3,5},{5,3},{7,1},{8,14},{10,12},{12... | collective-permute-start | bytes 786440 | tf_op jit(solution)/shard_map/ppermute | solution.py:327

commit v8 on v7

--- a/solution.py
+++ b/solution.py
@@ -17,8 +17,9 @@
 RING = ("rep", "z")
 SWAP = ((0, 1), (1, 0))
 PAD = 384
-PROJECT, FIRST, THIRD = 2 * DK + 2 * DV, 2 * DK + 3 * DV, 3 * PAD
-Z_ISSUE = (4, 5, 6, 7, 3, 2, 1)
+FIRST, SECOND, THIRD = 2 * DK + 2 * DV, DV, 3 * PAD
+Z_SHIFTS = (4, 3, 2, 1, 0, -1, -2, -3)
+Z_ISSUE = (4, -3, 3, -2, 2, -1, 1)
 PARTNERS = (2, 1, 3)
 epsilon = 1e-06
 rope_base = 10000.0
@@ -58,14 +59,8 @@
     return [(i, i ^ k) for i in range(4)]
 
 
-def ring_pairs(k):
-    pairs = []
-    for i in range(16):
-        here = i // 8 * 8 + (i % 8 ^ k)
-        there = (here + 8) % 16
-        gap = min((here - i) % 16, (i - here) % 16)
-        pairs.append((i, here if gap <= 4 else there))
-    return pairs
+def ring_pairs(shift):
+    return [(i, (i + shift) % 16) for i in range(16)]
 
 
 def swap(value):
@@ -115,11 +110,12 @@
 
 
 def ring_order_body(index, *refs):
-    pieces, (one, three) = refs[:8], refs[8:]
-    for k, piece in enumerate(pieces):
-        at = index[2] ^ k
+    pieces, (one, two, three) = refs[:8], refs[8:]
+    for shift, piece in zip(Z_SHIFTS, pieces):
+        at = lax.rem(index[2] - shift + 8, 8)
         one[at] = piece[:, :FIRST]
-        three[at] = piece[:, FIRST:]
+        two[at] = piece[:, FIRST : FIRST + SECOND]
+        three[at] = piece[:, FIRST + SECOND :]
 
 
 def line_order_body(index, *refs):
@@ -161,15 +157,14 @@
 
 
 def attend_body(
-    index, logits, own, other, p0, p1, p2, p3, frequency, out_own, out_other, mo, w, qs, ks, vs, gs
+    index, logits, own, other, p0, p1, p2, p3, frequency, out_own, out_other, w, qs, ks, vs, gs
 ):
     y, core = index[1], index[3]
     for k, piece in enumerate((p0, p1, p2, p3)):
         at = (y ^ k) * 32
         for z in range(8):
             place = pl.ds(pl.multiple_of(z * 128 + at, 32), 32)
-            w[place, :] = piece[z * 32 : z * 32 + 32, :PROJECT]
-            mo[place, :] = piece[z * 32 : z * 32 + 32, PROJECT:]
+            w[place, :] = piece[z * 32 : z * 32 + 32, :]
     inside = lax.broadcasted_iota(jnp.int32, (128, DK), 0).astype(f32) * frequency[...]
     cos_in, sin_in = jnp.cos(inside), jnp.sin(inside)
     block = lax.broadcasted_iota(jnp.int32, (8, DK), 0)
@@ -323,6 +318,12 @@
     return [got[k].reshape(256, piece.shape[-1]) for k in range(4)]
 
 
+def in_line_order(pieces, place):
+    columns = pieces[0].shape[1]
+    ordered = call(line_order_body, shape((8, 4, 32, columns)), place, *pieces, smem=1)
+    return ordered.reshape(1024, columns)
+
+
 def sent(blocks):
     return [lax.ppermute(block, "x", line_pairs(k)) for k, block in zip(PARTNERS, blocks)]
 
@@ -376,7 +377,7 @@
     )
     packed = call(
         functools.partial(pack_body, width),
-        shape((32, FIRST + THIRD)),
+        shape((32, FIRST + SECOND + THIRD)),
         *parts,
         hbm=8,
         scratch=[pltpu.VMEM(part.shape, bf16) for part in parts]
@@ -390,14 +391,15 @@
     )
     normed_own = exchanged(spread).reshape(half, model)
     normed_other = swap(normed_own)
-    first_z, third_z = call(
+    first_z, second_z, third_z = call(
         ring_order_body,
-        [shape((8, 32, FIRST)), shape((8, 32, THIRD))],
+        [shape((8, 32, columns)) for columns in (FIRST, SECOND, THIRD)],
         place,
-        *[got[k] for k in range(8)],
+        *[got[k] for k in Z_SHIFTS],
         smem=1,
     )
     first_pieces = line_gather(first_z)
+    second_pieces = line_gather(second_z)
     third_pieces = line_gather(third_z)
     taps = call(
         functools.partial(taps_body, width),
@@ -408,9 +410,9 @@
         linear_bias,
     )
     taps_other = swap(taps)
-    gated_own, gated_other, out_own = call(
+    gated_own, gated_other = call(
         attend_body,
-        [shape((half, DV)), shape((half, DV)), shape((model, DV))],
+        [shape((half, DV)), shape((half, DV))],
         place,
         decay_logits[:, 0],
         normed_own,
@@ -421,7 +423,7 @@
         smem=2,
         limit=10,
         scratch=[
-            pltpu.VMEM((model, PROJECT), bf16),
+            pltpu.VMEM((model, FIRST), bf16),
             pltpu.VMEM((2 * half, DK), bf16),
             pltpu.VMEM((2 * half, DK), bf16),
             pltpu.VMEM((2 * half, DV), bf16),
@@ -429,6 +431,7 @@
         ],
     )
     gated_partner = swap(gated_other)
+    out_own = in_line_order(second_pieces, place)
     far, right, left, here = call(
         output_body,
         [shape((own, model))] * 4,
@@ -450,9 +453,7 @@
         row(mixer_out_gain),
         row(channel_in_gain),
     )
-    third_own = call(
-        line_order_body, shape((8, 4, 32, THIRD)), place, *third_pieces, smem=1
-    ).reshape(model, THIRD)
+    third_own = in_line_order(third_pieces, place)
     third_other = swap(third_own)
     blocks = (*sent([channel_in] * 3), channel_in)
     edges = call(edges_body, shape((8, model)), *blocks)

time: 209 us -> 213 us (1.019)
  the two profiles are of different devices: /device:TPU:128 before, /device:TPU:32 now
where the time goes in v8:
time: 213 us; the launch traced here: 212 us
  starting transfers between devices  112 us (53%)
  waiting for transfers between devices  80.1 us (38%)
  Pallas kernels  17.5 us (8%)
    ppermute x9, waiting for transfers between devices, line_gather(): got[k] = lax.ppermute(piece, 'y', line_pairs(k))  41.5 us
    ppermute x7, starting transfers between devices, layer(): got[k] = lax.ppermute(packed, RING, ring_pairs(k))  34.1 us
    ppermute x9, starting transfers between devices, line_gather(): got[k] = lax.ppermute(piece, 'y', line_pairs(k))  31.3 us
    ppermute x9, starting transfers between devices, sent(): lax.ppermute(block, 'x', line_pairs(k))  29.5 us
    ppermute x9, waiting for transfers between devices, sent(): lax.ppermute(block, 'x', line_pairs(k))  23.3 us
    pallas_call x12, Pallas kernels, call(): pl.pallas_call(body, out_shape=out_shapes, in_specs=specs, out_specs=VMEM...  17.5 us
    ppermute x7, waiting for transfers between devices, layer(): got[k] = lax.ppermute(packed, RING, ring_pairs(k))  13 us
    ppermute x6, starting transfers between devices, swap(): return lax.ppermute(value, 'c', SWAP)  12.6 us
  transfers between devices with their start and end apart: 32, of which 20 were waited for; matrix products, arithmetic and copies ran while one was open for 0% of the time, Pallas kernels for 5%

profile of v8, /device:TPU:32, one launch (start us, length us, event | category | flops | bytes accessed | tf_op | source)
XLA Modules:
  0.0 211.7 jit_solution(18208465782186620928)
XLA Ops:
  1.0 9.1 %collective-permute-start.1 = (bf16[32,2176]{1,0:T(8,128)(2,1)S(1)}, bf16[32,2176]{1,0:T(8,128)(2,1)S(1)}, u32[]{:S(2)}, u32[]{:S(2)}) collective-permute-start(bf16[32,2176]{1,0:T(8,128)(2,1)S(1)} %shard_map.182.refs_4_), channel_id=1, source_target_pairs={{0,128},{32,160},{64,192},{96,224},{128,256},{160,288},{192,320},{... | collective-permute-start | bytes 417800 | tf_op jit(solution)/shard_map/ppermute | solution.py:388
  10.1 7.7 %collective-permute-start.2 = (bf16[32,2176]{1,0:T(8,128)(2,1)S(1)}, bf16[32,2176]{1,0:T(8,128)(2,1)S(1)}, u32[]{:S(2)}, u32[]{:S(2)}) collective-permute-start(bf16[32,2176]{1,0:T(8,128)(2,1)S(1)} %shard_map.182.refs_4_), channel_id=1, source_target_pairs={{0,96},{32,128},{64,160},{96,192},{128,224},{160,256},{192,288},{2... | collective-permute-start | bytes 417800 | tf_op jit(solution)/shard_map/ppermute | solution.py:388
  17.9 2.1 shard_map.181
  20.0 4.3 %all-to-all-start = ((bf16[4,128,1024]{2,1,0:T(8,128)(2,1)}), bf16[4,128,1024]{2,1,0:T(8,128)(2,1)S(1)}, u32[]{:S(2)}, u32[]{:S(2)}) async-start(bf16[4,128,1024]{2,1,0:T(8,128)(2,1)} %shard_map.181), calls=%async_computation | async-start | bytes 2097152 | tf_op jit(solution)/shard_map/all_to_all | solution.py:71
  24.3 3.4 %collective-permute-start.3 = (bf16[32,2176]{1,0:T(8,128)(2,1)S(1)}, bf16[32,2176]{1,0:T(8,128)(2,1)S(1)}, u32[]{:S(2)}, u32[]{:S(2)}) collective-permute-start(bf16[32,2176]{1,0:T(8,128)(2,1)S(1)} %shard_map.182.refs_4_), channel_id=1, source_target_pairs={{0,64},{32,96},{64,128},{96,160},{128,192},{160,224},{192,256},{22... | collective-permute-start | bytes 417800 | tf_op jit(solution)/shard_map/ppermute | solution.py:388
  27.6 2.9 %collective-permute-start.4 = (bf16[32,2176]{1,0:T(8,128)(2,1)S(1)}, bf16[32,2176]{1,0:T(8,128)(2,1)S(1)}, u32[]{:S(2)}, u32[]{:S(2)}) collective-permute-start(bf16[32,2176]{1,0:T(8,128)(2,1)S(1)} %shard_map.182.refs_4_), channel_id=1, source_target_pairs={{0,32},{32,64},{64,96},{96,128},{128,160},{160,192},{192,224},{224... | collective-permute-start | bytes 417800 | tf_op jit(solution)/shard_map/ppermute | solution.py:388
  30.6 2.9 %collective-permute-start.5 = (bf16[32,2176]{1,0:T(8,128)(2,1)S(1)}, bf16[32,2176]{1,0:T(8,128)(2,1)S(1)}, u32[]{:S(2)}, u32[]{:S(2)}) collective-permute-start(bf16[32,2176]{1,0:T(8,128)(2,1)S(1)} %shard_map.182.refs_4_), channel_id=1, source_target_pairs={{0,480},{32,0},{64,32},{96,64},{128,96},{160,128},{192,160},{224,1... | collective-permute-start | bytes 417800 | tf_op jit(solution)/shard_map/ppermute | solution.py:388
  33.5 4.6 %collective-permute-start.6 = (bf16[32,2176]{1,0:T(8,128)(2,1)S(1)}, bf16[32,2176]{1,0:T(8,128)(2,1)S(1)}, u32[]{:S(2)}, u32[]{:S(2)}) collective-permute-start(bf16[32,2176]{1,0:T(8,128)(2,1)S(1)} %shard_map.182.refs_4_), channel_id=1, source_target_pairs={{0,448},{32,480},{64,0},{96,32},{128,64},{160,96},{192,128},{224,1... | collective-permute-start | bytes 417800 | tf_op jit(solution)/shard_map/ppermute | solution.py:388
  38.1 3.4 %collective-permute-start.7 = (bf16[32,2176]{1,0:T(8,128)(2,1)S(1)}, bf16[32,2176]{1,0:T(8,128)(2,1)S(1)}, u32[]{:S(2)}, u32[]{:S(2)}) collective-permute-start(bf16[32,2176]{1,0:T(8,128)(2,1)S(1)} %shard_map.182.refs_4_), channel_id=1, source_target_pairs={{0,416},{32,448},{64,480},{96,0},{128,32},{160,64},{192,96},{224,1... | collective-permute-start | bytes 417800 | tf_op jit(solution)/shard_map/ppermute | solution.py:388
  42.2 7.6 %collective-permute-done.6.refs_6_ = bf16[32,2176]{1,0:T(8,128)(2,1)S(1)} collective-permute-done((bf16[32,2176]{1,0:T(8,128)(2,1)S(1)}, bf16[32,2176]{1,0:T(8,128)(2,1)S(1)}, u32[]{:S(2)}, u32[]{:S(2)}) %collective-permute-start.6) | collective-permute-done | bytes 139296 | tf_op jit(solution)/shard_map/ppermute | solution.py:388
  49.8 4.8 %collective-permute-done.7.refs_7_ = bf16[32,2176]{1,0:T(8,128)(2,1)S(1)} collective-permute-done((bf16[32,2176]{1,0:T(8,128)(2,1)S(1)}, bf16[32,2176]{1,0:T(8,128)(2,1)S(1)}, u32[]{:S(2)}, u32[]{:S(2)}) %collective-permute-start.7) | collective-permute-done | bytes 139296 | tf_op jit(solution)/shard_map/ppermute | solution.py:388
  55.9 3.5 %collective-permute-start.23 = (bf16[8,32,1152]{2,1,0:T(8,128)(2,1)S(1)}, bf16[8,32,1152]{2,1,0:T(8,128)(2,1)S(1)}, u32[]{:S(2)}, u32[]{:S(2)}) collective-permute-start(bf16[8,32,1152]{2,1,0:T(8,128)(2,1)S(1)} %get-tuple-element.33), channel_id=1, source_target_pairs={{0,8},{8,0},{16,24},{24,16},{1,9},{9,1},{17,25},{25,17},{2,10},{10... | collective-permute-start | bytes 1769480 | tf_op jit(solution)/shard_map/ppermute | solution.py:317
  59.4 4.8 %collective-permute-start.24 = (bf16[8,32,1152]{2,1,0:T(8,128)(2,1)S(1)}, bf16[8,32,1152]{2,1,0:T(8,128)(2,1)S(1)}, u32[]{:S(2)}, u32[]{:S(2)}) collective-permute-start(bf16[8,32,1152]{2,1,0:T(8,128)(2,1)S(1)} %get-tuple-element.33), channel_id=1, source_target_pairs={{0,16},{8,24},{16,0},{24,8},{1,17},{9,25},{17,1},{25,9},{2,18},{10... | collective-permute-start | bytes 1769480 | tf_op jit(solution)/shard_map/ppermute | solution.py:317
  64.2 2.1 %collective-permute-start.25 = (bf16[8,32,1152]{2,1,0:T(8,128)(2,1)S(1)}, bf16[8,32,1152]{2,1,0:T(8,128)(2,1)S(1)}, u32[]{:S(2)}, u32[]{:S(2)}) collective-permute-start(bf16[8,32,1152]{2,1,0:T(8,128)(2,1)S(1)} %get-tuple-element.33), channel_id=1, source_target_pairs={{0,24},{8,16},{16,8},{24,0},{1,25},{9,17},{17,9},{25,1},{2,26},{10... | collective-permute-start | bytes 1769480 | tf_op jit(solution)/shard_map/ppermute | solution.py:317
  66.4 7.6 %collective-permute-done.23 = bf16[8,32,1152]{2,1,0:T(8,128)(2,1)S(1)} collective-permute-done((bf16[8,32,1152]{2,1,0:T(8,128)(2,1)S(1)}, bf16[8,32,1152]{2,1,0:T(8,128)(2,1)S(1)}, u32[]{:S(2)}, u32[]{:S(2)}) %collective-permute-start.23) | collective-permute-done | bytes 589856 | tf_op jit(solution)/shard_map/ppermute | solution.py:317
  74.0 13.4 %collective-permute-done.24 = bf16[8,32,1152]{2,1,0:T(8,128)(2,1)S(1)} collective-permute-done((bf16[8,32,1152]{2,1,0:T(8,128)(2,1)S(1)}, bf16[8,32,1152]{2,1,0:T(8,128)(2,1)S(1)}, u32[]{:S(2)}, u32[]{:S(2)}) %collective-permute-start.24) | collective-permute-done | bytes 589856 | tf_op jit(solution)/shard_map/ppermute | solution.py:317
  87.4 6.4 %collective-permute-done.25 = bf16[8,32,1152]{2,1,0:T(8,128)(2,1)S(1)} collective-permute-done((bf16[8,32,1152]{2,1,0:T(8,128)(2,1)S(1)}, bf16[8,32,1152]{2,1,0:T(8,128)(2,1)S(1)}, u32[]{:S(2)}, u32[]{:S(2)}) %collective-permute-start.25) | collective-permute-done | bytes 589856 | tf_op jit(solution)/shard_map/ppermute | solution.py:317
  94.6 1.9 collective-permute-start.26
  96.5 2.4 %collective-permute-start = (bf16[512,1024]{1,0:T(8,128)(2,1)S(1)}, bf16[512,1024]{1,0:T(8,128)(2,1)S(1)}, u32[]{:S(2)}, u32[]{:S(2)}) collective-permute-start(bf16[512,1024]{1,0:T(8,128)(2,1)S(1)} %bitcast.32), channel_id=1, source_target_pairs={{0,1},{1,0},{2,3},{3,2},{4,5},{5,4},{6,7},{7,6},{8,9},{9,8},{10,11... | collective-permute-start | bytes 3145736 | tf_op jit(solution)/shard_map/ppermute | solution.py:67
  98.9 1.9 collective-permute-start.12
  100.9 3.7 %collective-permute-start.13 = (bf16[8,32,256]{2,1,0:T(8,128)(2,1)S(1)}, bf16[8,32,256]{2,1,0:T(8,128)(2,1)S(1)}, u32[]{:S(2)}, u32[]{:S(2)}) collective-permute-start(bf16[8,32,256]{2,1,0:T(8,128)(2,1)S(1)} %get-tuple-element.27), channel_id=1, source_target_pairs={{0,16},{8,24},{16,0},{24,8},{1,17},{9,25},{17,1},{25,9},{2,18},{10... | collective-permute-start | bytes 393224 | tf_op jit(solution)/shard_map/ppermute | solution.py:317
  104.5 4.9 %collective-permute-start.14 = (bf16[8,32,256]{2,1,0:T(8,128)(2,1)S(1)}, bf16[8,32,256]{2,1,0:T(8,128)(2,1)S(1)}, u32[]{:S(2)}, u32[]{:S(2)}) collective-permute-start(bf16[8,32,256]{2,1,0:T(8,128)(2,1)S(1)} %get-tuple-element.27), channel_id=1, source_target_pairs={{0,24},{8,16},{16,8},{24,0},{1,25},{9,17},{17,9},{25,1},{2,26},{10... | collective-permute-start | bytes 393224 | tf_op jit(solution)/shard_map/ppermute | solution.py:317
  109.4 1.9 collective-permute-start.8
  111.3 3.7 %collective-permute-start.9 = (bf16[8,32,768]{2,1,0:T(8,128)(2,1)}, bf16[8,32,768]{2,1,0:T(8,128)(2,1)S(1)}, u32[]{:S(2)}, u32[]{:S(2)}) collective-permute-start(bf16[8,32,768]{2,1,0:T(8,128)(2,1)} %copy-done.4), channel_id=1, source_target_pairs={{0,16},{8,24},{16,0},{24,8},{1,17},{9,25},{17,1},{25,9},{2,18},{10... | collective-permute-start | bytes 1179656 | tf_op jit(solution)/shard_map/ppermute | solution.py:317
  115.0 4.9 %collective-permute-start.10 = (bf16[8,32,768]{2,1,0:T(8,128)(2,1)}, bf16[8,32,768]{2,1,0:T(8,128)(2,1)S(1)}, u32[]{:S(2)}, u32[]{:S(2)}) collective-permute-start(bf16[8,32,768]{2,1,0:T(8,128)(2,1)} %copy-done.4), channel_id=1, source_target_pairs={{0,24},{8,16},{16,8},{24,0},{1,25},{9,17},{17,9},{25,1},{2,26},{10... | collective-permute-start | bytes 1179656 | tf_op jit(solution)/shard_map/ppermute | solution.py:317
  120.4 3.0 %collective-permute-done.8 = bf16[8,32,768]{2,1,0:T(8,128)(2,1)S(1)} collective-permute-done((bf16[8,32,768]{2,1,0:T(8,128)(2,1)}, bf16[8,32,768]{2,1,0:T(8,128)(2,1)S(1)}, u32[]{:S(2)}, u32[]{:S(2)}) %collective-permute-start.8) | collective-permute-done | bytes 393248 | tf_op jit(solution)/shard_map/ppermute | solution.py:317
  125.4 4.5 %collective-permute-done.9 = bf16[8,32,768]{2,1,0:T(8,128)(2,1)S(1)} collective-permute-done((bf16[8,32,768]{2,1,0:T(8,128)(2,1)}, bf16[8,32,768]{2,1,0:T(8,128)(2,1)S(1)}, u32[]{:S(2)}, u32[]{:S(2)}) %collective-permute-start.9) | collective-permute-done | bytes 393248 | tf_op jit(solution)/shard_map/ppermute | solution.py:317
  129.9 6.4 %collective-permute-done.10 = bf16[8,32,768]{2,1,0:T(8,128)(2,1)S(1)} collective-permute-done((bf16[8,32,768]{2,1,0:T(8,128)(2,1)}, bf16[8,32,768]{2,1,0:T(8,128)(2,1)S(1)}, u32[]{:S(2)}, u32[]{:S(2)}) %collective-permute-start.10) | collective-permute-done | bytes 393248 | tf_op jit(solution)/shard_map/ppermute | solution.py:317
  137.4 4.1 %shard_map.184 = (bf16[512,256]{1,0:T(8,128)(2,1)S(1)}, bf16[512,256]{1,0:T(8,128)(2,1)S(1)}) custom-call(s32[4]{0:T(128)S(1)} %pad_add_fusion.index, f32[2]{0:T(128)S(1)} %bitcast.51, bf16[512,1024]{1,0:T(8,128)(2,1)S(1)} %bitcast.33, bf16[512,1024]{1,0:T(8,128)(2,1)S(1)} %collective-permute-done.other, bf16[256,768]{1,0:T(8,128)(2,1)S(1)} %bitcast.47, ...), custom_call_target="tpu_custom_call" | custom-call | flops 4294967296 | bytes 2097152 | tf_op jit(solution)/shard_map/pallas_call | solution.py:41
  141.5 2.1 collective-permute-start.11
  146.3 3.7 %collective-permute-start.16 = (bf16[128,1024]{1,0:T(8,128)(2,1)S(1)}, bf16[128,1024]{1,0:T(8,128)(2,1)S(1)}, u32[]{:S(2)}, u32[]{:S(2)}) collective-permute-start(bf16[128,1024]{1,0:T(8,128)(2,1)S(1)} %get-tuple-element.28), channel_id=1, source_target_pairs={{0,4},{2,6},{4,0},{6,2},{1,5},{3,7},{5,1},{7,3},{8,12},{10,14},{12... | collective-permute-start | bytes 786440 | tf_op jit(solution)/shard_map/ppermute | solution.py:328
  150.0 2.8 %collective-permute-start.17 = (bf16[128,1024]{1,0:T(8,128)(2,1)S(1)}, bf16[128,1024]{1,0:T(8,128)(2,1)S(1)}, u32[]{:S(2)}, u32[]{:S(2)}) collective-permute-start(bf16[128,1024]{1,0:T(8,128)(2,1)S(1)} %get-tuple-element.29), channel_id=1, source_target_pairs={{0,2},{2,0},{4,6},{6,4},{1,3},{3,1},{5,7},{7,5},{8,10},{10,8},{12,... | collective-permute-start | bytes 786440 | tf_op jit(solution)/shard_map/ppermute | solution.py:328
  152.8 3.3 %collective-permute-start.18 = (bf16[128,1024]{1,0:T(8,128)(2,1)S(1)}, bf16[128,1024]{1,0:T(8,128)(2,1)S(1)}, u32[]{:S(2)}, u32[]{:S(2)}) collective-permute-start(bf16[128,1024]{1,0:T(8,128)(2,1)S(1)} %get-tuple-element.30), channel_id=1, source_target_pairs={{0,6},{2,4},{4,2},{6,0},{1,7},{3,5},{5,3},{7,1},{8,14},{10,12},{12... | collective-permute-start | bytes 786440 | tf_op jit(solution)/shard_map/ppermute | solution.py:328
  156.2 2.7 %collective-permute-done.16.far = bf16[128,1024]{1,0:T(8,128)(2,1)S(1)} collective-permute-done((bf16[128,1024]{1,0:T(8,128)(2,1)S(1)}, bf16[128,1024]{1,0:T(8,128)(2,1)S(1)}, u32[]{:S(2)}, u32[]{:S(2)}) %collective-permute-start.16) | collective-permute-done | bytes 262176 | tf_op jit(solution)/shard_map/ppermute | solution.py:328
  158.9 3.9 %collective-permute-done.17.right = bf16[128,1024]{1,0:T(8,128)(2,1)S(1)} collective-permute-done((bf16[128,1024]{1,0:T(8,128)(2,1)S(1)}, bf16[128,1024]{1,0:T(8,128)(2,1)S(1)}, u32[]{:S(2)}, u32[]{:S(2)}) %collective-permute-start.17) | collective-permute-done | bytes 262176 | tf_op jit(solution)/shard_map/ppermute | solution.py:328
  164.5 3.2 %collective-permute-start.19 = (bf16[128,1024]{1,0:T(8,128)(2,1)S(1)}, bf16[128,1024]{1,0:T(8,128)(2,1)S(1)}, u32[]{:S(2)}, u32[]{:S(2)}) collective-permute-start(bf16[128,1024]{1,0:T(8,128)(2,1)S(1)} %get-tuple-element.32.own), channel_id=1, source_target_pairs={{0,4},{2,6},{4,0},{6,2},{1,5},{3,7},{5,1},{7,3},{8,12},{10,14},{12... | collective-permute-start | bytes 786440 | tf_op jit(solution)/shard_map/ppermute | solution.py:328
  167.8 3.0 %collective-permute-start.20 = (bf16[128,1024]{1,0:T(8,128)(2,1)S(1)}, bf16[128,1024]{1,0:T(8,128)(2,1)S(1)}, u32[]{:S(2)}, u32[]{:S(2)}) collective-permute-start(bf16[128,1024]{1,0:T(8,128)(2,1)S(1)} %get-tuple-element.32.own), channel_id=1, source_target_pairs={{0,2},{2,0},{4,6},{6,4},{1,3},{3,1},{5,7},{7,5},{8,10},{10,8},{12,... | collective-permute-start | bytes 786440 | tf_op jit(solution)/shard_map/ppermute | solution.py:328
  170.8 3.5 %collective-permute-start.21 = (bf16[128,1024]{1,0:T(8,128)(2,1)S(1)}, bf16[128,1024]{1,0:T(8,128)(2,1)S(1)}, u32[]{:S(2)}, u32[]{:S(2)}) collective-permute-start(bf16[128,1024]{1,0:T(8,128)(2,1)S(1)} %get-tuple-element.32.own), channel_id=1, source_target_pairs={{0,6},{2,4},{4,2},{6,0},{1,7},{3,5},{5,3},{7,1},{8,14},{10,12},{12... | collective-permute-start | bytes 786440 | tf_op jit(solution)/shard_map/ppermute | solution.py:328
  174.4 2.7 %collective-permute-done.19.far.got_far = bf16[128,1024]{1,0:T(8,128)(2,1)S(1)} collective-permute-done((bf16[128,1024]{1,0:T(8,128)(2,1)S(1)}, bf16[128,1024]{1,0:T(8,128)(2,1)S(1)}, u32[]{:S(2)}, u32[]{:S(2)}) %collective-permute-start.19) | collective-permute-done | bytes 262176 | tf_op jit(solution)/shard_map/ppermute | solution.py:328
  177.1 2.9 %collective-permute-done.20.after.got_next = bf16[128,1024]{1,0:T(8,128)(2,1)S(1)} collective-permute-done((bf16[128,1024]{1,0:T(8,128)(2,1)S(1)}, bf16[128,1024]{1,0:T(8,128)(2,1)S(1)}, u32[]{:S(2)}, u32[]{:S(2)}) %collective-permute-start.20) | collective-permute-done | bytes 262176 | tf_op jit(solution)/shard_map/ppermute | solution.py:328
  181.8 1.9 collective-permute-start.22
  183.8 2.4 %collective-permute-start.27 = (f32[8,384]{1,0:T(8,128)S(1)}, f32[8,384]{1,0:T(8,128)S(1)}, u32[]{:S(2)}, u32[]{:S(2)}) collective-permute-start(f32[8,384]{1,0:T(8,128)S(1)} %shard_map.190.my_taps), channel_id=1, source_target_pairs={{0,1},{1,0},{2,3},{3,2},{4,5},{5,4},{6,7},{7,6},{8,9},{9,8},{10,11... | collective-permute-start | bytes 36872 | tf_op jit(solution)/shard_map/ppermute | solution.py:67
  187.1 5.8 %shard_map.191 = (bf16[128,1024]{1,0:T(8,128)(2,1)S(1)}, bf16[128,1024]{1,0:T(8,128)(2,1)S(1)}, bf16[128,1024]{1,0:T(8,128)(2,1)S(1)}, bf16[128,1024]{1,0:T(8,128)(2,1)S(1)}) custom-call(s32[4]{0:T(128)S(1)} %pad_add_fusion.index, bf16[128,1024]{1,0:T(8,128)(2,1)S(1)} %collective-permute-done.19.far.got_far, ...), custom_call_target="tpu_custom_call" | custom-call | flops 4294967296 | bytes 2097152 | tf_op jit(solution)/shard_map/pallas_call | solution.py:41
  192.9 2.9 %collective-permute-start.28 = (bf16[128,1024]{1,0:T(8,128)(2,1)S(1)}, bf16[128,1024]{1,0:T(8,128)(2,1)S(1)}, u32[]{:S(2)}, u32[]{:S(2)}) collective-permute-start(bf16[128,1024]{1,0:T(8,128)(2,1)S(1)} %get-tuple-element.34), channel_id=1, source_target_pairs={{0,4},{2,6},{4,0},{6,2},{1,5},{3,7},{5,1},{7,3},{8,12},{10,14},{12... | collective-permute-start | bytes 786440 | tf_op jit(solution)/shard_map/ppermute | solution.py:328
  195.8 3.3 %collective-permute-start.29 = (bf16[128,1024]{1,0:T(8,128)(2,1)S(1)}, bf16[128,1024]{1,0:T(8,128)(2,1)S(1)}, u32[]{:S(2)}, u32[]{:S(2)}) collective-permute-start(bf16[128,1024]{1,0:T(8,128)(2,1)S(1)} %get-tuple-element.35), channel_id=1, source_target_pairs={{0,2},{2,0},{4,6},{6,4},{1,3},{3,1},{5,7},{7,5},{8,10},{10,8},{12,... | collective-permute-start | bytes 786440 | tf_op jit(solution)/shard_map/ppermute | solution.py:328
  199.1 3.6 %collective-permute-start.30 = (bf16[128,1024]{1,0:T(8,128)(2,1)S(1)}, bf16[128,1024]{1,0:T(8,128)(2,1)S(1)}, u32[]{:S(2)}, u32[]{:S(2)}) collective-permute-start(bf16[128,1024]{1,0:T(8,128)(2,1)S(1)} %get-tuple-element.36), channel_id=1, source_target_pairs={{0,6},{2,4},{4,2},{6,0},{1,7},{3,5},{5,3},{7,1},{8,14},{10,12},{12... | collective-permute-start | bytes 786440 | tf_op jit(solution)/shard_map/ppermute | solution.py:328
  202.8 2.7 %collective-permute-done.28.far = bf16[128,1024]{1,0:T(8,128)(2,1)S(1)} collective-permute-done((bf16[128,1024]{1,0:T(8,128)(2,1)S(1)}, bf16[128,1024]{1,0:T(8,128)(2,1)S(1)}, u32[]{:S(2)}, u32[]{:S(2)}) %collective-permute-start.28) | collective-permute-done | bytes 262176 | tf_op jit(solution)/shard_map/ppermute | solution.py:328
  205.5 3.8 %collective-permute-done.29.right = bf16[128,1024]{1,0:T(8,128)(2,1)S(1)} collective-permute-done((bf16[128,1024]{1,0:T(8,128)(2,1)S(1)}, bf16[128,1024]{1,0:T(8,128)(2,1)S(1)}, u32[]{:S(2)}, u32[]{:S(2)}) %collective-permute-start.29) | collective-permute-done | bytes 262176 | tf_op jit(solution)/shard_map/ppermute | solution.py:328
  (53 shorter events, 16.7 us)
Async XLA Ops:
  1.0 32.5 %collective-permute-start.1 = (bf16[32,2176]{1,0:T(8,128)(2,1)S(1)}, bf16[32,2176]{1,0:T(8,128)(2,1)S(1)}, u32[]{:S(2)}, u32[]{:S(2)}) collective-permute-start(bf16[32,2176]{1,0:T(8,128)(2,1)S(1)} %shard_map.182.refs_4_), channel_id=1, source_target_pairs={{0,128},{32,160},{64,192},{96,224},{128,256},{160,288},{192,320},{... | collective-permute-start | bytes 417800 | tf_op jit(solution)/shard_map/ppermute | solution.py:388
  10.1 28.0 %collective-permute-start.2 = (bf16[32,2176]{1,0:T(8,128)(2,1)S(1)}, bf16[32,2176]{1,0:T(8,128)(2,1)S(1)}, u32[]{:S(2)}, u32[]{:S(2)}) collective-permute-start(bf16[32,2176]{1,0:T(8,128)(2,1)S(1)} %shard_map.182.refs_4_), channel_id=1, source_target_pairs={{0,96},{32,128},{64,160},{96,192},{128,224},{160,256},{192,288},{2... | collective-permute-start | bytes 417800 | tf_op jit(solution)/shard_map/ppermute | solution.py:388
  20.0 76.5 %all-to-all-start = ((bf16[4,128,1024]{2,1,0:T(8,128)(2,1)}), bf16[4,128,1024]{2,1,0:T(8,128)(2,1)S(1)}, u32[]{:S(2)}, u32[]{:S(2)}) async-start(bf16[4,128,1024]{2,1,0:T(8,128)(2,1)} %shard_map.181), calls=%async_computation | async-start | bytes 2097152 | tf_op jit(solution)/shard_map/all_to_all | solution.py:71
  24.3 17.3 %collective-permute-start.3 = (bf16[32,2176]{1,0:T(8,128)(2,1)S(1)}, bf16[32,2176]{1,0:T(8,128)(2,1)S(1)}, u32[]{:S(2)}, u32[]{:S(2)}) collective-permute-start(bf16[32,2176]{1,0:T(8,128)(2,1)S(1)} %shard_map.182.refs_4_), channel_id=1, source_target_pairs={{0,64},{32,96},{64,128},{96,160},{128,192},{160,224},{192,256},{22... | collective-permute-start | bytes 417800 | tf_op jit(solution)/shard_map/ppermute | solution.py:388
  27.6 14.5 %collective-permute-start.4 = (bf16[32,2176]{1,0:T(8,128)(2,1)S(1)}, bf16[32,2176]{1,0:T(8,128)(2,1)S(1)}, u32[]{:S(2)}, u32[]{:S(2)}) collective-permute-start(bf16[32,2176]{1,0:T(8,128)(2,1)S(1)} %shard_map.182.refs_4_), channel_id=1, source_target_pairs={{0,32},{32,64},{64,96},{96,128},{128,160},{160,192},{192,224},{224... | collective-permute-start | bytes 417800 | tf_op jit(solution)/shard_map/ppermute | solution.py:388
  30.6 11.6 %collective-permute-start.5 = (bf16[32,2176]{1,0:T(8,128)(2,1)S(1)}, bf16[32,2176]{1,0:T(8,128)(2,1)S(1)}, u32[]{:S(2)}, u32[]{:S(2)}) collective-permute-start(bf16[32,2176]{1,0:T(8,128)(2,1)S(1)} %shard_map.182.refs_4_), channel_id=1, source_target_pairs={{0,480},{32,0},{64,32},{96,64},{128,96},{160,128},{192,160},{224,1... | collective-permute-start | bytes 417800 | tf_op jit(solution)/shard_map/ppermute | solution.py:388
  33.5 16.3 %collective-permute-start.6 = (bf16[32,2176]{1,0:T(8,128)(2,1)S(1)}, bf16[32,2176]{1,0:T(8,128)(2,1)S(1)}, u32[]{:S(2)}, u32[]{:S(2)}) collective-permute-start(bf16[32,2176]{1,0:T(8,128)(2,1)S(1)} %shard_map.182.refs_4_), channel_id=1, source_target_pairs={{0,448},{32,480},{64,0},{96,32},{128,64},{160,96},{192,128},{224,1... | collective-permute-start | bytes 417800 | tf_op jit(solution)/shard_map/ppermute | solution.py:388
  38.1 16.5 %collective-permute-start.7 = (bf16[32,2176]{1,0:T(8,128)(2,1)S(1)}, bf16[32,2176]{1,0:T(8,128)(2,1)S(1)}, u32[]{:S(2)}, u32[]{:S(2)}) collective-permute-start(bf16[32,2176]{1,0:T(8,128)(2,1)S(1)} %shard_map.182.refs_4_), channel_id=1, source_target_pairs={{0,416},{32,448},{64,480},{96,0},{128,32},{160,64},{192,96},{224,1... | collective-permute-start | bytes 417800 | tf_op jit(solution)/shard_map/ppermute | solution.py:388
  55.2 0.7 copy-start.4
  55.9 18.1 %collective-permute-start.23 = (bf16[8,32,1152]{2,1,0:T(8,128)(2,1)S(1)}, bf16[8,32,1152]{2,1,0:T(8,128)(2,1)S(1)}, u32[]{:S(2)}, u32[]{:S(2)}) collective-permute-start(bf16[8,32,1152]{2,1,0:T(8,128)(2,1)S(1)} %get-tuple-element.33), channel_id=1, source_target_pairs={{0,8},{8,0},{16,24},{24,16},{1,9},{9,1},{17,25},{25,17},{2,10},{10... | collective-permute-start | bytes 1769480 | tf_op jit(solution)/shard_map/ppermute | solution.py:317
  59.4 28.0 %collective-permute-start.24 = (bf16[8,32,1152]{2,1,0:T(8,128)(2,1)S(1)}, bf16[8,32,1152]{2,1,0:T(8,128)(2,1)S(1)}, u32[]{:S(2)}, u32[]{:S(2)}) collective-permute-start(bf16[8,32,1152]{2,1,0:T(8,128)(2,1)S(1)} %get-tuple-element.33), channel_id=1, source_target_pairs={{0,16},{8,24},{16,0},{24,8},{1,17},{9,25},{17,1},{25,9},{2,18},{10... | collective-permute-start | bytes 1769480 | tf_op jit(solution)/shard_map/ppermute | solution.py:317
  64.2 29.6 %collective-permute-start.25 = (bf16[8,32,1152]{2,1,0:T(8,128)(2,1)S(1)}, bf16[8,32,1152]{2,1,0:T(8,128)(2,1)S(1)}, u32[]{:S(2)}, u32[]{:S(2)}) collective-permute-start(bf16[8,32,1152]{2,1,0:T(8,128)(2,1)S(1)} %get-tuple-element.33), channel_id=1, source_target_pairs={{0,24},{8,16},{16,8},{24,0},{1,25},{9,17},{17,9},{25,1},{2,26},{10... | collective-permute-start | bytes 1769480 | tf_op jit(solution)/shard_map/ppermute | solution.py:317
  93.8 42.5 %copy-start.10 = (f32[2,1]{0,1:T(1,128)S(1)}, f32[2,1]{0,1:T(1,128)}, u32[]{:S(2)}) copy-start(f32[2,1]{0,1:T(1,128)} %param.25) | copy-start | bytes 28
  93.8 42.5 %copy-start.11 = (f32[1,128]{1,0:T(1,128)S(1)}, f32[1,128]{1,0:T(1,128)}, u32[]{:S(2)}) copy-start(f32[1,128]{1,0:T(1,128)} %constant.18.clone.frequency) | copy-start | bytes 1540
  94.6 92.5 %collective-permute-start.26 = (bf16[1024,1152]{1,0:T(8,128)(2,1)S(1)}, bf16[1024,1152]{1,0:T(8,128)(2,1)}, u32[]{:S(2)}, u32[]{:S(2)}) collective-permute-start(bf16[1024,1152]{1,0:T(8,128)(2,1)S(1)} %bitcast.28), channel_id=1, source_target_pairs={{0,1},{1,0},{2,3},{3,2},{4,5},{5,4},{6,7},{7,6},{8,9},{9,8},{10,11... | collective-permute-start | bytes 7077896 | tf_op jit(solution)/shard_map/ppermute | solution.py:67
  96.5 39.9 %collective-permute-start = (bf16[512,1024]{1,0:T(8,128)(2,1)S(1)}, bf16[512,1024]{1,0:T(8,128)(2,1)S(1)}, u32[]{:S(2)}, u32[]{:S(2)}) collective-permute-start(bf16[512,1024]{1,0:T(8,128)(2,1)S(1)} %bitcast.32), channel_id=1, source_target_pairs={{0,1},{1,0},{2,3},{3,2},{4,5},{5,4},{6,7},{7,6},{8,9},{9,8},{10,11... | collective-permute-start | bytes 3145736 | tf_op jit(solution)/shard_map/ppermute | solution.py:67
  98.9 10.4 %collective-permute-start.12 = (bf16[8,32,256]{2,1,0:T(8,128)(2,1)S(1)}, bf16[8,32,256]{2,1,0:T(8,128)(2,1)S(1)}, u32[]{:S(2)}, u32[]{:S(2)}) collective-permute-start(bf16[8,32,256]{2,1,0:T(8,128)(2,1)S(1)} %get-tuple-element.27), channel_id=1, source_target_pairs={{0,8},{8,0},{16,24},{24,16},{1,9},{9,1},{17,25},{25,17},{2,10},{10... | collective-permute-start | bytes 393224 | tf_op jit(solution)/shard_map/ppermute | solution.py:317
  100.9 10.5 %collective-permute-start.13 = (bf16[8,32,256]{2,1,0:T(8,128)(2,1)S(1)}, bf16[8,32,256]{2,1,0:T(8,128)(2,1)S(1)}, u32[]{:S(2)}, u32[]{:S(2)}) collective-permute-start(bf16[8,32,256]{2,1,0:T(8,128)(2,1)S(1)} %get-tuple-element.27), channel_id=1, source_target_pairs={{0,16},{8,24},{16,0},{24,8},{1,17},{9,25},{17,1},{25,9},{2,18},{10... | collective-permute-start | bytes 393224 | tf_op jit(solution)/shard_map/ppermute | solution.py:317
  104.5 10.5 %collective-permute-start.14 = (bf16[8,32,256]{2,1,0:T(8,128)(2,1)S(1)}, bf16[8,32,256]{2,1,0:T(8,128)(2,1)S(1)}, u32[]{:S(2)}, u32[]{:S(2)}) collective-permute-start(bf16[8,32,256]{2,1,0:T(8,128)(2,1)S(1)} %get-tuple-element.27), channel_id=1, source_target_pairs={{0,24},{8,16},{16,8},{24,0},{1,25},{9,17},{17,9},{25,1},{2,26},{10... | collective-permute-start | bytes 393224 | tf_op jit(solution)/shard_map/ppermute | solution.py:317
  109.4 14.1 %collective-permute-start.8 = (bf16[8,32,768]{2,1,0:T(8,128)(2,1)}, bf16[8,32,768]{2,1,0:T(8,128)(2,1)S(1)}, u32[]{:S(2)}, u32[]{:S(2)}) collective-permute-start(bf16[8,32,768]{2,1,0:T(8,128)(2,1)} %copy-done.4), channel_id=1, source_target_pairs={{0,8},{8,0},{16,24},{24,16},{1,9},{9,1},{17,25},{25,17},{2,10},{10... | collective-permute-start | bytes 1179656 | tf_op jit(solution)/shard_map/ppermute | solution.py:317
  111.3 18.6 %collective-permute-start.9 = (bf16[8,32,768]{2,1,0:T(8,128)(2,1)}, bf16[8,32,768]{2,1,0:T(8,128)(2,1)S(1)}, u32[]{:S(2)}, u32[]{:S(2)}) collective-permute-start(bf16[8,32,768]{2,1,0:T(8,128)(2,1)} %copy-done.4), channel_id=1, source_target_pairs={{0,16},{8,24},{16,0},{24,8},{1,17},{9,25},{17,1},{25,9},{2,18},{10... | collective-permute-start | bytes 1179656 | tf_op jit(solution)/shard_map/ppermute | solution.py:317
  115.0 21.4 %collective-permute-start.10 = (bf16[8,32,768]{2,1,0:T(8,128)(2,1)}, bf16[8,32,768]{2,1,0:T(8,128)(2,1)S(1)}, u32[]{:S(2)}, u32[]{:S(2)}) collective-permute-start(bf16[8,32,768]{2,1,0:T(8,128)(2,1)} %copy-done.4), channel_id=1, source_target_pairs={{0,24},{8,16},{16,8},{24,0},{1,25},{9,17},{17,9},{25,1},{2,26},{10... | collective-permute-start | bytes 1179656 | tf_op jit(solution)/shard_map/ppermute | solution.py:317
  123.5 20.1 %collective-permute-start.15 = (bf16[1024,256]{1,0:T(8,128)(2,1)S(1)}, bf16[1024,256]{1,0:T(8,128)(2,1)S(1)}, u32[]{:S(2)}, u32[]{:S(2)}) collective-permute-start(bf16[1024,256]{1,0:T(8,128)(2,1)S(1)} %bitcast.38), channel_id=1, source_target_pairs={{0,1},{1,0},{2,3},{3,2},{4,5},{5,4},{6,7},{7,6},{8,9},{9,8},{10,11... | collective-permute-start | bytes 1572872 | tf_op jit(solution)/shard_map/ppermute | solution.py:67
  136.4 1.0 copy-start.5
  141.4 22.7 %copy-start = (bf16[1,128,1024]{2,1,0:T(8,128)(2,1)S(1)}, bf16[1,128,1024]{2,1,0:T(8,128)(2,1)}, u32[]{:S(2)}) copy-start(bf16[1,128,1024]{2,1,0:T(8,128)(2,1)} %param.19) | copy-start | bytes 786436
  141.5 22.7 %copy-start.1 = (f32[1024]{0:T(1024)S(1)}, f32[1024]{0:T(1024)}, u32[]{:S(2)}) copy-start(f32[1024]{0:T(1024)} %param.27) | copy-start | bytes 12292
  141.5 22.7 %copy-start.2 = (f32[1024]{0:T(1024)S(1)}, f32[1024]{0:T(1024)}, u32[]{:S(2)}) copy-start(f32[1024]{0:T(1024)} %param.28) | copy-start | bytes 12292
  141.5 3.6 %collective-permute-start.11 = (bf16[512,256]{1,0:T(8,128)(2,1)S(1)}, bf16[512,256]{1,0:T(8,128)(2,1)S(1)}, u32[]{:S(2)}, u32[]{:S(2)}) collective-permute-start(bf16[512,256]{1,0:T(8,128)(2,1)S(1)} %get-tuple-element.26), channel_id=1, source_target_pairs={{0,1},{1,0},{2,3},{3,2},{4,5},{5,4},{6,7},{7,6},{8,9},{9,8},{10,11... | collective-permute-start | bytes 786440 | tf_op jit(solution)/shard_map/ppermute | solution.py:67
  145.0 38.7 %copy-start.6 = (f32[3,352]{1,0:T(4,128)S(1)}, f32[3,352]{1,0:T(4,128)}, u32[]{:S(2)}) copy-start(f32[3,352]{1,0:T(4,128)} %ge_kernel.1) | copy-start | bytes 12676
  145.0 38.7 %copy-start.7 = (f32[3,352]{1,0:T(4,128)S(1)}, f32[3,352]{1,0:T(4,128)}, u32[]{:S(2)}) copy-start(f32[3,352]{1,0:T(4,128)} %li_kernel.1) | copy-start | bytes 12676
  145.0 38.7 %copy-start.8 = (f32[352]{0:T(512)S(1)}, f32[352]{0:T(512)}, u32[]{:S(2)}) copy-start(f32[352]{0:T(512)} %ge_bias.1) | copy-start | bytes 4228
  145.0 38.8 %copy-start.9 = (f32[352]{0:T(512)S(1)}, f32[352]{0:T(512)}, u32[]{:S(2)}) copy-start(f32[352]{0:T(512)} %li_bias.1) | copy-start | bytes 4228
  146.3 12.6 %collective-permute-start.16 = (bf16[128,1024]{1,0:T(8,128)(2,1)S(1)}, bf16[128,1024]{1,0:T(8,128)(2,1)S(1)}, u32[]{:S(2)}, u32[]{:S(2)}) collective-permute-start(bf16[128,1024]{1,0:T(8,128)(2,1)S(1)} %get-tuple-element.28), channel_id=1, source_target_pairs={{0,4},{2,6},{4,0},{6,2},{1,5},{3,7},{5,1},{7,3},{8,12},{10,14},{12... | collective-permute-start | bytes 786440 | tf_op jit(solution)/shard_map/ppermute | solution.py:328
  150.0 12.8 %collective-permute-start.17 = (bf16[128,1024]{1,0:T(8,128)(2,1)S(1)}, bf16[128,1024]{1,0:T(8,128)(2,1)S(1)}, u32[]{:S(2)}, u32[]{:S(2)}) collective-permute-start(bf16[128,1024]{1,0:T(8,128)(2,1)S(1)} %get-tuple-element.29), channel_id=1, source_target_pairs={{0,2},{2,0},{4,6},{6,4},{1,3},{3,1},{5,7},{7,5},{8,10},{10,8},{12,... | collective-permute-start | bytes 786440 | tf_op jit(solution)/shard_map/ppermute | solution.py:328
  152.8 11.3 %collective-permute-start.18 = (bf16[128,1024]{1,0:T(8,128)(2,1)S(1)}, bf16[128,1024]{1,0:T(8,128)(2,1)S(1)}, u32[]{:S(2)}, u32[]{:S(2)}) collective-permute-start(bf16[128,1024]{1,0:T(8,128)(2,1)S(1)} %get-tuple-element.30), channel_id=1, source_target_pairs={{0,6},{2,4},{4,2},{6,0},{1,7},{3,5},{5,3},{7,1},{8,14},{10,12},{12... | collective-permute-start | bytes 786440 | tf_op jit(solution)/shard_map/ppermute | solution.py:328
  164.5 12.6 %collective-permute-start.19 = (bf16[128,1024]{1,0:T(8,128)(2,1)S(1)}, bf16[128,1024]{1,0:T(8,128)(2,1)S(1)}, u32[]{:S(2)}, u32[]{:S(2)}) collective-permute-start(bf16[128,1024]{1,0:T(8,128)(2,1)S(1)} %get-tuple-element.32.own), channel_id=1, source_target_pairs={{0,4},{2,6},{4,0},{6,2},{1,5},{3,7},{5,1},{7,3},{8,12},{10,14},{12... | collective-permute-start | bytes 786440 | tf_op jit(solution)/shard_map/ppermute | solution.py:328
  167.8 12.2 %collective-permute-start.20 = (bf16[128,1024]{1,0:T(8,128)(2,1)S(1)}, bf16[128,1024]{1,0:T(8,128)(2,1)S(1)}, u32[]{:S(2)}, u32[]{:S(2)}) collective-permute-start(bf16[128,1024]{1,0:T(8,128)(2,1)S(1)} %get-tuple-element.32.own), channel_id=1, source_target_pairs={{0,2},{2,0},{4,6},{6,4},{1,3},{3,1},{5,7},{7,5},{8,10},{10,8},{12,... | collective-permute-start | bytes 786440 | tf_op jit(solution)/shard_map/ppermute | solution.py:328
  170.8 11.0 %collective-permute-start.21 = (bf16[128,1024]{1,0:T(8,128)(2,1)S(1)}, bf16[128,1024]{1,0:T(8,128)(2,1)S(1)}, u32[]{:S(2)}, u32[]{:S(2)}) collective-permute-start(bf16[128,1024]{1,0:T(8,128)(2,1)S(1)} %get-tuple-element.32.own), channel_id=1, source_target_pairs={{0,6},{2,4},{4,2},{6,0},{1,7},{3,5},{5,3},{7,1},{8,14},{10,12},{12... | collective-permute-start | bytes 786440 | tf_op jit(solution)/shard_map/ppermute | solution.py:328
  181.8 5.2 %collective-permute-start.22 = (bf16[8,1024]{1,0:T(8,128)(2,1)S(1)}, bf16[8,1024]{1,0:T(8,128)(2,1)S(1)}, u32[]{:S(2)}, u32[]{:S(2)}) collective-permute-start(bf16[8,1024]{1,0:T(8,128)(2,1)S(1)} %shard_map.188), channel_id=1, source_target_pairs={{0,1},{1,0},{2,3},{3,2},{4,5},{5,4},{6,7},{7,6},{8,9},{9,8},{10,11... | collective-permute-start | bytes 49160 | tf_op jit(solution)/shard_map/ppermute | solution.py:67
  183.8 26.9 %copy-start.3 = (f32[1024]{0:T(1024)S(1)}, f32[1024]{0:T(1024)}, u32[]{:S(2)}) copy-start(f32[1024]{0:T(1024)} %param.36) | copy-start | bytes 12292
  183.8 3.2 %collective-permute-start.27 = (f32[8,384]{1,0:T(8,128)S(1)}, f32[8,384]{1,0:T(8,128)S(1)}, u32[]{:S(2)}, u32[]{:S(2)}) collective-permute-start(f32[8,384]{1,0:T(8,128)S(1)} %shard_map.190.my_taps), channel_id=1, source_target_pairs={{0,1},{1,0},{2,3},{3,2},{4,5},{5,4},{6,7},{7,6},{8,9},{9,8},{10,11... | collective-permute-start | bytes 36872 | tf_op jit(solution)/shard_map/ppermute | solution.py:67
  192.9 12.6 %collective-permute-start.28 = (bf16[128,1024]{1,0:T(8,128)(2,1)S(1)}, bf16[128,1024]{1,0:T(8,128)(2,1)S(1)}, u32[]{:S(2)}, u32[]{:S(2)}) collective-permute-start(bf16[128,1024]{1,0:T(8,128)(2,1)S(1)} %get-tuple-element.34), channel_id=1, source_target_pairs={{0,4},{2,6},{4,0},{6,2},{1,5},{3,7},{5,1},{7,3},{8,12},{10,14},{12... | collective-permute-start | bytes 786440 | tf_op jit(solution)/shard_map/ppermute | solution.py:328
  195.8 13.5 %collective-permute-start.29 = (bf16[128,1024]{1,0:T(8,128)(2,1)S(1)}, bf16[128,1024]{1,0:T(8,128)(2,1)S(1)}, u32[]{:S(2)}, u32[]{:S(2)}) collective-permute-start(bf16[128,1024]{1,0:T(8,128)(2,1)S(1)} %get-tuple-element.35), channel_id=1, source_target_pairs={{0,2},{2,0},{4,6},{6,4},{1,3},{3,1},{5,7},{7,5},{8,10},{10,8},{12,... | collective-permute-start | bytes 786440 | tf_op jit(solution)/shard_map/ppermute | solution.py:328
  199.1 11.5 %collective-permute-start.30 = (bf16[128,1024]{1,0:T(8,128)(2,1)S(1)}, bf16[128,1024]{1,0:T(8,128)(2,1)S(1)}, u32[]{:S(2)}, u32[]{:S(2)}) collective-permute-start(bf16[128,1024]{1,0:T(8,128)(2,1)S(1)} %get-tuple-element.36), channel_id=1, source_target_pairs={{0,6},{2,4},{4,2},{6,0},{1,7},{3,5},{5,3},{7,1},{8,14},{10,12},{12... | collective-permute-start | bytes 786440 | tf_op jit(solution)/shard_map/ppermute | solution.py:328

commit v9 on v8

--- a/solution.py
+++ b/solution.py
@@ -13,13 +13,12 @@
 DK = 128
 DV = 256
 TP = ("x", "c")
-FS = ("z", "y")
-RING = ("rep", "z")
+FS = ("zh", "zl", "y")
+RING = ("rep", "zh", "zl")
 SWAP = ((0, 1), (1, 0))
 PAD = 384
 FIRST, SECOND, THIRD = 2 * DK + 2 * DV, DV, 3 * PAD
-Z_SHIFTS = (4, 3, 2, 1, 0, -1, -2, -3)
-Z_ISSUE = (4, -3, 3, -2, 2, -1, 1)
+Z_PAIRS = (5, 7, 6)
 PARTNERS = (2, 1, 3)
 epsilon = 1e-06
 rope_base = 10000.0
@@ -59,8 +58,17 @@
     return [(i, i ^ k) for i in range(4)]
 
 
-def ring_pairs(shift):
+def ring_shift(shift):
     return [(i, (i + shift) % 16) for i in range(16)]
+
+
+def ring_pairs(k):
+    pairs = []
+    for i in range(16):
+        here = i // 8 * 8 + (i % 8 ^ k)
+        gap = min((here - i) % 16, (i - here) % 16)
+        pairs.append((i, here if gap <= 4 else (here + 8) % 16))
+    return pairs
 
 
 def swap(value):
@@ -76,7 +84,8 @@
 
 
 def pack_body(width, *refs):
-    sources, out, places, arrived = refs[:8], refs[8], refs[9:17], refs[17]
+    sources, (out, spread, front, back) = refs[:8], refs[8:12]
+    places, arrived = refs[12:20], refs[20]
     copies = [
         pltpu.make_async_copy(source, place, arrived.at[k])
         for k, (source, place) in enumerate(zip(sources, places))
@@ -93,6 +102,10 @@
     for place in places[5:]:
         out[:, at : at + PAD] = jnp.concatenate([place[...], gap], axis=1)
         at += PAD
+    front[...] = out[:, : FIRST + SECOND]
+    back[...] = out[:, FIRST + SECOND :]
+    for k in range(spread.shape[0]):
+        spread[k] = out[...]
 
 
 def taps_body(width, ge_kernel, li_kernel, ge_bias, li_bias, out):
@@ -109,13 +122,18 @@
         out[k] = rows
 
 
-def ring_order_body(index, *refs):
-    pieces, (one, two, three) = refs[:8], refs[8:]
-    for shift, piece in zip(Z_SHIFTS, pieces):
-        at = lax.rem(index[2] - shift + 8, 8)
+def ring_order_body(index, quad, front, back, p5, p7, p6, one, two, three):
+    z = index[2]
+    pieces = [(quad.at[k], (z & 4) + k) for k in range(4)]
+    pieces += [(piece, z ^ k) for k, piece in zip(Z_PAIRS, (p5, p7, p6))]
+    for piece, at in pieces:
         one[at] = piece[:, :FIRST]
         two[at] = piece[:, FIRST : FIRST + SECOND]
         three[at] = piece[:, FIRST + SECOND :]
+    at = z ^ 4
+    one[at] = front[:, :FIRST]
+    two[at] = front[:, FIRST:]
+    three[at] = back[...]
 
 
 def line_order_body(index, *refs):
@@ -354,7 +372,7 @@
     down_weight,
     channel_out_gain,
 ):
-    place = jnp.stack([lax.axis_index(a).astype(jnp.int32) for a in ("x", "y", "z", "c")])
+    place = jnp.stack([lax.axis_index(a).astype(jnp.int32) for a in ("x", "y", ("zh", "zl"), "c")])
     place, query_weight = lax.optimization_barrier((place, query_weight))
     token_rows = tokens[0]
     own, model = token_rows.shape
@@ -375,17 +393,19 @@
         linear_weight,
         down_weight.T,
     )
-    packed = call(
+    total = FIRST + SECOND + THIRD
+    packed, quad_spread, front, back = call(
         functools.partial(pack_body, width),
-        shape((32, FIRST + SECOND + THIRD)),
+        [shape((32, total)), shape((4, 32, total)), shape((32, total - THIRD)), shape((32, THIRD))],
         *parts,
         hbm=8,
         scratch=[pltpu.VMEM(part.shape, bf16) for part in parts]
         + [pltpu.SemaphoreType.DMA((8,))],
     )
-    got = {0: packed}
-    for k in Z_ISSUE:
-        got[k] = lax.ppermute(packed, RING, ring_pairs(k))
+    quad = lax.all_to_all(quad_spread, "zl", 0, 0, tiled=True)
+    front = lax.ppermute(front, RING, ring_shift(4))
+    back = lax.ppermute(back, RING, ring_shift(-4))
+    ring_pieces = [lax.ppermute(packed, RING, ring_pairs(k)) for k in Z_PAIRS]
     spread = call(
         first_norm_body, shape((chips, own, model)), token_rows, row(mixer_in_gain), limit=60
     )
@@ -395,7 +415,10 @@
         ring_order_body,
         [shape((8, 32, columns)) for columns in (FIRST, SECOND, THIRD)],
         place,
-        *[got[k] for k in Z_SHIFTS],
+        quad,
+        front,
+        back,
+        *ring_pieces,
         smem=1,
     )
     first_pieces = line_gather(first_z)
@@ -491,11 +514,11 @@
     fs = mesh.shape["fs"]
     tp = mesh.shape["tp"]
     split = Mesh(
-        mesh.devices.reshape(mesh.shape["rep"], fs // 4, 4, tp // 2, 2),
-        ("rep", "z", "y", "x", "c"),
+        mesh.devices.reshape(mesh.shape["rep"], fs // 16, 4, 4, tp // 2, 2),
+        ("rep", "zh", "zl", "y", "x", "c"),
     )
     in_specs = (
-        P(("rep", "z", "y"), TP, None),
+        P(("rep", *FS), TP, None),
         P(),
         P(FS, TP),
         P(FS, TP),
@@ -514,5 +537,5 @@
         P(TP, FS),
         P(),
     )
-    out_specs = P(("rep", "z", "y"), TP, None)
+    out_specs = P(("rep", *FS), TP, None)
     return jax.shard_map(layer, mesh=split, in_specs=in_specs, out_specs=out_specs, check_vma=False)

time: 213 us -> 216 us (1.014)
  the two profiles are of different devices: /device:TPU:32 before, /device:TPU:1 now
where the time goes in v9:
time: 216 us; the launch traced here: 214 us
  starting transfers between devices  121 us (56%)
  waiting for transfers between devices  74.4 us (34%)
  Pallas kernels  17.9 us (8%)
    ppermute x9, waiting for transfers between devices, line_gather(): got[k] = lax.ppermute(piece, 'y', line_pairs(k))  32 us
    ppermute x9, starting transfers between devices, line_gather(): got[k] = lax.ppermute(piece, 'y', line_pairs(k))  28.8 us
    ppermute x9, starting transfers between devices, sent(): lax.ppermute(block, 'x', line_pairs(k))  27.8 us
    ppermute x6, starting transfers between devices, swap(): return lax.ppermute(value, 'c', SWAP)  25 us
    ppermute x9, waiting for transfers between devices, sent(): lax.ppermute(block, 'x', line_pairs(k))  23.4 us
    pallas_call x12, Pallas kernels, call(): pl.pallas_call(body, out_shape=out_shapes, in_specs=specs, out_specs=VMEM...  17.9 us
    ppermute x3, starting transfers between devices, layer(): ring_pieces = [lax.ppermute(packed, RING, ring_pairs(k)) for k in Z_PAIRS]  16.2 us
    all_to_all x1, waiting for transfers between devices, layer(): quad = lax.all_to_all(quad_spread, 'zl', 0, 0, tiled=True)  9.32 us
  transfers between devices with their start and end apart: 31, of which 18 were waited for; matrix products, arithmetic and copies ran while one was open for 0% of the time, Pallas kernels for 5%

profile of v9, /device:TPU:1, one launch (start us, length us, event | category | flops | bytes accessed | tf_op | source)
XLA Modules:
  0.0 214.5 jit_solution(12637066593034779593)
XLA Ops:
  0.1 1.8 shard_map.182
  1.9 6.4 %all-to-all-start.1 = ((bf16[4,32,2176]{2,1,0:T(8,128)(2,1)}), bf16[4,32,2176]{2,1,0:T(8,128)(2,1)S(1)}, u32[]{:S(2)}, u32[]{:S(2)}) async-start(bf16[4,32,2176]{2,1,0:T(8,128)(2,1)} %get-tuple-element.28), calls=%async_computation.1 | async-start | bytes 1114112 | tf_op jit(solution)/shard_map/all_to_all | solution.py:405
  8.4 2.1 shard_map.181
  10.5 9.3 %all-to-all-done.1.quad = bf16[4,32,2176]{2,1,0:T(8,128)(2,1)S(1)} async-done(((bf16[4,32,2176]{2,1,0:T(8,128)(2,1)}), bf16[4,32,2176]{2,1,0:T(8,128)(2,1)S(1)}, u32[]{:S(2)}, u32[]{:S(2)}) %all-to-all-start.1) | async-done | bytes 557088 | tf_op jit(solution)/shard_map/all_to_all | solution.py:405
  19.8 7.3 %all-to-all-start = ((bf16[4,128,1024]{2,1,0:T(8,128)(2,1)}), bf16[4,128,1024]{2,1,0:T(8,128)(2,1)S(1)}, u32[]{:S(2)}, u32[]{:S(2)}) async-start(bf16[4,128,1024]{2,1,0:T(8,128)(2,1)} %shard_map.181), calls=%async_computation | async-start | bytes 2097152 | tf_op jit(solution)/shard_map/all_to_all | solution.py:79
  27.1 7.4 %collective-permute-start.3 = (bf16[32,2176]{1,0:T(8,128)(2,1)S(1)}, bf16[32,2176]{1,0:T(8,128)(2,1)S(1)}, u32[]{:S(2)}, u32[]{:S(2)}) collective-permute-start(bf16[32,2176]{1,0:T(8,128)(2,1)S(1)} %get-tuple-element.31), channel_id=1, source_target_pairs={{0,416},{32,128},{64,480},{96,192},{128,32},{160,256},{192,96},{22... | collective-permute-start | bytes 417800 | tf_op jit(solution)/shard_map/ppermute | solution.py:408
  34.6 2.8 %collective-permute-start.4 = (bf16[32,2176]{1,0:T(8,128)(2,1)S(1)}, bf16[32,2176]{1,0:T(8,128)(2,1)S(1)}, u32[]{:S(2)}, u32[]{:S(2)}) collective-permute-start(bf16[32,2176]{1,0:T(8,128)(2,1)S(1)} %get-tuple-element.31), channel_id=1, source_target_pairs={{0,480},{32,448},{64,160},{96,128},{128,96},{160,64},{192,288},{22... | collective-permute-start | bytes 417800 | tf_op jit(solution)/shard_map/ppermute | solution.py:408
  37.4 5.9 %collective-permute-start.5 = (bf16[32,2176]{1,0:T(8,128)(2,1)S(1)}, bf16[32,2176]{1,0:T(8,128)(2,1)S(1)}, u32[]{:S(2)}, u32[]{:S(2)}) collective-permute-start(bf16[32,2176]{1,0:T(8,128)(2,1)S(1)} %get-tuple-element.31), channel_id=1, source_target_pairs={{0,448},{32,480},{64,128},{96,160},{128,64},{160,96},{192,256},{22... | collective-permute-start | bytes 417800 | tf_op jit(solution)/shard_map/ppermute | solution.py:408
  43.3 1.9 collective-permute-start.2
  45.3 7.3 %collective-permute-start.1 = (bf16[32,1024]{1,0:T(8,128)(2,1)S(1)}, bf16[32,1024]{1,0:T(8,128)(2,1)S(1)}, u32[]{:S(2)}, u32[]{:S(2)}) collective-permute-start(bf16[32,1024]{1,0:T(8,128)(2,1)S(1)} %get-tuple-element.29), channel_id=1, source_target_pairs={{0,128},{32,160},{64,192},{96,224},{128,256},{160,288},{192,320},{... | collective-permute-start | bytes 196616 | tf_op jit(solution)/shard_map/ppermute | solution.py:406
  52.5 3.8 %collective-permute-done.1.front = bf16[32,1024]{1,0:T(8,128)(2,1)S(1)} collective-permute-done((bf16[32,1024]{1,0:T(8,128)(2,1)S(1)}, bf16[32,1024]{1,0:T(8,128)(2,1)S(1)}, u32[]{:S(2)}, u32[]{:S(2)}) %collective-permute-start.1) | collective-permute-done | bytes 65568 | tf_op jit(solution)/shard_map/ppermute | solution.py:406
  56.4 3.5 %collective-permute-done.2.back = bf16[32,1152]{1,0:T(8,128)(2,1)S(1)} collective-permute-done((bf16[32,1152]{1,0:T(8,128)(2,1)S(1)}, bf16[32,1152]{1,0:T(8,128)(2,1)S(1)}, u32[]{:S(2)}, u32[]{:S(2)}) %collective-permute-start.2) | collective-permute-done | bytes 73760 | tf_op jit(solution)/shard_map/ppermute | solution.py:407
  61.3 3.2 %collective-permute-start.21 = (bf16[8,32,1152]{2,1,0:T(8,128)(2,1)S(1)}, bf16[8,32,1152]{2,1,0:T(8,128)(2,1)S(1)}, u32[]{:S(2)}, u32[]{:S(2)}) collective-permute-start(bf16[8,32,1152]{2,1,0:T(8,128)(2,1)S(1)} %get-tuple-element.41), channel_id=1, source_target_pairs={{0,8},{8,0},{16,24},{24,16},{1,9},{9,1},{17,25},{25,17},{2,10},{10... | collective-permute-start | bytes 1769480 | tf_op jit(solution)/shard_map/ppermute | solution.py:335
  64.5 4.5 %collective-permute-start.22 = (bf16[8,32,1152]{2,1,0:T(8,128)(2,1)S(1)}, bf16[8,32,1152]{2,1,0:T(8,128)(2,1)S(1)}, u32[]{:S(2)}, u32[]{:S(2)}) collective-permute-start(bf16[8,32,1152]{2,1,0:T(8,128)(2,1)S(1)} %get-tuple-element.41), channel_id=1, source_target_pairs={{0,16},{8,24},{16,0},{24,8},{1,17},{9,25},{17,1},{25,9},{2,18},{10... | collective-permute-start | bytes 1769480 | tf_op jit(solution)/shard_map/ppermute | solution.py:335
  69.0 1.9 collective-permute-start.23
  70.9 6.5 %collective-permute-start = (bf16[512,1024]{1,0:T(8,128)(2,1)S(1)}, bf16[512,1024]{1,0:T(8,128)(2,1)S(1)}, u32[]{:S(2)}, u32[]{:S(2)}) collective-permute-start(bf16[512,1024]{1,0:T(8,128)(2,1)S(1)} %bitcast.32), channel_id=1, source_target_pairs={{0,1},{1,0},{2,3},{3,2},{4,5},{5,4},{6,7},{7,6},{8,9},{9,8},{10,11... | collective-permute-start | bytes 3145736 | tf_op jit(solution)/shard_map/ppermute | solution.py:75
  77.5 11.9 %collective-permute-done.22 = bf16[8,32,1152]{2,1,0:T(8,128)(2,1)S(1)} collective-permute-done((bf16[8,32,1152]{2,1,0:T(8,128)(2,1)S(1)}, bf16[8,32,1152]{2,1,0:T(8,128)(2,1)S(1)}, u32[]{:S(2)}, u32[]{:S(2)}) %collective-permute-start.22) | collective-permute-done | bytes 589856 | tf_op jit(solution)/shard_map/ppermute | solution.py:335
  89.3 7.5 %collective-permute-done.23 = bf16[8,32,1152]{2,1,0:T(8,128)(2,1)} collective-permute-done((bf16[8,32,1152]{2,1,0:T(8,128)(2,1)S(1)}, bf16[8,32,1152]{2,1,0:T(8,128)(2,1)}, u32[]{:S(2)}, u32[]{:S(2)}) %collective-permute-start.23) | collective-permute-done | bytes 589856 | tf_op jit(solution)/shard_map/ppermute | solution.py:335
  96.9 1.3 shard_map.189
  98.2 5.7 %collective-permute-start.24 = (bf16[1024,1152]{1,0:T(8,128)(2,1)S(1)}, bf16[1024,1152]{1,0:T(8,128)(2,1)S(1)}, u32[]{:S(2)}, u32[]{:S(2)}) collective-permute-start(bf16[1024,1152]{1,0:T(8,128)(2,1)S(1)} %bitcast.28), channel_id=1, source_target_pairs={{0,1},{1,0},{2,3},{3,2},{4,5},{5,4},{6,7},{7,6},{8,9},{9,8},{10,11... | collective-permute-start | bytes 7077896 | tf_op jit(solution)/shard_map/ppermute | solution.py:75
  103.8 1.9 collective-permute-start.10
  105.7 3.1 %collective-permute-start.11 = (bf16[8,32,256]{2,1,0:T(8,128)(2,1)S(1)}, bf16[8,32,256]{2,1,0:T(8,128)(2,1)S(1)}, u32[]{:S(2)}, u32[]{:S(2)}) collective-permute-start(bf16[8,32,256]{2,1,0:T(8,128)(2,1)S(1)} %get-tuple-element.35), channel_id=1, source_target_pairs={{0,16},{8,24},{16,0},{24,8},{1,17},{9,25},{17,1},{25,9},{2,18},{10... | collective-permute-start | bytes 393224 | tf_op jit(solution)/shard_map/ppermute | solution.py:335
  108.8 4.6 %collective-permute-start.12 = (bf16[8,32,256]{2,1,0:T(8,128)(2,1)S(1)}, bf16[8,32,256]{2,1,0:T(8,128)(2,1)S(1)}, u32[]{:S(2)}, u32[]{:S(2)}) collective-permute-start(bf16[8,32,256]{2,1,0:T(8,128)(2,1)S(1)} %get-tuple-element.35), channel_id=1, source_target_pairs={{0,24},{8,16},{16,8},{24,0},{1,25},{9,17},{17,9},{25,1},{2,26},{10... | collective-permute-start | bytes 393224 | tf_op jit(solution)/shard_map/ppermute | solution.py:335
  113.4 1.9 collective-permute-start.6
  115.4 3.1 %collective-permute-start.7 = (bf16[8,32,768]{2,1,0:T(8,128)(2,1)S(1)}, bf16[8,32,768]{2,1,0:T(8,128)(2,1)S(1)}, u32[]{:S(2)}, u32[]{:S(2)}) collective-permute-start(bf16[8,32,768]{2,1,0:T(8,128)(2,1)S(1)} %copy-done.5), channel_id=1, source_target_pairs={{0,16},{8,24},{16,0},{24,8},{1,17},{9,25},{17,1},{25,9},{2,18},{10... | collective-permute-start | bytes 1179656 | tf_op jit(solution)/shard_map/ppermute | solution.py:335
  118.5 4.6 %collective-permute-start.8 = (bf16[8,32,768]{2,1,0:T(8,128)(2,1)S(1)}, bf16[8,32,768]{2,1,0:T(8,128)(2,1)S(1)}, u32[]{:S(2)}, u32[]{:S(2)}) collective-permute-start(bf16[8,32,768]{2,1,0:T(8,128)(2,1)S(1)} %copy-done.5), channel_id=1, source_target_pairs={{0,24},{8,16},{16,8},{24,0},{1,25},{9,17},{17,9},{25,1},{2,26},{10... | collective-permute-start | bytes 1179656 | tf_op jit(solution)/shard_map/ppermute | solution.py:335
  123.7 3.6 %collective-permute-start.13 = (bf16[1024,256]{1,0:T(8,128)(2,1)S(1)}, bf16[1024,256]{1,0:T(8,128)(2,1)S(1)}, u32[]{:S(2)}, u32[]{:S(2)}) collective-permute-start(bf16[1024,256]{1,0:T(8,128)(2,1)S(1)} %bitcast.37), channel_id=1, source_target_pairs={{0,1},{1,0},{2,3},{3,2},{4,5},{5,4},{6,7},{7,6},{8,9},{9,8},{10,11... | collective-permute-start | bytes 1572872 | tf_op jit(solution)/shard_map/ppermute | solution.py:75
  127.3 6.1 %collective-permute-done.7 = bf16[8,32,768]{2,1,0:T(8,128)(2,1)S(1)} collective-permute-done((bf16[8,32,768]{2,1,0:T(8,128)(2,1)S(1)}, bf16[8,32,768]{2,1,0:T(8,128)(2,1)S(1)}, u32[]{:S(2)}, u32[]{:S(2)}) %collective-permute-start.7) | collective-permute-done | bytes 393248 | tf_op jit(solution)/shard_map/ppermute | solution.py:335
  133.4 6.6 %collective-permute-done.8 = bf16[8,32,768]{2,1,0:T(8,128)(2,1)S(1)} collective-permute-done((bf16[8,32,768]{2,1,0:T(8,128)(2,1)S(1)}, bf16[8,32,768]{2,1,0:T(8,128)(2,1)S(1)}, u32[]{:S(2)}, u32[]{:S(2)}) %collective-permute-start.8) | collective-permute-done | bytes 393248 | tf_op jit(solution)/shard_map/ppermute | solution.py:335
  139.9 4.1 %shard_map.184 = (bf16[512,256]{1,0:T(8,128)(2,1)S(1)}, bf16[512,256]{1,0:T(8,128)(2,1)S(1)}) custom-call(s32[4]{0:T(128)S(1)} %pad_add_fusion.index, f32[2]{0:T(128)S(1)} %bitcast.50, bf16[512,1024]{1,0:T(8,128)(2,1)S(1)} %bitcast.33, bf16[512,1024]{1,0:T(8,128)(2,1)S(1)} %collective-permute-done.other, bf16[256,768]{1,0:T(8,128)(2,1)S(1)} %bitcast.46, ...), custom_call_target="tpu_custom_call" | custom-call | flops 4294967296 | bytes 2097152 | tf_op jit(solution)/shard_map/pallas_call | solution.py:40
  144.1 3.7 %collective-permute-start.9 = (bf16[512,256]{1,0:T(8,128)(2,1)S(1)}, bf16[512,256]{1,0:T(8,128)(2,1)S(1)}, u32[]{:S(2)}, u32[]{:S(2)}) collective-permute-start(bf16[512,256]{1,0:T(8,128)(2,1)S(1)} %get-tuple-element.34), channel_id=1, source_target_pairs={{0,1},{1,0},{2,3},{3,2},{4,5},{5,4},{6,7},{7,6},{8,9},{9,8},{10,11... | collective-permute-start | bytes 786440 | tf_op jit(solution)/shard_map/ppermute | solution.py:75
  150.2 4.9 %collective-permute-start.14 = (bf16[128,1024]{1,0:T(8,128)(2,1)S(1)}, bf16[128,1024]{1,0:T(8,128)(2,1)S(1)}, u32[]{:S(2)}, u32[]{:S(2)}) collective-permute-start(bf16[128,1024]{1,0:T(8,128)(2,1)S(1)} %get-tuple-element.36), channel_id=1, source_target_pairs={{0,4},{2,6},{4,0},{6,2},{1,5},{3,7},{5,1},{7,3},{8,12},{10,14},{12... | collective-permute-start | bytes 786440 | tf_op jit(solution)/shard_map/ppermute | solution.py:346
  155.1 2.2 %collective-permute-start.15 = (bf16[128,1024]{1,0:T(8,128)(2,1)S(1)}, bf16[128,1024]{1,0:T(8,128)(2,1)S(1)}, u32[]{:S(2)}, u32[]{:S(2)}) collective-permute-start(bf16[128,1024]{1,0:T(8,128)(2,1)S(1)} %get-tuple-element.37), channel_id=1, source_target_pairs={{0,2},{2,0},{4,6},{6,4},{1,3},{3,1},{5,7},{7,5},{8,10},{10,8},{12,... | collective-permute-start | bytes 786440 | tf_op jit(solution)/shard_map/ppermute | solution.py:346
  157.3 2.5 %collective-permute-start.16 = (bf16[128,1024]{1,0:T(8,128)(2,1)S(1)}, bf16[128,1024]{1,0:T(8,128)(2,1)S(1)}, u32[]{:S(2)}, u32[]{:S(2)}) collective-permute-start(bf16[128,1024]{1,0:T(8,128)(2,1)S(1)} %get-tuple-element.38), channel_id=1, source_target_pairs={{0,6},{2,4},{4,2},{6,0},{1,7},{3,5},{5,3},{7,1},{8,14},{10,12},{12... | collective-permute-start | bytes 786440 | tf_op jit(solution)/shard_map/ppermute | solution.py:346
  161.1 5.9 %collective-permute-done.15.right = bf16[128,1024]{1,0:T(8,128)(2,1)S(1)} collective-permute-done((bf16[128,1024]{1,0:T(8,128)(2,1)S(1)}, bf16[128,1024]{1,0:T(8,128)(2,1)S(1)}, u32[]{:S(2)}, u32[]{:S(2)}) %collective-permute-start.15) | collective-permute-done | bytes 262176 | tf_op jit(solution)/shard_map/ppermute | solution.py:346
  167.7 4.6 %collective-permute-start.17 = (bf16[128,1024]{1,0:T(8,128)(2,1)S(1)}, bf16[128,1024]{1,0:T(8,128)(2,1)S(1)}, u32[]{:S(2)}, u32[]{:S(2)}) collective-permute-start(bf16[128,1024]{1,0:T(8,128)(2,1)S(1)} %get-tuple-element.40.own), channel_id=1, source_target_pairs={{0,4},{2,6},{4,0},{6,2},{1,5},{3,7},{5,1},{7,3},{8,12},{10,14},{12... | collective-permute-start | bytes 786440 | tf_op jit(solution)/shard_map/ppermute | solution.py:346
  172.3 2.2 %collective-permute-start.18 = (bf16[128,1024]{1,0:T(8,128)(2,1)S(1)}, bf16[128,1024]{1,0:T(8,128)(2,1)S(1)}, u32[]{:S(2)}, u32[]{:S(2)}) collective-permute-start(bf16[128,1024]{1,0:T(8,128)(2,1)S(1)} %get-tuple-element.40.own), channel_id=1, source_target_pairs={{0,2},{2,0},{4,6},{6,4},{1,3},{3,1},{5,7},{7,5},{8,10},{10,8},{12,... | collective-permute-start | bytes 786440 | tf_op jit(solution)/shard_map/ppermute | solution.py:346
  174.5 2.5 %collective-permute-start.19 = (bf16[128,1024]{1,0:T(8,128)(2,1)S(1)}, bf16[128,1024]{1,0:T(8,128)(2,1)S(1)}, u32[]{:S(2)}, u32[]{:S(2)}) collective-permute-start(bf16[128,1024]{1,0:T(8,128)(2,1)S(1)} %get-tuple-element.40.own), channel_id=1, source_target_pairs={{0,6},{2,4},{4,2},{6,0},{1,7},{3,5},{5,3},{7,1},{8,14},{10,12},{12... | collective-permute-start | bytes 786440 | tf_op jit(solution)/shard_map/ppermute | solution.py:346
  177.2 6.4 %collective-permute-done.18.after.got_next = bf16[128,1024]{1,0:T(8,128)(2,1)S(1)} collective-permute-done((bf16[128,1024]{1,0:T(8,128)(2,1)S(1)}, bf16[128,1024]{1,0:T(8,128)(2,1)S(1)}, u32[]{:S(2)}, u32[]{:S(2)}) %collective-permute-start.18) | collective-permute-done | bytes 262176 | tf_op jit(solution)/shard_map/ppermute | solution.py:346
  183.6 1.4 collective-permute-done.19.before.got_prev
  185.1 3.7 %collective-permute-start.20 = (bf16[8,1024]{1,0:T(8,128)(2,1)S(1)}, bf16[8,1024]{1,0:T(8,128)(2,1)S(1)}, u32[]{:S(2)}, u32[]{:S(2)}) collective-permute-start(bf16[8,1024]{1,0:T(8,128)(2,1)S(1)} %shard_map.188), channel_id=1, source_target_pairs={{0,1},{1,0},{2,3},{3,2},{4,5},{5,4},{6,7},{7,6},{8,9},{9,8},{10,11... | collective-permute-start | bytes 49160 | tf_op jit(solution)/shard_map/ppermute | solution.py:75
  188.9 1.9 collective-permute-start.25
  192.0 4.7 %shard_map.191 = (bf16[128,1024]{1,0:T(8,128)(2,1)S(1)}, bf16[128,1024]{1,0:T(8,128)(2,1)S(1)}, bf16[128,1024]{1,0:T(8,128)(2,1)S(1)}, bf16[128,1024]{1,0:T(8,128)(2,1)S(1)}) custom-call(s32[4]{0:T(128)S(1)} %pad_add_fusion.index, bf16[128,1024]{1,0:T(8,128)(2,1)S(1)} %collective-permute-done.17.far.got_far, ...), custom_call_target="tpu_custom_call" | custom-call | flops 4294967296 | bytes 2097152 | tf_op jit(solution)/shard_map/pallas_call | solution.py:40
  196.7 3.2 %collective-permute-start.26 = (bf16[128,1024]{1,0:T(8,128)(2,1)S(1)}, bf16[128,1024]{1,0:T(8,128)(2,1)S(1)}, u32[]{:S(2)}, u32[]{:S(2)}) collective-permute-start(bf16[128,1024]{1,0:T(8,128)(2,1)S(1)} %get-tuple-element.42), channel_id=1, source_target_pairs={{0,4},{2,6},{4,0},{6,2},{1,5},{3,7},{5,1},{7,3},{8,12},{10,14},{12... | collective-permute-start | bytes 786440 | tf_op jit(solution)/shard_map/ppermute | solution.py:346
  199.9 2.4 %collective-permute-start.27 = (bf16[128,1024]{1,0:T(8,128)(2,1)S(1)}, bf16[128,1024]{1,0:T(8,128)(2,1)S(1)}, u32[]{:S(2)}, u32[]{:S(2)}) collective-permute-start(bf16[128,1024]{1,0:T(8,128)(2,1)S(1)} %get-tuple-element.43), channel_id=1, source_target_pairs={{0,2},{2,0},{4,6},{6,4},{1,3},{3,1},{5,7},{7,5},{8,10},{10,8},{12,... | collective-permute-start | bytes 786440 | tf_op jit(solution)/shard_map/ppermute | solution.py:346
  202.3 3.4 %collective-permute-start.28 = (bf16[128,1024]{1,0:T(8,128)(2,1)S(1)}, bf16[128,1024]{1,0:T(8,128)(2,1)S(1)}, u32[]{:S(2)}, u32[]{:S(2)}) collective-permute-start(bf16[128,1024]{1,0:T(8,128)(2,1)S(1)} %get-tuple-element.44), channel_id=1, source_target_pairs={{0,6},{2,4},{4,2},{6,0},{1,7},{3,5},{5,3},{7,1},{8,14},{10,12},{12... | collective-permute-start | bytes 786440 | tf_op jit(solution)/shard_map/ppermute | solution.py:346
  205.7 2.1 collective-permute-done.26.far
  207.8 4.4 %collective-permute-done.27.right = bf16[128,1024]{1,0:T(8,128)(2,1)S(1)} collective-permute-done((bf16[128,1024]{1,0:T(8,128)(2,1)S(1)}, bf16[128,1024]{1,0:T(8,128)(2,1)S(1)}, u32[]{:S(2)}, u32[]{:S(2)}) %collective-permute-start.27) | collective-permute-done | bytes 262176 | tf_op jit(solution)/shard_map/ppermute | solution.py:346
  (51 shorter events, 10.2 us)
Async XLA Ops:
  1.9 17.9 %all-to-all-start.1 = ((bf16[4,32,2176]{2,1,0:T(8,128)(2,1)}), bf16[4,32,2176]{2,1,0:T(8,128)(2,1)S(1)}, u32[]{:S(2)}, u32[]{:S(2)}) async-start(bf16[4,32,2176]{2,1,0:T(8,128)(2,1)} %get-tuple-element.28), calls=%async_computation.1 | async-start | bytes 1114112 | tf_op jit(solution)/shard_map/all_to_all | solution.py:405
  19.8 51.1 %all-to-all-start = ((bf16[4,128,1024]{2,1,0:T(8,128)(2,1)}), bf16[4,128,1024]{2,1,0:T(8,128)(2,1)S(1)}, u32[]{:S(2)}, u32[]{:S(2)}) async-start(bf16[4,128,1024]{2,1,0:T(8,128)(2,1)} %shard_map.181), calls=%async_computation | async-start | bytes 2097152 | tf_op jit(solution)/shard_map/all_to_all | solution.py:79
  27.1 32.8 %collective-permute-start.3 = (bf16[32,2176]{1,0:T(8,128)(2,1)S(1)}, bf16[32,2176]{1,0:T(8,128)(2,1)S(1)}, u32[]{:S(2)}, u32[]{:S(2)}) collective-permute-start(bf16[32,2176]{1,0:T(8,128)(2,1)S(1)} %get-tuple-element.31), channel_id=1, source_target_pairs={{0,416},{32,128},{64,480},{96,192},{128,32},{160,256},{192,96},{22... | collective-permute-start | bytes 417800 | tf_op jit(solution)/shard_map/ppermute | solution.py:408
  34.6 25.3 %collective-permute-start.4 = (bf16[32,2176]{1,0:T(8,128)(2,1)S(1)}, bf16[32,2176]{1,0:T(8,128)(2,1)S(1)}, u32[]{:S(2)}, u32[]{:S(2)}) collective-permute-start(bf16[32,2176]{1,0:T(8,128)(2,1)S(1)} %get-tuple-element.31), channel_id=1, source_target_pairs={{0,480},{32,448},{64,160},{96,128},{128,96},{160,64},{192,288},{22... | collective-permute-start | bytes 417800 | tf_op jit(solution)/shard_map/ppermute | solution.py:408
  37.4 22.5 %collective-permute-start.5 = (bf16[32,2176]{1,0:T(8,128)(2,1)S(1)}, bf16[32,2176]{1,0:T(8,128)(2,1)S(1)}, u32[]{:S(2)}, u32[]{:S(2)}) collective-permute-start(bf16[32,2176]{1,0:T(8,128)(2,1)S(1)} %get-tuple-element.31), channel_id=1, source_target_pairs={{0,448},{32,480},{64,128},{96,160},{128,64},{160,96},{192,256},{22... | collective-permute-start | bytes 417800 | tf_op jit(solution)/shard_map/ppermute | solution.py:408
  43.3 16.5 %collective-permute-start.2 = (bf16[32,1152]{1,0:T(8,128)(2,1)S(1)}, bf16[32,1152]{1,0:T(8,128)(2,1)S(1)}, u32[]{:S(2)}, u32[]{:S(2)}) collective-permute-start(bf16[32,1152]{1,0:T(8,128)(2,1)S(1)} %get-tuple-element.30), channel_id=1, source_target_pairs={{0,384},{32,416},{64,448},{96,480},{128,0},{160,32},{192,64},{224,... | collective-permute-start | bytes 221192 | tf_op jit(solution)/shard_map/ppermute | solution.py:407
  45.3 11.1 %collective-permute-start.1 = (bf16[32,1024]{1,0:T(8,128)(2,1)S(1)}, bf16[32,1024]{1,0:T(8,128)(2,1)S(1)}, u32[]{:S(2)}, u32[]{:S(2)}) collective-permute-start(bf16[32,1024]{1,0:T(8,128)(2,1)S(1)} %get-tuple-element.29), channel_id=1, source_target_pairs={{0,128},{32,160},{64,192},{96,224},{128,256},{160,288},{192,320},{... | collective-permute-start | bytes 196616 | tf_op jit(solution)/shard_map/ppermute | solution.py:406
  60.5 0.7 copy-start.4
  61.3 16.2 %collective-permute-start.21 = (bf16[8,32,1152]{2,1,0:T(8,128)(2,1)S(1)}, bf16[8,32,1152]{2,1,0:T(8,128)(2,1)S(1)}, u32[]{:S(2)}, u32[]{:S(2)}) collective-permute-start(bf16[8,32,1152]{2,1,0:T(8,128)(2,1)S(1)} %get-tuple-element.41), channel_id=1, source_target_pairs={{0,8},{8,0},{16,24},{24,16},{1,9},{9,1},{17,25},{25,17},{2,10},{10... | collective-permute-start | bytes 1769480 | tf_op jit(solution)/shard_map/ppermute | solution.py:335
  64.5 24.9 %collective-permute-start.22 = (bf16[8,32,1152]{2,1,0:T(8,128)(2,1)S(1)}, bf16[8,32,1152]{2,1,0:T(8,128)(2,1)S(1)}, u32[]{:S(2)}, u32[]{:S(2)}) collective-permute-start(bf16[8,32,1152]{2,1,0:T(8,128)(2,1)S(1)} %get-tuple-element.41), channel_id=1, source_target_pairs={{0,16},{8,24},{16,0},{24,8},{1,17},{9,25},{17,1},{25,9},{2,18},{10... | collective-permute-start | bytes 1769480 | tf_op jit(solution)/shard_map/ppermute | solution.py:335
  69.0 27.9 %collective-permute-start.23 = (bf16[8,32,1152]{2,1,0:T(8,128)(2,1)S(1)}, bf16[8,32,1152]{2,1,0:T(8,128)(2,1)}, u32[]{:S(2)}, u32[]{:S(2)}) collective-permute-start(bf16[8,32,1152]{2,1,0:T(8,128)(2,1)S(1)} %get-tuple-element.41), channel_id=1, source_target_pairs={{0,24},{8,16},{16,8},{24,0},{1,25},{9,17},{17,9},{25,1},{2,26},{10... | collective-permute-start | bytes 1769480 | tf_op jit(solution)/shard_map/ppermute | solution.py:335
  70.9 52.7 %collective-permute-start = (bf16[512,1024]{1,0:T(8,128)(2,1)S(1)}, bf16[512,1024]{1,0:T(8,128)(2,1)S(1)}, u32[]{:S(2)}, u32[]{:S(2)}) collective-permute-start(bf16[512,1024]{1,0:T(8,128)(2,1)S(1)} %bitcast.32), channel_id=1, source_target_pairs={{0,1},{1,0},{2,3},{3,2},{4,5},{5,4},{6,7},{7,6},{8,9},{9,8},{10,11... | collective-permute-start | bytes 3145736 | tf_op jit(solution)/shard_map/ppermute | solution.py:75
  96.9 16.6 %copy-start.5 = (bf16[8,32,768]{2,1,0:T(8,128)(2,1)S(1)}, bf16[8,32,768]{2,1,0:T(8,128)(2,1)}, u32[]{:S(2)}) copy-start(bf16[8,32,768]{2,1,0:T(8,128)(2,1)} %copy-done.4) | copy-start | bytes 1179652
  96.9 43.1 %copy-start.10 = (f32[2,1]{0,1:T(1,128)S(1)}, f32[2,1]{0,1:T(1,128)}, u32[]{:S(2)}) copy-start(f32[2,1]{0,1:T(1,128)} %param.25) | copy-start | bytes 28
  96.9 43.1 %copy-start.11 = (f32[1,128]{1,0:T(1,128)S(1)}, f32[1,128]{1,0:T(1,128)}, u32[]{:S(2)}) copy-start(f32[1,128]{1,0:T(1,128)} %constant.23.clone.frequency) | copy-start | bytes 1540
  98.2 93.8 %collective-permute-start.24 = (bf16[1024,1152]{1,0:T(8,128)(2,1)S(1)}, bf16[1024,1152]{1,0:T(8,128)(2,1)S(1)}, u32[]{:S(2)}, u32[]{:S(2)}) collective-permute-start(bf16[1024,1152]{1,0:T(8,128)(2,1)S(1)} %bitcast.28), channel_id=1, source_target_pairs={{0,1},{1,0},{2,3},{3,2},{4,5},{5,4},{6,7},{7,6},{8,9},{9,8},{10,11... | collective-permute-start | bytes 7077896 | tf_op jit(solution)/shard_map/ppermute | solution.py:75
  103.8 9.6 %collective-permute-start.10 = (bf16[8,32,256]{2,1,0:T(8,128)(2,1)S(1)}, bf16[8,32,256]{2,1,0:T(8,128)(2,1)S(1)}, u32[]{:S(2)}, u32[]{:S(2)}) collective-permute-start(bf16[8,32,256]{2,1,0:T(8,128)(2,1)S(1)} %get-tuple-element.35), channel_id=1, source_target_pairs={{0,8},{8,0},{16,24},{24,16},{1,9},{9,1},{17,25},{25,17},{2,10},{10... | collective-permute-start | bytes 393224 | tf_op jit(solution)/shard_map/ppermute | solution.py:335
  105.7 9.6 %collective-permute-start.11 = (bf16[8,32,256]{2,1,0:T(8,128)(2,1)S(1)}, bf16[8,32,256]{2,1,0:T(8,128)(2,1)S(1)}, u32[]{:S(2)}, u32[]{:S(2)}) collective-permute-start(bf16[8,32,256]{2,1,0:T(8,128)(2,1)S(1)} %get-tuple-element.35), channel_id=1, source_target_pairs={{0,16},{8,24},{16,0},{24,8},{1,17},{9,25},{17,1},{25,9},{2,18},{10... | collective-permute-start | bytes 393224 | tf_op jit(solution)/shard_map/ppermute | solution.py:335
  108.8 9.6 %collective-permute-start.12 = (bf16[8,32,256]{2,1,0:T(8,128)(2,1)S(1)}, bf16[8,32,256]{2,1,0:T(8,128)(2,1)S(1)}, u32[]{:S(2)}, u32[]{:S(2)}) collective-permute-start(bf16[8,32,256]{2,1,0:T(8,128)(2,1)S(1)} %get-tuple-element.35), channel_id=1, source_target_pairs={{0,24},{8,16},{16,8},{24,0},{1,25},{9,17},{17,9},{25,1},{2,26},{10... | collective-permute-start | bytes 393224 | tf_op jit(solution)/shard_map/ppermute | solution.py:335
  113.4 13.8 %collective-permute-start.6 = (bf16[8,32,768]{2,1,0:T(8,128)(2,1)S(1)}, bf16[8,32,768]{2,1,0:T(8,128)(2,1)S(1)}, u32[]{:S(2)}, u32[]{:S(2)}) collective-permute-start(bf16[8,32,768]{2,1,0:T(8,128)(2,1)S(1)} %copy-done.5), channel_id=1, source_target_pairs={{0,8},{8,0},{16,24},{24,16},{1,9},{9,1},{17,25},{25,17},{2,10},{10... | collective-permute-start | bytes 1179656 | tf_op jit(solution)/shard_map/ppermute | solution.py:335
  115.4 18.0 %collective-permute-start.7 = (bf16[8,32,768]{2,1,0:T(8,128)(2,1)S(1)}, bf16[8,32,768]{2,1,0:T(8,128)(2,1)S(1)}, u32[]{:S(2)}, u32[]{:S(2)}) collective-permute-start(bf16[8,32,768]{2,1,0:T(8,128)(2,1)S(1)} %copy-done.5), channel_id=1, source_target_pairs={{0,16},{8,24},{16,0},{24,8},{1,17},{9,25},{17,1},{25,9},{2,18},{10... | collective-permute-start | bytes 1179656 | tf_op jit(solution)/shard_map/ppermute | solution.py:335
  118.5 21.4 %collective-permute-start.8 = (bf16[8,32,768]{2,1,0:T(8,128)(2,1)S(1)}, bf16[8,32,768]{2,1,0:T(8,128)(2,1)S(1)}, u32[]{:S(2)}, u32[]{:S(2)}) collective-permute-start(bf16[8,32,768]{2,1,0:T(8,128)(2,1)S(1)} %copy-done.5), channel_id=1, source_target_pairs={{0,24},{8,16},{16,8},{24,0},{1,25},{9,17},{17,9},{25,1},{2,26},{10... | collective-permute-start | bytes 1179656 | tf_op jit(solution)/shard_map/ppermute | solution.py:335
  123.7 25.2 %collective-permute-start.13 = (bf16[1024,256]{1,0:T(8,128)(2,1)S(1)}, bf16[1024,256]{1,0:T(8,128)(2,1)S(1)}, u32[]{:S(2)}, u32[]{:S(2)}) collective-permute-start(bf16[1024,256]{1,0:T(8,128)(2,1)S(1)} %bitcast.37), channel_id=1, source_target_pairs={{0,1},{1,0},{2,3},{3,2},{4,5},{5,4},{6,7},{7,6},{8,9},{9,8},{10,11... | collective-permute-start | bytes 1572872 | tf_op jit(solution)/shard_map/ppermute | solution.py:75
  144.0 23.3 %copy-start = (bf16[1,128,1024]{2,1,0:T(8,128)(2,1)S(1)}, bf16[1,128,1024]{2,1,0:T(8,128)(2,1)}, u32[]{:S(2)}) copy-start(bf16[1,128,1024]{2,1,0:T(8,128)(2,1)} %param.19) | copy-start | bytes 786436
  144.0 23.3 %copy-start.1 = (f32[1024]{0:T(1024)S(1)}, f32[1024]{0:T(1024)}, u32[]{:S(2)}) copy-start(f32[1024]{0:T(1024)} %param.27) | copy-start | bytes 12292
  144.0 23.3 %copy-start.2 = (f32[1024]{0:T(1024)S(1)}, f32[1024]{0:T(1024)}, u32[]{:S(2)}) copy-start(f32[1024]{0:T(1024)} %param.28) | copy-start | bytes 12292
  144.1 4.8 %collective-permute-start.9 = (bf16[512,256]{1,0:T(8,128)(2,1)S(1)}, bf16[512,256]{1,0:T(8,128)(2,1)S(1)}, u32[]{:S(2)}, u32[]{:S(2)}) collective-permute-start(bf16[512,256]{1,0:T(8,128)(2,1)S(1)} %get-tuple-element.34), channel_id=1, source_target_pairs={{0,1},{1,0},{2,3},{3,2},{4,5},{5,4},{6,7},{7,6},{8,9},{9,8},{10,11... | collective-permute-start | bytes 786440 | tf_op jit(solution)/shard_map/ppermute | solution.py:75
  148.9 39.9 %copy-start.6 = (f32[3,352]{1,0:T(4,128)S(1)}, f32[3,352]{1,0:T(4,128)}, u32[]{:S(2)}) copy-start(f32[3,352]{1,0:T(4,128)} %ge_kernel.1) | copy-start | bytes 12676
  148.9 40.0 %copy-start.7 = (f32[3,352]{1,0:T(4,128)S(1)}, f32[3,352]{1,0:T(4,128)}, u32[]{:S(2)}) copy-start(f32[3,352]{1,0:T(4,128)} %li_kernel.1) | copy-start | bytes 12676
  148.9 40.0 %copy-start.8 = (f32[352]{0:T(512)S(1)}, f32[352]{0:T(512)}, u32[]{:S(2)}) copy-start(f32[352]{0:T(512)} %ge_bias.1) | copy-start | bytes 4228
  148.9 40.0 %copy-start.9 = (f32[352]{0:T(512)S(1)}, f32[352]{0:T(512)}, u32[]{:S(2)}) copy-start(f32[352]{0:T(512)} %li_bias.1) | copy-start | bytes 4228
  150.2 10.9 %collective-permute-start.14 = (bf16[128,1024]{1,0:T(8,128)(2,1)S(1)}, bf16[128,1024]{1,0:T(8,128)(2,1)S(1)}, u32[]{:S(2)}, u32[]{:S(2)}) collective-permute-start(bf16[128,1024]{1,0:T(8,128)(2,1)S(1)} %get-tuple-element.36), channel_id=1, source_target_pairs={{0,4},{2,6},{4,0},{6,2},{1,5},{3,7},{5,1},{7,3},{8,12},{10,14},{12... | collective-permute-start | bytes 786440 | tf_op jit(solution)/shard_map/ppermute | solution.py:346
  155.1 11.9 %collective-permute-start.15 = (bf16[128,1024]{1,0:T(8,128)(2,1)S(1)}, bf16[128,1024]{1,0:T(8,128)(2,1)S(1)}, u32[]{:S(2)}, u32[]{:S(2)}) collective-permute-start(bf16[128,1024]{1,0:T(8,128)(2,1)S(1)} %get-tuple-element.37), channel_id=1, source_target_pairs={{0,2},{2,0},{4,6},{6,4},{1,3},{3,1},{5,7},{7,5},{8,10},{10,8},{12,... | collective-permute-start | bytes 786440 | tf_op jit(solution)/shard_map/ppermute | solution.py:346
  157.3 10.0 %collective-permute-start.16 = (bf16[128,1024]{1,0:T(8,128)(2,1)S(1)}, bf16[128,1024]{1,0:T(8,128)(2,1)S(1)}, u32[]{:S(2)}, u32[]{:S(2)}) collective-permute-start(bf16[128,1024]{1,0:T(8,128)(2,1)S(1)} %get-tuple-element.38), channel_id=1, source_target_pairs={{0,6},{2,4},{4,2},{6,0},{1,7},{3,5},{5,3},{7,1},{8,14},{10,12},{12... | collective-permute-start | bytes 786440 | tf_op jit(solution)/shard_map/ppermute | solution.py:346
  167.7 9.5 %collective-permute-start.17 = (bf16[128,1024]{1,0:T(8,128)(2,1)S(1)}, bf16[128,1024]{1,0:T(8,128)(2,1)S(1)}, u32[]{:S(2)}, u32[]{:S(2)}) collective-permute-start(bf16[128,1024]{1,0:T(8,128)(2,1)S(1)} %get-tuple-element.40.own), channel_id=1, source_target_pairs={{0,4},{2,6},{4,0},{6,2},{1,5},{3,7},{5,1},{7,3},{8,12},{10,14},{12... | collective-permute-start | bytes 786440 | tf_op jit(solution)/shard_map/ppermute | solution.py:346
  172.3 11.3 %collective-permute-start.18 = (bf16[128,1024]{1,0:T(8,128)(2,1)S(1)}, bf16[128,1024]{1,0:T(8,128)(2,1)S(1)}, u32[]{:S(2)}, u32[]{:S(2)}) collective-permute-start(bf16[128,1024]{1,0:T(8,128)(2,1)S(1)} %get-tuple-element.40.own), channel_id=1, source_target_pairs={{0,2},{2,0},{4,6},{6,4},{1,3},{3,1},{5,7},{7,5},{8,10},{10,8},{12,... | collective-permute-start | bytes 786440 | tf_op jit(solution)/shard_map/ppermute | solution.py:346
  174.5 10.6 %collective-permute-start.19 = (bf16[128,1024]{1,0:T(8,128)(2,1)S(1)}, bf16[128,1024]{1,0:T(8,128)(2,1)S(1)}, u32[]{:S(2)}, u32[]{:S(2)}) collective-permute-start(bf16[128,1024]{1,0:T(8,128)(2,1)S(1)} %get-tuple-element.40.own), channel_id=1, source_target_pairs={{0,6},{2,4},{4,2},{6,0},{1,7},{3,5},{5,3},{7,1},{8,14},{10,12},{12... | collective-permute-start | bytes 786440 | tf_op jit(solution)/shard_map/ppermute | solution.py:346
  185.1 6.8 %collective-permute-start.20 = (bf16[8,1024]{1,0:T(8,128)(2,1)S(1)}, bf16[8,1024]{1,0:T(8,128)(2,1)S(1)}, u32[]{:S(2)}, u32[]{:S(2)}) collective-permute-start(bf16[8,1024]{1,0:T(8,128)(2,1)S(1)} %shard_map.188), channel_id=1, source_target_pairs={{0,1},{1,0},{2,3},{3,2},{4,5},{5,4},{6,7},{7,6},{8,9},{9,8},{10,11... | collective-permute-start | bytes 49160 | tf_op jit(solution)/shard_map/ppermute | solution.py:75
  188.9 24.6 %copy-start.3 = (f32[1024]{0:T(1024)S(1)}, f32[1024]{0:T(1024)}, u32[]{:S(2)}) copy-start(f32[1024]{0:T(1024)} %param.36) | copy-start | bytes 12292
  188.9 3.1 %collective-permute-start.25 = (f32[8,384]{1,0:T(8,128)S(1)}, f32[8,384]{1,0:T(8,128)S(1)}, u32[]{:S(2)}, u32[]{:S(2)}) collective-permute-start(f32[8,384]{1,0:T(8,128)S(1)} %shard_map.190.my_taps), channel_id=1, source_target_pairs={{0,1},{1,0},{2,3},{3,2},{4,5},{5,4},{6,7},{7,6},{8,9},{9,8},{10,11... | collective-permute-start | bytes 36872 | tf_op jit(solution)/shard_map/ppermute | solution.py:75
  196.7 11.1 %collective-permute-start.26 = (bf16[128,1024]{1,0:T(8,128)(2,1)S(1)}, bf16[128,1024]{1,0:T(8,128)(2,1)S(1)}, u32[]{:S(2)}, u32[]{:S(2)}) collective-permute-start(bf16[128,1024]{1,0:T(8,128)(2,1)S(1)} %get-tuple-element.42), channel_id=1, source_target_pairs={{0,4},{2,6},{4,0},{6,2},{1,5},{3,7},{5,1},{7,3},{8,12},{10,14},{12... | collective-permute-start | bytes 786440 | tf_op jit(solution)/shard_map/ppermute | solution.py:346
  199.9 12.3 %collective-permute-start.27 = (bf16[128,1024]{1,0:T(8,128)(2,1)S(1)}, bf16[128,1024]{1,0:T(8,128)(2,1)S(1)}, u32[]{:S(2)}, u32[]{:S(2)}) collective-permute-start(bf16[128,1024]{1,0:T(8,128)(2,1)S(1)} %get-tuple-element.43), channel_id=1, source_target_pairs={{0,2},{2,0},{4,6},{6,4},{1,3},{3,1},{5,7},{7,5},{8,10},{10,8},{12,... | collective-permute-start | bytes 786440 | tf_op jit(solution)/shard_map/ppermute | solution.py:346
  202.3 11.2 %collective-permute-start.28 = (bf16[128,1024]{1,0:T(8,128)(2,1)S(1)}, bf16[128,1024]{1,0:T(8,128)(2,1)S(1)}, u32[]{:S(2)}, u32[]{:S(2)}) collective-permute-start(bf16[128,1024]{1,0:T(8,128)(2,1)S(1)} %get-tuple-element.44), channel_id=1, source_target_pairs={{0,6},{2,4},{4,2},{6,0},{1,7},{3,5},{5,3},{7,1},{8,14},{10,12},{12... | collective-permute-start | bytes 786440 | tf_op jit(solution)/shard_map/ppermute | solution.py:346

commit v10 on v8

--- a/solution.py
+++ b/solution.py
@@ -216,25 +216,29 @@
         kept = head_norm(dot(weighted, vs[...]))
         gate = gs[rows, :]
         gated = (kept * (gate / (1.0 + jnp.exp(-gate)))).astype(bf16)
+        spot = index[0] ^ (r % 4)
+        spot = jnp.where(spot == 0, 3, jnp.where(spot == 2, 0, jnp.where(spot == 1, 1, 2)))
+        spot = pl.ds(pl.multiple_of(spot * 128, 128), 128)
         if r < 4:
-            out_own[rows, :] = gated
+            out_own[spot, :] = gated
         else:
-            out_other[r * 128 - 512 : r * 128 - 384, :] = gated
-
-
-def output_body(index, mine, theirs, my_weights, their_weights, far, right, left, here, lines):
-    for place, k in enumerate((2, 1, 3, 0)):
-        block = index[0] ^ k
-        rows = pl.ds(pl.multiple_of(block * 128, 128), 128)
-        lines[place * 128 : place * 128 + 128, :DV] = mine[rows, :]
-        lines[place * 128 : place * 128 + 128, DV:] = theirs[rows, :]
+            out_other[spot, :] = gated
+
+
+def other_body(gated, weights, out):
     for d in range(0, 1024, 256):
         columns = slice(d, d + 256)
-        total = dot_nt(lines[:, :DV], my_weights[columns, :]) + dot_nt(
-            lines[:, DV:], their_weights[columns, :]
-        )
-        for place, out in enumerate((far, right, left, here)):
-            out[:, columns] = total[place * 128 : place * 128 + 128, :].astype(bf16)
+        out[:, columns] = dot_nt(gated[...], weights[columns, :]).astype(bf16)
+
+
+def output_body(index, mine, weights, theirs, far, right, left, here):
+    for d in range(0, 1024, 256):
+        columns = slice(d, d + 256)
+        total = dot_nt(mine[...], weights[columns, :]) + theirs[:, columns].astype(f32)
+        far[:, columns] = total[:128, :].astype(bf16)
+        right[:, columns] = total[128:256, :].astype(bf16)
+        left[:, columns] = total[256:384, :].astype(bf16)
+        here[:, columns] = total[384:, :].astype(bf16)
 
 
 def feed_block(main, before, after, taps):
@@ -430,19 +434,18 @@
             pltpu.VMEM((2 * half, DV), f32),
         ],
     )
-    gated_partner = swap(gated_other)
     out_own = in_line_order(second_pieces, place)
+    for_partner = call(other_body, shape((half, model)), gated_other, out_own, flops=1 << 29)
+    from_partner = swap(for_partner)
     far, right, left, here = call(
         output_body,
         [shape((own, model))] * 4,
         place,
         gated_own,
-        gated_partner,
         out_own,
-        swap(out_own),
-        flops=1 << 30,
+        from_partner,
+        flops=1 << 29,
         smem=1,
-        scratch=[pltpu.VMEM((half, 2 * DV), bf16)],
     )
     after_mix, channel_in = call(
         middle_body,

time: 213 us -> 207 us (0.972)
  the two profiles are of different devices: /device:TPU:32 before, /device:TPU:80 now
where the time goes in v10:
time: 207 us; the launch traced here: 205 us
  starting transfers between devices  111 us (54%)
  waiting for transfers between devices  77.4 us (37%)
  Pallas kernels  16.6 us (8%)
    ppermute x7, starting transfers between devices, layer(): got[k] = lax.ppermute(packed, RING, ring_pairs(k))  35.2 us
    ppermute x9, waiting for transfers between devices, line_gather(): got[k] = lax.ppermute(piece, 'y', line_pairs(k))  33 us
    ppermute x9, starting transfers between devices, sent(): lax.ppermute(block, 'x', line_pairs(k))  31.2 us
    ppermute x9, starting transfers between devices, line_gather(): got[k] = lax.ppermute(piece, 'y', line_pairs(k))  29.9 us
    ppermute x9, waiting for transfers between devices, sent(): lax.ppermute(block, 'x', line_pairs(k))  25.2 us
    pallas_call x13, Pallas kernels, call(): pl.pallas_call(body, out_shape=out_shapes, in_specs=specs, out_specs=VMEM...  16.6 us
    ppermute x7, waiting for transfers between devices, layer(): got[k] = lax.ppermute(packed, RING, ring_pairs(k))  15.7 us
    ppermute x5, starting transfers between devices, swap(): return lax.ppermute(value, 'c', SWAP)  10.2 us
  transfers between devices with their start and end apart: 31, of which 16 were waited for; matrix products, arithmetic and copies ran while one was open for 0% of the time, Pallas kernels for 4%

profile of v10, /device:TPU:80, one launch (start us, length us, event | category | flops | bytes accessed | tf_op | source)
XLA Modules:
  0.0 205.5 jit_solution(18133364843436590156)
XLA Ops:
  0.0 2.1 %shard_map.181 = bf16[4,128,1024]{2,1,0:T(8,128)(2,1)} custom-call(bf16[128,1024]{1,0:T(8,128)(2,1)} %bitcast.30, f32[1,1024]{1,0:T(1,128)} %bitcast.54), custom_call_target="tpu_custom_call" | custom-call | flops 16777216 | bytes 2097152 | tf_op jit(solution)/shard_map/pallas_call | solution.py:41
  2.1 4.3 %all-to-all-start = ((bf16[4,128,1024]{2,1,0:T(8,128)(2,1)}), bf16[4,128,1024]{2,1,0:T(8,128)(2,1)S(1)}, u32[]{:S(2)}, u32[]{:S(2)}) async-start(bf16[4,128,1024]{2,1,0:T(8,128)(2,1)} %shard_map.181), calls=%async_computation | async-start | bytes 2097152 | tf_op jit(solution)/shard_map/all_to_all | solution.py:71
  7.4 10.5 %collective-permute-start.7 = (bf16[32,2176]{1,0:T(8,128)(2,1)S(1)}, bf16[32,2176]{1,0:T(8,128)(2,1)S(1)}, u32[]{:S(2)}, u32[]{:S(2)}) collective-permute-start(bf16[32,2176]{1,0:T(8,128)(2,1)S(1)} %shard_map.182.refs_4_), channel_id=1, source_target_pairs={{0,416},{32,448},{64,480},{96,0},{128,32},{160,64},{192,96},{224,1... | collective-permute-start | bytes 417800 | tf_op jit(solution)/shard_map/ppermute | solution.py:392
  17.9 3.4 %collective-permute-start.6 = (bf16[32,2176]{1,0:T(8,128)(2,1)S(1)}, bf16[32,2176]{1,0:T(8,128)(2,1)S(1)}, u32[]{:S(2)}, u32[]{:S(2)}) collective-permute-start(bf16[32,2176]{1,0:T(8,128)(2,1)S(1)} %shard_map.182.refs_4_), channel_id=1, source_target_pairs={{0,448},{32,480},{64,0},{96,32},{128,64},{160,96},{192,128},{224,1... | collective-permute-start | bytes 417800 | tf_op jit(solution)/shard_map/ppermute | solution.py:392
  21.3 2.9 %collective-permute-start.5 = (bf16[32,2176]{1,0:T(8,128)(2,1)S(1)}, bf16[32,2176]{1,0:T(8,128)(2,1)S(1)}, u32[]{:S(2)}, u32[]{:S(2)}) collective-permute-start(bf16[32,2176]{1,0:T(8,128)(2,1)S(1)} %shard_map.182.refs_4_), channel_id=1, source_target_pairs={{0,480},{32,0},{64,32},{96,64},{128,96},{160,128},{192,160},{224,1... | collective-permute-start | bytes 417800 | tf_op jit(solution)/shard_map/ppermute | solution.py:392
  24.2 2.9 %collective-permute-start.4 = (bf16[32,2176]{1,0:T(8,128)(2,1)S(1)}, bf16[32,2176]{1,0:T(8,128)(2,1)S(1)}, u32[]{:S(2)}, u32[]{:S(2)}) collective-permute-start(bf16[32,2176]{1,0:T(8,128)(2,1)S(1)} %shard_map.182.refs_4_), channel_id=1, source_target_pairs={{0,32},{32,64},{64,96},{96,128},{128,160},{160,192},{192,224},{224... | collective-permute-start | bytes 417800 | tf_op jit(solution)/shard_map/ppermute | solution.py:392
  27.2 4.6 %collective-permute-start.3 = (bf16[32,2176]{1,0:T(8,128)(2,1)S(1)}, bf16[32,2176]{1,0:T(8,128)(2,1)S(1)}, u32[]{:S(2)}, u32[]{:S(2)}) collective-permute-start(bf16[32,2176]{1,0:T(8,128)(2,1)S(1)} %shard_map.182.refs_4_), channel_id=1, source_target_pairs={{0,64},{32,96},{64,128},{96,160},{128,192},{160,224},{192,256},{22... | collective-permute-start | bytes 417800 | tf_op jit(solution)/shard_map/ppermute | solution.py:392
  31.8 1.9 collective-permute-start.2
  33.7 9.0 %collective-permute-start.1 = (bf16[32,2176]{1,0:T(8,128)(2,1)S(1)}, bf16[32,2176]{1,0:T(8,128)(2,1)S(1)}, u32[]{:S(2)}, u32[]{:S(2)}) collective-permute-start(bf16[32,2176]{1,0:T(8,128)(2,1)S(1)} %shard_map.182.refs_4_), channel_id=1, source_target_pairs={{0,128},{32,160},{64,192},{96,224},{128,256},{160,288},{192,320},{... | collective-permute-start | bytes 417800 | tf_op jit(solution)/shard_map/ppermute | solution.py:392
  42.7 1.9 collective-permute-start
  44.7 9.4 %collective-permute-done.2.refs_1_ = bf16[32,2176]{1,0:T(8,128)(2,1)S(1)} collective-permute-done((bf16[32,2176]{1,0:T(8,128)(2,1)S(1)}, bf16[32,2176]{1,0:T(8,128)(2,1)S(1)}, u32[]{:S(2)}, u32[]{:S(2)}) %collective-permute-start.2) | collective-permute-done | bytes 139296 | tf_op jit(solution)/shard_map/ppermute | solution.py:392
  54.1 6.3 %collective-permute-done.1.refs_0_ = bf16[32,2176]{1,0:T(8,128)(2,1)S(1)} collective-permute-done((bf16[32,2176]{1,0:T(8,128)(2,1)S(1)}, bf16[32,2176]{1,0:T(8,128)(2,1)S(1)}, u32[]{:S(2)}, u32[]{:S(2)}) %collective-permute-start.1) | collective-permute-done | bytes 139296 | tf_op jit(solution)/shard_map/ppermute | solution.py:392
  61.0 2.4 %collective-permute-start.24 = (bf16[8,32,1152]{2,1,0:T(8,128)(2,1)S(1)}, bf16[8,32,1152]{2,1,0:T(8,128)(2,1)S(1)}, u32[]{:S(2)}, u32[]{:S(2)}) collective-permute-start(bf16[8,32,1152]{2,1,0:T(8,128)(2,1)S(1)} %get-tuple-element.33), channel_id=1, source_target_pairs={{0,24},{8,16},{16,8},{24,0},{1,25},{9,17},{17,9},{25,1},{2,26},{10... | collective-permute-start | bytes 1769480 | tf_op jit(solution)/shard_map/ppermute | solution.py:321
  63.4 4.8 %collective-permute-start.23 = (bf16[8,32,1152]{2,1,0:T(8,128)(2,1)S(1)}, bf16[8,32,1152]{2,1,0:T(8,128)(2,1)S(1)}, u32[]{:S(2)}, u32[]{:S(2)}) collective-permute-start(bf16[8,32,1152]{2,1,0:T(8,128)(2,1)S(1)} %get-tuple-element.33), channel_id=1, source_target_pairs={{0,16},{8,24},{16,0},{24,8},{1,17},{9,25},{17,1},{25,9},{2,18},{10... | collective-permute-start | bytes 1769480 | tf_op jit(solution)/shard_map/ppermute | solution.py:321
  68.2 2.7 %collective-permute-start.22 = (bf16[8,32,1152]{2,1,0:T(8,128)(2,1)S(1)}, bf16[8,32,1152]{2,1,0:T(8,128)(2,1)S(1)}, u32[]{:S(2)}, u32[]{:S(2)}) collective-permute-start(bf16[8,32,1152]{2,1,0:T(8,128)(2,1)S(1)} %get-tuple-element.33), channel_id=1, source_target_pairs={{0,8},{8,0},{16,24},{24,16},{1,9},{9,1},{17,25},{25,17},{2,10},{10... | collective-permute-start | bytes 1769480 | tf_op jit(solution)/shard_map/ppermute | solution.py:321
  70.8 2.4 %collective-permute-start.13 = (bf16[8,32,256]{2,1,0:T(8,128)(2,1)S(1)}, bf16[8,32,256]{2,1,0:T(8,128)(2,1)S(1)}, u32[]{:S(2)}, u32[]{:S(2)}) collective-permute-start(bf16[8,32,256]{2,1,0:T(8,128)(2,1)S(1)} %get-tuple-element.26), channel_id=1, source_target_pairs={{0,24},{8,16},{16,8},{24,0},{1,25},{9,17},{17,9},{25,1},{2,26},{10... | collective-permute-start | bytes 393224 | tf_op jit(solution)/shard_map/ppermute | solution.py:321
  73.2 19.4 %collective-permute-done.13 = bf16[8,32,256]{2,1,0:T(8,128)(2,1)S(1)} collective-permute-done((bf16[8,32,256]{2,1,0:T(8,128)(2,1)S(1)}, bf16[8,32,256]{2,1,0:T(8,128)(2,1)S(1)}, u32[]{:S(2)}, u32[]{:S(2)}) %collective-permute-start.13) | collective-permute-done | bytes 131104 | tf_op jit(solution)/shard_map/ppermute | solution.py:321
  92.6 3.5 %collective-permute-start.12 = (bf16[8,32,256]{2,1,0:T(8,128)(2,1)S(1)}, bf16[8,32,256]{2,1,0:T(8,128)(2,1)S(1)}, u32[]{:S(2)}, u32[]{:S(2)}) collective-permute-start(bf16[8,32,256]{2,1,0:T(8,128)(2,1)S(1)} %get-tuple-element.26), channel_id=1, source_target_pairs={{0,16},{8,24},{16,0},{24,8},{1,17},{9,25},{17,1},{25,9},{2,18},{10... | collective-permute-start | bytes 393224 | tf_op jit(solution)/shard_map/ppermute | solution.py:321
  96.2 4.8 %collective-permute-done.12 = bf16[8,32,256]{2,1,0:T(8,128)(2,1)S(1)} collective-permute-done((bf16[8,32,256]{2,1,0:T(8,128)(2,1)S(1)}, bf16[8,32,256]{2,1,0:T(8,128)(2,1)S(1)}, u32[]{:S(2)}, u32[]{:S(2)}) %collective-permute-start.12) | collective-permute-done | bytes 131104 | tf_op jit(solution)/shard_map/ppermute | solution.py:321
  101.0 4.4 %collective-permute-start.11 = (bf16[8,32,256]{2,1,0:T(8,128)(2,1)S(1)}, bf16[8,32,256]{2,1,0:T(8,128)(2,1)S(1)}, u32[]{:S(2)}, u32[]{:S(2)}) collective-permute-start(bf16[8,32,256]{2,1,0:T(8,128)(2,1)S(1)} %get-tuple-element.26), channel_id=1, source_target_pairs={{0,8},{8,0},{16,24},{24,16},{1,9},{9,1},{17,25},{25,17},{2,10},{10... | collective-permute-start | bytes 393224 | tf_op jit(solution)/shard_map/ppermute | solution.py:321
  105.4 1.9 collective-permute-start.10
  107.3 4.0 %collective-permute-start.9 = (bf16[8,32,768]{2,1,0:T(8,128)(2,1)S(1)}, bf16[8,32,768]{2,1,0:T(8,128)(2,1)S(1)}, u32[]{:S(2)}, u32[]{:S(2)}) collective-permute-start(bf16[8,32,768]{2,1,0:T(8,128)(2,1)S(1)} %get-tuple-element.24), channel_id=1, source_target_pairs={{0,16},{8,24},{16,0},{24,8},{1,17},{9,25},{17,1},{25,9},{2,18},{10... | collective-permute-start | bytes 1179656 | tf_op jit(solution)/shard_map/ppermute | solution.py:321
  111.3 3.9 %collective-permute-start.8 = (bf16[8,32,768]{2,1,0:T(8,128)(2,1)S(1)}, bf16[8,32,768]{2,1,0:T(8,128)(2,1)S(1)}, u32[]{:S(2)}, u32[]{:S(2)}) collective-permute-start(bf16[8,32,768]{2,1,0:T(8,128)(2,1)S(1)} %get-tuple-element.24), channel_id=1, source_target_pairs={{0,8},{8,0},{16,24},{24,16},{1,9},{9,1},{17,25},{25,17},{2,10},{10... | collective-permute-start | bytes 1179656 | tf_op jit(solution)/shard_map/ppermute | solution.py:321
  116.0 1.9 collective-permute-start.25
  118.5 5.0 %collective-permute-done.10 = bf16[8,32,768]{2,1,0:T(8,128)(2,1)S(1)} collective-permute-done((bf16[8,32,768]{2,1,0:T(8,128)(2,1)S(1)}, bf16[8,32,768]{2,1,0:T(8,128)(2,1)S(1)}, u32[]{:S(2)}, u32[]{:S(2)}) %collective-permute-start.10) | collective-permute-done | bytes 393248 | tf_op jit(solution)/shard_map/ppermute | solution.py:321
  123.5 3.8 %collective-permute-done.8 = bf16[8,32,768]{2,1,0:T(8,128)(2,1)S(1)} collective-permute-done((bf16[8,32,768]{2,1,0:T(8,128)(2,1)S(1)}, bf16[8,32,768]{2,1,0:T(8,128)(2,1)S(1)}, u32[]{:S(2)}, u32[]{:S(2)}) %collective-permute-start.8) | collective-permute-done | bytes 393248 | tf_op jit(solution)/shard_map/ppermute | solution.py:321
  127.3 4.1 %shard_map.184 = (bf16[512,256]{1,0:T(8,128)(2,1)S(1)}, bf16[512,256]{1,0:T(8,128)(2,1)S(1)}) custom-call(s32[4]{0:T(128)S(1)} %pad_add_fusion.index, f32[2]{0:T(128)S(1)} %bitcast.51, bf16[512,1024]{1,0:T(8,128)(2,1)S(1)} %bitcast.33, bf16[512,1024]{1,0:T(8,128)(2,1)S(1)} %collective-permute-done.other, bf16[256,768]{1,0:T(8,128)(2,1)S(1)} %bitcast.47, ...), custom_call_target="tpu_custom_call" | custom-call | flops 4294967296 | bytes 2097152 | tf_op jit(solution)/shard_map/pallas_call | solution.py:41
  131.9 2.1 collective-permute-start.14
  134.0 2.6 %collective-permute-done.14.theirs = bf16[512,1024]{1,0:T(8,128)(2,1)S(1)} collective-permute-done((bf16[512,1024]{1,0:T(8,128)(2,1)S(1)}, bf16[512,1024]{1,0:T(8,128)(2,1)S(1)}, u32[]{:S(2)}, u32[]{:S(2)}) %collective-permute-start.14) | collective-permute-done | bytes 1048608 | tf_op jit(solution)/shard_map/ppermute | solution.py:67
  136.6 1.0 shard_map.187
  137.6 5.9 %collective-permute-start.15 = (bf16[128,1024]{1,0:T(8,128)(2,1)S(1)}, bf16[128,1024]{1,0:T(8,128)(2,1)S(1)}, u32[]{:S(2)}, u32[]{:S(2)}) collective-permute-start(bf16[128,1024]{1,0:T(8,128)(2,1)S(1)} %get-tuple-element.28), channel_id=1, source_target_pairs={{0,4},{2,6},{4,0},{6,2},{1,5},{3,7},{5,1},{7,3},{8,12},{10,14},{12... | collective-permute-start | bytes 786440 | tf_op jit(solution)/shard_map/ppermute | solution.py:332
  143.6 2.5 %collective-permute-start.16 = (bf16[128,1024]{1,0:T(8,128)(2,1)S(1)}, bf16[128,1024]{1,0:T(8,128)(2,1)S(1)}, u32[]{:S(2)}, u32[]{:S(2)}) collective-permute-start(bf16[128,1024]{1,0:T(8,128)(2,1)S(1)} %get-tuple-element.29), channel_id=1, source_target_pairs={{0,2},{2,0},{4,6},{6,4},{1,3},{3,1},{5,7},{7,5},{8,10},{10,8},{12,... | collective-permute-start | bytes 786440 | tf_op jit(solution)/shard_map/ppermute | solution.py:332
  146.0 2.5 %collective-permute-start.17 = (bf16[128,1024]{1,0:T(8,128)(2,1)S(1)}, bf16[128,1024]{1,0:T(8,128)(2,1)S(1)}, u32[]{:S(2)}, u32[]{:S(2)}) collective-permute-start(bf16[128,1024]{1,0:T(8,128)(2,1)S(1)} %get-tuple-element.30), channel_id=1, source_target_pairs={{0,6},{2,4},{4,2},{6,0},{1,7},{3,5},{5,3},{7,1},{8,14},{10,12},{12... | collective-permute-start | bytes 786440 | tf_op jit(solution)/shard_map/ppermute | solution.py:332
  148.6 2.1 %collective-permute-done.15.far = bf16[128,1024]{1,0:T(8,128)(2,1)S(1)} collective-permute-done((bf16[128,1024]{1,0:T(8,128)(2,1)S(1)}, bf16[128,1024]{1,0:T(8,128)(2,1)S(1)}, u32[]{:S(2)}, u32[]{:S(2)}) %collective-permute-start.15) | collective-permute-done | bytes 262176 | tf_op jit(solution)/shard_map/ppermute | solution.py:332
  150.7 5.3 %collective-permute-done.16.right = bf16[128,1024]{1,0:T(8,128)(2,1)S(1)} collective-permute-done((bf16[128,1024]{1,0:T(8,128)(2,1)S(1)}, bf16[128,1024]{1,0:T(8,128)(2,1)S(1)}, u32[]{:S(2)}, u32[]{:S(2)}) %collective-permute-start.16) | collective-permute-done | bytes 262176 | tf_op jit(solution)/shard_map/ppermute | solution.py:332
  157.3 3.7 %collective-permute-start.20 = (bf16[128,1024]{1,0:T(8,128)(2,1)S(1)}, bf16[128,1024]{1,0:T(8,128)(2,1)S(1)}, u32[]{:S(2)}, u32[]{:S(2)}) collective-permute-start(bf16[128,1024]{1,0:T(8,128)(2,1)S(1)} %get-tuple-element.32.own), channel_id=1, source_target_pairs={{0,6},{2,4},{4,2},{6,0},{1,7},{3,5},{5,3},{7,1},{8,14},{10,12},{12... | collective-permute-start | bytes 786440 | tf_op jit(solution)/shard_map/ppermute | solution.py:332
  161.0 2.2 %collective-permute-start.19 = (bf16[128,1024]{1,0:T(8,128)(2,1)S(1)}, bf16[128,1024]{1,0:T(8,128)(2,1)S(1)}, u32[]{:S(2)}, u32[]{:S(2)}) collective-permute-start(bf16[128,1024]{1,0:T(8,128)(2,1)S(1)} %get-tuple-element.32.own), channel_id=1, source_target_pairs={{0,2},{2,0},{4,6},{6,4},{1,3},{3,1},{5,7},{7,5},{8,10},{10,8},{12,... | collective-permute-start | bytes 786440 | tf_op jit(solution)/shard_map/ppermute | solution.py:332
  163.2 4.6 %collective-permute-start.18 = (bf16[128,1024]{1,0:T(8,128)(2,1)S(1)}, bf16[128,1024]{1,0:T(8,128)(2,1)S(1)}, u32[]{:S(2)}, u32[]{:S(2)}) collective-permute-start(bf16[128,1024]{1,0:T(8,128)(2,1)S(1)} %get-tuple-element.32.own), channel_id=1, source_target_pairs={{0,4},{2,6},{4,0},{6,2},{1,5},{3,7},{5,1},{7,3},{8,12},{10,14},{12... | collective-permute-start | bytes 786440 | tf_op jit(solution)/shard_map/ppermute | solution.py:332
  167.8 4.3 %collective-permute-done.19.after.got_next = bf16[128,1024]{1,0:T(8,128)(2,1)S(1)} collective-permute-done((bf16[128,1024]{1,0:T(8,128)(2,1)S(1)}, bf16[128,1024]{1,0:T(8,128)(2,1)S(1)}, u32[]{:S(2)}, u32[]{:S(2)}) %collective-permute-start.19) | collective-permute-done | bytes 262176 | tf_op jit(solution)/shard_map/ppermute | solution.py:332
  172.1 4.0 %collective-permute-done.18.far.got_far = bf16[128,1024]{1,0:T(8,128)(2,1)S(1)} collective-permute-done((bf16[128,1024]{1,0:T(8,128)(2,1)S(1)}, bf16[128,1024]{1,0:T(8,128)(2,1)S(1)}, u32[]{:S(2)}, u32[]{:S(2)}) %collective-permute-start.18) | collective-permute-done | bytes 262176 | tf_op jit(solution)/shard_map/ppermute | solution.py:332
  176.1 1.9 collective-permute-start.21
  178.1 2.4 %collective-permute-start.26 = (f32[8,384]{1,0:T(8,128)S(1)}, f32[8,384]{1,0:T(8,128)S(1)}, u32[]{:S(2)}, u32[]{:S(2)}) collective-permute-start(f32[8,384]{1,0:T(8,128)S(1)} %shard_map.191.my_taps), channel_id=1, source_target_pairs={{0,1},{1,0},{2,3},{3,2},{4,5},{5,4},{6,7},{7,6},{8,9},{9,8},{10,11... | collective-permute-start | bytes 36872 | tf_op jit(solution)/shard_map/ppermute | solution.py:67
  181.3 4.7 %shard_map.192 = (bf16[128,1024]{1,0:T(8,128)(2,1)S(1)}, bf16[128,1024]{1,0:T(8,128)(2,1)S(1)}, bf16[128,1024]{1,0:T(8,128)(2,1)S(1)}, bf16[128,1024]{1,0:T(8,128)(2,1)S(1)}) custom-call(s32[4]{0:T(128)S(1)} %pad_add_fusion.index, bf16[128,1024]{1,0:T(8,128)(2,1)S(1)} %collective-permute-done.18.far.got_far, ...), custom_call_target="tpu_custom_call" | custom-call | flops 4294967296 | bytes 2097152 | tf_op jit(solution)/shard_map/pallas_call | solution.py:41
  186.1 3.7 %collective-permute-start.27 = (bf16[128,1024]{1,0:T(8,128)(2,1)S(1)}, bf16[128,1024]{1,0:T(8,128)(2,1)S(1)}, u32[]{:S(2)}, u32[]{:S(2)}) collective-permute-start(bf16[128,1024]{1,0:T(8,128)(2,1)S(1)} %get-tuple-element.34), channel_id=1, source_target_pairs={{0,4},{2,6},{4,0},{6,2},{1,5},{3,7},{5,1},{7,3},{8,12},{10,14},{12... | collective-permute-start | bytes 786440 | tf_op jit(solution)/shard_map/ppermute | solution.py:332
  189.7 3.6 %collective-permute-start.28 = (bf16[128,1024]{1,0:T(8,128)(2,1)S(1)}, bf16[128,1024]{1,0:T(8,128)(2,1)S(1)}, u32[]{:S(2)}, u32[]{:S(2)}) collective-permute-start(bf16[128,1024]{1,0:T(8,128)(2,1)S(1)} %get-tuple-element.35), channel_id=1, source_target_pairs={{0,2},{2,0},{4,6},{6,4},{1,3},{3,1},{5,7},{7,5},{8,10},{10,8},{12,... | collective-permute-start | bytes 786440 | tf_op jit(solution)/shard_map/ppermute | solution.py:332
  193.4 2.5 %collective-permute-start.29 = (bf16[128,1024]{1,0:T(8,128)(2,1)S(1)}, bf16[128,1024]{1,0:T(8,128)(2,1)S(1)}, u32[]{:S(2)}, u32[]{:S(2)}) collective-permute-start(bf16[128,1024]{1,0:T(8,128)(2,1)S(1)} %get-tuple-element.36), channel_id=1, source_target_pairs={{0,6},{2,4},{4,2},{6,0},{1,7},{3,5},{5,3},{7,1},{8,14},{10,12},{12... | collective-permute-start | bytes 786440 | tf_op jit(solution)/shard_map/ppermute | solution.py:332
  195.9 2.7 %collective-permute-done.27.far = bf16[128,1024]{1,0:T(8,128)(2,1)S(1)} collective-permute-done((bf16[128,1024]{1,0:T(8,128)(2,1)S(1)}, bf16[128,1024]{1,0:T(8,128)(2,1)S(1)}, u32[]{:S(2)}, u32[]{:S(2)}) %collective-permute-start.27) | collective-permute-done | bytes 262176 | tf_op jit(solution)/shard_map/ppermute | solution.py:332
  198.6 5.0 %collective-permute-done.28.right = bf16[128,1024]{1,0:T(8,128)(2,1)S(1)} collective-permute-done((bf16[128,1024]{1,0:T(8,128)(2,1)S(1)}, bf16[128,1024]{1,0:T(8,128)(2,1)S(1)}, u32[]{:S(2)}, u32[]{:S(2)}) %collective-permute-start.28) | collective-permute-done | bytes 262176 | tf_op jit(solution)/shard_map/ppermute | solution.py:332
  (48 shorter events, 7.5 us)
Async XLA Ops:
  2.1 40.6 %all-to-all-start = ((bf16[4,128,1024]{2,1,0:T(8,128)(2,1)}), bf16[4,128,1024]{2,1,0:T(8,128)(2,1)S(1)}, u32[]{:S(2)}, u32[]{:S(2)}) async-start(bf16[4,128,1024]{2,1,0:T(8,128)(2,1)} %shard_map.181), calls=%async_computation | async-start | bytes 2097152 | tf_op jit(solution)/shard_map/all_to_all | solution.py:71
  7.4 24.3 %collective-permute-start.7 = (bf16[32,2176]{1,0:T(8,128)(2,1)S(1)}, bf16[32,2176]{1,0:T(8,128)(2,1)S(1)}, u32[]{:S(2)}, u32[]{:S(2)}) collective-permute-start(bf16[32,2176]{1,0:T(8,128)(2,1)S(1)} %shard_map.182.refs_4_), channel_id=1, source_target_pairs={{0,416},{32,448},{64,480},{96,0},{128,32},{160,64},{192,96},{224,1... | collective-permute-start | bytes 417800 | tf_op jit(solution)/shard_map/ppermute | solution.py:392
  17.9 15.8 %collective-permute-start.6 = (bf16[32,2176]{1,0:T(8,128)(2,1)S(1)}, bf16[32,2176]{1,0:T(8,128)(2,1)S(1)}, u32[]{:S(2)}, u32[]{:S(2)}) collective-permute-start(bf16[32,2176]{1,0:T(8,128)(2,1)S(1)} %shard_map.182.refs_4_), channel_id=1, source_target_pairs={{0,448},{32,480},{64,0},{96,32},{128,64},{160,96},{192,128},{224,1... | collective-permute-start | bytes 417800 | tf_op jit(solution)/shard_map/ppermute | solution.py:392
  21.3 21.4 %collective-permute-start.5 = (bf16[32,2176]{1,0:T(8,128)(2,1)S(1)}, bf16[32,2176]{1,0:T(8,128)(2,1)S(1)}, u32[]{:S(2)}, u32[]{:S(2)}) collective-permute-start(bf16[32,2176]{1,0:T(8,128)(2,1)S(1)} %shard_map.182.refs_4_), channel_id=1, source_target_pairs={{0,480},{32,0},{64,32},{96,64},{128,96},{160,128},{192,160},{224,1... | collective-permute-start | bytes 417800 | tf_op jit(solution)/shard_map/ppermute | solution.py:392
  24.2 20.4 %collective-permute-start.4 = (bf16[32,2176]{1,0:T(8,128)(2,1)S(1)}, bf16[32,2176]{1,0:T(8,128)(2,1)S(1)}, u32[]{:S(2)}, u32[]{:S(2)}) collective-permute-start(bf16[32,2176]{1,0:T(8,128)(2,1)S(1)} %shard_map.182.refs_4_), channel_id=1, source_target_pairs={{0,32},{32,64},{64,96},{96,128},{128,160},{160,192},{192,224},{224... | collective-permute-start | bytes 417800 | tf_op jit(solution)/shard_map/ppermute | solution.py:392
  27.2 17.5 %collective-permute-start.3 = (bf16[32,2176]{1,0:T(8,128)(2,1)S(1)}, bf16[32,2176]{1,0:T(8,128)(2,1)S(1)}, u32[]{:S(2)}, u32[]{:S(2)}) collective-permute-start(bf16[32,2176]{1,0:T(8,128)(2,1)S(1)} %shard_map.182.refs_4_), channel_id=1, source_target_pairs={{0,64},{32,96},{64,128},{96,160},{128,192},{160,224},{192,256},{22... | collective-permute-start | bytes 417800 | tf_op jit(solution)/shard_map/ppermute | solution.py:392
  31.8 22.3 %collective-permute-start.2 = (bf16[32,2176]{1,0:T(8,128)(2,1)S(1)}, bf16[32,2176]{1,0:T(8,128)(2,1)S(1)}, u32[]{:S(2)}, u32[]{:S(2)}) collective-permute-start(bf16[32,2176]{1,0:T(8,128)(2,1)S(1)} %shard_map.182.refs_4_), channel_id=1, source_target_pairs={{0,96},{32,128},{64,160},{96,192},{128,224},{160,256},{192,288},{2... | collective-permute-start | bytes 417800 | tf_op jit(solution)/shard_map/ppermute | solution.py:392
  33.7 26.6 %collective-permute-start.1 = (bf16[32,2176]{1,0:T(8,128)(2,1)S(1)}, bf16[32,2176]{1,0:T(8,128)(2,1)S(1)}, u32[]{:S(2)}, u32[]{:S(2)}) collective-permute-start(bf16[32,2176]{1,0:T(8,128)(2,1)S(1)} %shard_map.182.refs_4_), channel_id=1, source_target_pairs={{0,128},{32,160},{64,192},{96,224},{128,256},{160,288},{192,320},{... | collective-permute-start | bytes 417800 | tf_op jit(solution)/shard_map/ppermute | solution.py:392
  42.7 84.6 %collective-permute-start = (bf16[512,1024]{1,0:T(8,128)(2,1)S(1)}, bf16[512,1024]{1,0:T(8,128)(2,1)S(1)}, u32[]{:S(2)}, u32[]{:S(2)}) collective-permute-start(bf16[512,1024]{1,0:T(8,128)(2,1)S(1)} %bitcast.32), channel_id=1, source_target_pairs={{0,1},{1,0},{2,3},{3,2},{4,5},{5,4},{6,7},{7,6},{8,9},{9,8},{10,11... | collective-permute-start | bytes 3145736 | tf_op jit(solution)/shard_map/ppermute | solution.py:67
  61.0 44.4 %collective-permute-start.24 = (bf16[8,32,1152]{2,1,0:T(8,128)(2,1)S(1)}, bf16[8,32,1152]{2,1,0:T(8,128)(2,1)S(1)}, u32[]{:S(2)}, u32[]{:S(2)}) collective-permute-start(bf16[8,32,1152]{2,1,0:T(8,128)(2,1)S(1)} %get-tuple-element.33), channel_id=1, source_target_pairs={{0,24},{8,16},{16,8},{24,0},{1,25},{9,17},{17,9},{25,1},{2,26},{10... | collective-permute-start | bytes 1769480 | tf_op jit(solution)/shard_map/ppermute | solution.py:321
  63.4 44.0 %collective-permute-start.23 = (bf16[8,32,1152]{2,1,0:T(8,128)(2,1)S(1)}, bf16[8,32,1152]{2,1,0:T(8,128)(2,1)S(1)}, u32[]{:S(2)}, u32[]{:S(2)}) collective-permute-start(bf16[8,32,1152]{2,1,0:T(8,128)(2,1)S(1)} %get-tuple-element.33), channel_id=1, source_target_pairs={{0,16},{8,24},{16,0},{24,8},{1,17},{9,25},{17,1},{25,9},{2,18},{10... | collective-permute-start | bytes 1769480 | tf_op jit(solution)/shard_map/ppermute | solution.py:321
  68.2 43.2 %collective-permute-start.22 = (bf16[8,32,1152]{2,1,0:T(8,128)(2,1)S(1)}, bf16[8,32,1152]{2,1,0:T(8,128)(2,1)S(1)}, u32[]{:S(2)}, u32[]{:S(2)}) collective-permute-start(bf16[8,32,1152]{2,1,0:T(8,128)(2,1)S(1)} %get-tuple-element.33), channel_id=1, source_target_pairs={{0,8},{8,0},{16,24},{24,16},{1,9},{9,1},{17,25},{25,17},{2,10},{10... | collective-permute-start | bytes 1769480 | tf_op jit(solution)/shard_map/ppermute | solution.py:321
  70.8 21.8 %collective-permute-start.13 = (bf16[8,32,256]{2,1,0:T(8,128)(2,1)S(1)}, bf16[8,32,256]{2,1,0:T(8,128)(2,1)S(1)}, u32[]{:S(2)}, u32[]{:S(2)}) collective-permute-start(bf16[8,32,256]{2,1,0:T(8,128)(2,1)S(1)} %get-tuple-element.26), channel_id=1, source_target_pairs={{0,24},{8,16},{16,8},{24,0},{1,25},{9,17},{17,9},{25,1},{2,26},{10... | collective-permute-start | bytes 393224 | tf_op jit(solution)/shard_map/ppermute | solution.py:321
  92.6 8.4 %collective-permute-start.12 = (bf16[8,32,256]{2,1,0:T(8,128)(2,1)S(1)}, bf16[8,32,256]{2,1,0:T(8,128)(2,1)S(1)}, u32[]{:S(2)}, u32[]{:S(2)}) collective-permute-start(bf16[8,32,256]{2,1,0:T(8,128)(2,1)S(1)} %get-tuple-element.26), channel_id=1, source_target_pairs={{0,16},{8,24},{16,0},{24,8},{1,17},{9,25},{17,1},{25,9},{2,18},{10... | collective-permute-start | bytes 393224 | tf_op jit(solution)/shard_map/ppermute | solution.py:321
  101.0 15.0 %collective-permute-start.11 = (bf16[8,32,256]{2,1,0:T(8,128)(2,1)S(1)}, bf16[8,32,256]{2,1,0:T(8,128)(2,1)S(1)}, u32[]{:S(2)}, u32[]{:S(2)}) collective-permute-start(bf16[8,32,256]{2,1,0:T(8,128)(2,1)S(1)} %get-tuple-element.26), channel_id=1, source_target_pairs={{0,8},{8,0},{16,24},{24,16},{1,9},{9,1},{17,25},{25,17},{2,10},{10... | collective-permute-start | bytes 393224 | tf_op jit(solution)/shard_map/ppermute | solution.py:321
  105.4 18.1 %collective-permute-start.10 = (bf16[8,32,768]{2,1,0:T(8,128)(2,1)S(1)}, bf16[8,32,768]{2,1,0:T(8,128)(2,1)S(1)}, u32[]{:S(2)}, u32[]{:S(2)}) collective-permute-start(bf16[8,32,768]{2,1,0:T(8,128)(2,1)S(1)} %get-tuple-element.24), channel_id=1, source_target_pairs={{0,24},{8,16},{16,8},{24,0},{1,25},{9,17},{17,9},{25,1},{2,26},{10... | collective-permute-start | bytes 1179656 | tf_op jit(solution)/shard_map/ppermute | solution.py:321
  107.3 16.2 %collective-permute-start.9 = (bf16[8,32,768]{2,1,0:T(8,128)(2,1)S(1)}, bf16[8,32,768]{2,1,0:T(8,128)(2,1)S(1)}, u32[]{:S(2)}, u32[]{:S(2)}) collective-permute-start(bf16[8,32,768]{2,1,0:T(8,128)(2,1)S(1)} %get-tuple-element.24), channel_id=1, source_target_pairs={{0,16},{8,24},{16,0},{24,8},{1,17},{9,25},{17,1},{25,9},{2,18},{10... | collective-permute-start | bytes 1179656 | tf_op jit(solution)/shard_map/ppermute | solution.py:321
  111.3 16.0 %collective-permute-start.8 = (bf16[8,32,768]{2,1,0:T(8,128)(2,1)S(1)}, bf16[8,32,768]{2,1,0:T(8,128)(2,1)S(1)}, u32[]{:S(2)}, u32[]{:S(2)}) collective-permute-start(bf16[8,32,768]{2,1,0:T(8,128)(2,1)S(1)} %get-tuple-element.24), channel_id=1, source_target_pairs={{0,8},{8,0},{16,24},{24,16},{1,9},{9,1},{17,25},{25,17},{2,10},{10... | collective-permute-start | bytes 1179656 | tf_op jit(solution)/shard_map/ppermute | solution.py:321
  115.3 12.0 %copy-start.8 = (f32[2,1]{0,1:T(1,128)S(1)}, f32[2,1]{0,1:T(1,128)}, u32[]{:S(2)}) copy-start(f32[2,1]{0,1:T(1,128)} %param.25) | copy-start | bytes 28
  115.3 12.0 %copy-start.9 = (f32[1,128]{1,0:T(1,128)S(1)}, f32[1,128]{1,0:T(1,128)}, u32[]{:S(2)}) copy-start(f32[1,128]{1,0:T(1,128)} %constant.18.clone.frequency) | copy-start | bytes 1540
  116.0 65.3 %collective-permute-start.25 = (bf16[1024,1152]{1,0:T(8,128)(2,1)S(1)}, bf16[1024,1152]{1,0:T(8,128)(2,1)S(1)}, u32[]{:S(2)}, u32[]{:S(2)}) collective-permute-start(bf16[1024,1152]{1,0:T(8,128)(2,1)S(1)} %bitcast.28), channel_id=1, source_target_pairs={{0,1},{1,0},{2,3},{3,2},{4,5},{5,4},{6,7},{7,6},{8,9},{9,8},{10,11... | collective-permute-start | bytes 7077896 | tf_op jit(solution)/shard_map/ppermute | solution.py:67
  131.4 25.6 %copy-start = (bf16[1,128,1024]{2,1,0:T(8,128)(2,1)S(1)}, bf16[1,128,1024]{2,1,0:T(8,128)(2,1)}, u32[]{:S(2)}) copy-start(bf16[1,128,1024]{2,1,0:T(8,128)(2,1)} %param.19) | copy-start | bytes 786436
  131.4 25.6 %copy-start.1 = (f32[1024]{0:T(1024)S(1)}, f32[1024]{0:T(1024)}, u32[]{:S(2)}) copy-start(f32[1024]{0:T(1024)} %param.27) | copy-start | bytes 12292
  131.4 25.6 %copy-start.2 = (f32[1024]{0:T(1024)S(1)}, f32[1024]{0:T(1024)}, u32[]{:S(2)}) copy-start(f32[1024]{0:T(1024)} %param.28) | copy-start | bytes 12292
  131.9 46.2 %copy-start.4 = (f32[3,352]{1,0:T(4,128)S(1)}, f32[3,352]{1,0:T(4,128)}, u32[]{:S(2)}) copy-start(f32[3,352]{1,0:T(4,128)} %ge_kernel.1) | copy-start | bytes 12676
  131.9 46.2 %copy-start.5 = (f32[3,352]{1,0:T(4,128)S(1)}, f32[3,352]{1,0:T(4,128)}, u32[]{:S(2)}) copy-start(f32[3,352]{1,0:T(4,128)} %li_kernel.1) | copy-start | bytes 12676
  131.9 46.2 %copy-start.6 = (f32[352]{0:T(512)S(1)}, f32[352]{0:T(512)}, u32[]{:S(2)}) copy-start(f32[352]{0:T(512)} %ge_bias.1) | copy-start | bytes 4228
  131.9 46.2 %copy-start.7 = (f32[352]{0:T(512)S(1)}, f32[352]{0:T(512)}, u32[]{:S(2)}) copy-start(f32[352]{0:T(512)} %li_bias.1) | copy-start | bytes 4228
  131.9 4.7 %collective-permute-start.14 = (bf16[512,1024]{1,0:T(8,128)(2,1)S(1)}, bf16[512,1024]{1,0:T(8,128)(2,1)S(1)}, u32[]{:S(2)}, u32[]{:S(2)}) collective-permute-start(bf16[512,1024]{1,0:T(8,128)(2,1)S(1)} %shard_map.186), channel_id=1, source_target_pairs={{0,1},{1,0},{2,3},{3,2},{4,5},{5,4},{6,7},{7,6},{8,9},{9,8},{10,11... | collective-permute-start | bytes 3145736 | tf_op jit(solution)/shard_map/ppermute | solution.py:67
  137.6 13.1 %collective-permute-start.15 = (bf16[128,1024]{1,0:T(8,128)(2,1)S(1)}, bf16[128,1024]{1,0:T(8,128)(2,1)S(1)}, u32[]{:S(2)}, u32[]{:S(2)}) collective-permute-start(bf16[128,1024]{1,0:T(8,128)(2,1)S(1)} %get-tuple-element.28), channel_id=1, source_target_pairs={{0,4},{2,6},{4,0},{6,2},{1,5},{3,7},{5,1},{7,3},{8,12},{10,14},{12... | collective-permute-start | bytes 786440 | tf_op jit(solution)/shard_map/ppermute | solution.py:332
  143.6 12.5 %collective-permute-start.16 = (bf16[128,1024]{1,0:T(8,128)(2,1)S(1)}, bf16[128,1024]{1,0:T(8,128)(2,1)S(1)}, u32[]{:S(2)}, u32[]{:S(2)}) collective-permute-start(bf16[128,1024]{1,0:T(8,128)(2,1)S(1)} %get-tuple-element.29), channel_id=1, source_target_pairs={{0,2},{2,0},{4,6},{6,4},{1,3},{3,1},{5,7},{7,5},{8,10},{10,8},{12,... | collective-permute-start | bytes 786440 | tf_op jit(solution)/shard_map/ppermute | solution.py:332
  146.0 10.9 %collective-permute-start.17 = (bf16[128,1024]{1,0:T(8,128)(2,1)S(1)}, bf16[128,1024]{1,0:T(8,128)(2,1)S(1)}, u32[]{:S(2)}, u32[]{:S(2)}) collective-permute-start(bf16[128,1024]{1,0:T(8,128)(2,1)S(1)} %get-tuple-element.30), channel_id=1, source_target_pairs={{0,6},{2,4},{4,2},{6,0},{1,7},{3,5},{5,3},{7,1},{8,14},{10,12},{12... | collective-permute-start | bytes 786440 | tf_op jit(solution)/shard_map/ppermute | solution.py:332
  157.3 10.5 %collective-permute-start.20 = (bf16[128,1024]{1,0:T(8,128)(2,1)S(1)}, bf16[128,1024]{1,0:T(8,128)(2,1)S(1)}, u32[]{:S(2)}, u32[]{:S(2)}) collective-permute-start(bf16[128,1024]{1,0:T(8,128)(2,1)S(1)} %get-tuple-element.32.own), channel_id=1, source_target_pairs={{0,6},{2,4},{4,2},{6,0},{1,7},{3,5},{5,3},{7,1},{8,14},{10,12},{12... | collective-permute-start | bytes 786440 | tf_op jit(solution)/shard_map/ppermute | solution.py:332
  161.0 11.1 %collective-permute-start.19 = (bf16[128,1024]{1,0:T(8,128)(2,1)S(1)}, bf16[128,1024]{1,0:T(8,128)(2,1)S(1)}, u32[]{:S(2)}, u32[]{:S(2)}) collective-permute-start(bf16[128,1024]{1,0:T(8,128)(2,1)S(1)} %get-tuple-element.32.own), channel_id=1, source_target_pairs={{0,2},{2,0},{4,6},{6,4},{1,3},{3,1},{5,7},{7,5},{8,10},{10,8},{12,... | collective-permute-start | bytes 786440 | tf_op jit(solution)/shard_map/ppermute | solution.py:332
  163.2 12.9 %collective-permute-start.18 = (bf16[128,1024]{1,0:T(8,128)(2,1)S(1)}, bf16[128,1024]{1,0:T(8,128)(2,1)S(1)}, u32[]{:S(2)}, u32[]{:S(2)}) collective-permute-start(bf16[128,1024]{1,0:T(8,128)(2,1)S(1)} %get-tuple-element.32.own), channel_id=1, source_target_pairs={{0,4},{2,6},{4,0},{6,2},{1,5},{3,7},{5,1},{7,3},{8,12},{10,14},{12... | collective-permute-start | bytes 786440 | tf_op jit(solution)/shard_map/ppermute | solution.py:332
  176.1 5.2 %collective-permute-start.21 = (bf16[8,1024]{1,0:T(8,128)(2,1)S(1)}, bf16[8,1024]{1,0:T(8,128)(2,1)S(1)}, u32[]{:S(2)}, u32[]{:S(2)}) collective-permute-start(bf16[8,1024]{1,0:T(8,128)(2,1)S(1)} %shard_map.189), channel_id=1, source_target_pairs={{0,1},{1,0},{2,3},{3,2},{4,5},{5,4},{6,7},{7,6},{8,9},{9,8},{10,11... | collective-permute-start | bytes 49160 | tf_op jit(solution)/shard_map/ppermute | solution.py:67
  178.1 26.4 %copy-start.3 = (f32[1024]{0:T(1024)S(1)}, f32[1024]{0:T(1024)}, u32[]{:S(2)}) copy-start(f32[1024]{0:T(1024)} %param.36) | copy-start | bytes 12292
  178.1 3.2 %collective-permute-start.26 = (f32[8,384]{1,0:T(8,128)S(1)}, f32[8,384]{1,0:T(8,128)S(1)}, u32[]{:S(2)}, u32[]{:S(2)}) collective-permute-start(f32[8,384]{1,0:T(8,128)S(1)} %shard_map.191.my_taps), channel_id=1, source_target_pairs={{0,1},{1,0},{2,3},{3,2},{4,5},{5,4},{6,7},{7,6},{8,9},{9,8},{10,11... | collective-permute-start | bytes 36872 | tf_op jit(solution)/shard_map/ppermute | solution.py:67
  186.1 12.6 %collective-permute-start.27 = (bf16[128,1024]{1,0:T(8,128)(2,1)S(1)}, bf16[128,1024]{1,0:T(8,128)(2,1)S(1)}, u32[]{:S(2)}, u32[]{:S(2)}) collective-permute-start(bf16[128,1024]{1,0:T(8,128)(2,1)S(1)} %get-tuple-element.34), channel_id=1, source_target_pairs={{0,4},{2,6},{4,0},{6,2},{1,5},{3,7},{5,1},{7,3},{8,12},{10,14},{12... | collective-permute-start | bytes 786440 | tf_op jit(solution)/shard_map/ppermute | solution.py:332
  189.7 13.8 %collective-permute-start.28 = (bf16[128,1024]{1,0:T(8,128)(2,1)S(1)}, bf16[128,1024]{1,0:T(8,128)(2,1)S(1)}, u32[]{:S(2)}, u32[]{:S(2)}) collective-permute-start(bf16[128,1024]{1,0:T(8,128)(2,1)S(1)} %get-tuple-element.35), channel_id=1, source_target_pairs={{0,2},{2,0},{4,6},{6,4},{1,3},{3,1},{5,7},{7,5},{8,10},{10,8},{12,... | collective-permute-start | bytes 786440 | tf_op jit(solution)/shard_map/ppermute | solution.py:332
  193.4 11.1 %collective-permute-start.29 = (bf16[128,1024]{1,0:T(8,128)(2,1)S(1)}, bf16[128,1024]{1,0:T(8,128)(2,1)S(1)}, u32[]{:S(2)}, u32[]{:S(2)}) collective-permute-start(bf16[128,1024]{1,0:T(8,128)(2,1)S(1)} %get-tuple-element.36), channel_id=1, source_target_pairs={{0,6},{2,4},{4,2},{6,0},{1,7},{3,5},{5,3},{7,1},{8,14},{10,12},{12... | collective-permute-start | bytes 786440 | tf_op jit(solution)/shard_map/ppermute | solution.py:332
